TPU v7x, 512 devices: a whole 4x8x8 slice. The times are simulated.
512 devices in a mesh: sp: 32 (over z, x), tp: 16 (over y, core).
Axes of the slice: x: 4, y: 8, z: 8, core: 2. Of those that a mesh axis runs over, the one named last changes fastest.
Arguments:
- queries: bfloat16 [8192, 2048], P('sp', 'tp'), may hold values from -6 to 6
- key_matrix: bfloat16 [8192, 2048], P('sp', 'tp'), may hold values from -6 to 6
- value_matrix: bfloat16 [8192, 4096], P('sp', 'tp'), may hold values from -6 to 6
- output_gate_preactivation: bfloat16 [8192, 4096], P('sp', 'tp'), may hold values from -6 to 6
- decay_preactivation: bfloat16 [8192, 2048], P('sp', 'tp')
- extra_log_decay: float32 [8192, 16], P('sp', 'tp'), may hold values from -0.7 to 0
- head_norm_gain: bfloat16 [256], replicated, may hold values from 0.099609375 to 1.8984375
- output_projection: bfloat16 [4096, 2048], P(None, 'tp'), may hold values from -0.09375 to 0.09375
- residual: bfloat16 [8192, 2048], P('sp', 'tp'), may hold values from -210 to 210
- feedforward_gain: bfloat16 [2048], replicated, may hold values from 0.099609375 to 1.8984375
- routing: int32 [8192, 4], P('sp'), may hold values from 0 to 127, all different within a row; in each aligned block of 256 rows (0 to 255, 256 to 511, ...) at most 12 rows name the same one
- router_score: float32 [8192, 4], P('sp'), may hold values from 0.05 to 1
- expert_gate_weight: bfloat16 [2048, 131072], P(None, ('sp', 'tp')), may hold values from -0.125 to 0.125
- expert_up_weight: bfloat16 [2048, 131072], P(None, ('sp', 'tp')), may hold values from -0.125 to 0.125
- expert_down_weight: bfloat16 [131072, 2048], P(('sp', 'tp')), may hold values from -0.1875 to 0.1875
- shared_expert_gate: bfloat16 [2048, 512], P(None, 'tp'), may hold values from -0.125 to 0.125
- shared_expert_up: bfloat16 [2048, 512], P(None, 'tp'), may hold values from -0.125 to 0.125
- shared_expert_down: bfloat16 [512, 2048], P(None, 'tp'), may hold values from -0.25 to 0.25
Outputs:
- layer_out: bfloat16 [8192, 2048], P('sp', 'tp')
Inputs may be any that keep to these rules, and one draw needn't show every extreme that they name: `routing`: each row names 4 different experts. In each aligned block of 256 rows, the rows of one index of sp, no expert is named by more than 12 rows, a bound that some expert reaches in some blocks.
All inputs are finite; a program needn't handle non-finite values.
Results may differ from a plain program's by a relative error of at most 0.01.
Values may be sent and summed in bfloat16 or wider, within the bound.
No kernel may reach another device: no remote copies, remote signals or barrier semaphores. Data moves between devices by JAX's collectives and lax.ppermute only.
A program may use at most 64 MiB of HBM per device.

v0:
```python
import jax
import jax.numpy as jnp
from jax import lax
from jax.sharding import Mesh
from jax.sharding import PartitionSpec as P

DK = 128
DV = 256
BLOCK_POSITIONS = 64
FF_PARTS = 4
SP = ("sp_0", "sp_1")
SP_TP = ("sp_0", "sp_1", "tp")


HIGHEST = lax.Precision.HIGHEST
EPSILON = 1e-06
ROUTE_SCALE = 2.5
GATE_TEMPER = 16.0


def nothing_yet(value, identity):
    return jax.tree.map(
        lambda part, zero: jnp.zeros_like(part) + jnp.asarray(zero, part.dtype), value, identity
    )


def prefix_by_axis(value, axes, combine, identity):
    before = start = nothing_yet(value, identity)
    total = value
    for axis in reversed(axes):
        count, position = (lax.axis_size(axis), lax.axis_index(axis))
        pieces = jax.tree.map(
            lambda part, kind: lax.all_gather(part.astype(kind), axis),
            total,
            (jnp.bfloat16, jnp.bfloat16),
        )
        inside, total = (start, start)
        for k in range(count):
            passed = k < position
            total = combine(
                total, jax.tree.map(lambda part, own: part[k].astype(own.dtype), pieces, value)
            )
            inside = jax.tree.map(lambda new, old: jnp.where(passed, new, old), total, inside)
        before = combine(inside, before)
    return before


def laid_out(blocks, dim):
    blocks = jnp.moveaxis(blocks, 0, dim)
    dims = blocks.shape
    return blocks.reshape(*dims[:dim], dims[dim] * dims[dim + 1], *dims[dim + 2 :])


def sent_to_all(value, axis):
    copies = jnp.broadcast_to(value, (lax.axis_size(axis), *value.shape))
    return lax.all_to_all(copies, axis, split_axis=0, concat_axis=0, tiled=True)


def gather_directly(value, axis, dim):
    return laid_out(sent_to_all(value, axis), dim)


def from_partner(value, axis, bit):
    mask = 2**bit
    pairs = [(source, source ^ mask) for source in range(lax.axis_size(axis))]
    return lax.ppermute(value, axis, pairs)


def carry_combine(first_part, second_part):
    return (
        first_part[0] * second_part[0],
        second_part[0][..., None] * first_part[1] + second_part[1],
    )


def attention_heads(queries, key_matrix, value_matrix, decay_preactivation, extra_log_decay):
    tokens = queries.shape[0]
    local_head_count = extra_log_decay.shape[1]
    block_count = tokens // BLOCK_POSITIONS
    query_block = queries.astype(jnp.float32).reshape(
        block_count, BLOCK_POSITIONS, local_head_count, DK
    ) * DK ** (-0.5)
    key_block = key_matrix.astype(jnp.float32).reshape(
        block_count, BLOCK_POSITIONS, local_head_count, DK
    )
    value_block = value_matrix.astype(jnp.float32).reshape(
        block_count, BLOCK_POSITIONS, local_head_count, DV
    )
    log_decay_rows = (
        jax.nn.log_sigmoid(decay_preactivation.astype(jnp.float32)).reshape(
            block_count, BLOCK_POSITIONS, local_head_count, DK
        )
        / GATE_TEMPER
    )
    log_decay_rows = (
        log_decay_rows
        + extra_log_decay.reshape(block_count, BLOCK_POSITIONS, local_head_count)[..., None]
    )
    inside = jnp.cumsum(log_decay_rows, axis=1)
    block_total = inside[:, -1]
    query_decay = query_block * jnp.exp(inside)
    key_decay = key_block * jnp.exp(-inside)
    causal = jnp.tril(jnp.ones((BLOCK_POSITIONS, BLOCK_POSITIONS), dtype=bool))
    scores = jnp.where(
        causal, jnp.einsum("nthd,nshd->nhts", query_decay, key_decay, precision=HIGHEST), 0.0
    )
    within = jnp.einsum("nhts,nshv->nthv", scores, value_block, precision=HIGHEST)
    key_end = key_block * jnp.exp(block_total[:, None] - inside)
    update = jnp.einsum("nshd,nshv->nhdv", key_end, value_block, precision=HIGHEST)
    before = jnp.cumsum(block_total, axis=0) - block_total
    ending = jnp.concatenate([before, (before[-1] + block_total[-1])[None]], axis=0)
    after_block = before + block_total
    earlier_mask = jnp.arange(block_count + 1)[:, None] > jnp.arange(block_count)[None, :]
    span_logs = jnp.where(
        earlier_mask[:, :, None, None], ending[:, None] - after_block[None], -1e30
    )
    states = jnp.einsum("nmhd,mhdv->nhdv", jnp.exp(span_logs), update, precision=HIGHEST)
    passed = jnp.einsum("nthd,nhdv->nthv", query_decay, states[:block_count], precision=HIGHEST)
    query_start = query_block * jnp.exp(inside + before[:, None])
    return (within + passed, query_start, jnp.exp(ending[block_count]), states[block_count])


def body(
    queries,
    key_matrix,
    value_matrix,
    output_gate_preactivation,
    decay_preactivation,
    extra_log_decay,
    head_norm_gain,
    output_projection,
    residual,
    feedforward_gain,
    routing,
    router_score,
    expert_gate_weight,
    expert_up_weight,
    expert_down_weight,
    shared_expert_gate,
    shared_expert_up,
    shared_expert_down,
):
    tokens = queries.shape[0]
    local_head_count = extra_log_decay.shape[1]
    local_part, query_start, dev_decay, dev_update = attention_heads(
        queries, key_matrix, value_matrix, decay_preactivation, extra_log_decay
    )
    _, entering = prefix_by_axis(
        (dev_decay, dev_update),
        SP,
        carry_combine,
        (jnp.ones_like(dev_decay), jnp.zeros_like(dev_update)),
    )
    attention_output = local_part + jnp.einsum(
        "nthd,hdv->nthv", query_start, entering, precision=HIGHEST
    )
    attention_output = attention_output.reshape(tokens, local_head_count, DV)
    inverse_rms = lax.rsqrt(
        jnp.mean(attention_output * attention_output, axis=-1, keepdims=True) + EPSILON
    )
    gate_act = jax.nn.silu(
        output_gate_preactivation.astype(jnp.float32).reshape(tokens, local_head_count, DV)
    )
    head_rows = (
        (attention_output * inverse_rms * head_norm_gain.astype(jnp.float32) * gate_act)
        .reshape(tokens, local_head_count * DV)
        .astype(jnp.bfloat16)
    )
    projected = jnp.dot(
        lax.all_gather(head_rows, "tp", axis=1, tiled=True),
        output_projection,
        preferred_element_type=jnp.float32,
    )
    mid_local = (residual.astype(jnp.float32) + projected).astype(jnp.bfloat16)
    mid_rows = gather_directly(mid_local, "tp", 1).astype(jnp.float32)
    normed = (
        mid_rows
        * lax.rsqrt(jnp.mean(mid_rows * mid_rows, axis=-1, keepdims=True) + EPSILON)
        * feedforward_gain.astype(jnp.float32)
    ).astype(jnp.bfloat16)
    shared_pre = jnp.dot(normed, shared_expert_gate, preferred_element_type=jnp.float32)
    shared_lin = jnp.dot(normed, shared_expert_up, preferred_element_type=jnp.float32)
    shared_hidden = (jax.nn.silu(shared_pre) * shared_lin).astype(jnp.bfloat16)
    senders = lax.axis_size(SP)
    tp_count = lax.axis_size("tp")
    tp_bits = tp_count.bit_length() - 1
    tp_index = lax.axis_index("tp")
    groups = tp_count // FF_PARTS
    group_here = tp_index // FF_PARTS
    part_here = tp_index % FF_PARTS
    model_width = normed.shape[1]
    picks = routing.shape[1]
    expert_total = senders * groups
    rows_most = max(2, 3 * tokens * picks // (2 * expert_total))
    slot_count = senders * rows_most
    flat_expert = routing.reshape(-1)
    one_hot = (flat_expert[:, None] == jnp.arange(expert_total, dtype=jnp.int32)[None, :]).astype(
        jnp.int32
    )
    rank_before = jnp.sum((jnp.cumsum(one_hot, axis=0) - one_hot) * one_hot, axis=1)
    owned = flat_expert % groups == group_here
    slot_index = jnp.where(owned, flat_expert // groups * rows_most + rank_before, slot_count)
    token_index = jnp.arange(flat_expert.shape[0], dtype=jnp.int32) // picks
    part_width = model_width // FF_PARTS
    normed_part = lax.dynamic_slice_in_dim(normed, part_here * part_width, part_width, 1)
    outgoing = (
        jnp.zeros((slot_count, part_width), jnp.bfloat16)
        .at[slot_index]
        .set(normed_part[token_index], mode="drop")
    )
    arrived = lax.all_to_all(
        outgoing.reshape(senders, rows_most, part_width),
        SP,
        split_axis=0,
        concat_axis=0,
        tiled=True,
    )
    for bit in range(2):
        partner_cols = from_partner(arrived, "tp", bit)
        upper = (tp_index >> bit) % 2
        arrived = jnp.where(
            upper == 1,
            jnp.concatenate([partner_cols, arrived], axis=2),
            jnp.concatenate([arrived, partner_cols], axis=2),
        )
    rows_in = arrived.reshape(slot_count, model_width)
    gate_pre = jnp.dot(rows_in, expert_gate_weight, preferred_element_type=jnp.float32)
    up_pre = jnp.dot(rows_in, expert_up_weight, preferred_element_type=jnp.float32)
    routed_hidden = (jax.nn.silu(gate_pre) * up_pre).astype(jnp.bfloat16)
    partial_out = jnp.dot(routed_hidden, expert_down_weight, preferred_element_type=jnp.float32)
    slab_width = model_width // tp_count
    partial_out = partial_out.reshape(slot_count, groups, FF_PARTS, slab_width)
    for bit in (1, 0):
        paired = partial_out.reshape(slot_count, groups, 2, 2**bit, slab_width)
        upper = (tp_index >> bit) % 2
        kept = lax.dynamic_index_in_dim(paired, upper, 2, keepdims=False)
        given = lax.dynamic_index_in_dim(paired, 1 - upper, 2, keepdims=False)
        partial_out = kept + from_partner(given.astype(jnp.bfloat16), "tp", bit).astype(given.dtype)
    expert_out = partial_out.reshape(senders, rows_most, groups, slab_width).astype(jnp.bfloat16)
    shared_out = jnp.dot(
        lax.all_gather(shared_hidden, "tp", axis=1, tiled=True),
        shared_expert_down,
        preferred_element_type=jnp.float32,
    )
    returned = lax.all_to_all(expert_out, SP, split_axis=0, concat_axis=0, tiled=True).reshape(
        slot_count, groups, slab_width
    )
    safe_slot = jnp.minimum(slot_index, slot_count - 1)
    route_weight = ROUTE_SCALE * router_score / jnp.sum(router_score, axis=1, keepdims=True)
    pair_weight = jnp.where(owned, route_weight.reshape(-1), 0.0)
    picked = returned[safe_slot].astype(jnp.float32) * pair_weight[:, None, None]
    routed_part = jnp.sum(picked.reshape(tokens, picks, groups, slab_width), axis=1)
    for bit in range(tp_bits - 1, 1, -1):
        paired = routed_part.reshape(tokens, 2, 2 ** (bit - 2), slab_width)
        upper = (tp_index >> bit) % 2
        kept = lax.dynamic_index_in_dim(paired, upper, 1, keepdims=False)
        given = lax.dynamic_index_in_dim(paired, 1 - upper, 1, keepdims=False)
        routed_part = kept + from_partner(given.astype(jnp.bfloat16), "tp", bit).astype(given.dtype)
    routed = routed_part.reshape(tokens, slab_width)
    return (mid_local.astype(jnp.float32) + routed + shared_out).astype(jnp.bfloat16)


def solution(mesh):
    finer = Mesh(mesh.devices.reshape(8, 4, mesh.shape["tp"]), ("sp_0", "sp_1", "tp"))
    in_specs = (
        P(SP, "tp"),
        P(SP, "tp"),
        P(SP, "tp"),
        P(SP, "tp"),
        P(SP, "tp"),
        P(SP, "tp"),
        P(),
        P(None, "tp"),
        P(SP, "tp"),
        P(),
        P(SP, None),
        P(SP, None),
        P(None, SP_TP),
        P(None, SP_TP),
        P(SP_TP, None),
        P(None, "tp"),
        P(None, "tp"),
        P(None, "tp"),
    )
    out_specs = P(SP, "tp")
    return jax.shard_map(body, mesh=finer, in_specs=in_specs, out_specs=out_specs, check_vma=False)
```

profile of v0, /device:TPU:1, one launch (start us, length us, event | category | flops | bytes accessed | tf_op | source)
XLA Modules:
  0.0 347.6 jit_solution(1330581877182747626)
XLA Ops:
  6.6 1.0 fusion.52
  7.6 0.5 broadcast.932
  8.1 1.3 reduce.7
  9.5 0.3 fusion.86
  10.2 1.4 fusion.49
  11.6 1.7 convolution_bitcast_fusion
  13.6 8.5 %all_gather.22 = bf16[4,1,128]{2,1,0:T(2,128)(2,1)S(1)} all-gather(bf16[1,1,128]{2,1,0:T(2,128)(2,1)S(1)} %get-tuple-element.7), channel_id=1, replica_groups=mesh['sp_0'=8,'sp_1'=4,'tp'=16] {'sp_1'}, dimensions={0}, use_global_device_ids=true | all-gather | bytes 1280 | tf_op jit(solution)/shard_map/all_gather | solution.py:33
  22.1 18.6 %all_gather.23 = bf16[8,1,128]{2,1,0:T(2,128)(2,1)S(1)} all-gather(bf16[1,1,128]{2,1,0:T(2,128)(2,1)S(1)} %multiply_convert_fusion.1), channel_id=1, replica_groups=mesh['sp_0'=8,'sp_1'=4,'tp'=16] {'sp_0'}, dimensions={0}, use_global_device_ids=true | all-gather | bytes 2304 | tf_op jit(solution)/shard_map/all_gather | solution.py:33
  40.7 0.6 fusion.124
  41.2 0.6 fusion.131
  41.9 0.4 convolution_select_fusion
  42.3 0.3 convolution_bitcast_fusion.2
  42.6 9.4 %all_gather.24 = bf16[4,1,128,256]{3,2,1,0:T(8,128)(2,1)S(1)} all-gather(bf16[1,1,128,256]{3,2,1,0:T(8,128)(2,1)S(1)} %copy.45), channel_id=1, replica_groups=mesh['sp_0'=8,'sp_1'=4,'tp'=16] {'sp_1'}, dimensions={0}, use_global_device_ids=true | all-gather | bytes 327680 | tf_op jit(solution)/shard_map/all_gather | solution.py:33
  51.9 0.5 broadcast_select_fusion.3
  52.6 21.8 %all_gather.25 = bf16[8,1,128,256]{3,2,1,0:T(8,128)(2,1)} all-gather(bf16[1,1,128,256]{3,2,1,0:T(8,128)(2,1)S(1)} %fusion.46), channel_id=1, replica_groups=mesh['sp_0'=8,'sp_1'=4,'tp'=16] {'sp_0'}, dimensions={0}, use_global_device_ids=true | all-gather | bytes 589824 | tf_op jit(solution)/shard_map/all_gather | solution.py:33
  74.4 0.6 convert_element_type.645
  74.9 0.5 fusion.4
  75.4 1.9 multiply_reduce_fusion
  77.4 1.7 fusion.29
  79.1 53.5 %all-gather.2.cloned.1.call-done = bf16[256,4096]{1,0:T(8,128)(2,1)} async-done(((bf16[256,256]{1,0:T(8,128)(2,1)}), bf16[256,4096]{1,0:T(8,128)(2,1)}) %all-gather.2.cloned.1.call-update) | async-done | bytes 2097168 | tf_op jit(solution)/shard_map/all_gather | solution.py:170
  132.6 2.3 fusion.6
  134.9 0.6 copy-done.4
  135.5 1.2 broadcast_in_dim.52
  136.7 5.1 %all-to-all-start = ((bf16[16,256,128]{2,1,0:T(8,128)(2,1)}), bf16[16,256,128]{2,1,0:T(8,128)(2,1)S(1)}, u32[]{:S(2)}, u32[]{:S(2)}) async-start(bf16[16,256,128]{2,1,0:T(8,128)(2,1)} %broadcast_in_dim.52), calls=%async_computation | async-start | bytes 2097152 | tf_op jit(solution)/shard_map/all_to_all | solution.py:56
  142.9 0.4 fusion.12
  143.4 26.5 %all-to-all-done = bf16[16,256,128]{2,1,0:T(8,128)(2,1)S(1)} async-done(((bf16[16,256,128]{2,1,0:T(8,128)(2,1)}), bf16[16,256,128]{2,1,0:T(8,128)(2,1)S(1)}, u32[]{:S(2)}, u32[]{:S(2)}) %all-to-all-start) | async-done | bytes 1048608 | tf_op jit(solution)/shard_map/all_to_all | solution.py:56
  169.8 0.3 fusion
  170.1 0.3 fusion.2
  170.5 9.7 %scatter_custom_fusion = bf16[384,512]{1,0:T(8,128)(2,1)S(1)} fusion(s32[1024]{0:T(1024)S(1)} %bitcast.324, bf16[256,512]{1,0:T(8,128)(2,1)S(1)} %constant_dynamic-slice_fusion.2, s32[1024]{0:T(1024)S(1)} %broadcast_clamp_fusion.1, bf16[]{:T(256)} %constant.181.clone.1), kind=kCustom, calls=%fused_computation.26 | custom fusion | bytes 393218 | tf_op jit(solution)/shard_map/scatter | solution.py:209
  180.3 27.1 %all_to_all.15 = bf16[32,12,512]{2,1,0:T(8,128)(2,1)S(1)} all-to-all(bf16[32,12,512]{2,1,0:T(8,128)(2,1)S(1)} %reshape.1386), channel_id=1, replica_groups=mesh['sp_0'=8,'sp_1'=4,'tp'=16] {'sp_0','sp_1'}, dimensions={0} | all-to-all | bytes 786432 | tf_op jit(solution)/shard_map/all_to_all | solution.py:211
  207.4 1.9 collective-permute-start
  209.3 1.9 collective-permute-done
  211.2 0.4 maximum_select_fusion.1
  211.5 1.3 copy.52
  212.9 2.1 collective-permute-start.1
  215.2 1.1 maximum_select_fusion.2
  216.3 17.7 %collective-permute-done.1 = bf16[32,12,1024]{2,0,1:T(8,128)(2,1)} collective-permute-done((bf16[32,12,1024]{2,0,1:T(8,128)(2,1)}, bf16[32,12,1024]{2,0,1:T(8,128)(2,1)}, u32[]{:S(2)}, u32[]{:S(2)}) %collective-permute-start.1) | collective-permute-done | bytes 786464 | tf_op jit(solution)/shard_map/ppermute | solution.py:66
  234.0 1.6 copy.53
  235.6 1.1 concatenate.32
  236.7 2.8 fusion.18
  239.5 5.1 %fusion.19 = f32[384,2048]{1,0:T(8,128)} fusion(bf16[256,2048]{1,0:T(8,128)(2,1)S(1)} %copy-done, f32[384,256]{1,0:T(8,128)S(1)} %fusion.18, bf16[2048,256]{1,0:T(8,128)(2,1)} %param.31, bf16[384,1024]{1,0:T(8,128)(2,1)} %maximum_select_fusion.2, bf16[384,1024]{1,0:T(8,128)(2,1)S(1)} %copy-done.3, pred[]{:T(512)S(6)} %eq.66), kind=kOutput, calls=%fused_computation.48 | convolution fusion | flops 812974080 | bytes 7208961 | tf_op jit(solution)/shard_map/dot_general | solution.py:230
  244.7 5.6 %reshape_reshape.3 = f32[384,4,2,2,128]{4,3,2,1,0:T(2,128)} reshape(f32[384,2048]{1,0:T(8,128)} %fusion.19) | data formatting | bytes 6291456 | tf_op jit(solution)/shard_map/reshape;reshape | solution.py:234
  250.3 1.9 constant_dynamic-slice_fusion
  252.4 2.2 collective-permute-start.2
  254.7 2.0 constant_dynamic-slice_fusion.1
  256.6 15.9 %collective-permute-done.2 = bf16[384,4,2,128]{3,1,0,2:T(4,128)(2,1)} collective-permute-done((bf16[384,4,2,128]{3,1,0,2:T(4,128)(2,1)S(1)}, bf16[384,4,2,128]{3,1,0,2:T(4,128)(2,1)}, u32[]{:S(2)}, u32[]{:S(2)}) %collective-permute-start.2) | collective-permute-done | bytes 786464 | tf_op jit(solution)/shard_map/ppermute | solution.py:66
  272.6 1.7 bitcast_add_fusion
  274.3 1.1 copy-done.1
  275.6 3.8 %collective-permute-start.3 = (bf16[384,4,1,128]{3,1,0,2:T(4,128)(2,1)S(1)}, bf16[384,4,1,128]{3,1,0,2:T(4,128)(2,1)S(1)}, u32[]{:S(2)}, u32[]{:S(2)}) collective-permute-start(bf16[384,4,1,128]{3,1,0,2:T(4,128)(2,1)S(1)} %dynamic-slice_convert_fusion), channel_id=1, source_target_pairs={{0,1},{1,0},{2,3},{3,2},{4,5},{5,4},{6,7},{7,6},{8,9},{9,8},{10,11... | collective-permute-start | bytes 1179656 | tf_op jit(solution)/shard_map/ppermute | solution.py:66
  279.3 1.3 collective-permute-done.3
  280.6 2.1 add_convert_fusion
  282.7 4.3 %all-to-all-start.2 = ((bf16[32,12,4,128]{3,2,1,0:T(4,128)(2,1)}), bf16[32,12,4,128]{3,2,1,0:T(4,128)(2,1)S(1)}, u32[]{:S(2)}, u32[]{:S(2)}) async-start(bf16[32,12,4,128]{3,2,1,0:T(4,128)(2,1)} %bitcast.64), calls=%async_computation.2 | async-start | bytes 786432 | tf_op jit(solution)/shard_map/all_to_all | solution.py:245
  287.1 0.8 copy.56
  287.9 1.0 fusion.143
  289.0 12.0 %all-to-all-done.2 = bf16[32,12,4,128]{3,2,1,0:T(4,128)(2,1)S(1)} async-done(((bf16[32,12,4,128]{3,2,1,0:T(4,128)(2,1)}), bf16[32,12,4,128]{3,2,1,0:T(4,128)(2,1)S(1)}, u32[]{:S(2)}, u32[]{:S(2)}) %all-to-all-start.2) | async-done | bytes 393248 | tf_op jit(solution)/shard_map/all_to_all | solution.py:245
  300.9 3.6 %gather_fusion = bf16[1024,4,128]{2,1,0:T(4,128)(2,1)S(1)} fusion(bf16[384,4,128]{2,1,0:T(4,128)(2,1)S(1)} %bitcast.299, s32[1024]{0:T(1024)S(1)} %broadcast_clamp_fusion), kind=kCustom, calls=%fused_computation.1 | custom fusion | bytes 2101248 | tf_op jit(solution)/shard_map/gather | solution.py:251
  304.5 2.7 fusion.3
  307.4 4.1 %collective-permute-start.4 = (bf16[256,2,128]{2,0,1:T(8,128)(2,1)S(1)}, bf16[256,2,128]{2,0,1:T(8,128)(2,1)S(1)}, u32[]{:S(2)}, u32[]{:S(2)}) collective-permute-start(bf16[256,2,128]{2,0,1:T(8,128)(2,1)S(1)} %fusion.50), channel_id=1, source_target_pairs={{0,8},{1,9},{2,10},{3,11},{4,12},{5,13},{6,14},{7,15},{8,0},{9,1},... | collective-permute-start | bytes 393224 | tf_op jit(solution)/shard_map/ppermute | solution.py:66
  311.6 0.4 fusion.7
  312.0 19.9 %all_gather.27 = bf16[256,512]{0,1:T(8,128)(2,1)S(1)} all-gather(bf16[256,32]{0,1:T(8,128)(2,1)S(1)} %fusion.7), channel_id=1, replica_groups=mesh['sp_0'=8,'sp_1'=4,'tp'=16] {'tp'}, dimensions={1}, use_global_device_ids=true | all-gather | bytes 278528 | tf_op jit(solution)/shard_map/all_gather | solution.py:241
  331.9 1.9 collective-permute-start.5
  333.9 0.3 fusion.144
  334.1 6.0 %collective-permute-done.5 = bf16[256,1,128]{2,0,1:T(8,128)(2,1)S(1)} collective-permute-done((bf16[256,1,128]{2,0,1:T(8,128)(2,1)S(1)}, bf16[256,1,128]{2,0,1:T(8,128)(2,1)S(1)}, u32[]{:S(2)}, u32[]{:S(2)}) %collective-permute-start.5) | collective-permute-done | bytes 65568 | tf_op jit(solution)/shard_map/ppermute | solution.py:66
  340.1 0.7 fusion.66
  (89 shorter events, 2.9 us)
Async XLA Ops:
  6.5 233.0 %copy-start = (bf16[256,2048]{1,0:T(8,128)(2,1)S(1)}, bf16[256,2048]{1,0:T(8,128)(2,1)}, u32[]{:S(2)}) copy-start(bf16[256,2048]{1,0:T(8,128)(2,1)} %param.32) | copy-start | bytes 3145732
  6.5 126.1 %all-gather.2.cloned.1.call-start = ((), (), s32[]{:S(2)}) async-start(), calls=%async_computation.3 | async-start | bytes 2228224 | tf_op jit(solution)/shard_map/all_gather | solution.py:170
  9.9 32.0 %copy-start.12 = (bf16[256,128]{1,0:T(8,128)(2,1)S(1)}, bf16[256,128]{1,0:T(8,128)(2,1)}, u32[]{:S(2)}) copy-start(bf16[256,128]{1,0:T(8,128)(2,1)} %param.18) | copy-start | bytes 196612
  10.2 31.7 %copy-start.7 = (bf16[256,128]{1,0:T(8,128)(2,1)S(1)}, bf16[256,128]{1,0:T(8,128)(2,1)}, u32[]{:S(2)}) copy-start(bf16[256,128]{1,0:T(8,128)(2,1)} %param.19) | copy-start | bytes 196612
  11.6 30.7 %copy-start.6 = (bf16[256,256]{1,0:T(8,128)(2,1)S(1)}, bf16[256,256]{1,0:T(8,128)(2,1)}, u32[]{:S(2)}) copy-start(bf16[256,256]{1,0:T(8,128)(2,1)} %param.20) | copy-start | bytes 393220
  13.3 61.0 %copy-start.18 = (bf16[256]{0:T(256)(128)(2,1)S(1)}, bf16[256]{0:T(256)(128)(2,1)}, u32[]{:S(2)}) copy-start(bf16[256]{0:T(256)(128)(2,1)} %param.24) | copy-start | bytes 1540
  74.9 57.7 %copy-start.2 = (bf16[4096,128]{1,0:T(8,128)(2,1)S(1)}, bf16[4096,128]{1,0:T(8,128)(2,1)}, u32[]{:S(2)}) copy-start(bf16[4096,128]{1,0:T(8,128)(2,1)} %param.25) | copy-start | bytes 3145732
  75.4 2.0 copy-start.17
  75.4 57.2 %copy-start.13 = (bf16[256,128]{1,0:T(8,128)(2,1)S(1)}, bf16[256,128]{1,0:T(8,128)(2,1)}, u32[]{:S(2)}) copy-start(bf16[256,128]{1,0:T(8,128)(2,1)} %param.26) | copy-start | bytes 196612
  134.9 0.6 copy-start.4
  135.5 6.3 %copy-start.14 = (s32[256,4]{0,1:T(4,128)S(1)}, s32[256,4]{0,1:T(4,128)}, u32[]{:S(2)}) copy-start(s32[256,4]{0,1:T(4,128)} %param.28) | copy-start | bytes 12292
  135.5 6.8 %copy-start.16 = (bf16[2048]{0:T(1024)(128)(2,1)S(1)}, bf16[2048]{0:T(1024)(128)(2,1)}, u32[]{:S(2)}) copy-start(bf16[2048]{0:T(1024)(128)(2,1)} %param.27) | copy-start | bytes 12292
  136.7 33.1 %all-to-all-start = ((bf16[16,256,128]{2,1,0:T(8,128)(2,1)}), bf16[16,256,128]{2,1,0:T(8,128)(2,1)S(1)}, u32[]{:S(2)}, u32[]{:S(2)}) async-start(bf16[16,256,128]{2,1,0:T(8,128)(2,1)} %broadcast_in_dim.52), calls=%async_computation | async-start | bytes 2097152 | tf_op jit(solution)/shard_map/all_to_all | solution.py:56
  207.4 3.8 %collective-permute-start = (bf16[32,12,512]{2,1,0:T(8,128)(2,1)S(1)}, bf16[32,12,512]{2,1,0:T(8,128)(2,1)S(1)}, u32[]{:S(2)}, u32[]{:S(2)}) collective-permute-start(bf16[32,12,512]{2,1,0:T(8,128)(2,1)S(1)} %all_to_all.15), channel_id=1, source_target_pairs={{0,1},{1,0},{2,3},{3,2},{4,5},{5,4},{6,7},{7,6},{8,9},{9,8},{10,11... | collective-permute-start | bytes 1179656 | tf_op jit(solution)/shard_map/ppermute | solution.py:66
  212.9 21.2 %collective-permute-start.1 = (bf16[32,12,1024]{2,0,1:T(8,128)(2,1)}, bf16[32,12,1024]{2,0,1:T(8,128)(2,1)}, u32[]{:S(2)}, u32[]{:S(2)}) collective-permute-start(bf16[32,12,1024]{2,0,1:T(8,128)(2,1)} %copy.52), channel_id=1, source_target_pairs={{0,2},{1,3},{2,0},{3,1},{4,6},{5,7},{6,4},{7,5},{8,10},{9,11},{10,... | collective-permute-start | bytes 2359304 | tf_op jit(solution)/shard_map/ppermute | solution.py:66
  236.7 2.8 copy-start.3
  252.4 20.1 %collective-permute-start.2 = (bf16[384,4,2,128]{3,1,0,2:T(4,128)(2,1)S(1)}, bf16[384,4,2,128]{3,1,0,2:T(4,128)(2,1)}, u32[]{:S(2)}, u32[]{:S(2)}) collective-permute-start(bf16[384,4,2,128]{3,1,0,2:T(4,128)(2,1)S(1)} %bitcast.308), channel_id=1, source_target_pairs={{0,2},{1,3},{2,0},{3,1},{4,6},{5,7},{6,4},{7,5},{8,10},{9,11},{10,... | collective-permute-start | bytes 2359304 | tf_op jit(solution)/shard_map/ppermute | solution.py:66
  274.3 1.1 copy-start.1
  275.4 11.7 %copy-start.15 = (f32[256,4]{0,1:T(4,128)S(1)}, f32[256,4]{0,1:T(4,128)}, u32[]{:S(2)}) copy-start(f32[256,4]{0,1:T(4,128)} %param.29) | copy-start | bytes 12292
  275.4 12.5 %copy-start.8 = (bf16[2048,32]{0,1:T(8,128)(2,1)S(1)}, bf16[2048,32]{0,1:T(8,128)(2,1)}, u32[]{:S(2)}) copy-start(bf16[2048,32]{0,1:T(8,128)(2,1)} %param.33) | copy-start | bytes 393220
  275.6 5.1 %collective-permute-start.3 = (bf16[384,4,1,128]{3,1,0,2:T(4,128)(2,1)S(1)}, bf16[384,4,1,128]{3,1,0,2:T(4,128)(2,1)S(1)}, u32[]{:S(2)}, u32[]{:S(2)}) collective-permute-start(bf16[384,4,1,128]{3,1,0,2:T(4,128)(2,1)S(1)} %dynamic-slice_convert_fusion), channel_id=1, source_target_pairs={{0,1},{1,0},{2,3},{3,2},{4,5},{5,4},{6,7},{7,6},{8,9},{9,8},{10,11... | collective-permute-start | bytes 1179656 | tf_op jit(solution)/shard_map/ppermute | solution.py:66
  282.7 18.2 %all-to-all-start.2 = ((bf16[32,12,4,128]{3,2,1,0:T(4,128)(2,1)}), bf16[32,12,4,128]{3,2,1,0:T(4,128)(2,1)S(1)}, u32[]{:S(2)}, u32[]{:S(2)}) async-start(bf16[32,12,4,128]{3,2,1,0:T(4,128)(2,1)} %bitcast.64), calls=%async_computation.2 | async-start | bytes 786432 | tf_op jit(solution)/shard_map/all_to_all | solution.py:245
  304.5 7.0 %copy-start.9 = (bf16[2048,32]{0,1:T(8,128)(2,1)S(1)}, bf16[2048,32]{0,1:T(8,128)(2,1)}, u32[]{:S(2)}) copy-start(bf16[2048,32]{0,1:T(8,128)(2,1)} %param.34) | copy-start | bytes 393220
  304.5 7.0 %copy-start.10 = (f32[256,32]{0,1:T(8,128)S(1)}, f32[256,32]{0,1:T(8,128)}, u32[]{:S(2)}) copy-start(f32[256,32]{0,1:T(8,128)} %fusion.143) | copy-start | bytes 98308
  307.3 26.6 %copy-start.11 = (bf16[512,128]{1,0:T(8,128)(2,1)S(1)}, bf16[512,128]{1,0:T(8,128)(2,1)}, u32[]{:S(2)}) copy-start(bf16[512,128]{1,0:T(8,128)(2,1)} %param.35) | copy-start | bytes 393220
  307.3 32.8 %copy-start.5 = (bf16[256,128]{1,0:T(8,128)(2,1)S(1)}, bf16[256,128]{1,0:T(8,128)(2,1)}, u32[]{:S(2)}) copy-start(bf16[256,128]{1,0:T(8,128)(2,1)} %copy-done.4) | copy-start | bytes 196612
  307.4 24.5 %collective-permute-start.4 = (bf16[256,2,128]{2,0,1:T(8,128)(2,1)S(1)}, bf16[256,2,128]{2,0,1:T(8,128)(2,1)S(1)}, u32[]{:S(2)}, u32[]{:S(2)}) collective-permute-start(bf16[256,2,128]{2,0,1:T(8,128)(2,1)S(1)} %fusion.50), channel_id=1, source_target_pairs={{0,8},{1,9},{2,10},{3,11},{4,12},{5,13},{6,14},{7,15},{8,0},{9,1},... | collective-permute-start | bytes 393224 | tf_op jit(solution)/shard_map/ppermute | solution.py:66
  331.9 8.2 %collective-permute-start.5 = (bf16[256,1,128]{2,0,1:T(8,128)(2,1)S(1)}, bf16[256,1,128]{2,0,1:T(8,128)(2,1)S(1)}, u32[]{:S(2)}, u32[]{:S(2)}) collective-permute-start(bf16[256,1,128]{2,0,1:T(8,128)(2,1)S(1)} %dynamic-slice_convert_fusion.2), channel_id=1, source_target_pairs={{0,4},{1,5},{2,6},{3,7},{4,0},{5,1},{6,2},{7,3},{8,12},{9,13},{10,... | collective-permute-start | bytes 196616 | tf_op jit(solution)/shard_map/ppermute | solution.py:66
Sparse Core Ops, SparseCore 0:
  79.2 53.3 all-gather.1
where the time goes:
time: 349 us; the launch traced here: 348 us
  waiting for transfers between devices  135 us (39%)
  blocking collectives  105 us (30%)
  local copies, waits for them, and re-layouts  33.1 us (9%)
  starting transfers between devices  25.5 us (7%)
  matrix products  18 us (5%)
  other arithmetic  16.9 us (5%)
  between operations  14.1 us (4%)
    all_gather x4, blocking collectives, prefix_by_axis(): lax.all_gather(part.astype(kind), axis)  58.2 us
    all_gather x1, waiting for transfers between devices, body(): lax.all_gather(head_rows, 'tp', axis=1, tiled=True)  53.5 us
    ppermute x6, waiting for transfers between devices, from_partner(): return lax.ppermute(value, axis, pairs)  42.8 us
    all_to_all x1, blocking collectives, body(): lax.all_to_all(outgoing.reshape(senders, rows_most, part_width), SP, spli...  27.1 us
    all_to_all x1, waiting for transfers between devices, sent_to_all(): return lax.all_to_all(copies, axis, split_axis=0, concat_axis=0, tiled=True)  26.5 us
    all_gather x1, blocking collectives, body(): lax.all_gather(shared_hidden, 'tp', axis=1, tiled=True)  19.9 us
    ppermute x6, starting transfers between devices, from_partner(): return lax.ppermute(value, axis, pairs)  16.1 us
    all_to_all x1, waiting for transfers between devices, body(): lax.all_to_all(expert_out, SP, split_axis=0, concat_axis=0, tiled=True)  12 us
  transfers between devices with their start and end apart: 9, of which 8 were waited for; matrix products, arithmetic and copies ran while one was open for 2% of the time, Pallas kernels for 0%

commit v1 on v0

v1 whole, which is shorter than its diff:
```python
import jax
import jax.numpy as jnp
from jax import lax
from jax.experimental import pallas as pl
from jax.experimental.pallas import tpu as pltpu
from jax.sharding import Mesh
from jax.sharding import PartitionSpec as P

DK = 128
DV = 256
BLOCK = 64
TOK = 256
MOST = 12
SLOTS = 384
D = 2048
SP = ("z", "x")
TP = ("yg", "yn", "c")
Y = ("yg", "yn")
GROUP = ("yn", "c")
F32 = jnp.float32
BF16 = jnp.bfloat16
HIGHEST = lax.Precision.HIGHEST
EPSILON = 1e-06
ROUTE_SCALE = 2.5
GATE_TEMPER = 16.0
VMEM = pl.BlockSpec(memory_space=pltpu.VMEM)
SMEM = pl.BlockSpec(memory_space=pltpu.SMEM)


def call(kernel, outs, *args, scratch=(), smem=0, flops=1000000, limit=24):
    single = not isinstance(outs, list)
    shapes = [jax.ShapeDtypeStruct(s, t) for s, t in ([outs] if single else outs)]
    got = pl.pallas_call(
        kernel,
        out_shape=shapes,
        in_specs=[SMEM] * smem + [VMEM] * (len(args) - smem),
        out_specs=[VMEM] * len(shapes),
        scratch_shapes=list(scratch),
        compiler_params=pltpu.CompilerParams(vmem_limit_bytes=limit * 2**20),
        cost_estimate=pl.CostEstimate(flops=flops, bytes_accessed=1000000, transcendentals=0),
        name=kernel.__name__,
    )(*args)
    return got[0] if single else got


def nt(a, b, **kw):
    return lax.dot_general(
        a, b, (((1,), (1,)), ((), ())), preferred_element_type=F32, **kw
    )


def decays(decay_ref, extra_ref):
    raw = decay_ref[...].astype(F32)
    logs = jax.nn.log_sigmoid(raw) / GATE_TEMPER + extra_ref[...]
    rows = lax.broadcasted_iota(jnp.int32, (BLOCK, BLOCK), 0)
    cols = lax.broadcasted_iota(jnp.int32, (BLOCK, BLOCK), 1)
    lower = (rows >= cols).astype(F32)
    inside = [
        jnp.dot(lower, logs[b * BLOCK : (b + 1) * BLOCK], precision=HIGHEST,
                preferred_element_type=F32)
        for b in range(TOK // BLOCK)
    ]
    return inside


def block_states(inside, key_ref, value_ref):
    state = jnp.zeros((DV, DK), F32)
    states = []
    total = jnp.zeros((1, DK), F32)
    for b, cum in enumerate(inside):
        states.append(state)
        rows = pl.ds(b * BLOCK, BLOCK)
        end = cum[BLOCK - 1 : BLOCK]
        key_end = key_ref[rows, :].astype(F32) * jnp.exp(end - cum)
        value = value_ref[rows, :].astype(F32)
        fresh = jnp.dot(value.T, key_end, precision=HIGHEST, preferred_element_type=F32)
        state = jnp.exp(end) * state + fresh
        total = total + end
    return states, state, total


def state_kernel(key_ref, value_ref, decay_ref, extra_ref, out_ref):
    inside = decays(decay_ref, extra_ref)
    _, state, total = block_states(inside, key_ref, value_ref)
    out_ref[:, 0:8, :] = state.reshape(32, 8, DK).astype(BF16)
    decay = jnp.exp(total)
    high = decay.astype(BF16).astype(F32)
    row = lax.broadcasted_iota(jnp.int32, (8, DK), 0)
    tail = jnp.where(row == 0, high, jnp.where(row == 1, decay - high, 0.0))
    out_ref[:, 8:16, :] = jnp.broadcast_to(tail[None], (32, 8, DK)).astype(BF16)


def scan_kernel(in_ref, out_ref):
    state = jnp.zeros((8, DK), F32)
    for s in range(32):
        out_ref[s] = state.astype(BF16)
        block = in_ref[s].astype(F32)
        decay = block[8:9] + block[9:10]
        state = decay * state + block[0:8]


def local_kernel(query_ref, key_ref, value_ref, decay_ref, extra_ref, local_ref, start_ref):
    inside = decays(decay_ref, extra_ref)
    states, _, _ = block_states(inside, key_ref, value_ref)
    rows_at = lax.broadcasted_iota(jnp.int32, (BLOCK, BLOCK), 0)
    cols_at = lax.broadcasted_iota(jnp.int32, (BLOCK, BLOCK), 1)
    before = jnp.zeros((1, DK), F32)
    for b, cum in enumerate(inside):
        rows = pl.ds(b * BLOCK, BLOCK)
        query = query_ref[rows, :].astype(F32) * DK ** (-0.5)
        key = key_ref[rows, :].astype(F32)
        value = value_ref[rows, :].astype(F32)
        query_decay = query * jnp.exp(cum)
        scores = nt(query_decay, key * jnp.exp(-cum), precision=HIGHEST)
        scores = jnp.where(rows_at >= cols_at, scores, 0.0)
        mixed = jnp.dot(scores, value, precision=HIGHEST, preferred_element_type=F32)
        if b > 0:
            mixed = mixed + nt(query_decay, states[b], precision=HIGHEST)
        local_ref[rows, :] = mixed
        start_ref[rows, :] = query * jnp.exp(cum + before)
        before = before + cum[BLOCK - 1 : BLOCK]


def head_kernel(local_ref, start_ref, enter_ref, gate_ref, gain_ref, out_ref):
    mixed = local_ref[...] + nt(start_ref[...], enter_ref[...].astype(F32), precision=HIGHEST)
    scale = lax.rsqrt(jnp.mean(mixed * mixed, axis=-1, keepdims=True) + EPSILON)
    gate = jax.nn.silu(gate_ref[...].astype(F32))
    out_ref[...] = (mixed * scale * gain_ref[...].astype(F32) * gate).astype(BF16)


def project_kernel(ids_ref, own_ref, other_ref, weight_ref, residual_ref, out_ref):
    y, c = ids_ref[0], ids_ref[1]
    mine = pl.ds(pl.multiple_of(c * DV, DV), DV)
    theirs = pl.ds(pl.multiple_of((1 - c) * DV, DV), DV)
    own, other = own_ref[...], other_ref[...]
    residual = residual_ref[...].astype(F32)
    for k in range(0, 8, 2):
        w_mine = jnp.concatenate([weight_ref[k, mine, :], weight_ref[k + 1, mine, :]], axis=1)
        w_theirs = jnp.concatenate([weight_ref[k, theirs, :], weight_ref[k + 1, theirs, :]], axis=1)
        part = jnp.dot(own, w_mine, preferred_element_type=F32)
        part = part + jnp.dot(other, w_theirs, preferred_element_type=F32)
        for j in range(2):
            slab = part[:, j * 128 : (j + 1) * 128]
            slab = slab + residual * (y == k + j).astype(F32)
            out_ref[:, k + j] = slab.reshape(8, 32, 128).astype(BF16)


def reduce_kernel(in_ref, out_ref):
    total = in_ref[0].astype(F32)
    for s in range(1, 8):
        total = total + in_ref[s].astype(F32)
    mid = total.astype(BF16)
    for dest in range(8):
        for q in range(4):
            out_ref[dest, q] = mid[2 * q + dest % 2]


def routing_kernel(ids_ref, routing_ref, score_ref, pick_ref, high_ref, low_ref):
    group = ids_ref[2]
    experts = lax.broadcasted_iota(jnp.int32, (TOK, 128), 1)
    hot = [(routing_ref[:, k : k + 1] == experts).astype(F32) for k in range(4)]
    named = hot[0] + hot[1] + hot[2] + hot[3]
    rows = lax.broadcasted_iota(jnp.int32, (TOK, TOK), 0)
    cols = lax.broadcasted_iota(jnp.int32, (TOK, TOK), 1)
    earlier = (rows > cols).astype(BF16)
    ranks = jnp.dot(earlier, named.astype(BF16), preferred_element_type=F32)
    scores = [score_ref[:, k : k + 1] for k in range(4)]
    total = scores[0] + scores[1] + scores[2] + scores[3]
    slots = lax.broadcasted_iota(jnp.int32, (TOK, SLOTS), 1)
    picked = jnp.zeros((TOK, SLOTS), F32)
    weighted = jnp.zeros((TOK, SLOTS), F32)
    for k in range(4):
        expert = routing_ref[:, k : k + 1]
        rank = jnp.sum(hot[k] * ranks, axis=1, keepdims=True).astype(jnp.int32)
        place = lax.shift_right_logical(expert, 2) * MOST + rank
        place = jnp.where((expert & 3) == group, place, -1)
        here = (place == slots).astype(F32)
        picked = picked + here
        weighted = weighted + here * (ROUTE_SCALE * scores[k] / total)
    pick_ref[...] = picked.T.astype(BF16)
    high = weighted.astype(BF16)
    high_ref[...] = high
    low_ref[...] = (weighted - high.astype(F32)).astype(BF16)


def dispatch_kernel(pick_ref, mid_ref, out_ref, wide_ref):
    pick = pick_ref[...]
    for q in range(4):
        tile = mid_ref[:, q].reshape(TOK, 128)
        wide_ref[pl.ds(q, SLOTS, stride=4), :] = jnp.dot(pick, tile, preferred_element_type=F32)
    out_ref[...] = wide_ref[...].astype(BF16)


def expert_kernel(ids_ref, x0, x1, x2, x3, gate_ref, up_ref, gain_ref, out_ref, wide_ref, rows_ref):
    part = ids_ref[3]
    squares = jnp.zeros((SLOTS, 128), F32)
    for m, x_ref in enumerate((x0, x1, x2, x3)):
        wide_ref[...] = x_ref[...].astype(F32)
        for q in range(4):
            slab = q * 4 + (part ^ m)
            tile = wide_ref[pl.ds(q, SLOTS, stride=4), :]
            squares = squares + tile * tile
            scaled = (tile * gain_ref[pl.ds(slab, 1), :]).astype(BF16)
            rows_ref[:, pl.ds(pl.multiple_of(slab * 128, 128), 128)] = scaled
    scale = lax.rsqrt(jnp.sum(squares, axis=1, keepdims=True) * (1.0 / D) + EPSILON)
    gate = jnp.dot(rows_ref[...], gate_ref[...], preferred_element_type=F32) * scale
    up = jnp.dot(rows_ref[...], up_ref[...], preferred_element_type=F32) * scale
    out_ref[...] = (jax.nn.silu(gate) * up).astype(BF16)


def down_kernel(ids_ref, h0, h1, h2, h3, down_ref, out_ref, wide_ref):
    part = ids_ref[3]
    total = jnp.dot(h0[...], down_ref[part], preferred_element_type=F32)
    for m, h_ref in ((1, h1), (2, h2), (3, h3)):
        total = total + jnp.dot(h_ref[...], down_ref[part ^ m], preferred_element_type=F32)
    for q in range(4):
        wide_ref[pl.ds(q, SLOTS, stride=4), :] = total[:, q * 128 : (q + 1) * 128]
    out_ref[...] = wide_ref[...].astype(BF16)


def shared_in_kernel(ids_ref, mid_ref, weight_ref, gain_ref, out_ref):
    part = ids_ref[3]
    squares = jnp.zeros((TOK, 128), F32)
    pre = jnp.zeros((TOK, 256), F32)
    for q in range(4):
        tile = mid_ref[:, q].reshape(TOK, 128).astype(F32)
        squares = squares + tile * tile
        scaled = (tile * gain_ref[pl.ds(q * 4 + part, 1), :]).astype(BF16)
        weight = jnp.concatenate(
            [weight_ref[p, q, 0:32, :] for p in range(4)]
            + [weight_ref[p, q, 32:64, :] for p in range(4)],
            axis=0,
        )
        pre = pre + nt(scaled, weight)
    out_ref[:, 0:256] = pre.astype(BF16)
    ssq = jnp.sum(squares, axis=1, keepdims=True)
    high = ssq.astype(BF16).astype(F32)
    lane = lax.broadcasted_iota(jnp.int32, (TOK, 128), 1)
    tail = jnp.where(lane == 0, high, jnp.where(lane == 1, ssq - high, 0.0))
    out_ref[:, 256:384] = tail.astype(BF16)


def shared_hidden_kernel(in_ref, out_ref):
    total = in_ref[0].astype(F32)
    for s in range(1, 4):
        total = total + in_ref[s].astype(F32)
    ssq = jnp.sum(total[:, 256:384], axis=1, keepdims=True)
    scale = lax.rsqrt(ssq * (1.0 / D) + EPSILON)
    hidden = jax.nn.silu(total[:, 0:128] * scale) * (total[:, 128:256] * scale)
    hidden = hidden.astype(BF16)
    for dest in range(4):
        out_ref[dest] = hidden


def combine_kernel(back_ref, high_ref, low_ref, hidden_ref, down_ref, out_ref, wide_ref):
    wide_ref[...] = back_ref[...].astype(F32)
    hidden = hidden_ref[...].reshape(TOK, 128)
    for q in range(4):
        tile = wide_ref[pl.ds(q, SLOTS, stride=4), :].astype(BF16)
        total = jnp.dot(high_ref[...], tile, preferred_element_type=F32)
        total = total + jnp.dot(low_ref[...], tile, preferred_element_type=F32)
        total = total + jnp.dot(hidden, down_ref[q], preferred_element_type=F32)
        out_ref[q] = total.astype(BF16)


def final_kernel(ids_ref, in_ref, mid_ref, out_ref):
    group = ids_ref[2]
    total = mid_ref[:, group].reshape(TOK, 128).astype(F32)
    for s in range(4):
        total = total + in_ref[s].astype(F32)
    out_ref[...] = total.astype(BF16)


def exchange(value, axes):
    return lax.all_to_all(value, axes, split_axis=0, concat_axis=0, tiled=True)


def swapped(value, axis):
    return lax.ppermute(value, axis, [(0, 1), (1, 0)])


def body(
    queries,
    key_matrix,
    value_matrix,
    output_gate_preactivation,
    decay_preactivation,
    extra_log_decay,
    head_norm_gain,
    output_projection,
    residual,
    feedforward_gain,
    routing,
    router_score,
    expert_gate_weight,
    expert_up_weight,
    expert_down_weight,
    shared_expert_gate,
    shared_expert_up,
    shared_expert_down,
):
    y, c, g, p = (lax.axis_index(a) for a in (Y, "c", "yg", GROUP))
    ids = jnp.stack([y, c, g, p]).astype(jnp.int32)
    gain = feedforward_gain.astype(F32).reshape(16, 128)
    head_gain = head_norm_gain.reshape(1, DV)

    payload = call(
        state_kernel, ((32, 16, DK), BF16),
        key_matrix, value_matrix, decay_preactivation, extra_log_decay,
    )
    weights = exchange(output_projection.reshape(8, 512, 128), Y)
    payload, down, gate_t, up_t, shared_down = lax.optimization_barrier(
        (payload, expert_down_weight, shared_expert_gate, shared_expert_up, shared_expert_down)
    )
    states = exchange(payload, SP)
    local, start = call(
        local_kernel, [((TOK, DV), F32), ((TOK, DK), F32)],
        queries, key_matrix, value_matrix, decay_preactivation, extra_log_decay,
    )
    down = exchange(
        down.reshape(256, 4, 4, 128).transpose(2, 0, 1, 3).reshape(4, 256, 512), GROUP
    )
    shared_in = jnp.concatenate(
        [w.T.reshape(32, 4, 4, 128).transpose(2, 1, 0, 3) for w in (gate_t, up_t)], axis=2
    )
    shared_in = exchange(shared_in, GROUP)
    shared_down = exchange(shared_down.reshape(4, 128, 128), "yg")
    pick, high, low = call(
        routing_kernel,
        [((SLOTS, TOK), BF16), ((TOK, SLOTS), BF16), ((TOK, SLOTS), BF16)],
        ids, routing, router_score, smem=1,
    )

    entering = exchange(call(scan_kernel, ((32, 8, DK), BF16), states), SP).reshape(DV, DK)
    head_rows = call(
        head_kernel, ((TOK, DV), BF16),
        local, start, entering, output_gate_preactivation, head_gain,
    )
    partial = call(
        project_kernel, ((8, 8, 32, 128), BF16),
        ids, head_rows, swapped(head_rows, "c"), weights, residual, smem=1,
    )
    mid_send = call(reduce_kernel, ((8, 4, 32, 128), BF16), exchange(partial, Y))
    mid = exchange(mid_send, Y)

    outgoing = call(
        dispatch_kernel, ((4 * SLOTS, 128), BF16), pick, mid,
        scratch=[pltpu.VMEM((4 * SLOTS, 128), F32)],
    )
    own = exchange(outgoing.reshape(32, 48, 128), SP).reshape(4 * SLOTS, 128)

    pre = call(
        shared_in_kernel, ((TOK, 384), BF16), ids, mid, shared_in, gain, smem=1,
    )
    hidden = call(
        shared_hidden_kernel, ((4, 64, 128), BF16), exchange(pre.reshape(4, 64, 384), GROUP)
    )
    hidden = exchange(hidden, GROUP)

    across = swapped(own, "yn")
    beside = swapped(own, "c")
    rows_far = swapped(across, "c")
    routed = call(
        expert_kernel, ((SLOTS, 256), BF16),
        ids, own, beside, across, rows_far, expert_gate_weight, expert_up_weight, gain,
        smem=1,
        scratch=[pltpu.VMEM((4 * SLOTS, 128), F32), pltpu.VMEM((SLOTS, D), BF16)],
    )
    routed_across = swapped(routed, "yn")
    routed_beside = swapped(routed, "c")
    routed_far = swapped(routed_across, "c")
    expert_out = call(
        down_kernel, ((4 * SLOTS, 128), BF16),
        ids, routed, routed_beside, routed_across, routed_far, down,
        smem=1, scratch=[pltpu.VMEM((4 * SLOTS, 128), F32)],
    )
    back = exchange(expert_out.reshape(32, 48, 128), SP).reshape(4 * SLOTS, 128)
    sums = call(
        combine_kernel, ((4, TOK, 128), BF16),
        back, high, low, hidden, shared_down,
        scratch=[pltpu.VMEM((4 * SLOTS, 128), F32)],
    )
    return call(final_kernel, ((TOK, 128), BF16), ids, exchange(sums, "yg"), mid, smem=1)


def solution(mesh):
    finer = Mesh(mesh.devices.reshape(8, 4, 4, 2, 2), ("z", "x", "yg", "yn", "c"))
    in_specs = (
        P(SP, TP),
        P(SP, TP),
        P(SP, TP),
        P(SP, TP),
        P(SP, TP),
        P(SP, TP),
        P(),
        P(None, TP),
        P(SP, TP),
        P(),
        P(SP, None),
        P(SP, None),
        P(None, SP + TP),
        P(None, SP + TP),
        P(SP + TP, None),
        P(None, TP),
        P(None, TP),
        P(None, TP),
    )
    return jax.shard_map(
        body, mesh=finer, in_specs=in_specs, out_specs=P(SP, TP), check_vma=False
    )
```

time: 349 us -> 245 us (0.70)
  waiting for transfers between devices: 135 us -> 75.1 us
  starting transfers between devices: 25.5 us -> 63.4 us
  blocking collectives: 105 us -> 76.2 us
  local copies, waits for them, and re-layouts: 33.1 us -> 9.83 us
  matrix products: 18 us -> 0 us
  other arithmetic: 16.9 us -> 0.82 us
  Pallas kernels: 0 us -> 15.9 us
  between operations: 14.1 us -> 0.35 us
    all_gather x5 -> x0, blocking collectives: 78.1 us -> none  [the longest x4 58.2 us: prefix_by_axis(): lax.all_gather(part.astype(kind), axis)]
    all_gather x1 -> x0, waiting for transfers between devices: 53.5 us -> none  [body(): lax.all_gather(head_rows, 'tp', axis=1, tiled=True)]
    all_to_all x1 -> x5, blocking collectives: 27.1 us -> 76.2 us  [exchange(): return lax.all_to_all(value, axes, split_axis=0, concat_axis=0, tiled=True)]
    all_to_all x2 -> x8, starting transfers between devices: 9.44 us -> 41.6 us  [exchange(): return lax.all_to_all(value, axes, split_axis=0, concat_axis=0, tiled=True)]
    ppermute x6 -> x7, waiting for transfers between devices: 42.8 us -> 21.6 us  [swapped(): return lax.ppermute(value, axis, [(0, 1), (1, 0)])]
    dot_general x12 -> x0, matrix products: 18 us -> none  [the longest x1 5.15 us: body(): jnp.dot(routed_hidden, expert_down_weight, preferred_element_type=jnp.flo...]
    pallas_call x0 -> x14, Pallas kernels: none -> 15.9 us  [call(): pl.pallas_call(kernel, out_shape=shapes, in_specs=[SMEM] * smem + [VMEM]...]
    all_to_all x2 -> x8, waiting for transfers between devices: 38.4 us -> 53.5 us  [exchange(): return lax.all_to_all(value, axes, split_axis=0, concat_axis=0, tiled=True)]
  transfers between devices with their start and end apart: 9 -> 15, of which waited for: 8 -> 10; matrix products, arithmetic and copies ran while one was open for 2% -> 2% of each run, Pallas kernels for 0% -> 5%
where the time goes in v1:
time: 245 us; the launch traced here: 242 us
  blocking collectives  76.2 us (31%)
  waiting for transfers between devices  75.1 us (31%)
  starting transfers between devices  63.4 us (26%)
  Pallas kernels  15.9 us (6%)
  local copies, waits for them, and re-layouts  9.83 us (4%)
    all_to_all x5, blocking collectives, exchange(): return lax.all_to_all(value, axes, split_axis=0, concat_axis=0, tiled=True)  76.2 us
    all_to_all x8, waiting for transfers between devices, exchange(): return lax.all_to_all(value, axes, split_axis=0, concat_axis=0, tiled=True)  53.5 us
    all_to_all x8, starting transfers between devices, exchange(): return lax.all_to_all(value, axes, split_axis=0, concat_axis=0, tiled=True)  41.6 us
    ppermute x7, starting transfers between devices, swapped(): return lax.ppermute(value, axis, [(0, 1), (1, 0)])  21.8 us
    ppermute x7, waiting for transfers between devices, swapped(): return lax.ppermute(value, axis, [(0, 1), (1, 0)])  21.6 us
    pallas_call x14, Pallas kernels, call(): pl.pallas_call(kernel, out_shape=shapes, in_specs=[SMEM] * smem + [VMEM]...  15.9 us
    unnamed x39, local copies, waits for them, and re-layouts  6.17 us
  transfers between devices with their start and end apart: 15, of which 10 were waited for; matrix products, arithmetic and copies ran while one was open for 2% of the time, Pallas kernels for 5%

profile of v1, /device:TPU:1, one launch (start us, length us, event | category | flops | bytes accessed | tf_op | source)
XLA Modules:
  0.0 241.7 jit_solution(12492555121784822107)
XLA Ops:
  0.0 0.8 copy.26.extra_ref
  0.9 0.1 copy-done.2
  0.9 0.8 copy-done.3
  1.8 0.8 copy-done.5
  2.6 0.8 state_kernel.1
  3.5 22.8 %all_to_all.65.in_ref = bf16[32,16,128]{2,1,0:T(8,128)(2,1)S(1)} all-to-all(bf16[32,16,128]{2,1,0:T(8,128)(2,1)S(1)} %state_kernel.1), channel_id=1, replica_groups=mesh['z'=8,'x'=4,'yg'=4,'yn'=2,'c'=2] {'z','x'}, dimensions={0} | all-to-all | bytes 262144 | tf_op jit(solution)/shard_map/all_to_all | solution.py:275
  26.3 0.1 scan_kernel.1
  26.4 12.1 %all_to_all.66 = bf16[32,8,128]{2,1,0:T(8,128)(2,1)S(1)} all-to-all(bf16[32,8,128]{2,1,0:T(8,128)(2,1)S(1)} %scan_kernel.1), channel_id=1, replica_groups=mesh['z'=8,'x'=4,'yg'=4,'yn'=2,'c'=2] {'z','x'}, dimensions={0} | all-to-all | bytes 131072 | tf_op jit(solution)/shard_map/all_to_all | solution.py:275
  38.5 7.0 %all-to-all-start.2 = ((bf16[8,512,128]{2,1,0:T(8,128)(2,1)}), bf16[8,512,128]{2,1,0:T(8,128)(2,1)S(1)}, u32[]{:S(2)}, u32[]{:S(2)}) async-start(bf16[8,512,128]{2,1,0:T(8,128)(2,1)} %bitcast.5), calls=%async_computation.2 | async-start | bytes 2097152 | tf_op jit(solution)/shard_map/all_to_all | solution.py:275
  45.5 0.0 copy-start.9
  45.5 1.8 local_kernel.1
  47.4 0.0 copy-start.11
  47.4 0.5 head_kernel.1.own_ref
  47.9 5.4 %collective-permute-start = (bf16[256,256]{1,0:T(8,128)(2,1)S(1)}, bf16[256,256]{1,0:T(8,128)(2,1)S(1)}, u32[]{:S(2)}, u32[]{:S(2)}) collective-permute-start(bf16[256,256]{1,0:T(8,128)(2,1)S(1)} %head_kernel.1.own_ref), channel_id=1, source_target_pairs={{0,1},{1,0},{2,3},{3,2},{4,5},{5,4},{6,7},{7,6},{8,9},{9,8},{10,11... | collective-permute-start | bytes 393224 | tf_op jit(solution)/shard_map/ppermute | solution.py:279
  53.3 0.1 pad_add_fusion.ids_ref
  53.4 0.9 collective-permute-done.other_ref
  54.3 17.8 %all-to-all-done.2.weight_ref = bf16[8,512,128]{2,1,0:T(8,128)(2,1)S(1)} async-done(((bf16[8,512,128]{2,1,0:T(8,128)(2,1)}), bf16[8,512,128]{2,1,0:T(8,128)(2,1)S(1)}, u32[]{:S(2)}, u32[]{:S(2)}) %all-to-all-start.2) | async-done | bytes 1048608 | tf_op jit(solution)/shard_map/all_to_all | solution.py:275
  72.0 1.8 project_kernel.1
  73.8 3.6 %all-to-all-start.3 = ((bf16[8,8,32,128]{3,2,1,0:T(8,128)(2,1)}), bf16[8,8,32,128]{3,2,1,0:T(8,128)(2,1)S(1)}, u32[]{:S(2)}, u32[]{:S(2)}) async-start(bf16[8,8,32,128]{3,2,1,0:T(8,128)(2,1)} %project_kernel.1), calls=%async_computation.3 | async-start | bytes 1048576 | tf_op jit(solution)/shard_map/all_to_all | solution.py:275
  77.4 0.1 reshape.55
  77.5 0.8 copy-done.13
  78.3 0.1 reshape.56
  78.4 0.1 copy_bitcast_fusion.1
  78.5 0.7 pad_maximum_fusion
  79.2 12.5 %all-to-all-done.3.in_ref = bf16[8,8,32,128]{3,2,1,0:T(8,128)(2,1)S(1)} async-done(((bf16[8,8,32,128]{3,2,1,0:T(8,128)(2,1)}), bf16[8,8,32,128]{3,2,1,0:T(8,128)(2,1)S(1)}, u32[]{:S(2)}, u32[]{:S(2)}) %all-to-all-start.3) | async-done | bytes 524320 | tf_op jit(solution)/shard_map/all_to_all | solution.py:275
  91.7 7.5 %all-to-all-start.8 = ((bf16[4,4,64,128]{3,2,1,0:T(8,128)(2,1)}), bf16[4,4,64,128]{3,2,1,0:T(8,128)(2,1)S(1)}, u32[]{:S(2)}, u32[]{:S(2)}) async-start(bf16[4,4,64,128]{3,2,1,0:T(8,128)(2,1)} %pad_maximum_fusion), calls=%async_computation.8 | async-start | bytes 524288 | tf_op jit(solution)/shard_map/all_to_all | solution.py:275
  99.2 0.1 reduce_kernel.1
  99.2 5.0 %all-to-all-done.8.weight_ref = bf16[4,4,64,128]{3,2,1,0:T(8,128)(2,1)S(1)} async-done(((bf16[4,4,64,128]{3,2,1,0:T(8,128)(2,1)}), bf16[4,4,64,128]{3,2,1,0:T(8,128)(2,1)S(1)}, u32[]{:S(2)}, u32[]{:S(2)}) %all-to-all-start.8) | async-done | bytes 262176 | tf_op jit(solution)/shard_map/all_to_all | solution.py:275
  104.2 12.9 %all_to_all.67.mid_ref = bf16[8,4,32,128]{3,2,1,0:T(8,128)(2,1)S(1)} all-to-all(bf16[8,4,32,128]{3,2,1,0:T(8,128)(2,1)S(1)} %reduce_kernel.1), channel_id=1, replica_groups=mesh['z'=8,'x'=4,'yg'=4,'yn'=2,'c'=2] {'yg','yn'}, dimensions={0} | all-to-all | bytes 524288 | tf_op jit(solution)/shard_map/all_to_all | solution.py:275
  117.1 3.5 %all-to-all-start.11 = ((bf16[4,128,128]{2,1,0:T(8,128)(2,1)}), bf16[4,128,128]{2,1,0:T(8,128)(2,1)S(1)}, u32[]{:S(2)}, u32[]{:S(2)}) async-start(bf16[4,128,128]{2,1,0:T(8,128)(2,1)} %bitcast.18), calls=%async_computation.11 | async-start | bytes 262144 | tf_op jit(solution)/shard_map/all_to_all | solution.py:275
  120.6 1.5 shared_in_kernel.1
  122.1 5.7 %all-to-all-done.11.down_ref = bf16[4,128,128]{2,1,0:T(8,128)(2,1)S(1)} async-done(((bf16[4,128,128]{2,1,0:T(8,128)(2,1)}), bf16[4,128,128]{2,1,0:T(8,128)(2,1)S(1)}, u32[]{:S(2)}, u32[]{:S(2)}) %all-to-all-start.11) | async-done | bytes 131104 | tf_op jit(solution)/shard_map/all_to_all | solution.py:275
  127.9 7.2 %all-to-all-start.9 = ((bf16[4,64,384]{2,1,0:T(8,128)(2,1)}), bf16[4,64,384]{2,1,0:T(8,128)(2,1)S(1)}, u32[]{:S(2)}, u32[]{:S(2)}) async-start(bf16[4,64,384]{2,1,0:T(8,128)(2,1)} %bitcast.17), calls=%async_computation.9 | async-start | bytes 393216 | tf_op jit(solution)/shard_map/all_to_all | solution.py:275
  135.1 0.1 copy.24.routing_ref
  135.2 0.5 copy-done.16
  135.7 0.1 copy.25.score_ref
  135.9 2.0 routing_kernel.1
  137.9 0.7 copy-done.7
  138.6 1.2 dispatch_kernel.1
  139.8 3.9 %all-to-all-start.5 = ((bf16[32,48,128]{2,1,0:T(8,128)(2,1)}), bf16[32,48,128]{2,1,0:T(8,128)(2,1)S(1)}, u32[]{:S(2)}, u32[]{:S(2)}) async-start(bf16[32,48,128]{2,1,0:T(8,128)(2,1)} %bitcast.6), calls=%async_computation.5 | async-start | bytes 786432 | tf_op jit(solution)/shard_map/all_to_all | solution.py:275
  143.6 1.8 reshape.51
  145.4 0.4 copy.34
  145.8 1.2 reshape.52
  147.1 10.5 %all-to-all-done.5 = bf16[32,48,128]{2,1,0:T(8,128)(2,1)S(1)} async-done(((bf16[32,48,128]{2,1,0:T(8,128)(2,1)}), bf16[32,48,128]{2,1,0:T(8,128)(2,1)S(1)}, u32[]{:S(2)}, u32[]{:S(2)}) %all-to-all-start.5) | async-done | bytes 393248 | tf_op jit(solution)/shard_map/all_to_all | solution.py:275
  157.6 5.7 %all-to-all-start.6 = ((bf16[4,256,512]{2,1,0:T(8,128)(2,1)}), bf16[4,256,512]{2,1,0:T(8,128)(2,1)S(1)}, u32[]{:S(2)}, u32[]{:S(2)}) async-start(bf16[4,256,512]{2,1,0:T(8,128)(2,1)} %reshape.52), calls=%async_computation.6 | async-start | bytes 2097152 | tf_op jit(solution)/shard_map/all_to_all | solution.py:275
  163.3 3.3 %collective-permute-start.2 = (bf16[1536,128]{1,0:T(8,128)(2,1)S(1)}, bf16[1536,128]{1,0:T(8,128)(2,1)S(1)}, u32[]{:S(2)}, u32[]{:S(2)}) collective-permute-start(bf16[1536,128]{1,0:T(8,128)(2,1)S(1)} %bitcast.24), channel_id=1, source_target_pairs={{0,2},{2,0},{1,3},{3,1},{4,6},{6,4},{5,7},{7,5},{8,10},{10,8},{9,1... | collective-permute-start | bytes 1179656 | tf_op jit(solution)/shard_map/ppermute | solution.py:279
  166.6 2.6 %collective-permute-start.1 = (bf16[1536,128]{1,0:T(8,128)(2,1)S(1)}, bf16[1536,128]{1,0:T(8,128)(2,1)S(1)}, u32[]{:S(2)}, u32[]{:S(2)}) collective-permute-start(bf16[1536,128]{1,0:T(8,128)(2,1)S(1)} %bitcast.25), channel_id=1, source_target_pairs={{0,1},{1,0},{2,3},{3,2},{4,5},{5,4},{6,7},{7,6},{8,9},{9,8},{10,11... | collective-permute-start | bytes 1179656 | tf_op jit(solution)/shard_map/ppermute | solution.py:279
  169.2 16.0 %collective-permute-done.2.x2 = bf16[1536,128]{1,0:T(8,128)(2,1)S(1)} collective-permute-done((bf16[1536,128]{1,0:T(8,128)(2,1)S(1)}, bf16[1536,128]{1,0:T(8,128)(2,1)S(1)}, u32[]{:S(2)}, u32[]{:S(2)}) %collective-permute-start.2) | collective-permute-done | bytes 393248 | tf_op jit(solution)/shard_map/ppermute | solution.py:279
  185.2 2.9 %collective-permute-start.3 = (bf16[1536,128]{1,0:T(8,128)(2,1)S(1)}, bf16[1536,128]{1,0:T(8,128)(2,1)S(1)}, u32[]{:S(2)}, u32[]{:S(2)}) collective-permute-start(bf16[1536,128]{1,0:T(8,128)(2,1)S(1)} %collective-permute-done.2.x2), channel_id=1, source_target_pairs={{0,1},{1,0},{2,3},{3,2},{4,5},{5,4},{6,7},{7,6},{8,9},{9,8},{10,11... | collective-permute-start | bytes 1179656 | tf_op jit(solution)/shard_map/ppermute | solution.py:279
  188.1 1.3 collective-permute-done.3.x3
  189.4 1.2 copy-done.1
  190.7 2.4 expert_kernel.1.h0
  193.1 2.0 collective-permute-start.5
  195.1 2.6 %collective-permute-start.4 = (bf16[384,256]{1,0:T(8,128)(2,1)S(1)}, bf16[384,256]{1,0:T(8,128)(2,1)S(1)}, u32[]{:S(2)}, u32[]{:S(2)}) collective-permute-start(bf16[384,256]{1,0:T(8,128)(2,1)S(1)} %expert_kernel.1.h0), channel_id=1, source_target_pairs={{0,1},{1,0},{2,3},{3,2},{4,5},{5,4},{6,7},{7,6},{8,9},{9,8},{10,11... | collective-permute-start | bytes 589832 | tf_op jit(solution)/shard_map/ppermute | solution.py:279
  197.7 3.4 %collective-permute-done.5.h2 = bf16[384,256]{1,0:T(8,128)(2,1)S(1)} collective-permute-done((bf16[384,256]{1,0:T(8,128)(2,1)S(1)}, bf16[384,256]{1,0:T(8,128)(2,1)S(1)}, u32[]{:S(2)}, u32[]{:S(2)}) %collective-permute-start.5) | collective-permute-done | bytes 196640 | tf_op jit(solution)/shard_map/ppermute | solution.py:279
  201.1 3.1 %collective-permute-start.6 = (bf16[384,256]{1,0:T(8,128)(2,1)S(1)}, bf16[384,256]{1,0:T(8,128)(2,1)S(1)}, u32[]{:S(2)}, u32[]{:S(2)}) collective-permute-start(bf16[384,256]{1,0:T(8,128)(2,1)S(1)} %collective-permute-done.5.h2), channel_id=1, source_target_pairs={{0,1},{1,0},{2,3},{3,2},{4,5},{5,4},{6,7},{7,6},{8,9},{9,8},{10,11... | collective-permute-start | bytes 589832 | tf_op jit(solution)/shard_map/ppermute | solution.py:279
  204.2 0.7 shared_hidden_kernel.1
  204.9 3.3 %all-to-all-start.10 = ((bf16[4,64,128]{2,1,0:T(8,128)(2,1)}), bf16[4,64,128]{2,1,0:T(8,128)(2,1)S(1)}, u32[]{:S(2)}, u32[]{:S(2)}) async-start(bf16[4,64,128]{2,1,0:T(8,128)(2,1)} %shared_hidden_kernel.1), calls=%async_computation.10 | async-start | bytes 131072 | tf_op jit(solution)/shard_map/all_to_all | solution.py:275
  208.2 1.2 down_kernel.1
  209.4 2.1 all-to-all-done.10.hidden_ref
  211.5 17.8 %all_to_all.68 = bf16[32,48,128]{2,1,0:T(8,128)(2,1)S(1)} all-to-all(bf16[32,48,128]{2,1,0:T(8,128)(2,1)S(1)} %bitcast.27), channel_id=1, replica_groups=mesh['z'=8,'x'=4,'yg'=4,'yn'=2,'c'=2] {'z','x'}, dimensions={0} | all-to-all | bytes 786432 | tf_op jit(solution)/shard_map/all_to_all | solution.py:275
  229.3 0.7 combine_kernel.1
  230.0 10.5 %all_to_all.69.in_ref = bf16[4,256,128]{2,1,0:T(8,128)(2,1)S(1)} all-to-all(bf16[4,256,128]{2,1,0:T(8,128)(2,1)S(1)} %combine_kernel.1), channel_id=1, replica_groups=mesh['z'=8,'x'=4,'yg'=4,'yn'=2,'c'=2] {'yg'}, dimensions={0} | all-to-all | bytes 524288 | tf_op jit(solution)/shard_map/all_to_all | solution.py:275
  240.5 1.2 final_kernel.1
  (34 shorter events, 0.1 us)
Async XLA Ops:
  0.0 0.9 copy-start.2
  0.9 0.8 copy-start.3
  1.8 0.8 copy-start.5
  38.5 7.0 %copy-start.17 = (bf16[256]{0:T(256)(128)(2,1)S(1)}, bf16[256]{0:T(256)(128)(2,1)}, u32[]{:S(2)}) copy-start(bf16[256]{0:T(256)(128)(2,1)} %param.24) | copy-start | bytes 1540
  38.5 7.0 %copy-start.4 = (bf16[256,128]{1,0:T(8,128)(2,1)S(1)}, bf16[256,128]{1,0:T(8,128)(2,1)}, u32[]{:S(2)}) copy-start(bf16[256,128]{1,0:T(8,128)(2,1)} %key_ref.3) | copy-start | bytes 196612
  38.5 7.0 %copy-start.6 = (bf16[256,128]{1,0:T(8,128)(2,1)S(1)}, bf16[256,128]{1,0:T(8,128)(2,1)}, u32[]{:S(2)}) copy-start(bf16[256,128]{1,0:T(8,128)(2,1)} %decay_ref.3) | copy-start | bytes 196612
  38.5 7.0 %copy-start.10 = (bf16[256,128]{1,0:T(8,128)(2,1)S(1)}, bf16[256,128]{1,0:T(8,128)(2,1)}, u32[]{:S(2)}) copy-start(bf16[256,128]{1,0:T(8,128)(2,1)} %query_ref.1) | copy-start | bytes 196612
  38.5 33.5 %all-to-all-start.2 = ((bf16[8,512,128]{2,1,0:T(8,128)(2,1)}), bf16[8,512,128]{2,1,0:T(8,128)(2,1)S(1)}, u32[]{:S(2)}, u32[]{:S(2)}) async-start(bf16[8,512,128]{2,1,0:T(8,128)(2,1)} %bitcast.5), calls=%async_computation.2 | async-start | bytes 2097152 | tf_op jit(solution)/shard_map/all_to_all | solution.py:275
  45.5 1.8 copy-start.9
  47.4 24.6 %copy-start.11 = (bf16[256,128]{1,0:T(8,128)(2,1)S(1)}, bf16[256,128]{1,0:T(8,128)(2,1)}, u32[]{:S(2)}) copy-start(bf16[256,128]{1,0:T(8,128)(2,1)} %residual_ref.1) | copy-start | bytes 196612
  47.9 6.4 %collective-permute-start = (bf16[256,256]{1,0:T(8,128)(2,1)S(1)}, bf16[256,256]{1,0:T(8,128)(2,1)S(1)}, u32[]{:S(2)}, u32[]{:S(2)}) collective-permute-start(bf16[256,256]{1,0:T(8,128)(2,1)S(1)} %head_kernel.1.own_ref), channel_id=1, source_target_pairs={{0,1},{1,0},{2,3},{3,2},{4,5},{5,4},{6,7},{7,6},{8,9},{9,8},{10,11... | collective-permute-start | bytes 393224 | tf_op jit(solution)/shard_map/ppermute | solution.py:279
  73.8 3.6 %copy-start.12 = (bf16[2048,32]{0,1:T(8,128)(2,1)S(1)}, bf16[2048,32]{0,1:T(8,128)(2,1)}, u32[]{:S(2)}) copy-start(bf16[2048,32]{0,1:T(8,128)(2,1)} %param.33) | copy-start | bytes 393220
  73.8 17.9 %all-to-all-start.3 = ((bf16[8,8,32,128]{3,2,1,0:T(8,128)(2,1)}), bf16[8,8,32,128]{3,2,1,0:T(8,128)(2,1)S(1)}, u32[]{:S(2)}, u32[]{:S(2)}) async-start(bf16[8,8,32,128]{3,2,1,0:T(8,128)(2,1)} %project_kernel.1), calls=%async_computation.3 | async-start | bytes 1048576 | tf_op jit(solution)/shard_map/all_to_all | solution.py:275
  77.4 0.9 copy-start.13
  91.7 12.5 %all-to-all-start.8 = ((bf16[4,4,64,128]{3,2,1,0:T(8,128)(2,1)}), bf16[4,4,64,128]{3,2,1,0:T(8,128)(2,1)S(1)}, u32[]{:S(2)}, u32[]{:S(2)}) async-start(bf16[4,4,64,128]{3,2,1,0:T(8,128)(2,1)} %pad_maximum_fusion), calls=%async_computation.8 | async-start | bytes 524288 | tf_op jit(solution)/shard_map/all_to_all | solution.py:275
  117.1 3.5 %copy-start.14 = (bf16[2048]{0:T(1024)(128)(2,1)S(1)}, bf16[2048]{0:T(1024)(128)(2,1)}, u32[]{:S(2)}) copy-start(bf16[2048]{0:T(1024)(128)(2,1)} %param.27) | copy-start | bytes 12292
  117.1 10.8 %all-to-all-start.11 = ((bf16[4,128,128]{2,1,0:T(8,128)(2,1)}), bf16[4,128,128]{2,1,0:T(8,128)(2,1)S(1)}, u32[]{:S(2)}, u32[]{:S(2)}) async-start(bf16[4,128,128]{2,1,0:T(8,128)(2,1)} %bitcast.18), calls=%async_computation.11 | async-start | bytes 262144 | tf_op jit(solution)/shard_map/all_to_all | solution.py:275
  127.9 7.2 %copy-start.15 = (s32[256,4]{0,1:T(4,128)S(1)}, s32[256,4]{0,1:T(4,128)}, u32[]{:S(2)}) copy-start(s32[256,4]{0,1:T(4,128)} %param.28) | copy-start | bytes 12292
  127.9 11.9 %all-to-all-start.9 = ((bf16[4,64,384]{2,1,0:T(8,128)(2,1)}), bf16[4,64,384]{2,1,0:T(8,128)(2,1)S(1)}, u32[]{:S(2)}, u32[]{:S(2)}) async-start(bf16[4,64,384]{2,1,0:T(8,128)(2,1)} %bitcast.17), calls=%async_computation.9 | async-start | bytes 393216 | tf_op jit(solution)/shard_map/all_to_all | solution.py:275
  135.1 0.7 copy-start.16
  137.9 0.7 copy-start.7
  139.8 17.9 %all-to-all-start.5 = ((bf16[32,48,128]{2,1,0:T(8,128)(2,1)}), bf16[32,48,128]{2,1,0:T(8,128)(2,1)S(1)}, u32[]{:S(2)}, u32[]{:S(2)}) async-start(bf16[32,48,128]{2,1,0:T(8,128)(2,1)} %bitcast.6), calls=%async_computation.5 | async-start | bytes 786432 | tf_op jit(solution)/shard_map/all_to_all | solution.py:275
  147.1 42.3 %copy-start = (bf16[2048,256]{1,0:T(8,128)(2,1)S(1)}, bf16[2048,256]{1,0:T(8,128)(2,1)}, u32[]{:S(2)}) copy-start(bf16[2048,256]{1,0:T(8,128)(2,1)} %gate_ref.3) | copy-start | bytes 3145732
  157.6 47.3 %all-to-all-start.6 = ((bf16[4,256,512]{2,1,0:T(8,128)(2,1)}), bf16[4,256,512]{2,1,0:T(8,128)(2,1)S(1)}, u32[]{:S(2)}, u32[]{:S(2)}) async-start(bf16[4,256,512]{2,1,0:T(8,128)(2,1)} %reshape.52), calls=%async_computation.6 | async-start | bytes 2097152 | tf_op jit(solution)/shard_map/all_to_all | solution.py:275
  163.3 21.9 %collective-permute-start.2 = (bf16[1536,128]{1,0:T(8,128)(2,1)S(1)}, bf16[1536,128]{1,0:T(8,128)(2,1)S(1)}, u32[]{:S(2)}, u32[]{:S(2)}) collective-permute-start(bf16[1536,128]{1,0:T(8,128)(2,1)S(1)} %bitcast.24), channel_id=1, source_target_pairs={{0,2},{2,0},{1,3},{3,1},{4,6},{6,4},{5,7},{7,5},{8,10},{10,8},{9,1... | collective-permute-start | bytes 1179656 | tf_op jit(solution)/shard_map/ppermute | solution.py:279
  166.6 21.5 %collective-permute-start.1 = (bf16[1536,128]{1,0:T(8,128)(2,1)S(1)}, bf16[1536,128]{1,0:T(8,128)(2,1)S(1)}, u32[]{:S(2)}, u32[]{:S(2)}) collective-permute-start(bf16[1536,128]{1,0:T(8,128)(2,1)S(1)} %bitcast.25), channel_id=1, source_target_pairs={{0,1},{1,0},{2,3},{3,2},{4,5},{5,4},{6,7},{7,6},{8,9},{9,8},{10,11... | collective-permute-start | bytes 1179656 | tf_op jit(solution)/shard_map/ppermute | solution.py:279
  185.2 4.2 %collective-permute-start.3 = (bf16[1536,128]{1,0:T(8,128)(2,1)S(1)}, bf16[1536,128]{1,0:T(8,128)(2,1)S(1)}, u32[]{:S(2)}, u32[]{:S(2)}) collective-permute-start(bf16[1536,128]{1,0:T(8,128)(2,1)S(1)} %collective-permute-done.2.x2), channel_id=1, source_target_pairs={{0,1},{1,0},{2,3},{3,2},{4,5},{5,4},{6,7},{7,6},{8,9},{9,8},{10,11... | collective-permute-start | bytes 1179656 | tf_op jit(solution)/shard_map/ppermute | solution.py:279
  189.4 1.2 copy-start.1
  193.1 8.0 %collective-permute-start.5 = (bf16[384,256]{1,0:T(8,128)(2,1)S(1)}, bf16[384,256]{1,0:T(8,128)(2,1)S(1)}, u32[]{:S(2)}, u32[]{:S(2)}) collective-permute-start(bf16[384,256]{1,0:T(8,128)(2,1)S(1)} %expert_kernel.1.h0), channel_id=1, source_target_pairs={{0,2},{2,0},{1,3},{3,1},{4,6},{6,4},{5,7},{7,5},{8,10},{10,8},{9,1... | collective-permute-start | bytes 589832 | tf_op jit(solution)/shard_map/ppermute | solution.py:279
  195.1 13.1 %collective-permute-start.4 = (bf16[384,256]{1,0:T(8,128)(2,1)S(1)}, bf16[384,256]{1,0:T(8,128)(2,1)S(1)}, u32[]{:S(2)}, u32[]{:S(2)}) collective-permute-start(bf16[384,256]{1,0:T(8,128)(2,1)S(1)} %expert_kernel.1.h0), channel_id=1, source_target_pairs={{0,1},{1,0},{2,3},{3,2},{4,5},{5,4},{6,7},{7,6},{8,9},{9,8},{10,11... | collective-permute-start | bytes 589832 | tf_op jit(solution)/shard_map/ppermute | solution.py:279
  201.1 7.2 %collective-permute-start.6 = (bf16[384,256]{1,0:T(8,128)(2,1)S(1)}, bf16[384,256]{1,0:T(8,128)(2,1)S(1)}, u32[]{:S(2)}, u32[]{:S(2)}) collective-permute-start(bf16[384,256]{1,0:T(8,128)(2,1)S(1)} %collective-permute-done.5.h2), channel_id=1, source_target_pairs={{0,1},{1,0},{2,3},{3,2},{4,5},{5,4},{6,7},{7,6},{8,9},{9,8},{10,11... | collective-permute-start | bytes 589832 | tf_op jit(solution)/shard_map/ppermute | solution.py:279
  204.9 6.5 %all-to-all-start.10 = ((bf16[4,64,128]{2,1,0:T(8,128)(2,1)}), bf16[4,64,128]{2,1,0:T(8,128)(2,1)S(1)}, u32[]{:S(2)}, u32[]{:S(2)}) async-start(bf16[4,64,128]{2,1,0:T(8,128)(2,1)} %shared_hidden_kernel.1), calls=%async_computation.10 | async-start | bytes 131072 | tf_op jit(solution)/shard_map/all_to_all | solution.py:275
  211.5 17.8 %copy-start.8 = (bf16[256,384]{1,0:T(8,128)(2,1)S(1)}, bf16[256,384]{1,0:T(8,128)(2,1)}, u32[]{:S(2)}) copy-start(bf16[256,384]{1,0:T(8,128)(2,1)} %copy-done.7) | copy-start | bytes 589828

commit v2 on v1

v2 whole, which is shorter than its diff:
```python
import jax
import jax.numpy as jnp
from jax import lax
from jax.experimental import pallas as pl
from jax.experimental.pallas import tpu as pltpu
from jax.sharding import Mesh
from jax.sharding import PartitionSpec as P

DK = 128
DV = 256
BLOCK = 64
TOK = 256
MOST = 12
SLOTS = 384
ALL_SLOTS = 1536
PITCH = 56
D = 2048
SP = ("z", "x")
SPG = ("z", "x", "yg")
TP = ("yg", "yn", "c")
GROUP = ("yn", "c")
F32 = jnp.float32
BF16 = jnp.bfloat16
HIGHEST = lax.Precision.HIGHEST
EPSILON = 1e-06
ROUTE_SCALE = 2.5
GATE_TEMPER = 16.0
VMEM = pl.BlockSpec(memory_space=pltpu.VMEM)
SMEM = pl.BlockSpec(memory_space=pltpu.SMEM)


def call(kernel, outs, *args, scratch=(), smem=0, limit=24):
    single = not isinstance(outs, list)
    shapes = [jax.ShapeDtypeStruct(s, t) for s, t in ([outs] if single else outs)]
    got = pl.pallas_call(
        kernel,
        out_shape=shapes,
        in_specs=[SMEM] * smem + [VMEM] * (len(args) - smem),
        out_specs=[VMEM] * len(shapes),
        scratch_shapes=list(scratch),
        compiler_params=pltpu.CompilerParams(vmem_limit_bytes=limit * 2**20),
        cost_estimate=pl.CostEstimate(
            flops=1000000, bytes_accessed=1000000, transcendentals=0
        ),
    )(*args)
    return got[0] if single else got


def nt(a, b, **kw):
    return lax.dot_general(
        a, b, (((1,), (1,)), ((), ())), preferred_element_type=F32, **kw
    )


def decays(decay_ref, extra_ref):
    raw = decay_ref[...].astype(F32)
    logs = jax.nn.log_sigmoid(raw) / GATE_TEMPER + extra_ref[...]
    rows = lax.broadcasted_iota(jnp.int32, (BLOCK, BLOCK), 0)
    cols = lax.broadcasted_iota(jnp.int32, (BLOCK, BLOCK), 1)
    lower = (rows >= cols).astype(F32)
    inside = [
        jnp.dot(lower, logs[b * BLOCK : (b + 1) * BLOCK], precision=HIGHEST,
                preferred_element_type=F32)
        for b in range(TOK // BLOCK)
    ]
    return inside


def block_states(inside, key_ref, value_ref):
    state = jnp.zeros((DV, DK), F32)
    states = []
    total = jnp.zeros((1, DK), F32)
    for b, cum in enumerate(inside):
        states.append(state)
        rows = pl.ds(b * BLOCK, BLOCK)
        end = cum[BLOCK - 1 : BLOCK]
        key_end = key_ref[rows, :].astype(F32) * jnp.exp(end - cum)
        value = value_ref[rows, :].astype(F32)
        fresh = jnp.dot(value.T, key_end, precision=HIGHEST, preferred_element_type=F32)
        state = jnp.exp(end) * state + fresh
        total = total + end
    return states, state, total


def state_kernel(key_ref, value_ref, decay_ref, extra_ref, out_ref):
    inside = decays(decay_ref, extra_ref)
    _, state, total = block_states(inside, key_ref, value_ref)
    out_ref[:, 0:8, :] = state.reshape(32, 8, DK).astype(BF16)
    decay = jnp.exp(total)
    high = decay.astype(BF16).astype(F32)
    row = lax.broadcasted_iota(jnp.int32, (8, DK), 0)
    tail = jnp.where(row == 0, high, jnp.where(row == 1, decay - high, 0.0))
    out_ref[:, 8:16, :] = jnp.broadcast_to(tail[None], (32, 8, DK)).astype(BF16)


def scan_kernel(in_ref, out_ref):
    state = jnp.zeros((8, DK), F32)
    for s in range(32):
        out_ref[s] = state.astype(BF16)
        block = in_ref[s].astype(F32)
        decay = block[8:9] + block[9:10]
        state = decay * state + block[0:8]


def local_kernel(query_ref, key_ref, value_ref, decay_ref, extra_ref, local_ref, start_ref):
    inside = decays(decay_ref, extra_ref)
    states, _, _ = block_states(inside, key_ref, value_ref)
    rows_at = lax.broadcasted_iota(jnp.int32, (BLOCK, BLOCK), 0)
    cols_at = lax.broadcasted_iota(jnp.int32, (BLOCK, BLOCK), 1)
    before = jnp.zeros((1, DK), F32)
    for b, cum in enumerate(inside):
        rows = pl.ds(b * BLOCK, BLOCK)
        query = query_ref[rows, :].astype(F32) * DK ** (-0.5)
        key = key_ref[rows, :].astype(F32)
        value = value_ref[rows, :].astype(F32)
        query_decay = query * jnp.exp(cum)
        scores = nt(query_decay, key * jnp.exp(-cum), precision=HIGHEST)
        scores = jnp.where(rows_at >= cols_at, scores, 0.0)
        mixed = jnp.dot(scores, value, precision=HIGHEST, preferred_element_type=F32)
        if b > 0:
            mixed = mixed + nt(query_decay, states[b], precision=HIGHEST)
        local_ref[rows, :] = mixed
        start_ref[rows, :] = query * jnp.exp(cum + before)
        before = before + cum[BLOCK - 1 : BLOCK]


def head_kernel(local_ref, start_ref, enter_ref, gate_ref, gain_ref, out_ref):
    mixed = local_ref[...] + nt(start_ref[...], enter_ref[...].astype(F32), precision=HIGHEST)
    scale = lax.rsqrt(jnp.mean(mixed * mixed, axis=-1, keepdims=True) + EPSILON)
    gate = jax.nn.silu(gate_ref[...].astype(F32))
    rows = (mixed * scale * gain_ref[...].astype(F32) * gate).astype(BF16)
    for dest in range(4):
        out_ref[dest] = rows


def project_kernel(ids_ref, heads_ref, w0, w1, w2, w3, out_ref):
    part = ids_ref[0]
    for m in (0, 2):
        pair = ((w0, w1), None, (w2, w3))[m]
        total = jnp.zeros((TOK, 256), F32)
        for h in range(4):
            lanes = slice(h * 128, (h + 1) * 128)
            weight = jnp.concatenate([w[0:256, lanes] for w in pair], axis=1)
            total = total + jnp.dot(heads_ref[h], weight, preferred_element_type=F32)
        out_ref[part ^ m] = total[:, :128].astype(BF16)
        out_ref[part ^ (m + 1)] = total[:, 128:].astype(BF16)


def places(routing_ref):
    experts = lax.broadcasted_iota(jnp.int32, (TOK, 128), 1)
    hot = [(routing_ref[:, k : k + 1] == experts).astype(F32) for k in range(4)]
    named = hot[0] + hot[1] + hot[2] + hot[3]
    rows = lax.broadcasted_iota(jnp.int32, (TOK, TOK), 0)
    cols = lax.broadcasted_iota(jnp.int32, (TOK, TOK), 1)
    earlier = (rows > cols).astype(BF16)
    ranks = jnp.dot(earlier, named.astype(BF16), preferred_element_type=F32)
    return [
        routing_ref[:, k : k + 1] * MOST
        + jnp.sum(hot[k] * ranks, axis=1, keepdims=True).astype(jnp.int32)
        for k in range(4)
    ]


def pick_kernel(routing_ref, pick_ref):
    place = places(routing_ref)
    slots = lax.broadcasted_iota(jnp.int32, (TOK, 512), 1)
    for j in range(ALL_SLOTS // 512):
        picked = jnp.zeros((TOK, 512), F32)
        for k in range(4):
            picked = picked + (place[k] - j * 512 == slots).astype(F32)
        pick_ref[j * 512 : (j + 1) * 512, :] = picked.T.astype(BF16)


def weigh_kernel(routing_ref, score_ref, high_ref, low_ref):
    place = places(routing_ref)
    scores = [score_ref[:, k : k + 1] for k in range(4)]
    total = scores[0] + scores[1] + scores[2] + scores[3]
    slots = lax.broadcasted_iota(jnp.int32, (TOK, 512), 1)
    for j in range(ALL_SLOTS // 512):
        weighted = jnp.zeros((TOK, 512), F32)
        for k in range(4):
            here = (place[k] - j * 512 == slots).astype(F32)
            weighted = weighted + here * (ROUTE_SCALE * scores[k] / total)
        high = weighted.astype(BF16)
        high_ref[:, j * 512 : (j + 1) * 512] = high
        low_ref[:, j * 512 : (j + 1) * 512] = (weighted - high.astype(F32)).astype(BF16)


def dispatch_kernel(pick_ref, in_ref, residual_ref, out_ref, mid_ref):
    total = residual_ref[...].astype(F32)
    for s in range(4):
        total = total + in_ref[s].astype(F32)
    mid = total.astype(BF16)
    mid_ref[...] = mid
    for j in range(4):
        rows = pl.ds(j * SLOTS, SLOTS)
        picked = jnp.dot(pick_ref[rows, :], mid, preferred_element_type=F32)
        out_ref[rows, :] = picked.astype(BF16)


def expert_kernel(ids_ref, x0, x1, x2, x3, gate_ref, up_ref, gain_ref, out_ref, wide_ref, rows_ref):
    part = ids_ref[0]
    squares = jnp.zeros((SLOTS, 128), F32)
    for m, x_ref in enumerate((x0, x1, x2, x3)):
        for s in range(32):
            wide_ref[m, s * PITCH : s * PITCH + 48, :] = x_ref[s * 48 : (s + 1) * 48, :].astype(F32)
    for m in range(4):
        for q in range(4):
            slab = q * 4 + (part ^ m)
            tile = jnp.concatenate(
                [wide_ref[m, pl.ds(q * MOST + r, 32, stride=PITCH), :] for r in range(MOST)], axis=0
            )
            squares = squares + tile * tile
            scaled = (tile * gain_ref[pl.ds(slab, 1), :]).astype(BF16)
            rows_ref[:, pl.ds(pl.multiple_of(slab * 128, 128), 128)] = scaled
    scale = lax.rsqrt(jnp.sum(squares, axis=1, keepdims=True) * (1.0 / D) + EPSILON)
    gate = jnp.dot(rows_ref[...], gate_ref[...], preferred_element_type=F32) * scale
    up = jnp.dot(rows_ref[...], up_ref[...], preferred_element_type=F32) * scale
    out_ref[...] = (jax.nn.silu(gate) * up).astype(BF16)


def down_kernel(h0, h1, h2, h3, d0, d1, d2, d3, out_ref, wide_ref):
    total = jnp.zeros((SLOTS, 512), F32)
    for h_ref, d_ref in ((h0, d0), (h1, d1), (h2, d2), (h3, d3)):
        total = total + jnp.dot(h_ref[...], d_ref[256:512, :], preferred_element_type=F32)
    for q in range(4):
        for r in range(MOST):
            wide_ref[pl.ds(q * MOST + r, 32, stride=PITCH), :] = total[
                r * 32 : (r + 1) * 32, q * 128 : (q + 1) * 128
            ]
    for s in range(32):
        out_ref[s * 48 : (s + 1) * 48, :] = wide_ref[s * PITCH : s * PITCH + 48, :].astype(BF16)


def parts_kernel(ids_ref, project_ref, down_ref, shared_ref, *out_refs):
    part = ids_ref[0]
    for m, out_ref in enumerate(out_refs):
        for q in range(4):
            slab = q * 4 + (part ^ m)
            lanes = slice(q * 128, (q + 1) * 128)
            out_ref[0:256, lanes] = project_ref[pl.ds(pl.multiple_of(slab * 256, 256), 256), :]
            columns = pl.ds(pl.multiple_of(slab * 128, 128), 128)
            out_ref[256:512, lanes] = down_ref[:, columns]
            out_ref[512:576, lanes] = shared_ref[:, columns]


def shared_in_kernel(ids_ref, m0, m1, m2, m3, w0, w1, w2, w3, gain_ref, out_ref, weight_ref, mid_ref):
    part, group = ids_ref[0], ids_ref[1]
    for m, w_ref in enumerate((w0, w1, w2, w3)):
        at = (part ^ m) * 32
        weight_ref[pl.ds(pl.multiple_of(at, 32), 32), :] = w_ref[512:544, :]
        weight_ref[pl.ds(pl.multiple_of(at + 128, 32), 32), :] = w_ref[544:576, :]
    for d, m_ref in enumerate((m0, m1, m2, m3)):
        mid_ref[(group - d) & 3] = m_ref[...]
    squares = jnp.zeros((TOK, 128), F32)
    pre = jnp.zeros((TOK, 256), F32)
    for q in range(4):
        tile = mid_ref[q].astype(F32)
        squares = squares + tile * tile
        scaled = (tile * gain_ref[pl.ds(q * 4 + part, 1), :]).astype(BF16)
        pre = pre + nt(scaled, weight_ref[:, q * 128 : (q + 1) * 128])
    ssq = jnp.sum(squares, axis=1, keepdims=True)
    high = ssq.astype(BF16).astype(F32)
    lane = lax.broadcasted_iota(jnp.int32, (TOK, 128), 1)
    tail = jnp.where(lane == 0, high, jnp.where(lane == 1, ssq - high, 0.0)).astype(BF16)
    pre = pre.astype(BF16)
    for dest in range(4):
        out_ref[dest, :, 0:256] = pre
        out_ref[dest, :, 256:384] = tail


def shared_hidden_kernel(in_ref, out_ref):
    total = sum(in_ref[s].astype(F32) for s in range(4))
    ssq = jnp.sum(total[:, 256:384], axis=1, keepdims=True)
    scale = lax.rsqrt(ssq * (1.0 / D) + EPSILON)
    hidden = jax.nn.silu(total[:, 0:128] * scale) * (total[:, 128:256] * scale)
    out_ref[...] = hidden.astype(BF16)


def final_kernel(ids_ref, back_ref, high_ref, low_ref, h0, h1, h2, h3, down_ref, mid_ref, out_ref):
    group = ids_ref[1]
    back = back_ref[...]
    total = mid_ref[...].astype(F32)
    total = total + jnp.dot(high_ref[...], back, preferred_element_type=F32)
    total = total + jnp.dot(low_ref[...], back, preferred_element_type=F32)
    for d, h in enumerate((h0, h1, h2, h3)):
        at = pl.multiple_of(((group - d) & 3) * 128, 128)
        total = total + jnp.dot(
            h[...], down_ref[pl.ds(at, 128), :], preferred_element_type=F32
        )
    out_ref[...] = total.astype(BF16)


def exchange(value, axes):
    return lax.all_to_all(value, axes, split_axis=0, concat_axis=0, tiled=True)


def moved(value, axes, target):
    count = lax.axis_size(axes)
    return lax.ppermute(value, axes, [(i, target(i) % count) for i in range(count)])


def shifted(values, axes):
    return [moved(v, axes, lambda i, d=d: i + d) for d, v in enumerate(values, 1)]


def swapped(value, axis):
    return moved(value, axis, lambda i: i ^ 1)


def grouped(values):
    return [moved(v, GROUP, lambda i, m=m: i ^ m) for m, v in enumerate(values, 1)]


def body(
    queries,
    key_matrix,
    value_matrix,
    output_gate_preactivation,
    decay_preactivation,
    extra_log_decay,
    head_norm_gain,
    output_projection,
    residual,
    feedforward_gain,
    routing,
    router_score,
    expert_gate_weight,
    expert_up_weight,
    expert_down_weight,
    shared_expert_gate,
    shared_expert_up,
    shared_expert_down,
):
    ids = jnp.stack([lax.axis_index(a) for a in (GROUP, "yg")]).astype(jnp.int32)
    gain = feedforward_gain.astype(F32).reshape(16, 128)
    head_gain = head_norm_gain.reshape(1, DV)

    payload = call(
        state_kernel, ((32, 16, DK), BF16),
        key_matrix, value_matrix, decay_preactivation, extra_log_decay,
    )
    states = exchange(payload, SP)
    local, start = call(
        local_kernel, [((TOK, DV), F32), ((TOK, DK), F32)],
        queries, key_matrix, value_matrix, decay_preactivation, extra_log_decay,
    )
    pick = call(pick_kernel, ((ALL_SLOTS, TOK), BF16), routing)
    high, low = call(
        weigh_kernel, [((TOK, ALL_SLOTS), BF16), ((TOK, ALL_SLOTS), BF16)], routing, router_score
    )
    shared_in = jnp.concatenate([shared_expert_gate.T, shared_expert_up.T], axis=0)
    own_part, *far_parts = call(
        parts_kernel, [((576, 512), BF16)] * 4,
        ids, output_projection, expert_down_weight, shared_in, smem=1,
    )
    parts = [own_part] + grouped(far_parts)

    entering = exchange(call(scan_kernel, ((32, 8, DK), BF16), states), SP)
    head_rows = call(
        head_kernel, ((4, TOK, DV), BF16),
        local, start, entering.reshape(DV, DK), output_gate_preactivation, head_gain,
    )
    partial = call(
        project_kernel, ((4, TOK, 128), BF16),
        ids, exchange(head_rows, "yg"), *parts, smem=1,
    )
    outgoing, mid = call(
        dispatch_kernel, [((ALL_SLOTS, 128), BF16), ((TOK, 128), BF16)],
        pick, exchange(partial, GROUP), residual,
    )
    own = exchange(outgoing.reshape(128, 3, 4, 128), SPG).reshape(ALL_SLOTS, 128)
    mids = [mid] + shifted([mid] * 3, "yg")

    across = swapped(own, "yn")
    beside = swapped(own, "c")
    far = swapped(across, "c")
    pre = call(
        shared_in_kernel, ((4, TOK, 384), BF16), ids, *mids, *parts, gain, smem=1,
        scratch=[pltpu.VMEM((256, 512), BF16), pltpu.VMEM((4, TOK, 128), BF16)],
    )
    pre = exchange(pre, GROUP)
    routed = call(
        expert_kernel, ((SLOTS, 256), BF16),
        ids, own, beside, across, far, expert_gate_weight, expert_up_weight, gain,
        smem=1,
        scratch=[pltpu.VMEM((4, 32 * PITCH, 128), F32), pltpu.VMEM((SLOTS, D), BF16)],
    )
    routed_across = swapped(routed, "yn")
    routed_beside = swapped(routed, "c")
    routed_far = swapped(routed_across, "c")
    expert_out = call(
        down_kernel, ((ALL_SLOTS, 128), BF16),
        routed, routed_beside, routed_across, routed_far, *parts,
        scratch=[pltpu.VMEM((32 * PITCH, 128), F32)],
    )
    back = exchange(expert_out.reshape(128, 3, 4, 128), SPG).reshape(ALL_SLOTS, 128)
    hidden = call(shared_hidden_kernel, ((TOK, 128), BF16), pre)
    hidden = [hidden] + shifted([hidden] * 3, "yg")
    return call(
        final_kernel, ((TOK, 128), BF16),
        ids, back, high, low, *hidden, shared_expert_down, mid, smem=1,
    )


def solution(mesh):
    finer = Mesh(mesh.devices.reshape(8, 4, 4, 2, 2), ("z", "x", "yg", "yn", "c"))
    in_specs = (
        P(SP, TP),
        P(SP, TP),
        P(SP, TP),
        P(SP, TP),
        P(SP, TP),
        P(SP, TP),
        P(),
        P(None, TP),
        P(SP, TP),
        P(),
        P(SP, None),
        P(SP, None),
        P(None, SP + TP),
        P(None, SP + TP),
        P(SP + TP, None),
        P(None, TP),
        P(None, TP),
        P(None, TP),
    )
    return jax.shard_map(body, mesh=finer, in_specs=in_specs, out_specs=P(SP, TP), check_vma=False)
```

time: 245 us -> 197 us (0.80)
  blocking collectives: 76.2 us -> 22.8 us
  starting transfers between devices: 63.4 us -> 94.7 us
  waiting for transfers between devices: 75.1 us -> 47.3 us
  Pallas kernels: 15.9 us -> 18.5 us
    all_to_all x5 -> x1, blocking collectives: 76.2 us -> 22.8 us  [exchange(): return lax.all_to_all(value, axes, split_axis=0, concat_axis=0, tiled=True)]
    all_to_all x8 -> x6, waiting for transfers between devices: 53.5 us -> 14.9 us  [exchange(): return lax.all_to_all(value, axes, split_axis=0, concat_axis=0, tiled=True)]
    ppermute x7 -> x15, starting transfers between devices: 21.8 us -> 53 us  [moved(): lax.ppermute(value, axes, [(i, target(i) % count) for i in range(count)])]
    ppermute x7 -> x15, waiting for transfers between devices: 21.6 us -> 32.4 us  [moved(): lax.ppermute(value, axes, [(i, target(i) % count) for i in range(count)])]
    reshape x5 -> x0, local copies, waits for them, and re-layouts: 3.59 us -> none  [the longest x3 3.44 us: body(): down.reshape(256, 4, 4, 128).transpose(2, 0, 1, 3).reshape(4, 256, 512)]
    unnamed x39 -> x53, local copies, waits for them, and re-layouts: 6.17 us -> 9.73 us
    pallas_call x14, Pallas kernels: 15.9 us -> 18.5 us  [call(): pl.pallas_call(kernel, out_shape=shapes, in_specs=[SMEM] * smem + [VMEM]...]
    all_to_all x8 -> x6, starting transfers between devices: 41.6 us -> 41.8 us  [exchange(): return lax.all_to_all(value, axes, split_axis=0, concat_axis=0, tiled=True)]
  transfers between devices with their start and end apart: 15 -> 21, of which waited for: 10 -> 10; matrix products, arithmetic and copies ran while one was open for 2% -> 0% of each run, Pallas kernels for 5% -> 6%
where the time goes in v2:
time: 197 us; the launch traced here: 194 us
  starting transfers between devices  94.7 us (48%)
  waiting for transfers between devices  47.3 us (24%)
  blocking collectives  22.8 us (12%)
  Pallas kernels  18.5 us (9%)
  local copies, waits for them, and re-layouts  9.73 us (5%)
    ppermute x15, starting transfers between devices, moved(): lax.ppermute(value, axes, [(i, target(i) % count) for i in range(count)])  53 us
    all_to_all x6, starting transfers between devices, exchange(): return lax.all_to_all(value, axes, split_axis=0, concat_axis=0, tiled=True)  41.8 us
    ppermute x15, waiting for transfers between devices, moved(): lax.ppermute(value, axes, [(i, target(i) % count) for i in range(count)])  32.4 us
    all_to_all x1, blocking collectives, exchange(): return lax.all_to_all(value, axes, split_axis=0, concat_axis=0, tiled=True)  22.8 us
    pallas_call x14, Pallas kernels, call(): pl.pallas_call(kernel, out_shape=shapes, in_specs=[SMEM] * smem + [VMEM]...  18.5 us
    all_to_all x6, waiting for transfers between devices, exchange(): return lax.all_to_all(value, axes, split_axis=0, concat_axis=0, tiled=True)  14.9 us
    unnamed x53, local copies, waits for them, and re-layouts  9.73 us
  transfers between devices with their start and end apart: 21, of which 10 were waited for; matrix products, arithmetic and copies ran while one was open for 0% of the time, Pallas kernels for 6%

profile of v2, /device:TPU:1, one launch (start us, length us, event | category | flops | bytes accessed | tf_op | source)
XLA Modules:
  0.0 193.7 jit_solution(8072030922141527447)
XLA Ops:
  0.0 0.8 copy.20.extra_ref
  0.9 0.1 copy-done.7
  0.9 0.8 copy-done.11
  1.8 0.8 copy-done.13
  2.6 0.8 shard_map.174
  3.5 22.8 %all_to_all.35.in_ref = bf16[32,16,128]{2,1,0:T(8,128)(2,1)S(1)} all-to-all(bf16[32,16,128]{2,1,0:T(8,128)(2,1)S(1)} %shard_map.174), channel_id=1, replica_groups=mesh['z'=8,'x'=4,'yg'=4,'yn'=2,'c'=2] {'z','x'}, dimensions={0} | all-to-all | bytes 262144 | tf_op jit(solution)/shard_map/all_to_all | solution.py:295
  26.3 0.7 shard_map.175
  27.0 4.0 %all-to-all-start.1 = ((bf16[32,8,128]{2,1,0:T(8,128)(2,1)}), bf16[32,8,128]{2,1,0:T(8,128)(2,1)S(1)}, u32[]{:S(2)}, u32[]{:S(2)}) async-start(bf16[32,8,128]{2,1,0:T(8,128)(2,1)} %shard_map.175), calls=%async_computation.1 | async-start | bytes 131072 | tf_op jit(solution)/shard_map/all_to_all | solution.py:295
  31.0 0.0 copy-start.24
  31.0 0.6 copy-done.24
  31.7 0.0 copy-start.15
  31.7 1.8 shard_map.173
  33.5 0.1 pad_add_fusion.ids_ref
  33.6 6.3 %all-to-all-done.1 = bf16[32,8,128]{2,1,0:T(8,128)(2,1)S(1)} async-done(((bf16[32,8,128]{2,1,0:T(8,128)(2,1)}), bf16[32,8,128]{2,1,0:T(8,128)(2,1)S(1)}, u32[]{:S(2)}, u32[]{:S(2)}) %all-to-all-start.1) | async-done | bytes 65568 | tf_op jit(solution)/shard_map/all_to_all | solution.py:295
  39.9 1.3 shard_map.176
  41.2 6.9 %all-to-all-start.2 = ((bf16[4,256,256]{2,1,0:T(8,128)(2,1)}), bf16[4,256,256]{2,1,0:T(8,128)(2,1)S(1)}, u32[]{:S(2)}, u32[]{:S(2)}) async-start(bf16[4,256,256]{2,1,0:T(8,128)(2,1)} %shard_map.176), calls=%async_computation.2 | async-start | bytes 1048576 | tf_op jit(solution)/shard_map/all_to_all | solution.py:295
  48.1 0.0 copy-start.4
  48.1 1.2 copy-done.4
  49.4 1.0 shard_map.177
  50.4 5.4 %collective-permute-start = (bf16[576,512]{1,0:T(8,128)(2,1)S(1)}, bf16[576,512]{1,0:T(8,128)(2,1)S(1)}, u32[]{:S(2)}, u32[]{:S(2)}) collective-permute-start(bf16[576,512]{1,0:T(8,128)(2,1)S(1)} %get-tuple-element.18), channel_id=1, source_target_pairs={{0,1},{1,0},{2,3},{3,2},{4,5},{5,4},{6,7},{7,6},{8,9},{9,8},{10,11... | collective-permute-start | bytes 1769480 | tf_op jit(solution)/shard_map/ppermute | solution.py:300
  55.8 2.3 %collective-permute-start.1 = (bf16[576,512]{1,0:T(8,128)(2,1)S(1)}, bf16[576,512]{1,0:T(8,128)(2,1)S(1)}, u32[]{:S(2)}, u32[]{:S(2)}) collective-permute-start(bf16[576,512]{1,0:T(8,128)(2,1)S(1)} %get-tuple-element.19), channel_id=1, source_target_pairs={{0,2},{1,3},{2,0},{3,1},{4,6},{5,7},{6,4},{7,5},{8,10},{9,11},{10,... | collective-permute-start | bytes 1769480 | tf_op jit(solution)/shard_map/ppermute | solution.py:300
  58.1 3.2 %collective-permute-start.2 = (bf16[576,512]{1,0:T(8,128)(2,1)S(1)}, bf16[576,512]{1,0:T(8,128)(2,1)S(1)}, u32[]{:S(2)}, u32[]{:S(2)}) collective-permute-start(bf16[576,512]{1,0:T(8,128)(2,1)S(1)} %get-tuple-element.20), channel_id=1, source_target_pairs={{0,3},{1,2},{2,1},{3,0},{4,7},{5,6},{6,5},{7,4},{8,11},{9,10},{10,... | collective-permute-start | bytes 1769480 | tf_op jit(solution)/shard_map/ppermute | solution.py:300
  61.3 13.1 %collective-permute-done.1.w2.d2 = bf16[576,512]{1,0:T(8,128)(2,1)S(1)} collective-permute-done((bf16[576,512]{1,0:T(8,128)(2,1)S(1)}, bf16[576,512]{1,0:T(8,128)(2,1)S(1)}, u32[]{:S(2)}, u32[]{:S(2)}) %collective-permute-start.1) | collective-permute-done | bytes 589856 | tf_op jit(solution)/shard_map/ppermute | solution.py:300
  74.4 12.6 %collective-permute-done.2.w3.d3 = bf16[576,512]{1,0:T(8,128)(2,1)S(1)} collective-permute-done((bf16[576,512]{1,0:T(8,128)(2,1)S(1)}, bf16[576,512]{1,0:T(8,128)(2,1)S(1)}, u32[]{:S(2)}, u32[]{:S(2)}) %collective-permute-start.2) | collective-permute-done | bytes 589856 | tf_op jit(solution)/shard_map/ppermute | solution.py:300
  87.0 1.7 shard_map.178
  88.7 3.9 %all-to-all-start.3 = ((bf16[4,256,128]{2,1,0:T(8,128)(2,1)}), bf16[4,256,128]{2,1,0:T(8,128)(2,1)S(1)}, u32[]{:S(2)}, u32[]{:S(2)}) async-start(bf16[4,256,128]{2,1,0:T(8,128)(2,1)} %shard_map.178), calls=%async_computation.3 | async-start | bytes 524288 | tf_op jit(solution)/shard_map/all_to_all | solution.py:295
  92.6 0.1 copy.19.routing_ref
  92.8 1.5 shard_map.172.pick_ref
  94.3 3.4 %all-to-all-done.3.in_ref = bf16[4,256,128]{2,1,0:T(8,128)(2,1)S(1)} async-done(((bf16[4,256,128]{2,1,0:T(8,128)(2,1)}), bf16[4,256,128]{2,1,0:T(8,128)(2,1)S(1)}, u32[]{:S(2)}, u32[]{:S(2)}) %all-to-all-start.3) | async-done | bytes 262176 | tf_op jit(solution)/shard_map/all_to_all | solution.py:295
  97.7 0.8 copy-done.18
  98.5 0.4 shard_map.179
  98.9 0.8 copy-done.8
  99.6 9.4 %all-to-all-start.4 = ((bf16[128,3,4,128]{3,2,1,0:T(4,128)(2,1)}), bf16[128,3,4,128]{3,2,1,0:T(4,128)(2,1)S(1)}, u32[]{:S(2)}, u32[]{:S(2)}) async-start(bf16[128,3,4,128]{3,2,1,0:T(4,128)(2,1)} %bitcast.16), calls=%async_computation.4 | async-start | bytes 786432 | tf_op jit(solution)/shard_map/all_to_all | solution.py:295
  109.1 6.4 %collective-permute-start.10 = (bf16[256,128]{1,0:T(8,128)(2,1)S(1)}, bf16[256,128]{1,0:T(8,128)(2,1)S(1)}, u32[]{:S(2)}, u32[]{:S(2)}) collective-permute-start(bf16[256,128]{1,0:T(8,128)(2,1)S(1)} %get-tuple-element.24.m0.mid_ref), channel_id=1, source_target_pairs={{0,8},{4,12},{8,0},{12,4},{1,9},{5,13},{9,1},{13,5},{2,10},{6,14},... | collective-permute-start | bytes 196616 | tf_op jit(solution)/shard_map/ppermute | solution.py:300
  115.5 2.2 %collective-permute-start.11 = (bf16[256,128]{1,0:T(8,128)(2,1)S(1)}, bf16[256,128]{1,0:T(8,128)(2,1)S(1)}, u32[]{:S(2)}, u32[]{:S(2)}) collective-permute-start(bf16[256,128]{1,0:T(8,128)(2,1)S(1)} %get-tuple-element.24.m0.mid_ref), channel_id=1, source_target_pairs={{0,12},{4,0},{8,4},{12,8},{1,13},{5,1},{9,5},{13,9},{2,14},{6,2},{... | collective-permute-start | bytes 196616 | tf_op jit(solution)/shard_map/ppermute | solution.py:300
  117.7 4.0 %collective-permute-start.9 = (bf16[256,128]{1,0:T(8,128)(2,1)S(1)}, bf16[256,128]{1,0:T(8,128)(2,1)S(1)}, u32[]{:S(2)}, u32[]{:S(2)}) collective-permute-start(bf16[256,128]{1,0:T(8,128)(2,1)S(1)} %get-tuple-element.24.m0.mid_ref), channel_id=1, source_target_pairs={{0,4},{4,8},{8,12},{12,0},{1,5},{5,9},{9,13},{13,1},{2,6},{6,10},{... | collective-permute-start | bytes 196616 | tf_op jit(solution)/shard_map/ppermute | solution.py:300
  121.7 5.2 %all-to-all-done.4 = bf16[128,3,4,128]{3,2,1,0:T(4,128)(2,1)S(1)} async-done(((bf16[128,3,4,128]{3,2,1,0:T(4,128)(2,1)}), bf16[128,3,4,128]{3,2,1,0:T(4,128)(2,1)S(1)}, u32[]{:S(2)}, u32[]{:S(2)}) %all-to-all-start.4) | async-done | bytes 393248 | tf_op jit(solution)/shard_map/all_to_all | solution.py:295
  126.9 2.3 %collective-permute-start.4 = (bf16[1536,128]{1,0:T(8,128)(2,1)S(1)}, bf16[1536,128]{1,0:T(8,128)(2,1)}, u32[]{:S(2)}, u32[]{:S(2)}) collective-permute-start(bf16[1536,128]{1,0:T(8,128)(2,1)S(1)} %bitcast.12), channel_id=1, source_target_pairs={{0,2},{2,0},{1,3},{3,1},{4,6},{6,4},{5,7},{7,5},{8,10},{10,8},{9,1... | collective-permute-start | bytes 1179656 | tf_op jit(solution)/shard_map/ppermute | solution.py:300
  129.3 0.9 shard_map.183
  130.2 0.9 copy-done
  131.1 9.0 %all-to-all-start.6 = ((bf16[4,256,384]{2,1,0:T(8,128)(2,1)}), bf16[4,256,384]{2,1,0:T(8,128)(2,1)S(1)}, u32[]{:S(2)}, u32[]{:S(2)}) async-start(bf16[4,256,384]{2,1,0:T(8,128)(2,1)} %copy-done), calls=%async_computation.6 | async-start | bytes 1572864 | tf_op jit(solution)/shard_map/all_to_all | solution.py:295
  140.1 1.9 %collective-permute-start.3 = (bf16[1536,128]{1,0:T(8,128)(2,1)S(1)}, bf16[1536,128]{1,0:T(8,128)(2,1)S(1)}, u32[]{:S(2)}, u32[]{:S(2)}) collective-permute-start(bf16[1536,128]{1,0:T(8,128)(2,1)S(1)} %bitcast.13), channel_id=1, source_target_pairs={{0,1},{1,0},{2,3},{3,2},{4,5},{5,4},{6,7},{7,6},{8,9},{9,8},{10,11... | collective-permute-start | bytes 1179656 | tf_op jit(solution)/shard_map/ppermute | solution.py:300
  142.1 2.4 %collective-permute-start.5 = (bf16[1536,128]{1,0:T(8,128)(2,1)}, bf16[1536,128]{1,0:T(8,128)(2,1)S(1)}, u32[]{:S(2)}, u32[]{:S(2)}) collective-permute-start(bf16[1536,128]{1,0:T(8,128)(2,1)} %collective-permute-done.4.x2), channel_id=1, source_target_pairs={{0,1},{1,0},{2,3},{3,2},{4,5},{5,4},{6,7},{7,6},{8,9},{9,8},{10,11... | collective-permute-start | bytes 1179656 | tf_op jit(solution)/shard_map/ppermute | solution.py:300
  144.4 1.5 collective-permute-done.5.x3
  146.0 1.2 copy-done.5
  147.2 1.2 copy-done.6
  148.4 3.1 %shard_map.180.h0 = bf16[384,256]{1,0:T(8,128)(2,1)S(1)} custom-call(s32[2]{0:T(128)S(1)} %pad_add_fusion.ids_ref, bf16[1536,128]{1,0:T(8,128)(2,1)S(1)} %bitcast.14, bf16[1536,128]{1,0:T(8,128)(2,1)S(1)} %collective-permute-done.3.x1, bf16[1536,128]{1,0:T(8,128)(2,1)} %collective-permute-done.4.x2, bf16[1536,128]{1,0:T(8,128)(2,1)S(1)} %collective-permute-done.5.x3, ...), custom_call_target="tpu_custom_call" | custom-call | flops 1000000 | bytes 1000000 | tf_op jit(solution)/shard_map/pallas_call | solution.py:35
  151.5 3.5 %collective-permute-start.7 = (bf16[384,256]{1,0:T(8,128)(2,1)S(1)}, bf16[384,256]{1,0:T(8,128)(2,1)S(1)}, u32[]{:S(2)}, u32[]{:S(2)}) collective-permute-start(bf16[384,256]{1,0:T(8,128)(2,1)S(1)} %shard_map.180.h0), channel_id=1, source_target_pairs={{0,2},{2,0},{1,3},{3,1},{4,6},{6,4},{5,7},{7,5},{8,10},{10,8},{9,1... | collective-permute-start | bytes 589832 | tf_op jit(solution)/shard_map/ppermute | solution.py:300
  155.1 2.3 %collective-permute-start.6 = (bf16[384,256]{1,0:T(8,128)(2,1)S(1)}, bf16[384,256]{1,0:T(8,128)(2,1)S(1)}, u32[]{:S(2)}, u32[]{:S(2)}) collective-permute-start(bf16[384,256]{1,0:T(8,128)(2,1)S(1)} %shard_map.180.h0), channel_id=1, source_target_pairs={{0,1},{1,0},{2,3},{3,2},{4,5},{5,4},{6,7},{7,6},{8,9},{9,8},{10,11... | collective-permute-start | bytes 589832 | tf_op jit(solution)/shard_map/ppermute | solution.py:300
  157.4 2.4 %collective-permute-done.7.h2 = bf16[384,256]{1,0:T(8,128)(2,1)S(1)} collective-permute-done((bf16[384,256]{1,0:T(8,128)(2,1)S(1)}, bf16[384,256]{1,0:T(8,128)(2,1)S(1)}, u32[]{:S(2)}, u32[]{:S(2)}) %collective-permute-start.7) | collective-permute-done | bytes 196640 | tf_op jit(solution)/shard_map/ppermute | solution.py:300
  159.8 3.1 %collective-permute-start.8 = (bf16[384,256]{1,0:T(8,128)(2,1)S(1)}, bf16[384,256]{1,0:T(8,128)(2,1)S(1)}, u32[]{:S(2)}, u32[]{:S(2)}) collective-permute-start(bf16[384,256]{1,0:T(8,128)(2,1)S(1)} %collective-permute-done.7.h2), channel_id=1, source_target_pairs={{0,1},{1,0},{2,3},{3,2},{4,5},{5,4},{6,7},{7,6},{8,9},{9,8},{10,11... | collective-permute-start | bytes 589832 | tf_op jit(solution)/shard_map/ppermute | solution.py:300
  163.0 0.9 collective-permute-done.8.h3
  163.9 1.4 shard_map.181
  165.3 8.5 %all-to-all-start.5 = ((bf16[128,3,4,128]{3,2,1,0:T(4,128)(2,1)}), bf16[128,3,4,128]{3,2,1,0:T(4,128)(2,1)S(1)}, u32[]{:S(2)}, u32[]{:S(2)}) async-start(bf16[128,3,4,128]{3,2,1,0:T(4,128)(2,1)} %bitcast.8), calls=%async_computation.5 | async-start | bytes 786432 | tf_op jit(solution)/shard_map/all_to_all | solution.py:295
  173.8 0.0 copy-start.23
  173.8 0.1 shard_map.184.h0
  174.0 3.5 %collective-permute-start.12 = (bf16[256,128]{1,0:T(8,128)(2,1)S(1)}, bf16[256,128]{1,0:T(8,128)(2,1)S(1)}, u32[]{:S(2)}, u32[]{:S(2)}) collective-permute-start(bf16[256,128]{1,0:T(8,128)(2,1)S(1)} %shard_map.184.h0), channel_id=1, source_target_pairs={{0,4},{4,8},{8,12},{12,0},{1,5},{5,9},{9,13},{13,1},{2,6},{6,10},{... | collective-permute-start | bytes 196616 | tf_op jit(solution)/shard_map/ppermute | solution.py:300
  177.5 5.2 %collective-permute-start.13 = (bf16[256,128]{1,0:T(8,128)(2,1)S(1)}, bf16[256,128]{1,0:T(8,128)(2,1)S(1)}, u32[]{:S(2)}, u32[]{:S(2)}) collective-permute-start(bf16[256,128]{1,0:T(8,128)(2,1)S(1)} %shard_map.184.h0), channel_id=1, source_target_pairs={{0,8},{4,12},{8,0},{12,4},{1,9},{5,13},{9,1},{13,5},{2,10},{6,14},... | collective-permute-start | bytes 196616 | tf_op jit(solution)/shard_map/ppermute | solution.py:300
  182.7 5.2 %collective-permute-start.14 = (bf16[256,128]{1,0:T(8,128)(2,1)S(1)}, bf16[256,128]{1,0:T(8,128)(2,1)S(1)}, u32[]{:S(2)}, u32[]{:S(2)}) collective-permute-start(bf16[256,128]{1,0:T(8,128)(2,1)S(1)} %shard_map.184.h0), channel_id=1, source_target_pairs={{0,12},{4,0},{8,4},{12,8},{1,13},{5,1},{9,5},{13,9},{2,14},{6,2},{... | collective-permute-start | bytes 196616 | tf_op jit(solution)/shard_map/ppermute | solution.py:300
  187.9 0.1 copy.23.score_ref
  188.1 2.0 %shard_map.182 = (bf16[256,1536]{1,0:T(8,128)(2,1)S(1)}, bf16[256,1536]{1,0:T(8,128)(2,1)S(1)}) custom-call(s32[256,4]{1,0:T(8,128)S(1)} %copy-done.2, f32[256,4]{1,0:T(8,128)S(1)} %copy.23.score_ref), custom_call_target="tpu_custom_call" | custom-call | flops 1000000 | bytes 1000000 | tf_op jit(solution)/shard_map/pallas_call | solution.py:35
  190.1 0.7 collective-permute-done.13.h2
  190.8 1.1 collective-permute-done.14.h3
  191.9 1.8 shard_map.185
  (50 shorter events, 0.1 us)
Async XLA Ops:
  0.0 0.9 copy-start.7
  0.9 0.8 copy-start.11
  1.8 0.8 copy-start.13
  26.3 5.4 %copy-start.17 = (bf16[256,128]{1,0:T(8,128)(2,1)S(1)}, bf16[256,128]{1,0:T(8,128)(2,1)}, u32[]{:S(2)}) copy-start(bf16[256,128]{1,0:T(8,128)(2,1)} %query_ref.1) | copy-start | bytes 196612
  27.0 4.7 %copy-start.12 = (bf16[256,128]{1,0:T(8,128)(2,1)S(1)}, bf16[256,128]{1,0:T(8,128)(2,1)}, u32[]{:S(2)}) copy-start(bf16[256,128]{1,0:T(8,128)(2,1)} %key_ref.3) | copy-start | bytes 196612
  27.0 4.7 %copy-start.14 = (bf16[256,128]{1,0:T(8,128)(2,1)S(1)}, bf16[256,128]{1,0:T(8,128)(2,1)}, u32[]{:S(2)}) copy-start(bf16[256,128]{1,0:T(8,128)(2,1)} %decay_ref.3) | copy-start | bytes 196612
  27.0 12.9 %all-to-all-start.1 = ((bf16[32,8,128]{2,1,0:T(8,128)(2,1)}), bf16[32,8,128]{2,1,0:T(8,128)(2,1)S(1)}, u32[]{:S(2)}, u32[]{:S(2)}) async-start(bf16[32,8,128]{2,1,0:T(8,128)(2,1)} %shard_map.175), calls=%async_computation.1 | async-start | bytes 131072 | tf_op jit(solution)/shard_map/all_to_all | solution.py:295
  31.0 0.7 copy-start.24
  31.7 8.2 %copy-start.15 = (bf16[256,256]{1,0:T(8,128)(2,1)S(1)}, bf16[256,256]{1,0:T(8,128)(2,1)}, u32[]{:S(2)}) copy-start(bf16[256,256]{1,0:T(8,128)(2,1)} %gate_ref.2) | copy-start | bytes 393220
  39.9 8.2 %copy-start.19 = (bf16[2048,32]{0,1:T(8,128)(2,1)S(1)}, bf16[2048,32]{0,1:T(8,128)(2,1)}, u32[]{:S(2)}) copy-start(bf16[2048,32]{0,1:T(8,128)(2,1)} %param.34) | copy-start | bytes 393220
  39.9 8.2 %copy-start.20 = (bf16[2048,32]{0,1:T(8,128)(2,1)S(1)}, bf16[2048,32]{0,1:T(8,128)(2,1)}, u32[]{:S(2)}) copy-start(bf16[2048,32]{0,1:T(8,128)(2,1)} %param.33) | copy-start | bytes 393220
  41.2 7.0 %copy-start.3 = (bf16[4096,128]{1,0:T(8,128)(2,1)S(1)}, bf16[4096,128]{1,0:T(8,128)(2,1)}, u32[]{:S(2)}) copy-start(bf16[4096,128]{1,0:T(8,128)(2,1)} %project_ref.1) | copy-start | bytes 3145732
  41.2 45.9 %all-to-all-start.2 = ((bf16[4,256,256]{2,1,0:T(8,128)(2,1)}), bf16[4,256,256]{2,1,0:T(8,128)(2,1)S(1)}, u32[]{:S(2)}, u32[]{:S(2)}) async-start(bf16[4,256,256]{2,1,0:T(8,128)(2,1)} %shard_map.176), calls=%async_computation.2 | async-start | bytes 1048576 | tf_op jit(solution)/shard_map/all_to_all | solution.py:295
  48.1 1.2 copy-start.4
  50.4 10.9 %collective-permute-start = (bf16[576,512]{1,0:T(8,128)(2,1)S(1)}, bf16[576,512]{1,0:T(8,128)(2,1)S(1)}, u32[]{:S(2)}, u32[]{:S(2)}) collective-permute-start(bf16[576,512]{1,0:T(8,128)(2,1)S(1)} %get-tuple-element.18), channel_id=1, source_target_pairs={{0,1},{1,0},{2,3},{3,2},{4,5},{5,4},{6,7},{7,6},{8,9},{9,8},{10,11... | collective-permute-start | bytes 1769480 | tf_op jit(solution)/shard_map/ppermute | solution.py:300
  55.8 18.6 %collective-permute-start.1 = (bf16[576,512]{1,0:T(8,128)(2,1)S(1)}, bf16[576,512]{1,0:T(8,128)(2,1)S(1)}, u32[]{:S(2)}, u32[]{:S(2)}) collective-permute-start(bf16[576,512]{1,0:T(8,128)(2,1)S(1)} %get-tuple-element.19), channel_id=1, source_target_pairs={{0,2},{1,3},{2,0},{3,1},{4,6},{5,7},{6,4},{7,5},{8,10},{9,11},{10,... | collective-permute-start | bytes 1769480 | tf_op jit(solution)/shard_map/ppermute | solution.py:300
  58.1 28.9 %collective-permute-start.2 = (bf16[576,512]{1,0:T(8,128)(2,1)S(1)}, bf16[576,512]{1,0:T(8,128)(2,1)S(1)}, u32[]{:S(2)}, u32[]{:S(2)}) collective-permute-start(bf16[576,512]{1,0:T(8,128)(2,1)S(1)} %get-tuple-element.20), channel_id=1, source_target_pairs={{0,3},{1,2},{2,1},{3,0},{4,7},{5,6},{6,5},{7,4},{8,11},{9,10},{10,... | collective-permute-start | bytes 1769480 | tf_op jit(solution)/shard_map/ppermute | solution.py:300
  88.7 3.9 %copy-start.21 = (s32[256,4]{0,1:T(4,128)S(1)}, s32[256,4]{0,1:T(4,128)}, u32[]{:S(2)}) copy-start(s32[256,4]{0,1:T(4,128)} %param.28) | copy-start | bytes 12292
  88.7 8.9 %all-to-all-start.3 = ((bf16[4,256,128]{2,1,0:T(8,128)(2,1)}), bf16[4,256,128]{2,1,0:T(8,128)(2,1)S(1)}, u32[]{:S(2)}, u32[]{:S(2)}) async-start(bf16[4,256,128]{2,1,0:T(8,128)(2,1)} %shard_map.178), calls=%async_computation.3 | async-start | bytes 524288 | tf_op jit(solution)/shard_map/all_to_all | solution.py:295
  92.8 1.5 copy-start.1
  97.7 0.8 copy-start.18
  98.9 0.8 copy-start.8
  99.6 29.7 %copy-start.9 = (bf16[256,128]{1,0:T(8,128)(2,1)}, bf16[256,128]{1,0:T(8,128)(2,1)S(1)}, u32[]{:S(2)}) copy-start(bf16[256,128]{1,0:T(8,128)(2,1)S(1)} %get-tuple-element.24.m0.mid_ref) | copy-start | bytes 196612
  99.6 29.6 %copy-start.22 = (bf16[2048]{0:T(1024)(128)(2,1)S(1)}, bf16[2048]{0:T(1024)(128)(2,1)}, u32[]{:S(2)}) copy-start(bf16[2048]{0:T(1024)(128)(2,1)} %param.27) | copy-start | bytes 12292
  99.6 27.3 %all-to-all-start.4 = ((bf16[128,3,4,128]{3,2,1,0:T(4,128)(2,1)}), bf16[128,3,4,128]{3,2,1,0:T(4,128)(2,1)S(1)}, u32[]{:S(2)}, u32[]{:S(2)}) async-start(bf16[128,3,4,128]{3,2,1,0:T(4,128)(2,1)} %bitcast.16), calls=%async_computation.4 | async-start | bytes 786432 | tf_op jit(solution)/shard_map/all_to_all | solution.py:295
  109.1 20.2 %collective-permute-start.10 = (bf16[256,128]{1,0:T(8,128)(2,1)S(1)}, bf16[256,128]{1,0:T(8,128)(2,1)S(1)}, u32[]{:S(2)}, u32[]{:S(2)}) collective-permute-start(bf16[256,128]{1,0:T(8,128)(2,1)S(1)} %get-tuple-element.24.m0.mid_ref), channel_id=1, source_target_pairs={{0,8},{4,12},{8,0},{12,4},{1,9},{5,13},{9,1},{13,5},{2,10},{6,14},... | collective-permute-start | bytes 196616 | tf_op jit(solution)/shard_map/ppermute | solution.py:300
  115.5 13.8 %collective-permute-start.11 = (bf16[256,128]{1,0:T(8,128)(2,1)S(1)}, bf16[256,128]{1,0:T(8,128)(2,1)S(1)}, u32[]{:S(2)}, u32[]{:S(2)}) collective-permute-start(bf16[256,128]{1,0:T(8,128)(2,1)S(1)} %get-tuple-element.24.m0.mid_ref), channel_id=1, source_target_pairs={{0,12},{4,0},{8,4},{12,8},{1,13},{5,1},{9,5},{13,9},{2,14},{6,2},{... | collective-permute-start | bytes 196616 | tf_op jit(solution)/shard_map/ppermute | solution.py:300
  117.7 11.6 %collective-permute-start.9 = (bf16[256,128]{1,0:T(8,128)(2,1)S(1)}, bf16[256,128]{1,0:T(8,128)(2,1)S(1)}, u32[]{:S(2)}, u32[]{:S(2)}) collective-permute-start(bf16[256,128]{1,0:T(8,128)(2,1)S(1)} %get-tuple-element.24.m0.mid_ref), channel_id=1, source_target_pairs={{0,4},{4,8},{8,12},{12,0},{1,5},{5,9},{9,13},{13,1},{2,6},{6,10},{... | collective-permute-start | bytes 196616 | tf_op jit(solution)/shard_map/ppermute | solution.py:300
  126.9 15.1 %collective-permute-start.4 = (bf16[1536,128]{1,0:T(8,128)(2,1)S(1)}, bf16[1536,128]{1,0:T(8,128)(2,1)}, u32[]{:S(2)}, u32[]{:S(2)}) collective-permute-start(bf16[1536,128]{1,0:T(8,128)(2,1)S(1)} %bitcast.12), channel_id=1, source_target_pairs={{0,2},{2,0},{1,3},{3,1},{4,6},{6,4},{5,7},{7,5},{8,10},{10,8},{9,1... | collective-permute-start | bytes 1179656 | tf_op jit(solution)/shard_map/ppermute | solution.py:300
  130.2 0.9 copy-start
  131.1 34.2 %all-to-all-start.6 = ((bf16[4,256,384]{2,1,0:T(8,128)(2,1)}), bf16[4,256,384]{2,1,0:T(8,128)(2,1)S(1)}, u32[]{:S(2)}, u32[]{:S(2)}) async-start(bf16[4,256,384]{2,1,0:T(8,128)(2,1)} %copy-done), calls=%async_computation.6 | async-start | bytes 1572864 | tf_op jit(solution)/shard_map/all_to_all | solution.py:295
  140.1 4.3 %collective-permute-start.3 = (bf16[1536,128]{1,0:T(8,128)(2,1)S(1)}, bf16[1536,128]{1,0:T(8,128)(2,1)S(1)}, u32[]{:S(2)}, u32[]{:S(2)}) collective-permute-start(bf16[1536,128]{1,0:T(8,128)(2,1)S(1)} %bitcast.13), channel_id=1, source_target_pairs={{0,1},{1,0},{2,3},{3,2},{4,5},{5,4},{6,7},{7,6},{8,9},{9,8},{10,11... | collective-permute-start | bytes 1179656 | tf_op jit(solution)/shard_map/ppermute | solution.py:300
  142.1 3.9 %collective-permute-start.5 = (bf16[1536,128]{1,0:T(8,128)(2,1)}, bf16[1536,128]{1,0:T(8,128)(2,1)S(1)}, u32[]{:S(2)}, u32[]{:S(2)}) collective-permute-start(bf16[1536,128]{1,0:T(8,128)(2,1)} %collective-permute-done.4.x2), channel_id=1, source_target_pairs={{0,1},{1,0},{2,3},{3,2},{4,5},{5,4},{6,7},{7,6},{8,9},{9,8},{10,11... | collective-permute-start | bytes 1179656 | tf_op jit(solution)/shard_map/ppermute | solution.py:300
  146.0 1.2 copy-start.5
  147.2 1.2 copy-start.6
  151.5 8.3 %collective-permute-start.7 = (bf16[384,256]{1,0:T(8,128)(2,1)S(1)}, bf16[384,256]{1,0:T(8,128)(2,1)S(1)}, u32[]{:S(2)}, u32[]{:S(2)}) collective-permute-start(bf16[384,256]{1,0:T(8,128)(2,1)S(1)} %shard_map.180.h0), channel_id=1, source_target_pairs={{0,2},{2,0},{1,3},{3,1},{4,6},{6,4},{5,7},{7,5},{8,10},{10,8},{9,1... | collective-permute-start | bytes 589832 | tf_op jit(solution)/shard_map/ppermute | solution.py:300
  155.1 7.9 %collective-permute-start.6 = (bf16[384,256]{1,0:T(8,128)(2,1)S(1)}, bf16[384,256]{1,0:T(8,128)(2,1)S(1)}, u32[]{:S(2)}, u32[]{:S(2)}) collective-permute-start(bf16[384,256]{1,0:T(8,128)(2,1)S(1)} %shard_map.180.h0), channel_id=1, source_target_pairs={{0,1},{1,0},{2,3},{3,2},{4,5},{5,4},{6,7},{7,6},{8,9},{9,8},{10,11... | collective-permute-start | bytes 589832 | tf_op jit(solution)/shard_map/ppermute | solution.py:300
  159.8 4.0 %collective-permute-start.8 = (bf16[384,256]{1,0:T(8,128)(2,1)S(1)}, bf16[384,256]{1,0:T(8,128)(2,1)S(1)}, u32[]{:S(2)}, u32[]{:S(2)}) collective-permute-start(bf16[384,256]{1,0:T(8,128)(2,1)S(1)} %collective-permute-done.7.h2), channel_id=1, source_target_pairs={{0,1},{1,0},{2,3},{3,2},{4,5},{5,4},{6,7},{7,6},{8,9},{9,8},{10,11... | collective-permute-start | bytes 589832 | tf_op jit(solution)/shard_map/ppermute | solution.py:300
  165.3 26.6 %all-to-all-start.5 = ((bf16[128,3,4,128]{3,2,1,0:T(4,128)(2,1)}), bf16[128,3,4,128]{3,2,1,0:T(4,128)(2,1)S(1)}, u32[]{:S(2)}, u32[]{:S(2)}) async-start(bf16[128,3,4,128]{3,2,1,0:T(4,128)(2,1)} %bitcast.8), calls=%async_computation.5 | async-start | bytes 786432 | tf_op jit(solution)/shard_map/all_to_all | solution.py:295
  173.8 14.1 %copy-start.23 = (f32[256,4]{0,1:T(4,128)S(1)}, f32[256,4]{0,1:T(4,128)}, u32[]{:S(2)}) copy-start(f32[256,4]{0,1:T(4,128)} %param.29) | copy-start | bytes 12292
  174.0 14.1 %copy-start.2 = (s32[256,4]{1,0:T(8,128)S(1)}, s32[256,4]{1,0:T(8,128)}, u32[]{:S(2)}) copy-start(s32[256,4]{1,0:T(8,128)} %copy-done.1) | copy-start | bytes 12292
  174.0 16.1 %collective-permute-start.12 = (bf16[256,128]{1,0:T(8,128)(2,1)S(1)}, bf16[256,128]{1,0:T(8,128)(2,1)S(1)}, u32[]{:S(2)}, u32[]{:S(2)}) collective-permute-start(bf16[256,128]{1,0:T(8,128)(2,1)S(1)} %shard_map.184.h0), channel_id=1, source_target_pairs={{0,4},{4,8},{8,12},{12,0},{1,5},{5,9},{9,13},{13,1},{2,6},{6,10},{... | collective-permute-start | bytes 196616 | tf_op jit(solution)/shard_map/ppermute | solution.py:300
  177.5 13.3 %collective-permute-start.13 = (bf16[256,128]{1,0:T(8,128)(2,1)S(1)}, bf16[256,128]{1,0:T(8,128)(2,1)S(1)}, u32[]{:S(2)}, u32[]{:S(2)}) collective-permute-start(bf16[256,128]{1,0:T(8,128)(2,1)S(1)} %shard_map.184.h0), channel_id=1, source_target_pairs={{0,8},{4,12},{8,0},{12,4},{1,9},{5,13},{9,1},{13,5},{2,10},{6,14},... | collective-permute-start | bytes 196616 | tf_op jit(solution)/shard_map/ppermute | solution.py:300
  182.7 9.2 %collective-permute-start.14 = (bf16[256,128]{1,0:T(8,128)(2,1)S(1)}, bf16[256,128]{1,0:T(8,128)(2,1)S(1)}, u32[]{:S(2)}, u32[]{:S(2)}) collective-permute-start(bf16[256,128]{1,0:T(8,128)(2,1)S(1)} %shard_map.184.h0), channel_id=1, source_target_pairs={{0,12},{4,0},{8,4},{12,8},{1,13},{5,1},{9,5},{13,9},{2,14},{6,2},{... | collective-permute-start | bytes 196616 | tf_op jit(solution)/shard_map/ppermute | solution.py:300
  188.1 3.8 %copy-start.10 = (bf16[256,128]{1,0:T(8,128)(2,1)S(1)}, bf16[256,128]{1,0:T(8,128)(2,1)}, u32[]{:S(2)}) copy-start(bf16[256,128]{1,0:T(8,128)(2,1)} %copy-done.9) | copy-start | bytes 196612
  188.1 3.8 %copy-start.16 = (bf16[512,128]{1,0:T(8,128)(2,1)S(1)}, bf16[512,128]{1,0:T(8,128)(2,1)}, u32[]{:S(2)}) copy-start(bf16[512,128]{1,0:T(8,128)(2,1)} %down_ref.3) | copy-start | bytes 393220

commit v3 on v2

--- a/solution.py
+++ b/solution.py
@@ -29,15 +29,44 @@
 SMEM = pl.BlockSpec(memory_space=pltpu.SMEM)
 
 
-def call(kernel, outs, *args, scratch=(), smem=0, limit=24):
+def call(kernel, outs, *args, scratch=(), smem=0, fetch=(), late=False, limit=24):
     single = not isinstance(outs, list)
     shapes = [jax.ShapeDtypeStruct(s, t) for s, t in ([outs] if single else outs)]
+    n_in, n_out, n_scratch, n_fetch = len(args), len(shapes), len(scratch), len(fetch)
+    kept = n_in - n_fetch
+    buffers = []
+    for arg, rows in zip(args[kept:], fetch, strict=True):
+        buffers.append(pltpu.VMEM((rows[1], *arg.shape[1:]), arg.dtype))
+
+    def fetching(*refs):
+        sources, results = refs[kept:n_in], refs[n_in : n_in + n_out]
+        own = refs[n_in + n_out : n_in + n_out + n_scratch]
+        held, sems = refs[n_in + n_out + n_scratch : -1], refs[-1]
+        copies = [
+            pltpu.make_async_copy(src.at[pl.ds(rows[0], rows[1])], dst, sems.at[i])
+            for i, (src, dst, rows) in enumerate(zip(sources, held, fetch, strict=True))
+        ]
+        for copy in copies:
+            copy.start()
+
+        def ready():
+            for copy in copies:
+                copy.wait()
+
+        if late:
+            kernel(ready, *refs[:kept], *held, *results, *own)
+        else:
+            ready()
+            kernel(*refs[:kept], *held, *results, *own)
+
+    extra = buffers + [pltpu.SemaphoreType.DMA((n_fetch,))] if fetch else []
+    any_spec = pl.BlockSpec(memory_space=pl.ANY)
     got = pl.pallas_call(
-        kernel,
+        fetching if fetch else kernel,
         out_shape=shapes,
-        in_specs=[SMEM] * smem + [VMEM] * (len(args) - smem),
-        out_specs=[VMEM] * len(shapes),
-        scratch_shapes=list(scratch),
+        in_specs=[SMEM] * smem + [VMEM] * (kept - smem) + [any_spec] * n_fetch,
+        out_specs=[VMEM] * n_out,
+        scratch_shapes=list(scratch) + extra,
         compiler_params=pltpu.CompilerParams(vmem_limit_bytes=limit * 2**20),
         cost_estimate=pl.CostEstimate(
             flops=1000000, bytes_accessed=1000000, transcendentals=0
@@ -54,15 +83,22 @@
 
 def decays(decay_ref, extra_ref):
     raw = decay_ref[...].astype(F32)
-    logs = jax.nn.log_sigmoid(raw) / GATE_TEMPER + extra_ref[...]
+    logs = jax.nn.log_sigmoid(raw) / GATE_TEMPER
     rows = lax.broadcasted_iota(jnp.int32, (BLOCK, BLOCK), 0)
     cols = lax.broadcasted_iota(jnp.int32, (BLOCK, BLOCK), 1)
     lower = (rows >= cols).astype(F32)
-    inside = [
-        jnp.dot(lower, logs[b * BLOCK : (b + 1) * BLOCK], precision=HIGHEST,
-                preferred_element_type=F32)
-        for b in range(TOK // BLOCK)
-    ]
+    wide_rows = lax.broadcasted_iota(jnp.int32, (BLOCK, 128), 0)
+    wide_cols = lax.broadcasted_iota(jnp.int32, (BLOCK, 128), 1)
+    ones = jnp.ones((128, DK), F32)
+    inside = []
+    for b in range(TOK // BLOCK):
+        at = wide_cols - (b % 2) * BLOCK
+        extra = jnp.where((at >= 0) & (at <= wide_rows), extra_ref[b // 2 : b // 2 + 1, :], 0.0)
+        inside.append(
+            jnp.dot(lower, logs[b * BLOCK : (b + 1) * BLOCK], precision=HIGHEST,
+                    preferred_element_type=F32)
+            + jnp.dot(extra, ones, precision=HIGHEST, preferred_element_type=F32)
+        )
     return inside
 
 
@@ -124,7 +160,7 @@
         before = before + cum[BLOCK - 1 : BLOCK]
 
 
-def head_kernel(local_ref, start_ref, enter_ref, gate_ref, gain_ref, out_ref):
+def head_kernel(enter_ref, gain_ref, local_ref, start_ref, gate_ref, out_ref):
     mixed = local_ref[...] + nt(start_ref[...], enter_ref[...].astype(F32), precision=HIGHEST)
     scale = lax.rsqrt(jnp.mean(mixed * mixed, axis=-1, keepdims=True) + EPSILON)
     gate = jax.nn.silu(gate_ref[...].astype(F32))
@@ -140,7 +176,7 @@
         total = jnp.zeros((TOK, 256), F32)
         for h in range(4):
             lanes = slice(h * 128, (h + 1) * 128)
-            weight = jnp.concatenate([w[0:256, lanes] for w in pair], axis=1)
+            weight = jnp.concatenate([w[:, lanes] for w in pair], axis=1)
             total = total + jnp.dot(heads_ref[h], weight, preferred_element_type=F32)
         out_ref[part ^ m] = total[:, :128].astype(BF16)
         out_ref[part ^ (m + 1)] = total[:, 128:].astype(BF16)
@@ -198,7 +234,7 @@
         out_ref[rows, :] = picked.astype(BF16)
 
 
-def expert_kernel(ids_ref, x0, x1, x2, x3, gate_ref, up_ref, gain_ref, out_ref, wide_ref, rows_ref):
+def expert_kernel(ready, ids_ref, x0, x1, x2, x3, gain_ref, gate_ref, up_ref, out_ref, wide_ref, rows_ref):
     part = ids_ref[0]
     squares = jnp.zeros((SLOTS, 128), F32)
     for m, x_ref in enumerate((x0, x1, x2, x3)):
@@ -214,6 +250,7 @@
             scaled = (tile * gain_ref[pl.ds(slab, 1), :]).astype(BF16)
             rows_ref[:, pl.ds(pl.multiple_of(slab * 128, 128), 128)] = scaled
     scale = lax.rsqrt(jnp.sum(squares, axis=1, keepdims=True) * (1.0 / D) + EPSILON)
+    ready()
     gate = jnp.dot(rows_ref[...], gate_ref[...], preferred_element_type=F32) * scale
     up = jnp.dot(rows_ref[...], up_ref[...], preferred_element_type=F32) * scale
     out_ref[...] = (jax.nn.silu(gate) * up).astype(BF16)
@@ -263,14 +300,12 @@
     high = ssq.astype(BF16).astype(F32)
     lane = lax.broadcasted_iota(jnp.int32, (TOK, 128), 1)
     tail = jnp.where(lane == 0, high, jnp.where(lane == 1, ssq - high, 0.0)).astype(BF16)
-    pre = pre.astype(BF16)
-    for dest in range(4):
-        out_ref[dest, :, 0:256] = pre
-        out_ref[dest, :, 256:384] = tail
-
-
-def shared_hidden_kernel(in_ref, out_ref):
-    total = sum(in_ref[s].astype(F32) for s in range(4))
+    out_ref[:, 0:256] = pre.astype(BF16)
+    out_ref[:, 256:384] = tail
+
+
+def shared_hidden_kernel(r0, r1, r2, r3, out_ref):
+    total = sum(r[...].astype(F32) for r in (r0, r1, r2, r3))
     ssq = jnp.sum(total[:, 256:384], axis=1, keepdims=True)
     scale = lax.rsqrt(ssq * (1.0 / D) + EPSILON)
     hidden = jax.nn.silu(total[:, 0:128] * scale) * (total[:, 128:256] * scale)
@@ -335,15 +370,18 @@
     ids = jnp.stack([lax.axis_index(a) for a in (GROUP, "yg")]).astype(jnp.int32)
     gain = feedforward_gain.astype(F32).reshape(16, 128)
     head_gain = head_norm_gain.reshape(1, DV)
+    extra = extra_log_decay.reshape(2, 128)
+    whole = (0, TOK)
 
     payload = call(
         state_kernel, ((32, 16, DK), BF16),
-        key_matrix, value_matrix, decay_preactivation, extra_log_decay,
+        key_matrix, value_matrix, decay_preactivation, extra, fetch=(whole, whole, whole, (0, 2)), limit=60,
     )
     states = exchange(payload, SP)
     local, start = call(
         local_kernel, [((TOK, DV), F32), ((TOK, DK), F32)],
-        queries, key_matrix, value_matrix, decay_preactivation, extra_log_decay,
+        queries, key_matrix, value_matrix, decay_preactivation, extra,
+        fetch=(whole, whole, whole, whole, (0, 2)), limit=60,
     )
     pick = call(pick_kernel, ((ALL_SLOTS, TOK), BF16), routing)
     high, low = call(
@@ -359,11 +397,12 @@
     entering = exchange(call(scan_kernel, ((32, 8, DK), BF16), states), SP)
     head_rows = call(
         head_kernel, ((4, TOK, DV), BF16),
-        local, start, entering.reshape(DV, DK), output_gate_preactivation, head_gain,
+        entering.reshape(DV, DK), head_gain, local, start, output_gate_preactivation,
+        fetch=(whole, whole, whole),
     )
     partial = call(
         project_kernel, ((4, TOK, 128), BF16),
-        ids, exchange(head_rows, "yg"), *parts, smem=1,
+        ids, exchange(head_rows, "yg"), *parts, smem=1, fetch=(whole,) * 4,
     )
     outgoing, mid = call(
         dispatch_kernel, [((ALL_SLOTS, 128), BF16), ((TOK, 128), BF16)],
@@ -376,14 +415,14 @@
     beside = swapped(own, "c")
     far = swapped(across, "c")
     pre = call(
-        shared_in_kernel, ((4, TOK, 384), BF16), ids, *mids, *parts, gain, smem=1,
+        shared_in_kernel, ((TOK, 384), BF16), ids, *mids, *parts, gain, smem=1,
         scratch=[pltpu.VMEM((256, 512), BF16), pltpu.VMEM((4, TOK, 128), BF16)],
     )
-    pre = exchange(pre, GROUP)
+    pre = [pre] + grouped([pre] * 3)
     routed = call(
         expert_kernel, ((SLOTS, 256), BF16),
-        ids, own, beside, across, far, expert_gate_weight, expert_up_weight, gain,
-        smem=1,
+        ids, own, beside, across, far, gain, expert_gate_weight, expert_up_weight,
+        smem=1, fetch=((0, D), (0, D)), late=True,
         scratch=[pltpu.VMEM((4, 32 * PITCH, 128), F32), pltpu.VMEM((SLOTS, D), BF16)],
     )
     routed_across = swapped(routed, "yn")
@@ -395,7 +434,7 @@
         scratch=[pltpu.VMEM((32 * PITCH, 128), F32)],
     )
     back = exchange(expert_out.reshape(128, 3, 4, 128), SPG).reshape(ALL_SLOTS, 128)
-    hidden = call(shared_hidden_kernel, ((TOK, 128), BF16), pre)
+    hidden = call(shared_hidden_kernel, ((TOK, 128), BF16), *pre)
     hidden = [hidden] + shifted([hidden] * 3, "yg")
     return call(
         final_kernel, ((TOK, 128), BF16),

time: 197 us -> 225 us (1.14); the launches traced: 194 us -> 224 us
  blocking collectives: 22.8 us -> 51.6 us
  waiting for transfers between devices: 47.3 us -> 53.8 us
  starting transfers between devices: 94.7 us -> 89.8 us
  Pallas kernels: 18.5 us -> 22.3 us
  local copies, waits for them, and re-layouts: 9.73 us -> 6.11 us
    all_to_all x1 -> x2, blocking collectives: 22.8 us -> 51.6 us  [exchange(): return lax.all_to_all(value, axes, split_axis=0, concat_axis=0, tiled=True)]
    all_to_all x6 -> x4, starting transfers between devices: 41.8 us -> 22.3 us  [exchange(): return lax.all_to_all(value, axes, split_axis=0, concat_axis=0, tiled=True)]
    ppermute x15 -> x18, starting transfers between devices: 53 us -> 67.4 us  [moved(): lax.ppermute(value, axes, [(i, target(i) % count) for i in range(count)])]
    ppermute x15 -> x18, waiting for transfers between devices: 32.4 us -> 46 us  [moved(): lax.ppermute(value, axes, [(i, target(i) % count) for i in range(count)])]
    all_to_all x6 -> x4, waiting for transfers between devices: 14.9 us -> 7.88 us  [exchange(): return lax.all_to_all(value, axes, split_axis=0, concat_axis=0, tiled=True)]
    pallas_call x14, Pallas kernels: 18.5 us -> 22.3 us  [call(): pl.pallas_call(fetching if fetch else kernel, out_shape=shapes, in_specs=...]
    unnamed x53 -> x36, local copies, waits for them, and re-layouts: 9.73 us -> 6.11 us
  transfers between devices with their start and end apart: 21 -> 22, of which waited for: 10 -> 14; matrix products, arithmetic and copies ran while one was open for 0% -> 0% of each run, Pallas kernels for 6% -> 4%
where the time goes in v3:
time: 225 us; the launch traced here: 224 us
  starting transfers between devices  89.8 us (40%)
  waiting for transfers between devices  53.8 us (24%)
  blocking collectives  51.6 us (23%)
  Pallas kernels  22.3 us (10%)
  local copies, waits for them, and re-layouts  6.11 us (3%)
    ppermute x18, starting transfers between devices, moved(): lax.ppermute(value, axes, [(i, target(i) % count) for i in range(count)])  67.4 us
    all_to_all x2, blocking collectives, exchange(): return lax.all_to_all(value, axes, split_axis=0, concat_axis=0, tiled=True)  51.6 us
    ppermute x18, waiting for transfers between devices, moved(): lax.ppermute(value, axes, [(i, target(i) % count) for i in range(count)])  46 us
    all_to_all x4, starting transfers between devices, exchange(): return lax.all_to_all(value, axes, split_axis=0, concat_axis=0, tiled=True)  22.3 us
    pallas_call x14, Pallas kernels, call(): pl.pallas_call(fetching if fetch else kernel, out_shape=shapes, in_specs=...  22.3 us
    all_to_all x4, waiting for transfers between devices, exchange(): return lax.all_to_all(value, axes, split_axis=0, concat_axis=0, tiled=True)  7.88 us
    unnamed x36, local copies, waits for them, and re-layouts  6.11 us
  transfers between devices with their start and end apart: 22, of which 14 were waited for; matrix products, arithmetic and copies ran while one was open for 0% of the time, Pallas kernels for 4%

profile of v3, /device:TPU:1, one launch (start us, length us, event | category | flops | bytes accessed | tf_op | source)
XLA Modules:
  0.0 224.1 jit_solution(7628244977771242041)
XLA Ops:
  0.0 2.5 %shard_map.173 = bf16[32,16,128]{2,1,0:T(8,128)(2,1)} custom-call(bf16[256,128]{1,0:T(8,128)(2,1)} %refs_1_.3, bf16[256,256]{1,0:T(8,128)(2,1)} %refs_2_.3, bf16[256,128]{1,0:T(8,128)(2,1)} %refs_3_.1, f32[2,128]{1,0:T(2,128)} %bitcast.21), custom_call_target="tpu_custom_call" | custom-call | flops 1000000 | bytes 1000000 | tf_op jit(solution)/shard_map/pallas_call | solution.py:64
  2.5 23.1 %all_to_all.30.in_ref = bf16[32,16,128]{2,1,0:T(8,128)(2,1)S(1)} all-to-all(bf16[32,16,128]{2,1,0:T(8,128)(2,1)} %shard_map.173), channel_id=1, replica_groups=mesh['z'=8,'x'=4,'yg'=4,'yn'=2,'c'=2] {'z','x'}, dimensions={0} | all-to-all | bytes 262144 | tf_op jit(solution)/shard_map/all_to_all | solution.py:330
  25.6 0.7 shard_map.174
  26.3 3.9 %all-to-all-start.1 = ((bf16[32,8,128]{2,1,0:T(8,128)(2,1)}), bf16[32,8,128]{2,1,0:T(8,128)(2,1)S(1)}, u32[]{:S(2)}, u32[]{:S(2)}) async-start(bf16[32,8,128]{2,1,0:T(8,128)(2,1)} %shard_map.174), calls=%async_computation.1 | async-start | bytes 131072 | tf_op jit(solution)/shard_map/all_to_all | solution.py:330
  30.1 0.0 copy-start.16
  30.1 0.6 copy-done.16
  30.8 3.6 %shard_map.175 = (f32[256,256]{1,0:T(8,128)}, f32[256,128]{1,0:T(8,128)}) custom-call(bf16[256,128]{1,0:T(8,128)(2,1)} %refs_0_.3, bf16[256,128]{1,0:T(8,128)(2,1)} %refs_1_.3, bf16[256,256]{1,0:T(8,128)(2,1)} %refs_2_.3, bf16[256,128]{1,0:T(8,128)(2,1)} %refs_3_.1, f32[2,128]{1,0:T(2,128)} %bitcast.22), custom_call_target="tpu_custom_call" | custom-call | flops 1000000 | bytes 1000000 | tf_op jit(solution)/shard_map/pallas_call | solution.py:64
  34.4 0.1 pad_add_fusion.ids_ref.refs_0_
  34.5 4.5 %all-to-all-done.1 = bf16[32,8,128]{2,1,0:T(8,128)(2,1)S(1)} async-done(((bf16[32,8,128]{2,1,0:T(8,128)(2,1)}), bf16[32,8,128]{2,1,0:T(8,128)(2,1)S(1)}, u32[]{:S(2)}, u32[]{:S(2)}) %all-to-all-start.1) | async-done | bytes 65568 | tf_op jit(solution)/shard_map/all_to_all | solution.py:330
  39.0 0.9 copy-done.4
  40.0 0.9 copy-done.8
  40.9 1.6 shard_map.176
  42.5 0.0 copy-start
  42.5 7.0 %all-to-all-start.2 = ((bf16[4,256,256]{2,1,0:T(8,128)(2,1)}), bf16[4,256,256]{2,1,0:T(8,128)(2,1)S(1)}, u32[]{:S(2)}, u32[]{:S(2)}) async-start(bf16[4,256,256]{2,1,0:T(8,128)(2,1)} %shard_map.176), calls=%async_computation.2 | async-start | bytes 1048576 | tf_op jit(solution)/shard_map/all_to_all | solution.py:330
  49.5 1.2 copy-done.1
  50.8 1.0 shard_map.177
  51.8 5.4 %collective-permute-start = (bf16[576,512]{1,0:T(8,128)(2,1)S(1)}, bf16[576,512]{1,0:T(8,128)(2,1)S(1)}, u32[]{:S(2)}, u32[]{:S(2)}) collective-permute-start(bf16[576,512]{1,0:T(8,128)(2,1)S(1)} %get-tuple-element.18), channel_id=1, source_target_pairs={{0,1},{1,0},{2,3},{3,2},{4,5},{5,4},{6,7},{7,6},{8,9},{9,8},{10,11... | collective-permute-start | bytes 1769480 | tf_op jit(solution)/shard_map/ppermute | solution.py:335
  57.2 2.4 %collective-permute-start.1 = (bf16[576,512]{1,0:T(8,128)(2,1)S(1)}, bf16[576,512]{1,0:T(8,128)(2,1)S(1)}, u32[]{:S(2)}, u32[]{:S(2)}) collective-permute-start(bf16[576,512]{1,0:T(8,128)(2,1)S(1)} %get-tuple-element.19), channel_id=1, source_target_pairs={{0,2},{1,3},{2,0},{3,1},{4,6},{5,7},{6,4},{7,5},{8,10},{9,11},{10,... | collective-permute-start | bytes 1769480 | tf_op jit(solution)/shard_map/ppermute | solution.py:335
  59.5 3.1 %collective-permute-start.2 = (bf16[576,512]{1,0:T(8,128)(2,1)S(1)}, bf16[576,512]{1,0:T(8,128)(2,1)S(1)}, u32[]{:S(2)}, u32[]{:S(2)}) collective-permute-start(bf16[576,512]{1,0:T(8,128)(2,1)S(1)} %get-tuple-element.20), channel_id=1, source_target_pairs={{0,3},{1,2},{2,1},{3,0},{4,7},{5,6},{6,5},{7,4},{8,11},{9,10},{10,... | collective-permute-start | bytes 1769480 | tf_op jit(solution)/shard_map/ppermute | solution.py:335
  62.7 13.1 %collective-permute-done.1.refs_4_.d2.w2 = bf16[576,512]{1,0:T(8,128)(2,1)S(1)} collective-permute-done((bf16[576,512]{1,0:T(8,128)(2,1)S(1)}, bf16[576,512]{1,0:T(8,128)(2,1)S(1)}, u32[]{:S(2)}, u32[]{:S(2)}) %collective-permute-start.1) | collective-permute-done | bytes 589856 | tf_op jit(solution)/shard_map/ppermute | solution.py:335
  75.8 12.6 %collective-permute-done.2.refs_5_.d3.w3 = bf16[576,512]{1,0:T(8,128)(2,1)S(1)} collective-permute-done((bf16[576,512]{1,0:T(8,128)(2,1)S(1)}, bf16[576,512]{1,0:T(8,128)(2,1)S(1)}, u32[]{:S(2)}, u32[]{:S(2)}) %collective-permute-start.2) | collective-permute-done | bytes 589856 | tf_op jit(solution)/shard_map/ppermute | solution.py:335
  88.4 1.8 shard_map.178
  90.3 3.8 %all-to-all-start.3 = ((bf16[4,256,128]{2,1,0:T(8,128)(2,1)}), bf16[4,256,128]{2,1,0:T(8,128)(2,1)S(1)}, u32[]{:S(2)}, u32[]{:S(2)}) async-start(bf16[4,256,128]{2,1,0:T(8,128)(2,1)} %shard_map.178), calls=%async_computation.3 | async-start | bytes 524288 | tf_op jit(solution)/shard_map/all_to_all | solution.py:330
  94.1 0.1 copy.19.routing_ref
  94.2 1.5 shard_map.172.pick_ref
  95.7 3.4 %all-to-all-done.3.in_ref = bf16[4,256,128]{2,1,0:T(8,128)(2,1)S(1)} async-done(((bf16[4,256,128]{2,1,0:T(8,128)(2,1)}), bf16[4,256,128]{2,1,0:T(8,128)(2,1)S(1)}, u32[]{:S(2)}, u32[]{:S(2)}) %all-to-all-start.3) | async-done | bytes 262176 | tf_op jit(solution)/shard_map/all_to_all | solution.py:330
  99.1 0.8 copy-done.10
  99.9 0.4 shard_map.179
  100.3 0.0 copy-start.5
  100.3 28.5 %all_to_all.31 = bf16[128,3,4,128]{3,2,1,0:T(4,128)(2,1)S(1)} all-to-all(bf16[128,3,4,128]{3,2,1,0:T(4,128)(2,1)S(1)} %bitcast.17), channel_id=1, replica_groups=mesh['z'=8,'x'=4,'yg'=4,'yn'=2,'c'=2] {'z','x','yg'}, dimensions={0} | all-to-all | bytes 786432 | tf_op jit(solution)/shard_map/all_to_all | solution.py:330
  128.8 2.5 %collective-permute-start.4 = (bf16[1536,128]{1,0:T(8,128)(2,1)S(1)}, bf16[1536,128]{1,0:T(8,128)(2,1)S(1)}, u32[]{:S(2)}, u32[]{:S(2)}) collective-permute-start(bf16[1536,128]{1,0:T(8,128)(2,1)S(1)} %bitcast.13), channel_id=1, source_target_pairs={{0,2},{2,0},{1,3},{3,1},{4,6},{6,4},{5,7},{7,5},{8,10},{10,8},{9,1... | collective-permute-start | bytes 1179656 | tf_op jit(solution)/shard_map/ppermute | solution.py:335
  131.4 4.5 %collective-permute-start.3 = (bf16[1536,128]{1,0:T(8,128)(2,1)S(1)}, bf16[1536,128]{1,0:T(8,128)(2,1)S(1)}, u32[]{:S(2)}, u32[]{:S(2)}) collective-permute-start(bf16[1536,128]{1,0:T(8,128)(2,1)S(1)} %bitcast.14), channel_id=1, source_target_pairs={{0,1},{1,0},{2,3},{3,2},{4,5},{5,4},{6,7},{7,6},{8,9},{9,8},{10,11... | collective-permute-start | bytes 1179656 | tf_op jit(solution)/shard_map/ppermute | solution.py:335
  135.9 2.5 %collective-permute-done.4.refs_3_ = bf16[1536,128]{1,0:T(8,128)(2,1)S(1)} collective-permute-done((bf16[1536,128]{1,0:T(8,128)(2,1)S(1)}, bf16[1536,128]{1,0:T(8,128)(2,1)S(1)}, u32[]{:S(2)}, u32[]{:S(2)}) %collective-permute-start.4) | collective-permute-done | bytes 393248 | tf_op jit(solution)/shard_map/ppermute | solution.py:335
  138.4 5.7 %collective-permute-start.5 = (bf16[1536,128]{1,0:T(8,128)(2,1)S(1)}, bf16[1536,128]{1,0:T(8,128)(2,1)S(1)}, u32[]{:S(2)}, u32[]{:S(2)}) collective-permute-start(bf16[1536,128]{1,0:T(8,128)(2,1)S(1)} %collective-permute-done.4.refs_3_), channel_id=1, source_target_pairs={{0,1},{1,0},{2,3},{3,2},{4,5},{5,4},{6,7},{7,6},{8,9},{9,8},{10,11... | collective-permute-start | bytes 1179656 | tf_op jit(solution)/shard_map/ppermute | solution.py:335
  144.2 1.3 collective-permute-done.5.refs_4_
  145.5 1.2 copy-done.3
  146.7 2.9 %shard_map.180.h0 = bf16[384,256]{1,0:T(8,128)(2,1)S(1)} custom-call(s32[2]{0:T(128)S(1)} %pad_add_fusion.ids_ref.refs_0_, bf16[1536,128]{1,0:T(8,128)(2,1)S(1)} %bitcast.15, bf16[1536,128]{1,0:T(8,128)(2,1)S(1)} %collective-permute-done.3.refs_2_, bf16[1536,128]{1,0:T(8,128)(2,1)S(1)} %collective-permute-done.4.refs_3_, ...), custom_call_target="tpu_custom_call" | custom-call | flops 1000000 | bytes 1000000 | tf_op jit(solution)/shard_map/pallas_call | solution.py:64
  149.6 2.5 %collective-permute-start.7 = (bf16[384,256]{1,0:T(8,128)(2,1)S(1)}, bf16[384,256]{1,0:T(8,128)(2,1)S(1)}, u32[]{:S(2)}, u32[]{:S(2)}) collective-permute-start(bf16[384,256]{1,0:T(8,128)(2,1)S(1)} %shard_map.180.h0), channel_id=1, source_target_pairs={{0,2},{2,0},{1,3},{3,1},{4,6},{6,4},{5,7},{7,5},{8,10},{10,8},{9,1... | collective-permute-start | bytes 589832 | tf_op jit(solution)/shard_map/ppermute | solution.py:335
  152.2 2.6 %collective-permute-start.6 = (bf16[384,256]{1,0:T(8,128)(2,1)S(1)}, bf16[384,256]{1,0:T(8,128)(2,1)S(1)}, u32[]{:S(2)}, u32[]{:S(2)}) collective-permute-start(bf16[384,256]{1,0:T(8,128)(2,1)S(1)} %shard_map.180.h0), channel_id=1, source_target_pairs={{0,1},{1,0},{2,3},{3,2},{4,5},{5,4},{6,7},{7,6},{8,9},{9,8},{10,11... | collective-permute-start | bytes 589832 | tf_op jit(solution)/shard_map/ppermute | solution.py:335
  154.8 2.9 %collective-permute-done.7.h2 = bf16[384,256]{1,0:T(8,128)(2,1)S(1)} collective-permute-done((bf16[384,256]{1,0:T(8,128)(2,1)S(1)}, bf16[384,256]{1,0:T(8,128)(2,1)S(1)}, u32[]{:S(2)}, u32[]{:S(2)}) %collective-permute-start.7) | collective-permute-done | bytes 196640 | tf_op jit(solution)/shard_map/ppermute | solution.py:335
  157.6 3.1 %collective-permute-start.8 = (bf16[384,256]{1,0:T(8,128)(2,1)S(1)}, bf16[384,256]{1,0:T(8,128)(2,1)S(1)}, u32[]{:S(2)}, u32[]{:S(2)}) collective-permute-start(bf16[384,256]{1,0:T(8,128)(2,1)S(1)} %collective-permute-done.7.h2), channel_id=1, source_target_pairs={{0,1},{1,0},{2,3},{3,2},{4,5},{5,4},{6,7},{7,6},{8,9},{9,8},{10,11... | collective-permute-start | bytes 589832 | tf_op jit(solution)/shard_map/ppermute | solution.py:335
  160.8 1.0 collective-permute-done.8.h3
  161.8 1.4 shard_map.181
  163.2 7.7 %all-to-all-start.5 = ((bf16[128,3,4,128]{3,2,1,0:T(4,128)(2,1)}), bf16[128,3,4,128]{3,2,1,0:T(4,128)(2,1)S(1)}, u32[]{:S(2)}, u32[]{:S(2)}) async-start(bf16[128,3,4,128]{3,2,1,0:T(4,128)(2,1)} %bitcast.9), calls=%async_computation.5 | async-start | bytes 786432 | tf_op jit(solution)/shard_map/all_to_all | solution.py:330
  171.0 6.4 %collective-permute-start.10 = (bf16[256,128]{1,0:T(8,128)(2,1)S(1)}, bf16[256,128]{1,0:T(8,128)(2,1)S(1)}, u32[]{:S(2)}, u32[]{:S(2)}) collective-permute-start(bf16[256,128]{1,0:T(8,128)(2,1)S(1)} %copy-done.6), channel_id=1, source_target_pairs={{0,8},{4,12},{8,0},{12,4},{1,9},{5,13},{9,1},{13,5},{2,10},{6,14},... | collective-permute-start | bytes 196616 | tf_op jit(solution)/shard_map/ppermute | solution.py:335
  177.4 2.2 collective-permute-start.11
  179.6 4.0 %collective-permute-start.9 = (bf16[256,128]{1,0:T(8,128)(2,1)S(1)}, bf16[256,128]{1,0:T(8,128)(2,1)S(1)}, u32[]{:S(2)}, u32[]{:S(2)}) collective-permute-start(bf16[256,128]{1,0:T(8,128)(2,1)S(1)} %copy-done.6), channel_id=1, source_target_pairs={{0,4},{4,8},{8,12},{12,0},{1,5},{5,9},{9,13},{13,1},{2,6},{6,10},{... | collective-permute-start | bytes 196616 | tf_op jit(solution)/shard_map/ppermute | solution.py:335
  183.6 1.6 collective-permute-done.10.m2
  185.2 1.7 collective-permute-done.11.m3
  186.9 0.1 collective-permute-done.9.m1
  187.0 0.9 shard_map.183.r0
  187.9 5.5 %collective-permute-start.12 = (bf16[256,384]{1,0:T(8,128)(2,1)S(1)}, bf16[256,384]{1,0:T(8,128)(2,1)S(1)}, u32[]{:S(2)}, u32[]{:S(2)}) collective-permute-start(bf16[256,384]{1,0:T(8,128)(2,1)S(1)} %shard_map.183.r0), channel_id=1, source_target_pairs={{0,1},{1,0},{2,3},{3,2},{4,5},{5,4},{6,7},{7,6},{8,9},{9,8},{10,11... | collective-permute-start | bytes 589832 | tf_op jit(solution)/shard_map/ppermute | solution.py:335
  193.4 1.9 collective-permute-start.13
  195.3 3.5 %collective-permute-start.14 = (bf16[256,384]{1,0:T(8,128)(2,1)S(1)}, bf16[256,384]{1,0:T(8,128)(2,1)S(1)}, u32[]{:S(2)}, u32[]{:S(2)}) collective-permute-start(bf16[256,384]{1,0:T(8,128)(2,1)S(1)} %shard_map.183.r0), channel_id=1, source_target_pairs={{0,3},{1,2},{2,1},{3,0},{4,7},{5,6},{6,5},{7,4},{8,11},{9,10},{10,... | collective-permute-start | bytes 589832 | tf_op jit(solution)/shard_map/ppermute | solution.py:335
  198.9 2.9 %collective-permute-done.13.r2 = bf16[256,384]{1,0:T(8,128)(2,1)S(1)} collective-permute-done((bf16[256,384]{1,0:T(8,128)(2,1)S(1)}, bf16[256,384]{1,0:T(8,128)(2,1)S(1)}, u32[]{:S(2)}, u32[]{:S(2)}) %collective-permute-start.13) | collective-permute-done | bytes 196640 | tf_op jit(solution)/shard_map/ppermute | solution.py:335
  201.8 4.4 %collective-permute-done.14.r3 = bf16[256,384]{1,0:T(8,128)(2,1)S(1)} collective-permute-done((bf16[256,384]{1,0:T(8,128)(2,1)S(1)}, bf16[256,384]{1,0:T(8,128)(2,1)S(1)}, u32[]{:S(2)}, u32[]{:S(2)}) %collective-permute-start.14) | collective-permute-done | bytes 196640 | tf_op jit(solution)/shard_map/ppermute | solution.py:335
  206.2 0.1 shard_map.184.h0
  206.3 2.3 %collective-permute-start.15 = (bf16[256,128]{1,0:T(8,128)(2,1)S(1)}, bf16[256,128]{1,0:T(8,128)(2,1)S(1)}, u32[]{:S(2)}, u32[]{:S(2)}) collective-permute-start(bf16[256,128]{1,0:T(8,128)(2,1)S(1)} %shard_map.184.h0), channel_id=1, source_target_pairs={{0,4},{4,8},{8,12},{12,0},{1,5},{5,9},{9,13},{13,1},{2,6},{6,10},{... | collective-permute-start | bytes 196616 | tf_op jit(solution)/shard_map/ppermute | solution.py:335
  208.6 4.3 %collective-permute-start.16 = (bf16[256,128]{1,0:T(8,128)(2,1)S(1)}, bf16[256,128]{1,0:T(8,128)(2,1)S(1)}, u32[]{:S(2)}, u32[]{:S(2)}) collective-permute-start(bf16[256,128]{1,0:T(8,128)(2,1)S(1)} %shard_map.184.h0), channel_id=1, source_target_pairs={{0,8},{4,12},{8,0},{12,4},{1,9},{5,13},{9,1},{13,5},{2,10},{6,14},... | collective-permute-start | bytes 196616 | tf_op jit(solution)/shard_map/ppermute | solution.py:335
  212.9 5.5 %collective-permute-start.17 = (bf16[256,128]{1,0:T(8,128)(2,1)S(1)}, bf16[256,128]{1,0:T(8,128)(2,1)S(1)}, u32[]{:S(2)}, u32[]{:S(2)}) collective-permute-start(bf16[256,128]{1,0:T(8,128)(2,1)S(1)} %shard_map.184.h0), channel_id=1, source_target_pairs={{0,12},{4,0},{8,4},{12,8},{1,13},{5,1},{9,5},{13,9},{2,14},{6,2},{... | collective-permute-start | bytes 196616 | tf_op jit(solution)/shard_map/ppermute | solution.py:335
  218.4 0.1 copy.21.score_ref
  218.5 2.0 shard_map.182
  220.5 1.8 collective-permute-done.17.h3
  222.3 1.8 shard_map.185
  (36 shorter events, 0.1 us)
Async XLA Ops:
  26.3 12.7 %all-to-all-start.1 = ((bf16[32,8,128]{2,1,0:T(8,128)(2,1)}), bf16[32,8,128]{2,1,0:T(8,128)(2,1)S(1)}, u32[]{:S(2)}, u32[]{:S(2)}) async-start(bf16[32,8,128]{2,1,0:T(8,128)(2,1)} %shard_map.174), calls=%async_computation.1 | async-start | bytes 131072 | tf_op jit(solution)/shard_map/all_to_all | solution.py:330
  30.1 0.7 copy-start.16
  30.8 8.2 %copy-start.7 = (bf16[256,256]{1,0:T(8,128)(2,1)S(1)}, bf16[256,256]{1,0:T(8,128)(2,1)}, u32[]{:S(2)}) copy-start(bf16[256,256]{1,0:T(8,128)(2,1)} %refs_4_.1) | copy-start | bytes 393220
  39.0 1.0 copy-start.4
  40.0 0.9 copy-start.8
  40.9 8.6 %copy-start.11 = (bf16[2048,32]{0,1:T(8,128)(2,1)S(1)}, bf16[2048,32]{0,1:T(8,128)(2,1)}, u32[]{:S(2)}) copy-start(bf16[2048,32]{0,1:T(8,128)(2,1)} %param.34) | copy-start | bytes 393220
  40.9 8.6 %copy-start.12 = (bf16[2048,32]{0,1:T(8,128)(2,1)S(1)}, bf16[2048,32]{0,1:T(8,128)(2,1)}, u32[]{:S(2)}) copy-start(bf16[2048,32]{0,1:T(8,128)(2,1)} %param.33) | copy-start | bytes 393220
  42.5 7.0 %copy-start = (bf16[4096,128]{1,0:T(8,128)(2,1)S(1)}, bf16[4096,128]{1,0:T(8,128)(2,1)}, u32[]{:S(2)}) copy-start(bf16[4096,128]{1,0:T(8,128)(2,1)} %project_ref.1) | copy-start | bytes 3145732
  42.5 45.9 %all-to-all-start.2 = ((bf16[4,256,256]{2,1,0:T(8,128)(2,1)}), bf16[4,256,256]{2,1,0:T(8,128)(2,1)S(1)}, u32[]{:S(2)}, u32[]{:S(2)}) async-start(bf16[4,256,256]{2,1,0:T(8,128)(2,1)} %shard_map.176), calls=%async_computation.2 | async-start | bytes 1048576 | tf_op jit(solution)/shard_map/all_to_all | solution.py:330
  49.5 1.2 copy-start.1
  51.8 10.9 %collective-permute-start = (bf16[576,512]{1,0:T(8,128)(2,1)S(1)}, bf16[576,512]{1,0:T(8,128)(2,1)S(1)}, u32[]{:S(2)}, u32[]{:S(2)}) collective-permute-start(bf16[576,512]{1,0:T(8,128)(2,1)S(1)} %get-tuple-element.18), channel_id=1, source_target_pairs={{0,1},{1,0},{2,3},{3,2},{4,5},{5,4},{6,7},{7,6},{8,9},{9,8},{10,11... | collective-permute-start | bytes 1769480 | tf_op jit(solution)/shard_map/ppermute | solution.py:335
  57.2 18.6 %collective-permute-start.1 = (bf16[576,512]{1,0:T(8,128)(2,1)S(1)}, bf16[576,512]{1,0:T(8,128)(2,1)S(1)}, u32[]{:S(2)}, u32[]{:S(2)}) collective-permute-start(bf16[576,512]{1,0:T(8,128)(2,1)S(1)} %get-tuple-element.19), channel_id=1, source_target_pairs={{0,2},{1,3},{2,0},{3,1},{4,6},{5,7},{6,4},{7,5},{8,10},{9,11},{10,... | collective-permute-start | bytes 1769480 | tf_op jit(solution)/shard_map/ppermute | solution.py:335
  59.5 28.9 %collective-permute-start.2 = (bf16[576,512]{1,0:T(8,128)(2,1)S(1)}, bf16[576,512]{1,0:T(8,128)(2,1)S(1)}, u32[]{:S(2)}, u32[]{:S(2)}) collective-permute-start(bf16[576,512]{1,0:T(8,128)(2,1)S(1)} %get-tuple-element.20), channel_id=1, source_target_pairs={{0,3},{1,2},{2,1},{3,0},{4,7},{5,6},{6,5},{7,4},{8,11},{9,10},{10,... | collective-permute-start | bytes 1769480 | tf_op jit(solution)/shard_map/ppermute | solution.py:335
  90.3 3.8 %copy-start.13 = (s32[256,4]{0,1:T(4,128)S(1)}, s32[256,4]{0,1:T(4,128)}, u32[]{:S(2)}) copy-start(s32[256,4]{0,1:T(4,128)} %param.28) | copy-start | bytes 12292
  90.3 8.8 %all-to-all-start.3 = ((bf16[4,256,128]{2,1,0:T(8,128)(2,1)}), bf16[4,256,128]{2,1,0:T(8,128)(2,1)S(1)}, u32[]{:S(2)}, u32[]{:S(2)}) async-start(bf16[4,256,128]{2,1,0:T(8,128)(2,1)} %shard_map.178), calls=%async_computation.3 | async-start | bytes 524288 | tf_op jit(solution)/shard_map/all_to_all | solution.py:330
  99.1 0.8 copy-start.10
  99.9 45.6 %copy-start.2 = (bf16[2048,256]{1,0:T(8,128)(2,1)S(1)}, bf16[2048,256]{1,0:T(8,128)(2,1)}, u32[]{:S(2)}) copy-start(bf16[2048,256]{1,0:T(8,128)(2,1)} %refs_6_.1) | copy-start | bytes 3145732
  100.3 28.5 %copy-start.5 = (bf16[256,128]{1,0:T(8,128)(2,1)}, bf16[256,128]{1,0:T(8,128)(2,1)S(1)}, u32[]{:S(2)}) copy-start(bf16[256,128]{1,0:T(8,128)(2,1)S(1)} %get-tuple-element.24.m0.mid_ref) | copy-start | bytes 196612
  100.3 43.8 %copy-start.14 = (bf16[2048]{0:T(1024)(128)(2,1)S(1)}, bf16[2048]{0:T(1024)(128)(2,1)}, u32[]{:S(2)}) copy-start(bf16[2048]{0:T(1024)(128)(2,1)} %param.27) | copy-start | bytes 12292
  128.8 9.6 %collective-permute-start.4 = (bf16[1536,128]{1,0:T(8,128)(2,1)S(1)}, bf16[1536,128]{1,0:T(8,128)(2,1)S(1)}, u32[]{:S(2)}, u32[]{:S(2)}) collective-permute-start(bf16[1536,128]{1,0:T(8,128)(2,1)S(1)} %bitcast.13), channel_id=1, source_target_pairs={{0,2},{2,0},{1,3},{3,1},{4,6},{6,4},{5,7},{7,5},{8,10},{10,8},{9,1... | collective-permute-start | bytes 1179656 | tf_op jit(solution)/shard_map/ppermute | solution.py:335
  131.4 12.8 %collective-permute-start.3 = (bf16[1536,128]{1,0:T(8,128)(2,1)S(1)}, bf16[1536,128]{1,0:T(8,128)(2,1)S(1)}, u32[]{:S(2)}, u32[]{:S(2)}) collective-permute-start(bf16[1536,128]{1,0:T(8,128)(2,1)S(1)} %bitcast.14), channel_id=1, source_target_pairs={{0,1},{1,0},{2,3},{3,2},{4,5},{5,4},{6,7},{7,6},{8,9},{9,8},{10,11... | collective-permute-start | bytes 1179656 | tf_op jit(solution)/shard_map/ppermute | solution.py:335
  138.4 7.1 %collective-permute-start.5 = (bf16[1536,128]{1,0:T(8,128)(2,1)S(1)}, bf16[1536,128]{1,0:T(8,128)(2,1)S(1)}, u32[]{:S(2)}, u32[]{:S(2)}) collective-permute-start(bf16[1536,128]{1,0:T(8,128)(2,1)S(1)} %collective-permute-done.4.refs_3_), channel_id=1, source_target_pairs={{0,1},{1,0},{2,3},{3,2},{4,5},{5,4},{6,7},{7,6},{8,9},{9,8},{10,11... | collective-permute-start | bytes 1179656 | tf_op jit(solution)/shard_map/ppermute | solution.py:335
  145.5 1.2 copy-start.3
  149.6 8.0 %collective-permute-start.7 = (bf16[384,256]{1,0:T(8,128)(2,1)S(1)}, bf16[384,256]{1,0:T(8,128)(2,1)S(1)}, u32[]{:S(2)}, u32[]{:S(2)}) collective-permute-start(bf16[384,256]{1,0:T(8,128)(2,1)S(1)} %shard_map.180.h0), channel_id=1, source_target_pairs={{0,2},{2,0},{1,3},{3,1},{4,6},{6,4},{5,7},{7,5},{8,10},{10,8},{9,1... | collective-permute-start | bytes 589832 | tf_op jit(solution)/shard_map/ppermute | solution.py:335
  152.2 8.6 %collective-permute-start.6 = (bf16[384,256]{1,0:T(8,128)(2,1)S(1)}, bf16[384,256]{1,0:T(8,128)(2,1)S(1)}, u32[]{:S(2)}, u32[]{:S(2)}) collective-permute-start(bf16[384,256]{1,0:T(8,128)(2,1)S(1)} %shard_map.180.h0), channel_id=1, source_target_pairs={{0,1},{1,0},{2,3},{3,2},{4,5},{5,4},{6,7},{7,6},{8,9},{9,8},{10,11... | collective-permute-start | bytes 589832 | tf_op jit(solution)/shard_map/ppermute | solution.py:335
  157.6 4.2 %collective-permute-start.8 = (bf16[384,256]{1,0:T(8,128)(2,1)S(1)}, bf16[384,256]{1,0:T(8,128)(2,1)S(1)}, u32[]{:S(2)}, u32[]{:S(2)}) collective-permute-start(bf16[384,256]{1,0:T(8,128)(2,1)S(1)} %collective-permute-done.7.h2), channel_id=1, source_target_pairs={{0,1},{1,0},{2,3},{3,2},{4,5},{5,4},{6,7},{7,6},{8,9},{9,8},{10,11... | collective-permute-start | bytes 589832 | tf_op jit(solution)/shard_map/ppermute | solution.py:335
  163.2 7.7 %copy-start.6 = (bf16[256,128]{1,0:T(8,128)(2,1)S(1)}, bf16[256,128]{1,0:T(8,128)(2,1)}, u32[]{:S(2)}) copy-start(bf16[256,128]{1,0:T(8,128)(2,1)} %copy-done.5) | copy-start | bytes 196612
  163.2 59.1 %all-to-all-start.5 = ((bf16[128,3,4,128]{3,2,1,0:T(4,128)(2,1)}), bf16[128,3,4,128]{3,2,1,0:T(4,128)(2,1)S(1)}, u32[]{:S(2)}, u32[]{:S(2)}) async-start(bf16[128,3,4,128]{3,2,1,0:T(4,128)(2,1)} %bitcast.9), calls=%async_computation.5 | async-start | bytes 786432 | tf_op jit(solution)/shard_map/all_to_all | solution.py:330
  171.0 14.2 %collective-permute-start.10 = (bf16[256,128]{1,0:T(8,128)(2,1)S(1)}, bf16[256,128]{1,0:T(8,128)(2,1)S(1)}, u32[]{:S(2)}, u32[]{:S(2)}) collective-permute-start(bf16[256,128]{1,0:T(8,128)(2,1)S(1)} %copy-done.6), channel_id=1, source_target_pairs={{0,8},{4,12},{8,0},{12,4},{1,9},{5,13},{9,1},{13,5},{2,10},{6,14},... | collective-permute-start | bytes 196616 | tf_op jit(solution)/shard_map/ppermute | solution.py:335
  177.4 9.5 %collective-permute-start.11 = (bf16[256,128]{1,0:T(8,128)(2,1)S(1)}, bf16[256,128]{1,0:T(8,128)(2,1)S(1)}, u32[]{:S(2)}, u32[]{:S(2)}) collective-permute-start(bf16[256,128]{1,0:T(8,128)(2,1)S(1)} %copy-done.6), channel_id=1, source_target_pairs={{0,12},{4,0},{8,4},{12,8},{1,13},{5,1},{9,5},{13,9},{2,14},{6,2},{... | collective-permute-start | bytes 196616 | tf_op jit(solution)/shard_map/ppermute | solution.py:335
  179.6 7.4 %collective-permute-start.9 = (bf16[256,128]{1,0:T(8,128)(2,1)S(1)}, bf16[256,128]{1,0:T(8,128)(2,1)S(1)}, u32[]{:S(2)}, u32[]{:S(2)}) collective-permute-start(bf16[256,128]{1,0:T(8,128)(2,1)S(1)} %copy-done.6), channel_id=1, source_target_pairs={{0,4},{4,8},{8,12},{12,0},{1,5},{5,9},{9,13},{13,1},{2,6},{6,10},{... | collective-permute-start | bytes 196616 | tf_op jit(solution)/shard_map/ppermute | solution.py:335
  187.9 30.5 %copy-start.15 = (f32[256,4]{0,1:T(4,128)S(1)}, f32[256,4]{0,1:T(4,128)}, u32[]{:S(2)}) copy-start(f32[256,4]{0,1:T(4,128)} %param.29) | copy-start | bytes 12292
  187.9 11.0 %collective-permute-start.12 = (bf16[256,384]{1,0:T(8,128)(2,1)S(1)}, bf16[256,384]{1,0:T(8,128)(2,1)S(1)}, u32[]{:S(2)}, u32[]{:S(2)}) collective-permute-start(bf16[256,384]{1,0:T(8,128)(2,1)S(1)} %shard_map.183.r0), channel_id=1, source_target_pairs={{0,1},{1,0},{2,3},{3,2},{4,5},{5,4},{6,7},{7,6},{8,9},{9,8},{10,11... | collective-permute-start | bytes 589832 | tf_op jit(solution)/shard_map/ppermute | solution.py:335
  193.4 8.3 %collective-permute-start.13 = (bf16[256,384]{1,0:T(8,128)(2,1)S(1)}, bf16[256,384]{1,0:T(8,128)(2,1)S(1)}, u32[]{:S(2)}, u32[]{:S(2)}) collective-permute-start(bf16[256,384]{1,0:T(8,128)(2,1)S(1)} %shard_map.183.r0), channel_id=1, source_target_pairs={{0,2},{1,3},{2,0},{3,1},{4,6},{5,7},{6,4},{7,5},{8,10},{9,11},{10,... | collective-permute-start | bytes 589832 | tf_op jit(solution)/shard_map/ppermute | solution.py:335
  195.3 10.8 %collective-permute-start.14 = (bf16[256,384]{1,0:T(8,128)(2,1)S(1)}, bf16[256,384]{1,0:T(8,128)(2,1)S(1)}, u32[]{:S(2)}, u32[]{:S(2)}) collective-permute-start(bf16[256,384]{1,0:T(8,128)(2,1)S(1)} %shard_map.183.r0), channel_id=1, source_target_pairs={{0,3},{1,2},{2,1},{3,0},{4,7},{5,6},{6,5},{7,4},{8,11},{9,10},{10,... | collective-permute-start | bytes 589832 | tf_op jit(solution)/shard_map/ppermute | solution.py:335
  206.3 14.2 %collective-permute-start.15 = (bf16[256,128]{1,0:T(8,128)(2,1)S(1)}, bf16[256,128]{1,0:T(8,128)(2,1)S(1)}, u32[]{:S(2)}, u32[]{:S(2)}) collective-permute-start(bf16[256,128]{1,0:T(8,128)(2,1)S(1)} %shard_map.184.h0), channel_id=1, source_target_pairs={{0,4},{4,8},{8,12},{12,0},{1,5},{5,9},{9,13},{13,1},{2,6},{6,10},{... | collective-permute-start | bytes 196616 | tf_op jit(solution)/shard_map/ppermute | solution.py:335
  208.6 11.9 %collective-permute-start.16 = (bf16[256,128]{1,0:T(8,128)(2,1)S(1)}, bf16[256,128]{1,0:T(8,128)(2,1)S(1)}, u32[]{:S(2)}, u32[]{:S(2)}) collective-permute-start(bf16[256,128]{1,0:T(8,128)(2,1)S(1)} %shard_map.184.h0), channel_id=1, source_target_pairs={{0,8},{4,12},{8,0},{12,4},{1,9},{5,13},{9,1},{13,5},{2,10},{6,14},... | collective-permute-start | bytes 196616 | tf_op jit(solution)/shard_map/ppermute | solution.py:335
  212.9 9.5 %collective-permute-start.17 = (bf16[256,128]{1,0:T(8,128)(2,1)S(1)}, bf16[256,128]{1,0:T(8,128)(2,1)S(1)}, u32[]{:S(2)}, u32[]{:S(2)}) collective-permute-start(bf16[256,128]{1,0:T(8,128)(2,1)S(1)} %shard_map.184.h0), channel_id=1, source_target_pairs={{0,12},{4,0},{8,4},{12,8},{1,13},{5,1},{9,5},{13,9},{2,14},{6,2},{... | collective-permute-start | bytes 196616 | tf_op jit(solution)/shard_map/ppermute | solution.py:335
  218.5 3.8 %copy-start.9 = (bf16[512,128]{1,0:T(8,128)(2,1)S(1)}, bf16[512,128]{1,0:T(8,128)(2,1)}, u32[]{:S(2)}) copy-start(bf16[512,128]{1,0:T(8,128)(2,1)} %down_ref.3) | copy-start | bytes 393220

commit v4 on v3

--- a/solution.py
+++ b/solution.py
@@ -160,7 +160,7 @@
         before = before + cum[BLOCK - 1 : BLOCK]
 
 
-def head_kernel(enter_ref, gain_ref, local_ref, start_ref, gate_ref, out_ref):
+def head_kernel(gain_ref, enter_ref, local_ref, start_ref, gate_ref, out_ref):
     mixed = local_ref[...] + nt(start_ref[...], enter_ref[...].astype(F32), precision=HIGHEST)
     scale = lax.rsqrt(jnp.mean(mixed * mixed, axis=-1, keepdims=True) + EPSILON)
     gate = jax.nn.silu(gate_ref[...].astype(F32))
@@ -254,6 +254,10 @@
     gate = jnp.dot(rows_ref[...], gate_ref[...], preferred_element_type=F32) * scale
     up = jnp.dot(rows_ref[...], up_ref[...], preferred_element_type=F32) * scale
     out_ref[...] = (jax.nn.silu(gate) * up).astype(BF16)
+
+
+def gain_kernel(in_ref, out_ref):
+    out_ref[...] = in_ref[...].astype(F32)
 
 
 def down_kernel(h0, h1, h2, h3, d0, d1, d2, d3, out_ref, wide_ref):
@@ -312,17 +316,21 @@
     out_ref[...] = hidden.astype(BF16)
 
 
-def final_kernel(ids_ref, back_ref, high_ref, low_ref, h0, h1, h2, h3, down_ref, mid_ref, out_ref):
+def ahead_kernel(ids_ref, h0, h1, h2, h3, down_ref, mid_ref, out_ref):
     group = ids_ref[1]
-    back = back_ref[...]
     total = mid_ref[...].astype(F32)
-    total = total + jnp.dot(high_ref[...], back, preferred_element_type=F32)
-    total = total + jnp.dot(low_ref[...], back, preferred_element_type=F32)
     for d, h in enumerate((h0, h1, h2, h3)):
         at = pl.multiple_of(((group - d) & 3) * 128, 128)
         total = total + jnp.dot(
             h[...], down_ref[pl.ds(at, 128), :], preferred_element_type=F32
         )
+    out_ref[...] = total
+
+
+def final_kernel(back_ref, high_ref, low_ref, ahead_ref, out_ref):
+    back = back_ref[...]
+    total = ahead_ref[...] + jnp.dot(high_ref[...], back, preferred_element_type=F32)
+    total = total + jnp.dot(low_ref[...], back, preferred_element_type=F32)
     out_ref[...] = total.astype(BF16)
 
 
@@ -368,7 +376,7 @@
     shared_expert_down,
 ):
     ids = jnp.stack([lax.axis_index(a) for a in (GROUP, "yg")]).astype(jnp.int32)
-    gain = feedforward_gain.astype(F32).reshape(16, 128)
+    gain = call(gain_kernel, ((16, 128), F32), feedforward_gain.reshape(16, 128))
     head_gain = head_norm_gain.reshape(1, DV)
     extra = extra_log_decay.reshape(2, 128)
     whole = (0, TOK)
@@ -397,8 +405,8 @@
     entering = exchange(call(scan_kernel, ((32, 8, DK), BF16), states), SP)
     head_rows = call(
         head_kernel, ((4, TOK, DV), BF16),
-        entering.reshape(DV, DK), head_gain, local, start, output_gate_preactivation,
-        fetch=(whole, whole, whole),
+        head_gain, entering.reshape(DV, DK), local, start, output_gate_preactivation,
+        fetch=(whole,) * 4, limit=60,
     )
     partial = call(
         project_kernel, ((4, TOK, 128), BF16),
@@ -436,10 +444,10 @@
     back = exchange(expert_out.reshape(128, 3, 4, 128), SPG).reshape(ALL_SLOTS, 128)
     hidden = call(shared_hidden_kernel, ((TOK, 128), BF16), *pre)
     hidden = [hidden] + shifted([hidden] * 3, "yg")
-    return call(
-        final_kernel, ((TOK, 128), BF16),
-        ids, back, high, low, *hidden, shared_expert_down, mid, smem=1,
-    )
+    ahead = call(
+        ahead_kernel, ((TOK, 128), F32), ids, *hidden, shared_expert_down, mid, smem=1,
+    )
+    return call(final_kernel, ((TOK, 128), BF16), back, high, low, ahead)
 
 
 def solution(mesh):

time: 225 us -> 226 us (level)
    pallas_call x14 -> x16, Pallas kernels: 22.3 us -> 23.9 us  [call(): pl.pallas_call(fetching if fetch else kernel, out_shape=shapes, in_specs=...]
    unnamed x36 -> x32, local copies, waits for them, and re-layouts: 6.11 us -> 4.88 us
where the time goes in v4:
time: 226 us; the launch traced here: 225 us
  starting transfers between devices  89.7 us (40%)
  waiting for transfers between devices  53.3 us (24%)
  blocking collectives  52.1 us (23%)
  Pallas kernels  23.9 us (11%)
  local copies, waits for them, and re-layouts  5.48 us (2%)
    ppermute x18, starting transfers between devices, moved(): lax.ppermute(value, axes, [(i, target(i) % count) for i in range(count)])  67.4 us
    all_to_all x2, blocking collectives, exchange(): return lax.all_to_all(value, axes, split_axis=0, concat_axis=0, tiled=True)  52.1 us
    ppermute x18, waiting for transfers between devices, moved(): lax.ppermute(value, axes, [(i, target(i) % count) for i in range(count)])  46 us
    pallas_call x16, Pallas kernels, call(): pl.pallas_call(fetching if fetch else kernel, out_shape=shapes, in_specs=...  23.9 us
    all_to_all x4, starting transfers between devices, exchange(): return lax.all_to_all(value, axes, split_axis=0, concat_axis=0, tiled=True)  22.3 us
    all_to_all x4, waiting for transfers between devices, exchange(): return lax.all_to_all(value, axes, split_axis=0, concat_axis=0, tiled=True)  7.31 us
    unnamed x32, local copies, waits for them, and re-layouts  4.88 us
  transfers between devices with their start and end apart: 22, of which 14 were waited for; matrix products, arithmetic and copies ran while one was open for 0% of the time, Pallas kernels for 4%

profile of v4, /device:TPU:1, one launch (start us, length us, event | category | flops | bytes accessed | tf_op | source)
XLA Modules:
  0.0 225.1 jit_solution(17910098303662791666)
XLA Ops:
  0.0 2.5 %shard_map.173 = bf16[32,16,128]{2,1,0:T(8,128)(2,1)} custom-call(bf16[256,128]{1,0:T(8,128)(2,1)} %refs_1_.3, bf16[256,256]{1,0:T(8,128)(2,1)} %refs_2_.3, bf16[256,128]{1,0:T(8,128)(2,1)} %refs_3_.1, f32[2,128]{1,0:T(2,128)} %bitcast.20), custom_call_target="tpu_custom_call" | custom-call | flops 1000000 | bytes 1000000 | tf_op jit(solution)/shard_map/pallas_call | solution.py:64
  2.5 23.1 %all_to_all.30.in_ref = bf16[32,16,128]{2,1,0:T(8,128)(2,1)S(1)} all-to-all(bf16[32,16,128]{2,1,0:T(8,128)(2,1)} %shard_map.173), channel_id=1, replica_groups=mesh['z'=8,'x'=4,'yg'=4,'yn'=2,'c'=2] {'z','x'}, dimensions={0} | all-to-all | bytes 262144 | tf_op jit(solution)/shard_map/all_to_all | solution.py:338
  25.6 0.7 shard_map.174
  26.3 3.9 %all-to-all-start.1 = ((bf16[32,8,128]{2,1,0:T(8,128)(2,1)}), bf16[32,8,128]{2,1,0:T(8,128)(2,1)S(1)}, u32[]{:S(2)}, u32[]{:S(2)}) async-start(bf16[32,8,128]{2,1,0:T(8,128)(2,1)} %shard_map.174), calls=%async_computation.1 | async-start | bytes 131072 | tf_op jit(solution)/shard_map/all_to_all | solution.py:338
  30.1 0.6 copy-done.14
  30.8 0.6 reshape.24.refs_0_
  31.4 3.6 %shard_map.175 = (f32[256,256]{1,0:T(8,128)}, f32[256,128]{1,0:T(8,128)}) custom-call(bf16[256,128]{1,0:T(8,128)(2,1)} %refs_0_.3, bf16[256,128]{1,0:T(8,128)(2,1)} %refs_1_.3, bf16[256,256]{1,0:T(8,128)(2,1)} %refs_2_.3, bf16[256,128]{1,0:T(8,128)(2,1)} %refs_3_.1, f32[2,128]{1,0:T(2,128)} %bitcast.21), custom_call_target="tpu_custom_call" | custom-call | flops 1000000 | bytes 1000000 | tf_op jit(solution)/shard_map/pallas_call | solution.py:64
  35.0 0.1 pad_add_fusion.ids_ref.refs_0_
  35.1 3.9 %all-to-all-done.1 = bf16[32,8,128]{2,1,0:T(8,128)(2,1)S(1)} async-done(((bf16[32,8,128]{2,1,0:T(8,128)(2,1)}), bf16[32,8,128]{2,1,0:T(8,128)(2,1)S(1)}, u32[]{:S(2)}, u32[]{:S(2)}) %all-to-all-start.1) | async-done | bytes 65568 | tf_op jit(solution)/shard_map/all_to_all | solution.py:338
  39.0 0.6 copy-done.9
  39.6 3.1 %shard_map.176 = bf16[4,256,256]{2,1,0:T(8,128)(2,1)} custom-call(bf16[1,256]{1,0:T(2,128)(2,1)} %reshape.24.refs_0_, bf16[256,128]{1,0:T(8,128)(2,1)} %bitcast.17, f32[256,256]{1,0:T(8,128)} %get-tuple-element.15.refs_2_, f32[256,128]{1,0:T(8,128)} %get-tuple-element.16.refs_3_, bf16[256,256]{1,0:T(8,128)(2,1)} %refs_4_.1), custom_call_target="tpu_custom_call" | custom-call | flops 1000000 | bytes 1000000 | tf_op jit(solution)/shard_map/pallas_call | solution.py:64
  42.8 7.0 %all-to-all-start.2 = ((bf16[4,256,256]{2,1,0:T(8,128)(2,1)}), bf16[4,256,256]{2,1,0:T(8,128)(2,1)S(1)}, u32[]{:S(2)}, u32[]{:S(2)}) async-start(bf16[4,256,256]{2,1,0:T(8,128)(2,1)} %shard_map.176), calls=%async_computation.2 | async-start | bytes 1048576 | tf_op jit(solution)/shard_map/all_to_all | solution.py:338
  49.8 0.0 copy-start.1
  49.8 1.2 copy-done.1
  51.0 1.0 shard_map.177
  52.0 5.4 %collective-permute-start = (bf16[576,512]{1,0:T(8,128)(2,1)S(1)}, bf16[576,512]{1,0:T(8,128)(2,1)S(1)}, u32[]{:S(2)}, u32[]{:S(2)}) collective-permute-start(bf16[576,512]{1,0:T(8,128)(2,1)S(1)} %get-tuple-element.18), channel_id=1, source_target_pairs={{0,1},{1,0},{2,3},{3,2},{4,5},{5,4},{6,7},{7,6},{8,9},{9,8},{10,11... | collective-permute-start | bytes 1769480 | tf_op jit(solution)/shard_map/ppermute | solution.py:343
  57.4 2.4 %collective-permute-start.1 = (bf16[576,512]{1,0:T(8,128)(2,1)S(1)}, bf16[576,512]{1,0:T(8,128)(2,1)S(1)}, u32[]{:S(2)}, u32[]{:S(2)}) collective-permute-start(bf16[576,512]{1,0:T(8,128)(2,1)S(1)} %get-tuple-element.19), channel_id=1, source_target_pairs={{0,2},{1,3},{2,0},{3,1},{4,6},{5,7},{6,4},{7,5},{8,10},{9,11},{10,... | collective-permute-start | bytes 1769480 | tf_op jit(solution)/shard_map/ppermute | solution.py:343
  59.8 3.1 %collective-permute-start.2 = (bf16[576,512]{1,0:T(8,128)(2,1)S(1)}, bf16[576,512]{1,0:T(8,128)(2,1)S(1)}, u32[]{:S(2)}, u32[]{:S(2)}) collective-permute-start(bf16[576,512]{1,0:T(8,128)(2,1)S(1)} %get-tuple-element.20), channel_id=1, source_target_pairs={{0,3},{1,2},{2,1},{3,0},{4,7},{5,6},{6,5},{7,4},{8,11},{9,10},{10,... | collective-permute-start | bytes 1769480 | tf_op jit(solution)/shard_map/ppermute | solution.py:343
  62.9 13.1 %collective-permute-done.1.refs_4_.d2.w2 = bf16[576,512]{1,0:T(8,128)(2,1)S(1)} collective-permute-done((bf16[576,512]{1,0:T(8,128)(2,1)S(1)}, bf16[576,512]{1,0:T(8,128)(2,1)S(1)}, u32[]{:S(2)}, u32[]{:S(2)}) %collective-permute-start.1) | collective-permute-done | bytes 589856 | tf_op jit(solution)/shard_map/ppermute | solution.py:343
  76.0 12.6 %collective-permute-done.2.refs_5_.d3.w3 = bf16[576,512]{1,0:T(8,128)(2,1)S(1)} collective-permute-done((bf16[576,512]{1,0:T(8,128)(2,1)S(1)}, bf16[576,512]{1,0:T(8,128)(2,1)S(1)}, u32[]{:S(2)}, u32[]{:S(2)}) %collective-permute-start.2) | collective-permute-done | bytes 589856 | tf_op jit(solution)/shard_map/ppermute | solution.py:343
  88.7 1.8 shard_map.178
  90.5 3.8 %all-to-all-start.3 = ((bf16[4,256,128]{2,1,0:T(8,128)(2,1)}), bf16[4,256,128]{2,1,0:T(8,128)(2,1)S(1)}, u32[]{:S(2)}, u32[]{:S(2)}) async-start(bf16[4,256,128]{2,1,0:T(8,128)(2,1)} %shard_map.178), calls=%async_computation.3 | async-start | bytes 524288 | tf_op jit(solution)/shard_map/all_to_all | solution.py:338
  94.3 0.1 copy.19.routing_ref
  94.4 1.5 shard_map.172.pick_ref
  95.9 3.4 %all-to-all-done.3.in_ref = bf16[4,256,128]{2,1,0:T(8,128)(2,1)S(1)} async-done(((bf16[4,256,128]{2,1,0:T(8,128)(2,1)}), bf16[4,256,128]{2,1,0:T(8,128)(2,1)S(1)}, u32[]{:S(2)}, u32[]{:S(2)}) %all-to-all-start.3) | async-done | bytes 262176 | tf_op jit(solution)/shard_map/all_to_all | solution.py:338
  99.3 0.8 copy-done.7
  100.1 0.4 shard_map.179
  100.5 29.1 %all_to_all.31 = bf16[128,3,4,128]{3,2,1,0:T(4,128)(2,1)S(1)} all-to-all(bf16[128,3,4,128]{3,2,1,0:T(4,128)(2,1)S(1)} %bitcast.15), channel_id=1, replica_groups=mesh['z'=8,'x'=4,'yg'=4,'yn'=2,'c'=2] {'z','x','yg'}, dimensions={0} | all-to-all | bytes 786432 | tf_op jit(solution)/shard_map/all_to_all | solution.py:338
  129.6 2.5 %collective-permute-start.4 = (bf16[1536,128]{1,0:T(8,128)(2,1)S(1)}, bf16[1536,128]{1,0:T(8,128)(2,1)S(1)}, u32[]{:S(2)}, u32[]{:S(2)}) collective-permute-start(bf16[1536,128]{1,0:T(8,128)(2,1)S(1)} %bitcast.11), channel_id=1, source_target_pairs={{0,2},{2,0},{1,3},{3,1},{4,6},{6,4},{5,7},{7,5},{8,10},{10,8},{9,1... | collective-permute-start | bytes 1179656 | tf_op jit(solution)/shard_map/ppermute | solution.py:343
  132.1 4.5 %collective-permute-start.3 = (bf16[1536,128]{1,0:T(8,128)(2,1)S(1)}, bf16[1536,128]{1,0:T(8,128)(2,1)S(1)}, u32[]{:S(2)}, u32[]{:S(2)}) collective-permute-start(bf16[1536,128]{1,0:T(8,128)(2,1)S(1)} %bitcast.12), channel_id=1, source_target_pairs={{0,1},{1,0},{2,3},{3,2},{4,5},{5,4},{6,7},{7,6},{8,9},{9,8},{10,11... | collective-permute-start | bytes 1179656 | tf_op jit(solution)/shard_map/ppermute | solution.py:343
  136.7 2.5 %collective-permute-done.4.refs_3_ = bf16[1536,128]{1,0:T(8,128)(2,1)S(1)} collective-permute-done((bf16[1536,128]{1,0:T(8,128)(2,1)S(1)}, bf16[1536,128]{1,0:T(8,128)(2,1)S(1)}, u32[]{:S(2)}, u32[]{:S(2)}) %collective-permute-start.4) | collective-permute-done | bytes 393248 | tf_op jit(solution)/shard_map/ppermute | solution.py:343
  139.2 5.7 %collective-permute-start.5 = (bf16[1536,128]{1,0:T(8,128)(2,1)S(1)}, bf16[1536,128]{1,0:T(8,128)(2,1)S(1)}, u32[]{:S(2)}, u32[]{:S(2)}) collective-permute-start(bf16[1536,128]{1,0:T(8,128)(2,1)S(1)} %collective-permute-done.4.refs_3_), channel_id=1, source_target_pairs={{0,1},{1,0},{2,3},{3,2},{4,5},{5,4},{6,7},{7,6},{8,9},{9,8},{10,11... | collective-permute-start | bytes 1179656 | tf_op jit(solution)/shard_map/ppermute | solution.py:343
  145.0 1.3 collective-permute-done.5.refs_4_
  146.3 1.2 copy-done.3
  147.5 2.9 %shard_map.181.h0 = bf16[384,256]{1,0:T(8,128)(2,1)S(1)} custom-call(s32[2]{0:T(128)S(1)} %pad_add_fusion.ids_ref.refs_0_, bf16[1536,128]{1,0:T(8,128)(2,1)S(1)} %bitcast.13, bf16[1536,128]{1,0:T(8,128)(2,1)S(1)} %collective-permute-done.3.refs_2_, bf16[1536,128]{1,0:T(8,128)(2,1)S(1)} %collective-permute-done.4.refs_3_, ...), custom_call_target="tpu_custom_call" | custom-call | flops 1000000 | bytes 1000000 | tf_op jit(solution)/shard_map/pallas_call | solution.py:64
  150.4 2.5 %collective-permute-start.7 = (bf16[384,256]{1,0:T(8,128)(2,1)S(1)}, bf16[384,256]{1,0:T(8,128)(2,1)S(1)}, u32[]{:S(2)}, u32[]{:S(2)}) collective-permute-start(bf16[384,256]{1,0:T(8,128)(2,1)S(1)} %shard_map.181.h0), channel_id=1, source_target_pairs={{0,2},{2,0},{1,3},{3,1},{4,6},{6,4},{5,7},{7,5},{8,10},{10,8},{9,1... | collective-permute-start | bytes 589832 | tf_op jit(solution)/shard_map/ppermute | solution.py:343
  153.0 2.6 %collective-permute-start.6 = (bf16[384,256]{1,0:T(8,128)(2,1)S(1)}, bf16[384,256]{1,0:T(8,128)(2,1)S(1)}, u32[]{:S(2)}, u32[]{:S(2)}) collective-permute-start(bf16[384,256]{1,0:T(8,128)(2,1)S(1)} %shard_map.181.h0), channel_id=1, source_target_pairs={{0,1},{1,0},{2,3},{3,2},{4,5},{5,4},{6,7},{7,6},{8,9},{9,8},{10,11... | collective-permute-start | bytes 589832 | tf_op jit(solution)/shard_map/ppermute | solution.py:343
  155.5 2.9 %collective-permute-done.7.h2 = bf16[384,256]{1,0:T(8,128)(2,1)S(1)} collective-permute-done((bf16[384,256]{1,0:T(8,128)(2,1)S(1)}, bf16[384,256]{1,0:T(8,128)(2,1)S(1)}, u32[]{:S(2)}, u32[]{:S(2)}) %collective-permute-start.7) | collective-permute-done | bytes 196640 | tf_op jit(solution)/shard_map/ppermute | solution.py:343
  158.4 3.1 %collective-permute-start.8 = (bf16[384,256]{1,0:T(8,128)(2,1)S(1)}, bf16[384,256]{1,0:T(8,128)(2,1)S(1)}, u32[]{:S(2)}, u32[]{:S(2)}) collective-permute-start(bf16[384,256]{1,0:T(8,128)(2,1)S(1)} %collective-permute-done.7.h2), channel_id=1, source_target_pairs={{0,1},{1,0},{2,3},{3,2},{4,5},{5,4},{6,7},{7,6},{8,9},{9,8},{10,11... | collective-permute-start | bytes 589832 | tf_op jit(solution)/shard_map/ppermute | solution.py:343
  161.6 1.0 collective-permute-done.8.h3
  162.6 1.4 shard_map.182
  164.0 7.7 %all-to-all-start.5 = ((bf16[128,3,4,128]{3,2,1,0:T(4,128)(2,1)}), bf16[128,3,4,128]{3,2,1,0:T(4,128)(2,1)S(1)}, u32[]{:S(2)}, u32[]{:S(2)}) async-start(bf16[128,3,4,128]{3,2,1,0:T(4,128)(2,1)} %bitcast.9), calls=%async_computation.5 | async-start | bytes 786432 | tf_op jit(solution)/shard_map/all_to_all | solution.py:338
  171.7 6.4 %collective-permute-start.10 = (bf16[256,128]{1,0:T(8,128)(2,1)S(1)}, bf16[256,128]{1,0:T(8,128)(2,1)S(1)}, u32[]{:S(2)}, u32[]{:S(2)}) collective-permute-start(bf16[256,128]{1,0:T(8,128)(2,1)S(1)} %copy-done.5), channel_id=1, source_target_pairs={{0,8},{4,12},{8,0},{12,4},{1,9},{5,13},{9,1},{13,5},{2,10},{6,14},... | collective-permute-start | bytes 196616 | tf_op jit(solution)/shard_map/ppermute | solution.py:343
  178.1 2.2 collective-permute-start.11
  180.3 4.0 %collective-permute-start.9 = (bf16[256,128]{1,0:T(8,128)(2,1)S(1)}, bf16[256,128]{1,0:T(8,128)(2,1)S(1)}, u32[]{:S(2)}, u32[]{:S(2)}) collective-permute-start(bf16[256,128]{1,0:T(8,128)(2,1)S(1)} %copy-done.5), channel_id=1, source_target_pairs={{0,4},{4,8},{8,12},{12,0},{1,5},{5,9},{9,13},{13,1},{2,6},{6,10},{... | collective-permute-start | bytes 196616 | tf_op jit(solution)/shard_map/ppermute | solution.py:343
  184.3 1.6 collective-permute-done.10.m2
  186.0 1.7 collective-permute-done.11.m3
  187.7 0.1 collective-permute-done.9.m1
  187.7 0.9 shard_map.184.r0
  188.6 0.0 copy-start.13
  188.7 5.5 %collective-permute-start.12 = (bf16[256,384]{1,0:T(8,128)(2,1)S(1)}, bf16[256,384]{1,0:T(8,128)(2,1)S(1)}, u32[]{:S(2)}, u32[]{:S(2)}) collective-permute-start(bf16[256,384]{1,0:T(8,128)(2,1)S(1)} %shard_map.184.r0), channel_id=1, source_target_pairs={{0,1},{1,0},{2,3},{3,2},{4,5},{5,4},{6,7},{7,6},{8,9},{9,8},{10,11... | collective-permute-start | bytes 589832 | tf_op jit(solution)/shard_map/ppermute | solution.py:343
  194.2 1.9 collective-permute-start.13
  196.1 3.5 %collective-permute-start.14 = (bf16[256,384]{1,0:T(8,128)(2,1)S(1)}, bf16[256,384]{1,0:T(8,128)(2,1)S(1)}, u32[]{:S(2)}, u32[]{:S(2)}) collective-permute-start(bf16[256,384]{1,0:T(8,128)(2,1)S(1)} %shard_map.184.r0), channel_id=1, source_target_pairs={{0,3},{1,2},{2,1},{3,0},{4,7},{5,6},{6,5},{7,4},{8,11},{9,10},{10,... | collective-permute-start | bytes 589832 | tf_op jit(solution)/shard_map/ppermute | solution.py:343
  199.7 2.9 %collective-permute-done.13.r2 = bf16[256,384]{1,0:T(8,128)(2,1)S(1)} collective-permute-done((bf16[256,384]{1,0:T(8,128)(2,1)S(1)}, bf16[256,384]{1,0:T(8,128)(2,1)S(1)}, u32[]{:S(2)}, u32[]{:S(2)}) %collective-permute-start.13) | collective-permute-done | bytes 196640 | tf_op jit(solution)/shard_map/ppermute | solution.py:343
  202.5 4.4 %collective-permute-done.14.r3 = bf16[256,384]{1,0:T(8,128)(2,1)S(1)} collective-permute-done((bf16[256,384]{1,0:T(8,128)(2,1)S(1)}, bf16[256,384]{1,0:T(8,128)(2,1)S(1)}, u32[]{:S(2)}, u32[]{:S(2)}) %collective-permute-start.14) | collective-permute-done | bytes 196640 | tf_op jit(solution)/shard_map/ppermute | solution.py:343
  206.9 0.1 shard_map.185.h0
  207.1 2.3 %collective-permute-start.15 = (bf16[256,128]{1,0:T(8,128)(2,1)S(1)}, bf16[256,128]{1,0:T(8,128)(2,1)S(1)}, u32[]{:S(2)}, u32[]{:S(2)}) collective-permute-start(bf16[256,128]{1,0:T(8,128)(2,1)S(1)} %shard_map.185.h0), channel_id=1, source_target_pairs={{0,4},{4,8},{8,12},{12,0},{1,5},{5,9},{9,13},{13,1},{2,6},{6,10},{... | collective-permute-start | bytes 196616 | tf_op jit(solution)/shard_map/ppermute | solution.py:343
  209.4 4.3 %collective-permute-start.16 = (bf16[256,128]{1,0:T(8,128)(2,1)S(1)}, bf16[256,128]{1,0:T(8,128)(2,1)S(1)}, u32[]{:S(2)}, u32[]{:S(2)}) collective-permute-start(bf16[256,128]{1,0:T(8,128)(2,1)S(1)} %shard_map.185.h0), channel_id=1, source_target_pairs={{0,8},{4,12},{8,0},{12,4},{1,9},{5,13},{9,1},{13,5},{2,10},{6,14},... | collective-permute-start | bytes 196616 | tf_op jit(solution)/shard_map/ppermute | solution.py:343
  213.6 5.5 %collective-permute-start.17 = (bf16[256,128]{1,0:T(8,128)(2,1)S(1)}, bf16[256,128]{1,0:T(8,128)(2,1)S(1)}, u32[]{:S(2)}, u32[]{:S(2)}) collective-permute-start(bf16[256,128]{1,0:T(8,128)(2,1)S(1)} %shard_map.185.h0), channel_id=1, source_target_pairs={{0,12},{4,0},{8,4},{12,8},{1,13},{5,1},{9,5},{13,9},{2,14},{6,2},{... | collective-permute-start | bytes 196616 | tf_op jit(solution)/shard_map/ppermute | solution.py:343
  219.1 0.1 copy.21.score_ref
  219.3 2.0 shard_map.183
  221.3 1.8 collective-permute-done.17.h3
  223.1 0.8 shard_map.186.ahead_ref
  223.9 1.2 shard_map.187
  (33 shorter events, 0.1 us)
Async XLA Ops:
  26.3 12.7 %all-to-all-start.1 = ((bf16[32,8,128]{2,1,0:T(8,128)(2,1)}), bf16[32,8,128]{2,1,0:T(8,128)(2,1)S(1)}, u32[]{:S(2)}, u32[]{:S(2)}) async-start(bf16[32,8,128]{2,1,0:T(8,128)(2,1)} %shard_map.174), calls=%async_computation.1 | async-start | bytes 131072 | tf_op jit(solution)/shard_map/all_to_all | solution.py:338
  30.1 0.7 copy-start.14
  39.0 0.6 copy-start.9
  39.6 10.1 %copy-start.10 = (bf16[2048,32]{0,1:T(8,128)(2,1)S(1)}, bf16[2048,32]{0,1:T(8,128)(2,1)}, u32[]{:S(2)}) copy-start(bf16[2048,32]{0,1:T(8,128)(2,1)} %param.34) | copy-start | bytes 393220
  39.6 10.1 %copy-start.11 = (bf16[2048,32]{0,1:T(8,128)(2,1)S(1)}, bf16[2048,32]{0,1:T(8,128)(2,1)}, u32[]{:S(2)}) copy-start(bf16[2048,32]{0,1:T(8,128)(2,1)} %param.33) | copy-start | bytes 393220
  42.7 7.0 %copy-start = (bf16[4096,128]{1,0:T(8,128)(2,1)S(1)}, bf16[4096,128]{1,0:T(8,128)(2,1)}, u32[]{:S(2)}) copy-start(bf16[4096,128]{1,0:T(8,128)(2,1)} %project_ref.1) | copy-start | bytes 3145732
  42.8 45.9 %all-to-all-start.2 = ((bf16[4,256,256]{2,1,0:T(8,128)(2,1)}), bf16[4,256,256]{2,1,0:T(8,128)(2,1)S(1)}, u32[]{:S(2)}, u32[]{:S(2)}) async-start(bf16[4,256,256]{2,1,0:T(8,128)(2,1)} %shard_map.176), calls=%async_computation.2 | async-start | bytes 1048576 | tf_op jit(solution)/shard_map/all_to_all | solution.py:338
  49.8 1.2 copy-start.1
  52.0 10.9 %collective-permute-start = (bf16[576,512]{1,0:T(8,128)(2,1)S(1)}, bf16[576,512]{1,0:T(8,128)(2,1)S(1)}, u32[]{:S(2)}, u32[]{:S(2)}) collective-permute-start(bf16[576,512]{1,0:T(8,128)(2,1)S(1)} %get-tuple-element.18), channel_id=1, source_target_pairs={{0,1},{1,0},{2,3},{3,2},{4,5},{5,4},{6,7},{7,6},{8,9},{9,8},{10,11... | collective-permute-start | bytes 1769480 | tf_op jit(solution)/shard_map/ppermute | solution.py:343
  57.4 18.6 %collective-permute-start.1 = (bf16[576,512]{1,0:T(8,128)(2,1)S(1)}, bf16[576,512]{1,0:T(8,128)(2,1)S(1)}, u32[]{:S(2)}, u32[]{:S(2)}) collective-permute-start(bf16[576,512]{1,0:T(8,128)(2,1)S(1)} %get-tuple-element.19), channel_id=1, source_target_pairs={{0,2},{1,3},{2,0},{3,1},{4,6},{5,7},{6,4},{7,5},{8,10},{9,11},{10,... | collective-permute-start | bytes 1769480 | tf_op jit(solution)/shard_map/ppermute | solution.py:343
  59.8 28.9 %collective-permute-start.2 = (bf16[576,512]{1,0:T(8,128)(2,1)S(1)}, bf16[576,512]{1,0:T(8,128)(2,1)S(1)}, u32[]{:S(2)}, u32[]{:S(2)}) collective-permute-start(bf16[576,512]{1,0:T(8,128)(2,1)S(1)} %get-tuple-element.20), channel_id=1, source_target_pairs={{0,3},{1,2},{2,1},{3,0},{4,7},{5,6},{6,5},{7,4},{8,11},{9,10},{10,... | collective-permute-start | bytes 1769480 | tf_op jit(solution)/shard_map/ppermute | solution.py:343
  90.5 3.8 %copy-start.12 = (s32[256,4]{0,1:T(4,128)S(1)}, s32[256,4]{0,1:T(4,128)}, u32[]{:S(2)}) copy-start(s32[256,4]{0,1:T(4,128)} %param.28) | copy-start | bytes 12292
  90.5 8.8 %all-to-all-start.3 = ((bf16[4,256,128]{2,1,0:T(8,128)(2,1)}), bf16[4,256,128]{2,1,0:T(8,128)(2,1)S(1)}, u32[]{:S(2)}, u32[]{:S(2)}) async-start(bf16[4,256,128]{2,1,0:T(8,128)(2,1)} %shard_map.178), calls=%async_computation.3 | async-start | bytes 524288 | tf_op jit(solution)/shard_map/all_to_all | solution.py:338
  99.3 0.8 copy-start.7
  100.1 46.1 %copy-start.2 = (bf16[2048,256]{1,0:T(8,128)(2,1)S(1)}, bf16[2048,256]{1,0:T(8,128)(2,1)}, u32[]{:S(2)}) copy-start(bf16[2048,256]{1,0:T(8,128)(2,1)} %refs_6_.1) | copy-start | bytes 3145732
  100.5 29.1 %copy-start.4 = (bf16[256,128]{1,0:T(8,128)(2,1)}, bf16[256,128]{1,0:T(8,128)(2,1)S(1)}, u32[]{:S(2)}) copy-start(bf16[256,128]{1,0:T(8,128)(2,1)S(1)} %get-tuple-element.24.m0.mid_ref) | copy-start | bytes 196612
  100.5 44.4 %copy-start.8 = (bf16[2048]{0:T(1024)(128)(2,1)S(1)}, bf16[2048]{0:T(1024)(128)(2,1)}, u32[]{:S(2)}) copy-start(bf16[2048]{0:T(1024)(128)(2,1)} %param.27) | copy-start | bytes 12292
  129.6 9.6 %collective-permute-start.4 = (bf16[1536,128]{1,0:T(8,128)(2,1)S(1)}, bf16[1536,128]{1,0:T(8,128)(2,1)S(1)}, u32[]{:S(2)}, u32[]{:S(2)}) collective-permute-start(bf16[1536,128]{1,0:T(8,128)(2,1)S(1)} %bitcast.11), channel_id=1, source_target_pairs={{0,2},{2,0},{1,3},{3,1},{4,6},{6,4},{5,7},{7,5},{8,10},{10,8},{9,1... | collective-permute-start | bytes 1179656 | tf_op jit(solution)/shard_map/ppermute | solution.py:343
  132.1 12.8 %collective-permute-start.3 = (bf16[1536,128]{1,0:T(8,128)(2,1)S(1)}, bf16[1536,128]{1,0:T(8,128)(2,1)S(1)}, u32[]{:S(2)}, u32[]{:S(2)}) collective-permute-start(bf16[1536,128]{1,0:T(8,128)(2,1)S(1)} %bitcast.12), channel_id=1, source_target_pairs={{0,1},{1,0},{2,3},{3,2},{4,5},{5,4},{6,7},{7,6},{8,9},{9,8},{10,11... | collective-permute-start | bytes 1179656 | tf_op jit(solution)/shard_map/ppermute | solution.py:343
  139.2 7.1 %collective-permute-start.5 = (bf16[1536,128]{1,0:T(8,128)(2,1)S(1)}, bf16[1536,128]{1,0:T(8,128)(2,1)S(1)}, u32[]{:S(2)}, u32[]{:S(2)}) collective-permute-start(bf16[1536,128]{1,0:T(8,128)(2,1)S(1)} %collective-permute-done.4.refs_3_), channel_id=1, source_target_pairs={{0,1},{1,0},{2,3},{3,2},{4,5},{5,4},{6,7},{7,6},{8,9},{9,8},{10,11... | collective-permute-start | bytes 1179656 | tf_op jit(solution)/shard_map/ppermute | solution.py:343
  146.3 1.2 copy-start.3
  150.4 8.0 %collective-permute-start.7 = (bf16[384,256]{1,0:T(8,128)(2,1)S(1)}, bf16[384,256]{1,0:T(8,128)(2,1)S(1)}, u32[]{:S(2)}, u32[]{:S(2)}) collective-permute-start(bf16[384,256]{1,0:T(8,128)(2,1)S(1)} %shard_map.181.h0), channel_id=1, source_target_pairs={{0,2},{2,0},{1,3},{3,1},{4,6},{6,4},{5,7},{7,5},{8,10},{10,8},{9,1... | collective-permute-start | bytes 589832 | tf_op jit(solution)/shard_map/ppermute | solution.py:343
  153.0 8.6 %collective-permute-start.6 = (bf16[384,256]{1,0:T(8,128)(2,1)S(1)}, bf16[384,256]{1,0:T(8,128)(2,1)S(1)}, u32[]{:S(2)}, u32[]{:S(2)}) collective-permute-start(bf16[384,256]{1,0:T(8,128)(2,1)S(1)} %shard_map.181.h0), channel_id=1, source_target_pairs={{0,1},{1,0},{2,3},{3,2},{4,5},{5,4},{6,7},{7,6},{8,9},{9,8},{10,11... | collective-permute-start | bytes 589832 | tf_op jit(solution)/shard_map/ppermute | solution.py:343
  158.4 4.2 %collective-permute-start.8 = (bf16[384,256]{1,0:T(8,128)(2,1)S(1)}, bf16[384,256]{1,0:T(8,128)(2,1)S(1)}, u32[]{:S(2)}, u32[]{:S(2)}) collective-permute-start(bf16[384,256]{1,0:T(8,128)(2,1)S(1)} %collective-permute-done.7.h2), channel_id=1, source_target_pairs={{0,1},{1,0},{2,3},{3,2},{4,5},{5,4},{6,7},{7,6},{8,9},{9,8},{10,11... | collective-permute-start | bytes 589832 | tf_op jit(solution)/shard_map/ppermute | solution.py:343
  164.0 7.7 %copy-start.5 = (bf16[256,128]{1,0:T(8,128)(2,1)S(1)}, bf16[256,128]{1,0:T(8,128)(2,1)}, u32[]{:S(2)}) copy-start(bf16[256,128]{1,0:T(8,128)(2,1)} %copy-done.4) | copy-start | bytes 196612
  164.0 59.9 %all-to-all-start.5 = ((bf16[128,3,4,128]{3,2,1,0:T(4,128)(2,1)}), bf16[128,3,4,128]{3,2,1,0:T(4,128)(2,1)S(1)}, u32[]{:S(2)}, u32[]{:S(2)}) async-start(bf16[128,3,4,128]{3,2,1,0:T(4,128)(2,1)} %bitcast.9), calls=%async_computation.5 | async-start | bytes 786432 | tf_op jit(solution)/shard_map/all_to_all | solution.py:338
  171.7 14.2 %collective-permute-start.10 = (bf16[256,128]{1,0:T(8,128)(2,1)S(1)}, bf16[256,128]{1,0:T(8,128)(2,1)S(1)}, u32[]{:S(2)}, u32[]{:S(2)}) collective-permute-start(bf16[256,128]{1,0:T(8,128)(2,1)S(1)} %copy-done.5), channel_id=1, source_target_pairs={{0,8},{4,12},{8,0},{12,4},{1,9},{5,13},{9,1},{13,5},{2,10},{6,14},... | collective-permute-start | bytes 196616 | tf_op jit(solution)/shard_map/ppermute | solution.py:343
  178.1 9.5 %collective-permute-start.11 = (bf16[256,128]{1,0:T(8,128)(2,1)S(1)}, bf16[256,128]{1,0:T(8,128)(2,1)S(1)}, u32[]{:S(2)}, u32[]{:S(2)}) collective-permute-start(bf16[256,128]{1,0:T(8,128)(2,1)S(1)} %copy-done.5), channel_id=1, source_target_pairs={{0,12},{4,0},{8,4},{12,8},{1,13},{5,1},{9,5},{13,9},{2,14},{6,2},{... | collective-permute-start | bytes 196616 | tf_op jit(solution)/shard_map/ppermute | solution.py:343
  180.3 7.4 %collective-permute-start.9 = (bf16[256,128]{1,0:T(8,128)(2,1)S(1)}, bf16[256,128]{1,0:T(8,128)(2,1)S(1)}, u32[]{:S(2)}, u32[]{:S(2)}) collective-permute-start(bf16[256,128]{1,0:T(8,128)(2,1)S(1)} %copy-done.5), channel_id=1, source_target_pairs={{0,4},{4,8},{8,12},{12,0},{1,5},{5,9},{9,13},{13,1},{2,6},{6,10},{... | collective-permute-start | bytes 196616 | tf_op jit(solution)/shard_map/ppermute | solution.py:343
  188.6 30.5 %copy-start.13 = (f32[256,4]{0,1:T(4,128)S(1)}, f32[256,4]{0,1:T(4,128)}, u32[]{:S(2)}) copy-start(f32[256,4]{0,1:T(4,128)} %param.29) | copy-start | bytes 12292
  188.7 11.0 %collective-permute-start.12 = (bf16[256,384]{1,0:T(8,128)(2,1)S(1)}, bf16[256,384]{1,0:T(8,128)(2,1)S(1)}, u32[]{:S(2)}, u32[]{:S(2)}) collective-permute-start(bf16[256,384]{1,0:T(8,128)(2,1)S(1)} %shard_map.184.r0), channel_id=1, source_target_pairs={{0,1},{1,0},{2,3},{3,2},{4,5},{5,4},{6,7},{7,6},{8,9},{9,8},{10,11... | collective-permute-start | bytes 589832 | tf_op jit(solution)/shard_map/ppermute | solution.py:343
  194.2 8.3 %collective-permute-start.13 = (bf16[256,384]{1,0:T(8,128)(2,1)S(1)}, bf16[256,384]{1,0:T(8,128)(2,1)S(1)}, u32[]{:S(2)}, u32[]{:S(2)}) collective-permute-start(bf16[256,384]{1,0:T(8,128)(2,1)S(1)} %shard_map.184.r0), channel_id=1, source_target_pairs={{0,2},{1,3},{2,0},{3,1},{4,6},{5,7},{6,4},{7,5},{8,10},{9,11},{10,... | collective-permute-start | bytes 589832 | tf_op jit(solution)/shard_map/ppermute | solution.py:343
  196.1 10.8 %collective-permute-start.14 = (bf16[256,384]{1,0:T(8,128)(2,1)S(1)}, bf16[256,384]{1,0:T(8,128)(2,1)S(1)}, u32[]{:S(2)}, u32[]{:S(2)}) collective-permute-start(bf16[256,384]{1,0:T(8,128)(2,1)S(1)} %shard_map.184.r0), channel_id=1, source_target_pairs={{0,3},{1,2},{2,1},{3,0},{4,7},{5,6},{6,5},{7,4},{8,11},{9,10},{10,... | collective-permute-start | bytes 589832 | tf_op jit(solution)/shard_map/ppermute | solution.py:343
  207.1 14.2 %collective-permute-start.15 = (bf16[256,128]{1,0:T(8,128)(2,1)S(1)}, bf16[256,128]{1,0:T(8,128)(2,1)S(1)}, u32[]{:S(2)}, u32[]{:S(2)}) collective-permute-start(bf16[256,128]{1,0:T(8,128)(2,1)S(1)} %shard_map.185.h0), channel_id=1, source_target_pairs={{0,4},{4,8},{8,12},{12,0},{1,5},{5,9},{9,13},{13,1},{2,6},{6,10},{... | collective-permute-start | bytes 196616 | tf_op jit(solution)/shard_map/ppermute | solution.py:343
  209.4 11.9 %collective-permute-start.16 = (bf16[256,128]{1,0:T(8,128)(2,1)S(1)}, bf16[256,128]{1,0:T(8,128)(2,1)S(1)}, u32[]{:S(2)}, u32[]{:S(2)}) collective-permute-start(bf16[256,128]{1,0:T(8,128)(2,1)S(1)} %shard_map.185.h0), channel_id=1, source_target_pairs={{0,8},{4,12},{8,0},{12,4},{1,9},{5,13},{9,1},{13,5},{2,10},{6,14},... | collective-permute-start | bytes 196616 | tf_op jit(solution)/shard_map/ppermute | solution.py:343
  213.6 9.5 %collective-permute-start.17 = (bf16[256,128]{1,0:T(8,128)(2,1)S(1)}, bf16[256,128]{1,0:T(8,128)(2,1)S(1)}, u32[]{:S(2)}, u32[]{:S(2)}) collective-permute-start(bf16[256,128]{1,0:T(8,128)(2,1)S(1)} %shard_map.185.h0), channel_id=1, source_target_pairs={{0,12},{4,0},{8,4},{12,8},{1,13},{5,1},{9,5},{13,9},{2,14},{6,2},{... | collective-permute-start | bytes 196616 | tf_op jit(solution)/shard_map/ppermute | solution.py:343
  219.3 3.8 %copy-start.6 = (bf16[512,128]{1,0:T(8,128)(2,1)S(1)}, bf16[512,128]{1,0:T(8,128)(2,1)}, u32[]{:S(2)}) copy-start(bf16[512,128]{1,0:T(8,128)(2,1)} %down_ref.3) | copy-start | bytes 393220

commit v5 on v4

--- a/solution.py
+++ b/solution.py
@@ -160,7 +160,7 @@
         before = before + cum[BLOCK - 1 : BLOCK]
 
 
-def head_kernel(gain_ref, enter_ref, local_ref, start_ref, gate_ref, out_ref):
+def head_kernel(enter_ref, gain_ref, local_ref, start_ref, gate_ref, out_ref):
     mixed = local_ref[...] + nt(start_ref[...], enter_ref[...].astype(F32), precision=HIGHEST)
     scale = lax.rsqrt(jnp.mean(mixed * mixed, axis=-1, keepdims=True) + EPSILON)
     gate = jax.nn.silu(gate_ref[...].astype(F32))
@@ -263,7 +263,7 @@
 def down_kernel(h0, h1, h2, h3, d0, d1, d2, d3, out_ref, wide_ref):
     total = jnp.zeros((SLOTS, 512), F32)
     for h_ref, d_ref in ((h0, d0), (h1, d1), (h2, d2), (h3, d3)):
-        total = total + jnp.dot(h_ref[...], d_ref[256:512, :], preferred_element_type=F32)
+        total = total + jnp.dot(h_ref[...], d_ref[0:256, :], preferred_element_type=F32)
     for q in range(4):
         for r in range(MOST):
             wide_ref[pl.ds(q * MOST + r, 32, stride=PITCH), :] = total[
@@ -273,24 +273,30 @@
         out_ref[s * 48 : (s + 1) * 48, :] = wide_ref[s * PITCH : s * PITCH + 48, :].astype(BF16)
 
 
-def parts_kernel(ids_ref, project_ref, down_ref, shared_ref, *out_refs):
+def blocks_kernel(ids_ref, project_ref, *out_refs):
     part = ids_ref[0]
     for m, out_ref in enumerate(out_refs):
         for q in range(4):
-            slab = q * 4 + (part ^ m)
+            at = pl.multiple_of((q * 4 + (part ^ m)) * 256, 256)
+            out_ref[:, q * 128 : (q + 1) * 128] = project_ref[pl.ds(at, 256), :]
+
+
+def parts_kernel(ids_ref, down_ref, shared_ref, *out_refs):
+    part = ids_ref[0]
+    for m, out_ref in enumerate(out_refs):
+        for q in range(4):
             lanes = slice(q * 128, (q + 1) * 128)
-            out_ref[0:256, lanes] = project_ref[pl.ds(pl.multiple_of(slab * 256, 256), 256), :]
-            columns = pl.ds(pl.multiple_of(slab * 128, 128), 128)
-            out_ref[256:512, lanes] = down_ref[:, columns]
-            out_ref[512:576, lanes] = shared_ref[:, columns]
+            columns = pl.ds(pl.multiple_of((q * 4 + (part ^ m)) * 128, 128), 128)
+            out_ref[0:256, lanes] = down_ref[:, columns]
+            out_ref[256:320, lanes] = shared_ref[:, columns]
 
 
 def shared_in_kernel(ids_ref, m0, m1, m2, m3, w0, w1, w2, w3, gain_ref, out_ref, weight_ref, mid_ref):
     part, group = ids_ref[0], ids_ref[1]
     for m, w_ref in enumerate((w0, w1, w2, w3)):
         at = (part ^ m) * 32
-        weight_ref[pl.ds(pl.multiple_of(at, 32), 32), :] = w_ref[512:544, :]
-        weight_ref[pl.ds(pl.multiple_of(at + 128, 32), 32), :] = w_ref[544:576, :]
+        weight_ref[pl.ds(pl.multiple_of(at, 32), 32), :] = w_ref[256:288, :]
+        weight_ref[pl.ds(pl.multiple_of(at + 128, 32), 32), :] = w_ref[288:320, :]
     for d, m_ref in enumerate((m0, m1, m2, m3)):
         mid_ref[(group - d) & 3] = m_ref[...]
     squares = jnp.zeros((TOK, 128), F32)
@@ -396,21 +402,24 @@
         weigh_kernel, [((TOK, ALL_SLOTS), BF16), ((TOK, ALL_SLOTS), BF16)], routing, router_score
     )
     shared_in = jnp.concatenate([shared_expert_gate.T, shared_expert_up.T], axis=0)
+    own_block, *far_blocks = call(
+        blocks_kernel, [((256, 512), BF16)] * 4, ids, output_projection, smem=1,
+    )
+    blocks = [own_block] + grouped(far_blocks)
     own_part, *far_parts = call(
-        parts_kernel, [((576, 512), BF16)] * 4,
-        ids, output_projection, expert_down_weight, shared_in, smem=1,
+        parts_kernel, [((320, 512), BF16)] * 4, ids, expert_down_weight, shared_in, smem=1,
     )
     parts = [own_part] + grouped(far_parts)
 
     entering = exchange(call(scan_kernel, ((32, 8, DK), BF16), states), SP)
     head_rows = call(
         head_kernel, ((4, TOK, DV), BF16),
-        head_gain, entering.reshape(DV, DK), local, start, output_gate_preactivation,
-        fetch=(whole,) * 4, limit=60,
+        entering.reshape(DV, DK), head_gain, local, start, output_gate_preactivation,
+        fetch=(whole,) * 3,
     )
     partial = call(
         project_kernel, ((4, TOK, 128), BF16),
-        ids, exchange(head_rows, "yg"), *parts, smem=1, fetch=(whole,) * 4,
+        ids, exchange(head_rows, "yg"), *blocks, smem=1, fetch=(whole,) * 4,
     )
     outgoing, mid = call(
         dispatch_kernel, [((ALL_SLOTS, 128), BF16), ((TOK, 128), BF16)],

time: 226 us -> 221 us (0.978)
  waiting for transfers between devices: 53.3 us -> 45.9 us
  starting transfers between devices: 89.7 us -> 94.9 us
    ppermute x18 -> x21, waiting for transfers between devices: 46 us -> 37.4 us  [moved(): lax.ppermute(value, axes, [(i, target(i) % count) for i in range(count)])]
    ppermute x18 -> x21, starting transfers between devices: 67.4 us -> 73.3 us  [moved(): lax.ppermute(value, axes, [(i, target(i) % count) for i in range(count)])]
    pallas_call x16 -> x17, Pallas kernels: 23.9 us -> 23.1 us  [call(): pl.pallas_call(fetching if fetch else kernel, out_shape=shapes, in_specs=...]
  transfers between devices with their start and end apart: 22 -> 25, of which waited for: 14 -> 12; matrix products, arithmetic and copies ran while one was open for 0% -> 0% of each run, Pallas kernels for 4% -> 5%
where the time goes in v5:
time: 221 us; the launch traced here: 219 us
  starting transfers between devices  94.9 us (43%)
  blocking collectives  51.4 us (23%)
  waiting for transfers between devices  45.9 us (21%)
  Pallas kernels  23.1 us (10%)
  local copies, waits for them, and re-layouts  3.41 us (2%)
    ppermute x21, starting transfers between devices, moved(): lax.ppermute(value, axes, [(i, target(i) % count) for i in range(count)])  73.3 us
    all_to_all x2, blocking collectives, exchange(): return lax.all_to_all(value, axes, split_axis=0, concat_axis=0, tiled=True)  51.4 us
    ppermute x21, waiting for transfers between devices, moved(): lax.ppermute(value, axes, [(i, target(i) % count) for i in range(count)])  37.4 us
    pallas_call x17, Pallas kernels, call(): pl.pallas_call(fetching if fetch else kernel, out_shape=shapes, in_specs=...  23.1 us
    all_to_all x4, starting transfers between devices, exchange(): return lax.all_to_all(value, axes, split_axis=0, concat_axis=0, tiled=True)  21.7 us
    all_to_all x4, waiting for transfers between devices, exchange(): return lax.all_to_all(value, axes, split_axis=0, concat_axis=0, tiled=True)  8.51 us
  transfers between devices with their start and end apart: 25, of which 12 were waited for; matrix products, arithmetic and copies ran while one was open for 0% of the time, Pallas kernels for 5%

profile of v5, /device:TPU:1, one launch (start us, length us, event | category | flops | bytes accessed | tf_op | source)
XLA Modules:
  0.0 219.3 jit_solution(11192154113513732022)
XLA Ops:
  0.0 2.5 %shard_map.173 = bf16[32,16,128]{2,1,0:T(8,128)(2,1)} custom-call(bf16[256,128]{1,0:T(8,128)(2,1)} %refs_1_.3, bf16[256,256]{1,0:T(8,128)(2,1)} %refs_2_.3, bf16[256,128]{1,0:T(8,128)(2,1)} %refs_3_.1, f32[2,128]{1,0:T(2,128)} %bitcast.20), custom_call_target="tpu_custom_call" | custom-call | flops 1000000 | bytes 1000000 | tf_op jit(solution)/shard_map/pallas_call | solution.py:64
  2.5 23.1 %all_to_all.30.in_ref = bf16[32,16,128]{2,1,0:T(8,128)(2,1)S(1)} all-to-all(bf16[32,16,128]{2,1,0:T(8,128)(2,1)} %shard_map.173), channel_id=1, replica_groups=mesh['z'=8,'x'=4,'yg'=4,'yn'=2,'c'=2] {'z','x'}, dimensions={0} | all-to-all | bytes 262144 | tf_op jit(solution)/shard_map/all_to_all | solution.py:344
  25.6 0.7 shard_map.174
  26.3 4.0 %all-to-all-start.1 = ((bf16[32,8,128]{2,1,0:T(8,128)(2,1)}), bf16[32,8,128]{2,1,0:T(8,128)(2,1)S(1)}, u32[]{:S(2)}, u32[]{:S(2)}) async-start(bf16[32,8,128]{2,1,0:T(8,128)(2,1)} %shard_map.174), calls=%async_computation.1 | async-start | bytes 131072 | tf_op jit(solution)/shard_map/all_to_all | solution.py:344
  30.3 3.6 %shard_map.175 = (f32[256,256]{1,0:T(8,128)}, f32[256,128]{1,0:T(8,128)}) custom-call(bf16[256,128]{1,0:T(8,128)(2,1)} %refs_0_.3, bf16[256,128]{1,0:T(8,128)(2,1)} %refs_1_.3, bf16[256,256]{1,0:T(8,128)(2,1)} %refs_2_.3, bf16[256,128]{1,0:T(8,128)(2,1)} %refs_3_.1, f32[2,128]{1,0:T(2,128)} %bitcast.21), custom_call_target="tpu_custom_call" | custom-call | flops 1000000 | bytes 1000000 | tf_op jit(solution)/shard_map/pallas_call | solution.py:64
  33.9 5.2 %all-to-all-done.1 = bf16[32,8,128]{2,1,0:T(8,128)(2,1)S(1)} async-done(((bf16[32,8,128]{2,1,0:T(8,128)(2,1)}), bf16[32,8,128]{2,1,0:T(8,128)(2,1)S(1)}, u32[]{:S(2)}, u32[]{:S(2)}) %all-to-all-start.1) | async-done | bytes 65568 | tf_op jit(solution)/shard_map/all_to_all | solution.py:344
  39.2 0.9 copy-done.4
  40.1 0.9 copy-done.6
  41.0 1.6 shard_map.176
  42.7 6.8 %all-to-all-start.2 = ((bf16[4,256,256]{2,1,0:T(8,128)(2,1)}), bf16[4,256,256]{2,1,0:T(8,128)(2,1)S(1)}, u32[]{:S(2)}, u32[]{:S(2)}) async-start(bf16[4,256,256]{2,1,0:T(8,128)(2,1)} %shard_map.176), calls=%async_computation.2 | async-start | bytes 1048576 | tf_op jit(solution)/shard_map/all_to_all | solution.py:344
  49.5 0.1 pad_add_fusion.ids_ref.refs_0_
  49.6 0.7 shard_map.177
  50.3 5.4 %collective-permute-start = (bf16[256,512]{1,0:T(8,128)(2,1)S(1)}, bf16[256,512]{1,0:T(8,128)(2,1)S(1)}, u32[]{:S(2)}, u32[]{:S(2)}) collective-permute-start(bf16[256,512]{1,0:T(8,128)(2,1)S(1)} %get-tuple-element.22), channel_id=1, source_target_pairs={{0,1},{1,0},{2,3},{3,2},{4,5},{5,4},{6,7},{7,6},{8,9},{9,8},{10,11... | collective-permute-start | bytes 786440 | tf_op jit(solution)/shard_map/ppermute | solution.py:349
  55.7 2.4 %collective-permute-start.1 = (bf16[256,512]{1,0:T(8,128)(2,1)S(1)}, bf16[256,512]{1,0:T(8,128)(2,1)S(1)}, u32[]{:S(2)}, u32[]{:S(2)}) collective-permute-start(bf16[256,512]{1,0:T(8,128)(2,1)S(1)} %get-tuple-element.23), channel_id=1, source_target_pairs={{0,2},{1,3},{2,0},{3,1},{4,6},{5,7},{6,4},{7,5},{8,10},{9,11},{10,... | collective-permute-start | bytes 786440 | tf_op jit(solution)/shard_map/ppermute | solution.py:349
  58.1 3.1 %collective-permute-start.2 = (bf16[256,512]{1,0:T(8,128)(2,1)S(1)}, bf16[256,512]{1,0:T(8,128)(2,1)S(1)}, u32[]{:S(2)}, u32[]{:S(2)}) collective-permute-start(bf16[256,512]{1,0:T(8,128)(2,1)S(1)} %get-tuple-element.24), channel_id=1, source_target_pairs={{0,3},{1,2},{2,1},{3,0},{4,7},{5,6},{6,5},{7,4},{8,11},{9,10},{10,... | collective-permute-start | bytes 786440 | tf_op jit(solution)/shard_map/ppermute | solution.py:349
  61.2 6.9 %collective-permute-done.1.refs_4_ = bf16[256,512]{1,0:T(8,128)(2,1)S(1)} collective-permute-done((bf16[256,512]{1,0:T(8,128)(2,1)S(1)}, bf16[256,512]{1,0:T(8,128)(2,1)S(1)}, u32[]{:S(2)}, u32[]{:S(2)}) %collective-permute-start.1) | collective-permute-done | bytes 262176 | tf_op jit(solution)/shard_map/ppermute | solution.py:349
  68.1 6.0 %collective-permute-done.2.refs_5_ = bf16[256,512]{1,0:T(8,128)(2,1)S(1)} collective-permute-done((bf16[256,512]{1,0:T(8,128)(2,1)S(1)}, bf16[256,512]{1,0:T(8,128)(2,1)S(1)}, u32[]{:S(2)}, u32[]{:S(2)}) %collective-permute-start.2) | collective-permute-done | bytes 262176 | tf_op jit(solution)/shard_map/ppermute | solution.py:349
  74.1 1.8 shard_map.178
  76.0 0.0 copy-start.12
  76.0 3.4 %all-to-all-start.3 = ((bf16[4,256,128]{2,1,0:T(8,128)(2,1)}), bf16[4,256,128]{2,1,0:T(8,128)(2,1)S(1)}, u32[]{:S(2)}, u32[]{:S(2)}) async-start(bf16[4,256,128]{2,1,0:T(8,128)(2,1)} %shard_map.178), calls=%async_computation.3 | async-start | bytes 524288 | tf_op jit(solution)/shard_map/all_to_all | solution.py:344
  79.4 0.1 copy.19.routing_ref
  79.5 0.0 copy-start.8
  79.5 1.5 shard_map.172.pick_ref
  81.1 0.0 copy-start.2
  81.1 3.3 %all-to-all-done.3.in_ref = bf16[4,256,128]{2,1,0:T(8,128)(2,1)S(1)} async-done(((bf16[4,256,128]{2,1,0:T(8,128)(2,1)}), bf16[4,256,128]{2,1,0:T(8,128)(2,1)S(1)}, u32[]{:S(2)}, u32[]{:S(2)}) %all-to-all-start.3) | async-done | bytes 262176 | tf_op jit(solution)/shard_map/all_to_all | solution.py:344
  84.4 0.4 shard_map.179
  84.8 28.3 %all_to_all.31 = bf16[128,3,4,128]{3,2,1,0:T(4,128)(2,1)S(1)} all-to-all(bf16[128,3,4,128]{3,2,1,0:T(4,128)(2,1)S(1)} %bitcast.15), channel_id=1, replica_groups=mesh['z'=8,'x'=4,'yg'=4,'yn'=2,'c'=2] {'z','x','yg'}, dimensions={0} | all-to-all | bytes 786432 | tf_op jit(solution)/shard_map/all_to_all | solution.py:344
  113.1 2.5 %collective-permute-start.4 = (bf16[1536,128]{1,0:T(8,128)(2,1)S(1)}, bf16[1536,128]{1,0:T(8,128)(2,1)S(1)}, u32[]{:S(2)}, u32[]{:S(2)}) collective-permute-start(bf16[1536,128]{1,0:T(8,128)(2,1)S(1)} %bitcast.11), channel_id=1, source_target_pairs={{0,2},{2,0},{1,3},{3,1},{4,6},{6,4},{5,7},{7,5},{8,10},{10,8},{9,1... | collective-permute-start | bytes 1179656 | tf_op jit(solution)/shard_map/ppermute | solution.py:349
  115.6 4.5 %collective-permute-start.3 = (bf16[1536,128]{1,0:T(8,128)(2,1)S(1)}, bf16[1536,128]{1,0:T(8,128)(2,1)S(1)}, u32[]{:S(2)}, u32[]{:S(2)}) collective-permute-start(bf16[1536,128]{1,0:T(8,128)(2,1)S(1)} %bitcast.12), channel_id=1, source_target_pairs={{0,1},{1,0},{2,3},{3,2},{4,5},{5,4},{6,7},{7,6},{8,9},{9,8},{10,11... | collective-permute-start | bytes 1179656 | tf_op jit(solution)/shard_map/ppermute | solution.py:349
  120.2 2.5 %collective-permute-done.4.refs_3_ = bf16[1536,128]{1,0:T(8,128)(2,1)S(1)} collective-permute-done((bf16[1536,128]{1,0:T(8,128)(2,1)S(1)}, bf16[1536,128]{1,0:T(8,128)(2,1)S(1)}, u32[]{:S(2)}, u32[]{:S(2)}) %collective-permute-start.4) | collective-permute-done | bytes 393248 | tf_op jit(solution)/shard_map/ppermute | solution.py:349
  122.7 5.7 %collective-permute-start.5 = (bf16[1536,128]{1,0:T(8,128)(2,1)S(1)}, bf16[1536,128]{1,0:T(8,128)(2,1)S(1)}, u32[]{:S(2)}, u32[]{:S(2)}) collective-permute-start(bf16[1536,128]{1,0:T(8,128)(2,1)S(1)} %collective-permute-done.4.refs_3_), channel_id=1, source_target_pairs={{0,1},{1,0},{2,3},{3,2},{4,5},{5,4},{6,7},{7,6},{8,9},{9,8},{10,11... | collective-permute-start | bytes 1179656 | tf_op jit(solution)/shard_map/ppermute | solution.py:349
  128.4 1.3 collective-permute-done.5.refs_4_
  129.7 1.2 copy-done.3
  131.0 2.9 %shard_map.181.h0 = bf16[384,256]{1,0:T(8,128)(2,1)S(1)} custom-call(s32[2]{0:T(128)S(1)} %pad_add_fusion.ids_ref.refs_0_, bf16[1536,128]{1,0:T(8,128)(2,1)S(1)} %bitcast.13, bf16[1536,128]{1,0:T(8,128)(2,1)S(1)} %collective-permute-done.3.refs_2_, bf16[1536,128]{1,0:T(8,128)(2,1)S(1)} %collective-permute-done.4.refs_3_, ...), custom_call_target="tpu_custom_call" | custom-call | flops 1000000 | bytes 1000000 | tf_op jit(solution)/shard_map/pallas_call | solution.py:64
  133.9 2.5 %collective-permute-start.7 = (bf16[384,256]{1,0:T(8,128)(2,1)S(1)}, bf16[384,256]{1,0:T(8,128)(2,1)S(1)}, u32[]{:S(2)}, u32[]{:S(2)}) collective-permute-start(bf16[384,256]{1,0:T(8,128)(2,1)S(1)} %shard_map.181.h0), channel_id=1, source_target_pairs={{0,2},{2,0},{1,3},{3,1},{4,6},{6,4},{5,7},{7,5},{8,10},{10,8},{9,1... | collective-permute-start | bytes 589832 | tf_op jit(solution)/shard_map/ppermute | solution.py:349
  136.5 0.9 shard_map.182
  137.4 2.7 %collective-permute-start.10 = (bf16[320,512]{1,0:T(8,128)(2,1)S(1)}, bf16[320,512]{1,0:T(8,128)(2,1)S(1)}, u32[]{:S(2)}, u32[]{:S(2)}) collective-permute-start(bf16[320,512]{1,0:T(8,128)(2,1)S(1)} %get-tuple-element.28), channel_id=1, source_target_pairs={{0,2},{1,3},{2,0},{3,1},{4,6},{5,7},{6,4},{7,5},{8,10},{9,11},{10,... | collective-permute-start | bytes 983048 | tf_op jit(solution)/shard_map/ppermute | solution.py:349
  140.2 3.4 %collective-permute-start.11 = (bf16[320,512]{1,0:T(8,128)(2,1)S(1)}, bf16[320,512]{1,0:T(8,128)(2,1)S(1)}, u32[]{:S(2)}, u32[]{:S(2)}) collective-permute-start(bf16[320,512]{1,0:T(8,128)(2,1)S(1)} %get-tuple-element.29), channel_id=1, source_target_pairs={{0,3},{1,2},{2,1},{3,0},{4,7},{5,6},{6,5},{7,4},{8,11},{9,10},{10,... | collective-permute-start | bytes 983048 | tf_op jit(solution)/shard_map/ppermute | solution.py:349
  143.5 1.9 collective-permute-start.9
  145.5 2.4 %collective-permute-start.6 = (bf16[384,256]{1,0:T(8,128)(2,1)S(1)}, bf16[384,256]{1,0:T(8,128)(2,1)S(1)}, u32[]{:S(2)}, u32[]{:S(2)}) collective-permute-start(bf16[384,256]{1,0:T(8,128)(2,1)S(1)} %shard_map.181.h0), channel_id=1, source_target_pairs={{0,1},{1,0},{2,3},{3,2},{4,5},{5,4},{6,7},{7,6},{8,9},{9,8},{10,11... | collective-permute-start | bytes 589832 | tf_op jit(solution)/shard_map/ppermute | solution.py:349
  147.9 2.1 collective-permute-start.8
  150.0 6.5 %collective-permute-done.11.d3.w3 = bf16[320,512]{1,0:T(8,128)(2,1)S(1)} collective-permute-done((bf16[320,512]{1,0:T(8,128)(2,1)S(1)}, bf16[320,512]{1,0:T(8,128)(2,1)S(1)}, u32[]{:S(2)}, u32[]{:S(2)}) %collective-permute-start.11) | collective-permute-done | bytes 327712 | tf_op jit(solution)/shard_map/ppermute | solution.py:349
  156.5 1.4 shard_map.183
  157.9 7.4 %all-to-all-start.5 = ((bf16[128,3,4,128]{3,2,1,0:T(4,128)(2,1)}), bf16[128,3,4,128]{3,2,1,0:T(4,128)(2,1)S(1)}, u32[]{:S(2)}, u32[]{:S(2)}) async-start(bf16[128,3,4,128]{3,2,1,0:T(4,128)(2,1)} %bitcast.9), calls=%async_computation.5 | async-start | bytes 786432 | tf_op jit(solution)/shard_map/all_to_all | solution.py:344
  165.3 3.4 %collective-permute-start.12 = (bf16[256,128]{1,0:T(8,128)(2,1)S(1)}, bf16[256,128]{1,0:T(8,128)(2,1)S(1)}, u32[]{:S(2)}, u32[]{:S(2)}) collective-permute-start(bf16[256,128]{1,0:T(8,128)(2,1)S(1)} %get-tuple-element.32.m0.mid_ref), channel_id=1, source_target_pairs={{0,4},{4,8},{8,12},{12,0},{1,5},{5,9},{9,13},{13,1},{2,6},{6,10},{... | collective-permute-start | bytes 196616 | tf_op jit(solution)/shard_map/ppermute | solution.py:349
  168.7 5.2 %collective-permute-start.13 = (bf16[256,128]{1,0:T(8,128)(2,1)S(1)}, bf16[256,128]{1,0:T(8,128)(2,1)S(1)}, u32[]{:S(2)}, u32[]{:S(2)}) collective-permute-start(bf16[256,128]{1,0:T(8,128)(2,1)S(1)} %get-tuple-element.32.m0.mid_ref), channel_id=1, source_target_pairs={{0,8},{4,12},{8,0},{12,4},{1,9},{5,13},{9,1},{13,5},{2,10},{6,14},... | collective-permute-start | bytes 196616 | tf_op jit(solution)/shard_map/ppermute | solution.py:349
  173.9 5.2 %collective-permute-start.14 = (bf16[256,128]{1,0:T(8,128)(2,1)S(1)}, bf16[256,128]{1,0:T(8,128)(2,1)S(1)}, u32[]{:S(2)}, u32[]{:S(2)}) collective-permute-start(bf16[256,128]{1,0:T(8,128)(2,1)S(1)} %get-tuple-element.32.m0.mid_ref), channel_id=1, source_target_pairs={{0,12},{4,0},{8,4},{12,8},{1,13},{5,1},{9,5},{13,9},{2,14},{6,2},{... | collective-permute-start | bytes 196616 | tf_op jit(solution)/shard_map/ppermute | solution.py:349
  179.1 3.4 %collective-permute-done.13.m2 = bf16[256,128]{1,0:T(8,128)(2,1)S(1)} collective-permute-done((bf16[256,128]{1,0:T(8,128)(2,1)S(1)}, bf16[256,128]{1,0:T(8,128)(2,1)S(1)}, u32[]{:S(2)}, u32[]{:S(2)}) %collective-permute-start.13) | collective-permute-done | bytes 65568 | tf_op jit(solution)/shard_map/ppermute | solution.py:349
  182.5 0.4 collective-permute-done.14.m3
  182.9 0.9 shard_map.185.r0
  183.8 2.4 %collective-permute-start.15 = (bf16[256,384]{1,0:T(8,128)(2,1)S(1)}, bf16[256,384]{1,0:T(8,128)(2,1)S(1)}, u32[]{:S(2)}, u32[]{:S(2)}) collective-permute-start(bf16[256,384]{1,0:T(8,128)(2,1)S(1)} %shard_map.185.r0), channel_id=1, source_target_pairs={{0,1},{1,0},{2,3},{3,2},{4,5},{5,4},{6,7},{7,6},{8,9},{9,8},{10,11... | collective-permute-start | bytes 589832 | tf_op jit(solution)/shard_map/ppermute | solution.py:349
  186.3 1.9 collective-permute-start.16
  188.2 3.5 %collective-permute-start.17 = (bf16[256,384]{1,0:T(8,128)(2,1)S(1)}, bf16[256,384]{1,0:T(8,128)(2,1)S(1)}, u32[]{:S(2)}, u32[]{:S(2)}) collective-permute-start(bf16[256,384]{1,0:T(8,128)(2,1)S(1)} %shard_map.185.r0), channel_id=1, source_target_pairs={{0,3},{1,2},{2,1},{3,0},{4,7},{5,6},{6,5},{7,4},{8,11},{9,10},{10,... | collective-permute-start | bytes 589832 | tf_op jit(solution)/shard_map/ppermute | solution.py:349
  191.8 2.9 %collective-permute-done.16.r2 = bf16[256,384]{1,0:T(8,128)(2,1)S(1)} collective-permute-done((bf16[256,384]{1,0:T(8,128)(2,1)S(1)}, bf16[256,384]{1,0:T(8,128)(2,1)S(1)}, u32[]{:S(2)}, u32[]{:S(2)}) %collective-permute-start.16) | collective-permute-done | bytes 196640 | tf_op jit(solution)/shard_map/ppermute | solution.py:349
  194.6 4.4 %collective-permute-done.17.r3 = bf16[256,384]{1,0:T(8,128)(2,1)S(1)} collective-permute-done((bf16[256,384]{1,0:T(8,128)(2,1)S(1)}, bf16[256,384]{1,0:T(8,128)(2,1)S(1)}, u32[]{:S(2)}, u32[]{:S(2)}) %collective-permute-start.17) | collective-permute-done | bytes 196640 | tf_op jit(solution)/shard_map/ppermute | solution.py:349
  199.0 0.1 shard_map.186.h0
  199.2 4.5 %collective-permute-start.18 = (bf16[256,128]{1,0:T(8,128)(2,1)S(1)}, bf16[256,128]{1,0:T(8,128)(2,1)S(1)}, u32[]{:S(2)}, u32[]{:S(2)}) collective-permute-start(bf16[256,128]{1,0:T(8,128)(2,1)S(1)} %shard_map.186.h0), channel_id=1, source_target_pairs={{0,4},{4,8},{8,12},{12,0},{1,5},{5,9},{9,13},{13,1},{2,6},{6,10},{... | collective-permute-start | bytes 196616 | tf_op jit(solution)/shard_map/ppermute | solution.py:349
  203.6 5.4 %collective-permute-start.19 = (bf16[256,128]{1,0:T(8,128)(2,1)S(1)}, bf16[256,128]{1,0:T(8,128)(2,1)S(1)}, u32[]{:S(2)}, u32[]{:S(2)}) collective-permute-start(bf16[256,128]{1,0:T(8,128)(2,1)S(1)} %shard_map.186.h0), channel_id=1, source_target_pairs={{0,8},{4,12},{8,0},{12,4},{1,9},{5,13},{9,1},{13,5},{2,10},{6,14},... | collective-permute-start | bytes 196616 | tf_op jit(solution)/shard_map/ppermute | solution.py:349
  209.0 3.0 %collective-permute-start.20 = (bf16[256,128]{1,0:T(8,128)(2,1)S(1)}, bf16[256,128]{1,0:T(8,128)(2,1)S(1)}, u32[]{:S(2)}, u32[]{:S(2)}) collective-permute-start(bf16[256,128]{1,0:T(8,128)(2,1)S(1)} %shard_map.186.h0), channel_id=1, source_target_pairs={{0,12},{4,0},{8,4},{12,8},{1,13},{5,1},{9,5},{13,9},{2,14},{6,2},{... | collective-permute-start | bytes 196616 | tf_op jit(solution)/shard_map/ppermute | solution.py:349
  212.0 0.1 copy.21.score_ref
  212.2 2.0 shard_map.184
  214.2 3.1 %collective-permute-done.20.h3 = bf16[256,128]{1,0:T(8,128)(2,1)S(1)} collective-permute-done((bf16[256,128]{1,0:T(8,128)(2,1)S(1)}, bf16[256,128]{1,0:T(8,128)(2,1)S(1)}, u32[]{:S(2)}, u32[]{:S(2)}) %collective-permute-start.20) | collective-permute-done | bytes 65568 | tf_op jit(solution)/shard_map/ppermute | solution.py:349
  217.3 0.8 shard_map.187.ahead_ref
  218.1 1.2 shard_map.188
  (40 shorter events, 0.1 us)
Async XLA Ops:
  26.3 4.0 %copy-start.14 = (bf16[256]{0:T(256)(128)(2,1)S(1)}, bf16[256]{0:T(256)(128)(2,1)}, u32[]{:S(2)}) copy-start(bf16[256]{0:T(256)(128)(2,1)} %param.24) | copy-start | bytes 1540
  26.3 12.9 %all-to-all-start.1 = ((bf16[32,8,128]{2,1,0:T(8,128)(2,1)}), bf16[32,8,128]{2,1,0:T(8,128)(2,1)S(1)}, u32[]{:S(2)}, u32[]{:S(2)}) async-start(bf16[32,8,128]{2,1,0:T(8,128)(2,1)} %shard_map.174), calls=%async_computation.1 | async-start | bytes 131072 | tf_op jit(solution)/shard_map/all_to_all | solution.py:344
  30.3 8.9 %copy-start.5 = (bf16[256,256]{1,0:T(8,128)(2,1)S(1)}, bf16[256,256]{1,0:T(8,128)(2,1)}, u32[]{:S(2)}) copy-start(bf16[256,256]{1,0:T(8,128)(2,1)} %refs_4_.1) | copy-start | bytes 393220
  39.2 1.0 copy-start.4
  40.1 0.9 copy-start.6
  41.0 8.6 %copy-start.1 = (bf16[4096,128]{1,0:T(8,128)(2,1)S(1)}, bf16[4096,128]{1,0:T(8,128)(2,1)}, u32[]{:S(2)}) copy-start(bf16[4096,128]{1,0:T(8,128)(2,1)} %project_ref.1) | copy-start | bytes 3145732
  42.7 31.5 %all-to-all-start.2 = ((bf16[4,256,256]{2,1,0:T(8,128)(2,1)}), bf16[4,256,256]{2,1,0:T(8,128)(2,1)S(1)}, u32[]{:S(2)}, u32[]{:S(2)}) async-start(bf16[4,256,256]{2,1,0:T(8,128)(2,1)} %shard_map.176), calls=%async_computation.2 | async-start | bytes 1048576 | tf_op jit(solution)/shard_map/all_to_all | solution.py:344
  50.3 10.9 %collective-permute-start = (bf16[256,512]{1,0:T(8,128)(2,1)S(1)}, bf16[256,512]{1,0:T(8,128)(2,1)S(1)}, u32[]{:S(2)}, u32[]{:S(2)}) collective-permute-start(bf16[256,512]{1,0:T(8,128)(2,1)S(1)} %get-tuple-element.22), channel_id=1, source_target_pairs={{0,1},{1,0},{2,3},{3,2},{4,5},{5,4},{6,7},{7,6},{8,9},{9,8},{10,11... | collective-permute-start | bytes 786440 | tf_op jit(solution)/shard_map/ppermute | solution.py:349
  55.7 12.4 %collective-permute-start.1 = (bf16[256,512]{1,0:T(8,128)(2,1)S(1)}, bf16[256,512]{1,0:T(8,128)(2,1)S(1)}, u32[]{:S(2)}, u32[]{:S(2)}) collective-permute-start(bf16[256,512]{1,0:T(8,128)(2,1)S(1)} %get-tuple-element.23), channel_id=1, source_target_pairs={{0,2},{1,3},{2,0},{3,1},{4,6},{5,7},{6,4},{7,5},{8,10},{9,11},{10,... | collective-permute-start | bytes 786440 | tf_op jit(solution)/shard_map/ppermute | solution.py:349
  58.1 16.0 %collective-permute-start.2 = (bf16[256,512]{1,0:T(8,128)(2,1)S(1)}, bf16[256,512]{1,0:T(8,128)(2,1)S(1)}, u32[]{:S(2)}, u32[]{:S(2)}) collective-permute-start(bf16[256,512]{1,0:T(8,128)(2,1)S(1)} %get-tuple-element.24), channel_id=1, source_target_pairs={{0,3},{1,2},{2,1},{3,0},{4,7},{5,6},{6,5},{7,4},{8,11},{9,10},{10,... | collective-permute-start | bytes 786440 | tf_op jit(solution)/shard_map/ppermute | solution.py:349
  76.0 3.4 %copy-start.12 = (s32[256,4]{0,1:T(4,128)S(1)}, s32[256,4]{0,1:T(4,128)}, u32[]{:S(2)}) copy-start(s32[256,4]{0,1:T(4,128)} %param.28) | copy-start | bytes 12292
  76.0 8.4 %all-to-all-start.3 = ((bf16[4,256,128]{2,1,0:T(8,128)(2,1)}), bf16[4,256,128]{2,1,0:T(8,128)(2,1)S(1)}, u32[]{:S(2)}, u32[]{:S(2)}) async-start(bf16[4,256,128]{2,1,0:T(8,128)(2,1)} %shard_map.178), calls=%async_computation.3 | async-start | bytes 524288 | tf_op jit(solution)/shard_map/all_to_all | solution.py:344
  79.5 4.8 %copy-start.8 = (bf16[256,128]{1,0:T(8,128)(2,1)S(1)}, bf16[256,128]{1,0:T(8,128)(2,1)}, u32[]{:S(2)}) copy-start(bf16[256,128]{1,0:T(8,128)(2,1)} %residual_ref.1) | copy-start | bytes 196612
  81.1 48.7 %copy-start.2 = (bf16[2048,256]{1,0:T(8,128)(2,1)S(1)}, bf16[2048,256]{1,0:T(8,128)(2,1)}, u32[]{:S(2)}) copy-start(bf16[2048,256]{1,0:T(8,128)(2,1)} %refs_6_.1) | copy-start | bytes 3145732
  84.7 43.7 %copy-start.9 = (bf16[2048]{0:T(1024)(128)(2,1)S(1)}, bf16[2048]{0:T(1024)(128)(2,1)}, u32[]{:S(2)}) copy-start(bf16[2048]{0:T(1024)(128)(2,1)} %param.27) | copy-start | bytes 12292
  113.1 9.6 %collective-permute-start.4 = (bf16[1536,128]{1,0:T(8,128)(2,1)S(1)}, bf16[1536,128]{1,0:T(8,128)(2,1)S(1)}, u32[]{:S(2)}, u32[]{:S(2)}) collective-permute-start(bf16[1536,128]{1,0:T(8,128)(2,1)S(1)} %bitcast.11), channel_id=1, source_target_pairs={{0,2},{2,0},{1,3},{3,1},{4,6},{6,4},{5,7},{7,5},{8,10},{10,8},{9,1... | collective-permute-start | bytes 1179656 | tf_op jit(solution)/shard_map/ppermute | solution.py:349
  115.6 12.8 %collective-permute-start.3 = (bf16[1536,128]{1,0:T(8,128)(2,1)S(1)}, bf16[1536,128]{1,0:T(8,128)(2,1)S(1)}, u32[]{:S(2)}, u32[]{:S(2)}) collective-permute-start(bf16[1536,128]{1,0:T(8,128)(2,1)S(1)} %bitcast.12), channel_id=1, source_target_pairs={{0,1},{1,0},{2,3},{3,2},{4,5},{5,4},{6,7},{7,6},{8,9},{9,8},{10,11... | collective-permute-start | bytes 1179656 | tf_op jit(solution)/shard_map/ppermute | solution.py:349
  122.7 7.1 %collective-permute-start.5 = (bf16[1536,128]{1,0:T(8,128)(2,1)S(1)}, bf16[1536,128]{1,0:T(8,128)(2,1)S(1)}, u32[]{:S(2)}, u32[]{:S(2)}) collective-permute-start(bf16[1536,128]{1,0:T(8,128)(2,1)S(1)} %collective-permute-done.4.refs_3_), channel_id=1, source_target_pairs={{0,1},{1,0},{2,3},{3,2},{4,5},{5,4},{6,7},{7,6},{8,9},{9,8},{10,11... | collective-permute-start | bytes 1179656 | tf_op jit(solution)/shard_map/ppermute | solution.py:349
  129.7 1.2 copy-start.3
  131.0 5.5 %copy-start.10 = (bf16[2048,32]{0,1:T(8,128)(2,1)S(1)}, bf16[2048,32]{0,1:T(8,128)(2,1)}, u32[]{:S(2)}) copy-start(bf16[2048,32]{0,1:T(8,128)(2,1)} %param.34) | copy-start | bytes 393220
  131.0 5.5 %copy-start.11 = (bf16[2048,32]{0,1:T(8,128)(2,1)S(1)}, bf16[2048,32]{0,1:T(8,128)(2,1)}, u32[]{:S(2)}) copy-start(bf16[2048,32]{0,1:T(8,128)(2,1)} %param.33) | copy-start | bytes 393220
  131.0 5.5 %copy-start = (bf16[256,2048]{1,0:T(8,128)(2,1)S(1)}, bf16[256,2048]{1,0:T(8,128)(2,1)}, u32[]{:S(2)}) copy-start(bf16[256,2048]{1,0:T(8,128)(2,1)} %down_ref.2) | copy-start | bytes 3145732
  133.9 14.0 %collective-permute-start.7 = (bf16[384,256]{1,0:T(8,128)(2,1)S(1)}, bf16[384,256]{1,0:T(8,128)(2,1)S(1)}, u32[]{:S(2)}, u32[]{:S(2)}) collective-permute-start(bf16[384,256]{1,0:T(8,128)(2,1)S(1)} %shard_map.181.h0), channel_id=1, source_target_pairs={{0,2},{2,0},{1,3},{3,1},{4,6},{6,4},{5,7},{7,5},{8,10},{10,8},{9,1... | collective-permute-start | bytes 589832 | tf_op jit(solution)/shard_map/ppermute | solution.py:349
  137.4 12.6 %collective-permute-start.10 = (bf16[320,512]{1,0:T(8,128)(2,1)S(1)}, bf16[320,512]{1,0:T(8,128)(2,1)S(1)}, u32[]{:S(2)}, u32[]{:S(2)}) collective-permute-start(bf16[320,512]{1,0:T(8,128)(2,1)S(1)} %get-tuple-element.28), channel_id=1, source_target_pairs={{0,2},{1,3},{2,0},{3,1},{4,6},{5,7},{6,4},{7,5},{8,10},{9,11},{10,... | collective-permute-start | bytes 983048 | tf_op jit(solution)/shard_map/ppermute | solution.py:349
  140.2 16.3 %collective-permute-start.11 = (bf16[320,512]{1,0:T(8,128)(2,1)S(1)}, bf16[320,512]{1,0:T(8,128)(2,1)S(1)}, u32[]{:S(2)}, u32[]{:S(2)}) collective-permute-start(bf16[320,512]{1,0:T(8,128)(2,1)S(1)} %get-tuple-element.29), channel_id=1, source_target_pairs={{0,3},{1,2},{2,1},{3,0},{4,7},{5,6},{6,5},{7,4},{8,11},{9,10},{10,... | collective-permute-start | bytes 983048 | tf_op jit(solution)/shard_map/ppermute | solution.py:349
  143.5 12.9 %collective-permute-start.9 = (bf16[320,512]{1,0:T(8,128)(2,1)S(1)}, bf16[320,512]{1,0:T(8,128)(2,1)S(1)}, u32[]{:S(2)}, u32[]{:S(2)}) collective-permute-start(bf16[320,512]{1,0:T(8,128)(2,1)S(1)} %get-tuple-element.27), channel_id=1, source_target_pairs={{0,1},{1,0},{2,3},{3,2},{4,5},{5,4},{6,7},{7,6},{8,9},{9,8},{10,11... | collective-permute-start | bytes 983048 | tf_op jit(solution)/shard_map/ppermute | solution.py:349
  145.5 11.0 %collective-permute-start.6 = (bf16[384,256]{1,0:T(8,128)(2,1)S(1)}, bf16[384,256]{1,0:T(8,128)(2,1)S(1)}, u32[]{:S(2)}, u32[]{:S(2)}) collective-permute-start(bf16[384,256]{1,0:T(8,128)(2,1)S(1)} %shard_map.181.h0), channel_id=1, source_target_pairs={{0,1},{1,0},{2,3},{3,2},{4,5},{5,4},{6,7},{7,6},{8,9},{9,8},{10,11... | collective-permute-start | bytes 589832 | tf_op jit(solution)/shard_map/ppermute | solution.py:349
  147.9 8.6 %collective-permute-start.8 = (bf16[384,256]{1,0:T(8,128)(2,1)S(1)}, bf16[384,256]{1,0:T(8,128)(2,1)S(1)}, u32[]{:S(2)}, u32[]{:S(2)}) collective-permute-start(bf16[384,256]{1,0:T(8,128)(2,1)S(1)} %collective-permute-done.7.h2), channel_id=1, source_target_pairs={{0,1},{1,0},{2,3},{3,2},{4,5},{5,4},{6,7},{7,6},{8,9},{9,8},{10,11... | collective-permute-start | bytes 589832 | tf_op jit(solution)/shard_map/ppermute | solution.py:349
  157.9 60.2 %all-to-all-start.5 = ((bf16[128,3,4,128]{3,2,1,0:T(4,128)(2,1)}), bf16[128,3,4,128]{3,2,1,0:T(4,128)(2,1)S(1)}, u32[]{:S(2)}, u32[]{:S(2)}) async-start(bf16[128,3,4,128]{3,2,1,0:T(4,128)(2,1)} %bitcast.9), calls=%async_computation.5 | async-start | bytes 786432 | tf_op jit(solution)/shard_map/all_to_all | solution.py:344
  165.3 13.8 %collective-permute-start.12 = (bf16[256,128]{1,0:T(8,128)(2,1)S(1)}, bf16[256,128]{1,0:T(8,128)(2,1)S(1)}, u32[]{:S(2)}, u32[]{:S(2)}) collective-permute-start(bf16[256,128]{1,0:T(8,128)(2,1)S(1)} %get-tuple-element.32.m0.mid_ref), channel_id=1, source_target_pairs={{0,4},{4,8},{8,12},{12,0},{1,5},{5,9},{9,13},{13,1},{2,6},{6,10},{... | collective-permute-start | bytes 196616 | tf_op jit(solution)/shard_map/ppermute | solution.py:349
  168.7 13.8 %collective-permute-start.13 = (bf16[256,128]{1,0:T(8,128)(2,1)S(1)}, bf16[256,128]{1,0:T(8,128)(2,1)S(1)}, u32[]{:S(2)}, u32[]{:S(2)}) collective-permute-start(bf16[256,128]{1,0:T(8,128)(2,1)S(1)} %get-tuple-element.32.m0.mid_ref), channel_id=1, source_target_pairs={{0,8},{4,12},{8,0},{12,4},{1,9},{5,13},{9,1},{13,5},{2,10},{6,14},... | collective-permute-start | bytes 196616 | tf_op jit(solution)/shard_map/ppermute | solution.py:349
  173.9 9.0 %collective-permute-start.14 = (bf16[256,128]{1,0:T(8,128)(2,1)S(1)}, bf16[256,128]{1,0:T(8,128)(2,1)S(1)}, u32[]{:S(2)}, u32[]{:S(2)}) collective-permute-start(bf16[256,128]{1,0:T(8,128)(2,1)S(1)} %get-tuple-element.32.m0.mid_ref), channel_id=1, source_target_pairs={{0,12},{4,0},{8,4},{12,8},{1,13},{5,1},{9,5},{13,9},{2,14},{6,2},{... | collective-permute-start | bytes 196616 | tf_op jit(solution)/shard_map/ppermute | solution.py:349
  183.8 28.2 %copy-start.13 = (f32[256,4]{0,1:T(4,128)S(1)}, f32[256,4]{0,1:T(4,128)}, u32[]{:S(2)}) copy-start(f32[256,4]{0,1:T(4,128)} %param.29) | copy-start | bytes 12292
  183.8 7.9 %collective-permute-start.15 = (bf16[256,384]{1,0:T(8,128)(2,1)S(1)}, bf16[256,384]{1,0:T(8,128)(2,1)S(1)}, u32[]{:S(2)}, u32[]{:S(2)}) collective-permute-start(bf16[256,384]{1,0:T(8,128)(2,1)S(1)} %shard_map.185.r0), channel_id=1, source_target_pairs={{0,1},{1,0},{2,3},{3,2},{4,5},{5,4},{6,7},{7,6},{8,9},{9,8},{10,11... | collective-permute-start | bytes 589832 | tf_op jit(solution)/shard_map/ppermute | solution.py:349
  186.3 8.3 %collective-permute-start.16 = (bf16[256,384]{1,0:T(8,128)(2,1)S(1)}, bf16[256,384]{1,0:T(8,128)(2,1)S(1)}, u32[]{:S(2)}, u32[]{:S(2)}) collective-permute-start(bf16[256,384]{1,0:T(8,128)(2,1)S(1)} %shard_map.185.r0), channel_id=1, source_target_pairs={{0,2},{1,3},{2,0},{3,1},{4,6},{5,7},{6,4},{7,5},{8,10},{9,11},{10,... | collective-permute-start | bytes 589832 | tf_op jit(solution)/shard_map/ppermute | solution.py:349
  188.2 10.8 %collective-permute-start.17 = (bf16[256,384]{1,0:T(8,128)(2,1)S(1)}, bf16[256,384]{1,0:T(8,128)(2,1)S(1)}, u32[]{:S(2)}, u32[]{:S(2)}) collective-permute-start(bf16[256,384]{1,0:T(8,128)(2,1)S(1)} %shard_map.185.r0), channel_id=1, source_target_pairs={{0,3},{1,2},{2,1},{3,0},{4,7},{5,6},{6,5},{7,4},{8,11},{9,10},{10,... | collective-permute-start | bytes 589832 | tf_op jit(solution)/shard_map/ppermute | solution.py:349
  199.2 15.0 %collective-permute-start.18 = (bf16[256,128]{1,0:T(8,128)(2,1)S(1)}, bf16[256,128]{1,0:T(8,128)(2,1)S(1)}, u32[]{:S(2)}, u32[]{:S(2)}) collective-permute-start(bf16[256,128]{1,0:T(8,128)(2,1)S(1)} %shard_map.186.h0), channel_id=1, source_target_pairs={{0,4},{4,8},{8,12},{12,0},{1,5},{5,9},{9,13},{13,1},{2,6},{6,10},{... | collective-permute-start | bytes 196616 | tf_op jit(solution)/shard_map/ppermute | solution.py:349
  203.6 10.5 %collective-permute-start.19 = (bf16[256,128]{1,0:T(8,128)(2,1)S(1)}, bf16[256,128]{1,0:T(8,128)(2,1)S(1)}, u32[]{:S(2)}, u32[]{:S(2)}) collective-permute-start(bf16[256,128]{1,0:T(8,128)(2,1)S(1)} %shard_map.186.h0), channel_id=1, source_target_pairs={{0,8},{4,12},{8,0},{12,4},{1,9},{5,13},{9,1},{13,5},{2,10},{6,14},... | collective-permute-start | bytes 196616 | tf_op jit(solution)/shard_map/ppermute | solution.py:349
  209.0 8.3 %collective-permute-start.20 = (bf16[256,128]{1,0:T(8,128)(2,1)S(1)}, bf16[256,128]{1,0:T(8,128)(2,1)S(1)}, u32[]{:S(2)}, u32[]{:S(2)}) collective-permute-start(bf16[256,128]{1,0:T(8,128)(2,1)S(1)} %shard_map.186.h0), channel_id=1, source_target_pairs={{0,12},{4,0},{8,4},{12,8},{1,13},{5,1},{9,5},{13,9},{2,14},{6,2},{... | collective-permute-start | bytes 196616 | tf_op jit(solution)/shard_map/ppermute | solution.py:349
  212.2 5.2 %copy-start.7 = (bf16[512,128]{1,0:T(8,128)(2,1)S(1)}, bf16[512,128]{1,0:T(8,128)(2,1)}, u32[]{:S(2)}) copy-start(bf16[512,128]{1,0:T(8,128)(2,1)} %down_ref.3) | copy-start | bytes 393220

commit v6 on v4

--- a/solution.py
+++ b/solution.py
@@ -81,24 +81,34 @@
     )
 
 
+def split(value, count):
+    pieces = []
+    for _ in range(count):
+        piece = value.astype(BF16)
+        pieces.append(piece)
+        value = value - piece.astype(F32)
+    return pieces
+
+
+def dot(a, b):
+    return jnp.dot(a, b, preferred_element_type=F32)
+
+
 def decays(decay_ref, extra_ref):
     raw = decay_ref[...].astype(F32)
     logs = jax.nn.log_sigmoid(raw) / GATE_TEMPER
     rows = lax.broadcasted_iota(jnp.int32, (BLOCK, BLOCK), 0)
     cols = lax.broadcasted_iota(jnp.int32, (BLOCK, BLOCK), 1)
-    lower = (rows >= cols).astype(F32)
+    lower = (rows >= cols).astype(F32).astype(BF16)
     wide_rows = lax.broadcasted_iota(jnp.int32, (BLOCK, 128), 0)
     wide_cols = lax.broadcasted_iota(jnp.int32, (BLOCK, 128), 1)
-    ones = jnp.ones((128, DK), F32)
+    ones = jnp.ones((128, DK), BF16)
     inside = []
     for b in range(TOK // BLOCK):
         at = wide_cols - (b % 2) * BLOCK
         extra = jnp.where((at >= 0) & (at <= wide_rows), extra_ref[b // 2 : b // 2 + 1, :], 0.0)
-        inside.append(
-            jnp.dot(lower, logs[b * BLOCK : (b + 1) * BLOCK], precision=HIGHEST,
-                    preferred_element_type=F32)
-            + jnp.dot(extra, ones, precision=HIGHEST, preferred_element_type=F32)
-        )
+        total = sum(dot(lower, piece) for piece in split(logs[b * BLOCK : (b + 1) * BLOCK], 3))
+        inside.append(total + sum(dot(piece, ones) for piece in split(extra, 3)))
     return inside
 
 
@@ -120,9 +130,17 @@
 
 def state_kernel(key_ref, value_ref, decay_ref, extra_ref, out_ref):
     inside = decays(decay_ref, extra_ref)
-    _, state, total = block_states(inside, key_ref, value_ref)
+    later = jnp.zeros((1, DK), F32)
+    scaled = []
+    for cum in reversed(inside):
+        end = cum[BLOCK - 1 : BLOCK]
+        scaled.insert(0, jnp.exp(end - cum + later))
+        later = later + end
+    key_end = key_ref[...].astype(F32) * jnp.concatenate(scaled, axis=0)
+    value_t = value_ref[...].astype(F32).T.astype(BF16)
+    state = sum(dot(value_t, piece) for piece in split(key_end, 3))
     out_ref[:, 0:8, :] = state.reshape(32, 8, DK).astype(BF16)
-    decay = jnp.exp(total)
+    decay = jnp.exp(later)
     high = decay.astype(BF16).astype(F32)
     row = lax.broadcasted_iota(jnp.int32, (8, DK), 0)
     tail = jnp.where(row == 0, high, jnp.where(row == 1, decay - high, 0.0))
@@ -161,7 +179,8 @@
 
 
 def head_kernel(gain_ref, enter_ref, local_ref, start_ref, gate_ref, out_ref):
-    mixed = local_ref[...] + nt(start_ref[...], enter_ref[...].astype(F32), precision=HIGHEST)
+    enter = enter_ref[...]
+    mixed = local_ref[...] + sum(nt(piece, enter) for piece in split(start_ref[...], 3))
     scale = lax.rsqrt(jnp.mean(mixed * mixed, axis=-1, keepdims=True) + EPSILON)
     gate = jax.nn.silu(gate_ref[...].astype(F32))
     rows = (mixed * scale * gain_ref[...].astype(F32) * gate).astype(BF16)

time: 226 us -> 226 us (level)
  no operation moved by 1% of the time
where the time goes in v6:
time: 226 us; the launch traced here: 225 us
  starting transfers between devices  89.7 us (40%)
  waiting for transfers between devices  53.4 us (24%)
  blocking collectives  52.1 us (23%)
  Pallas kernels  23.5 us (10%)
  local copies, waits for them, and re-layouts  5.48 us (2%)
    ppermute x18, starting transfers between devices, moved(): lax.ppermute(value, axes, [(i, target(i) % count) for i in range(count)])  67.4 us
    all_to_all x2, blocking collectives, exchange(): return lax.all_to_all(value, axes, split_axis=0, concat_axis=0, tiled=True)  52.1 us
    ppermute x18, waiting for transfers between devices, moved(): lax.ppermute(value, axes, [(i, target(i) % count) for i in range(count)])  46 us
    pallas_call x16, Pallas kernels, call(): pl.pallas_call(fetching if fetch else kernel, out_shape=shapes, in_specs=...  23.5 us
    all_to_all x4, starting transfers between devices, exchange(): return lax.all_to_all(value, axes, split_axis=0, concat_axis=0, tiled=True)  22.3 us
    all_to_all x4, waiting for transfers between devices, exchange(): return lax.all_to_all(value, axes, split_axis=0, concat_axis=0, tiled=True)  7.35 us
    unnamed x32, local copies, waits for them, and re-layouts  4.88 us
  transfers between devices with their start and end apart: 22, of which 14 were waited for; matrix products, arithmetic and copies ran while one was open for 0% of the time, Pallas kernels for 4%

profile of v6, /device:TPU:1, one launch (start us, length us, event | category | flops | bytes accessed | tf_op | source)
XLA Modules:
  0.0 224.7 jit_solution(16160256010225120364)
XLA Ops:
  0.0 2.3 %shard_map.173 = bf16[32,16,128]{2,1,0:T(8,128)(2,1)} custom-call(bf16[256,128]{1,0:T(8,128)(2,1)} %refs_1_.3, bf16[256,256]{1,0:T(8,128)(2,1)} %refs_2_.3, bf16[256,128]{1,0:T(8,128)(2,1)} %refs_3_.1, f32[2,128]{1,0:T(2,128)} %bitcast.20), custom_call_target="tpu_custom_call" | custom-call | flops 1000000 | bytes 1000000 | tf_op jit(solution)/shard_map/pallas_call | solution.py:64
  2.3 23.1 %all_to_all.30.in_ref = bf16[32,16,128]{2,1,0:T(8,128)(2,1)S(1)} all-to-all(bf16[32,16,128]{2,1,0:T(8,128)(2,1)} %shard_map.173), channel_id=1, replica_groups=mesh['z'=8,'x'=4,'yg'=4,'yn'=2,'c'=2] {'z','x'}, dimensions={0} | all-to-all | bytes 262144 | tf_op jit(solution)/shard_map/all_to_all | solution.py:357
  25.3 0.7 shard_map.174
  26.0 3.9 %all-to-all-start.1 = ((bf16[32,8,128]{2,1,0:T(8,128)(2,1)}), bf16[32,8,128]{2,1,0:T(8,128)(2,1)S(1)}, u32[]{:S(2)}, u32[]{:S(2)}) async-start(bf16[32,8,128]{2,1,0:T(8,128)(2,1)} %shard_map.174), calls=%async_computation.1 | async-start | bytes 131072 | tf_op jit(solution)/shard_map/all_to_all | solution.py:357
  29.9 0.0 copy-start.14
  29.9 0.6 copy-done.14
  30.6 0.6 reshape.24.refs_0_
  31.2 3.6 %shard_map.175 = (f32[256,256]{1,0:T(8,128)}, f32[256,128]{1,0:T(8,128)}) custom-call(bf16[256,128]{1,0:T(8,128)(2,1)} %refs_0_.3, bf16[256,128]{1,0:T(8,128)(2,1)} %refs_1_.3, bf16[256,256]{1,0:T(8,128)(2,1)} %refs_2_.3, bf16[256,128]{1,0:T(8,128)(2,1)} %refs_3_.1, f32[2,128]{1,0:T(2,128)} %bitcast.21), custom_call_target="tpu_custom_call" | custom-call | flops 1000000 | bytes 1000000 | tf_op jit(solution)/shard_map/pallas_call | solution.py:64
  34.7 0.1 pad_add_fusion.ids_ref.refs_0_
  34.8 4.0 %all-to-all-done.1 = bf16[32,8,128]{2,1,0:T(8,128)(2,1)S(1)} async-done(((bf16[32,8,128]{2,1,0:T(8,128)(2,1)}), bf16[32,8,128]{2,1,0:T(8,128)(2,1)S(1)}, u32[]{:S(2)}, u32[]{:S(2)}) %all-to-all-start.1) | async-done | bytes 65568 | tf_op jit(solution)/shard_map/all_to_all | solution.py:357
  38.8 0.6 copy-done.9
  39.4 3.0 %shard_map.176 = bf16[4,256,256]{2,1,0:T(8,128)(2,1)} custom-call(bf16[1,256]{1,0:T(2,128)(2,1)} %reshape.24.refs_0_, bf16[256,128]{1,0:T(8,128)(2,1)} %bitcast.17, f32[256,256]{1,0:T(8,128)} %get-tuple-element.15.refs_2_, f32[256,128]{1,0:T(8,128)} %get-tuple-element.16.refs_3_, bf16[256,256]{1,0:T(8,128)(2,1)} %refs_4_.1), custom_call_target="tpu_custom_call" | custom-call | flops 1000000 | bytes 1000000 | tf_op jit(solution)/shard_map/pallas_call | solution.py:64
  42.4 0.0 copy-start
  42.4 7.0 %all-to-all-start.2 = ((bf16[4,256,256]{2,1,0:T(8,128)(2,1)}), bf16[4,256,256]{2,1,0:T(8,128)(2,1)S(1)}, u32[]{:S(2)}, u32[]{:S(2)}) async-start(bf16[4,256,256]{2,1,0:T(8,128)(2,1)} %shard_map.176), calls=%async_computation.2 | async-start | bytes 1048576 | tf_op jit(solution)/shard_map/all_to_all | solution.py:357
  49.4 1.2 copy-done.1
  50.6 1.0 shard_map.177
  51.7 5.4 %collective-permute-start = (bf16[576,512]{1,0:T(8,128)(2,1)S(1)}, bf16[576,512]{1,0:T(8,128)(2,1)S(1)}, u32[]{:S(2)}, u32[]{:S(2)}) collective-permute-start(bf16[576,512]{1,0:T(8,128)(2,1)S(1)} %get-tuple-element.18), channel_id=1, source_target_pairs={{0,1},{1,0},{2,3},{3,2},{4,5},{5,4},{6,7},{7,6},{8,9},{9,8},{10,11... | collective-permute-start | bytes 1769480 | tf_op jit(solution)/shard_map/ppermute | solution.py:362
  57.1 2.3 %collective-permute-start.1 = (bf16[576,512]{1,0:T(8,128)(2,1)S(1)}, bf16[576,512]{1,0:T(8,128)(2,1)S(1)}, u32[]{:S(2)}, u32[]{:S(2)}) collective-permute-start(bf16[576,512]{1,0:T(8,128)(2,1)S(1)} %get-tuple-element.19), channel_id=1, source_target_pairs={{0,2},{1,3},{2,0},{3,1},{4,6},{5,7},{6,4},{7,5},{8,10},{9,11},{10,... | collective-permute-start | bytes 1769480 | tf_op jit(solution)/shard_map/ppermute | solution.py:362
  59.4 3.2 %collective-permute-start.2 = (bf16[576,512]{1,0:T(8,128)(2,1)S(1)}, bf16[576,512]{1,0:T(8,128)(2,1)S(1)}, u32[]{:S(2)}, u32[]{:S(2)}) collective-permute-start(bf16[576,512]{1,0:T(8,128)(2,1)S(1)} %get-tuple-element.20), channel_id=1, source_target_pairs={{0,3},{1,2},{2,1},{3,0},{4,7},{5,6},{6,5},{7,4},{8,11},{9,10},{10,... | collective-permute-start | bytes 1769480 | tf_op jit(solution)/shard_map/ppermute | solution.py:362
  62.6 13.1 %collective-permute-done.1.refs_4_.d2.w2 = bf16[576,512]{1,0:T(8,128)(2,1)S(1)} collective-permute-done((bf16[576,512]{1,0:T(8,128)(2,1)S(1)}, bf16[576,512]{1,0:T(8,128)(2,1)S(1)}, u32[]{:S(2)}, u32[]{:S(2)}) %collective-permute-start.1) | collective-permute-done | bytes 589856 | tf_op jit(solution)/shard_map/ppermute | solution.py:362
  75.7 12.6 %collective-permute-done.2.refs_5_.d3.w3 = bf16[576,512]{1,0:T(8,128)(2,1)S(1)} collective-permute-done((bf16[576,512]{1,0:T(8,128)(2,1)S(1)}, bf16[576,512]{1,0:T(8,128)(2,1)S(1)}, u32[]{:S(2)}, u32[]{:S(2)}) %collective-permute-start.2) | collective-permute-done | bytes 589856 | tf_op jit(solution)/shard_map/ppermute | solution.py:362
  88.3 1.8 shard_map.178
  90.1 3.8 %all-to-all-start.3 = ((bf16[4,256,128]{2,1,0:T(8,128)(2,1)}), bf16[4,256,128]{2,1,0:T(8,128)(2,1)S(1)}, u32[]{:S(2)}, u32[]{:S(2)}) async-start(bf16[4,256,128]{2,1,0:T(8,128)(2,1)} %shard_map.178), calls=%async_computation.3 | async-start | bytes 524288 | tf_op jit(solution)/shard_map/all_to_all | solution.py:357
  93.9 0.1 copy.19.routing_ref
  94.0 1.5 shard_map.172.pick_ref
  95.6 3.4 %all-to-all-done.3.in_ref = bf16[4,256,128]{2,1,0:T(8,128)(2,1)S(1)} async-done(((bf16[4,256,128]{2,1,0:T(8,128)(2,1)}), bf16[4,256,128]{2,1,0:T(8,128)(2,1)S(1)}, u32[]{:S(2)}, u32[]{:S(2)}) %all-to-all-start.3) | async-done | bytes 262176 | tf_op jit(solution)/shard_map/all_to_all | solution.py:357
  98.9 0.8 copy-done.7
  99.8 0.4 shard_map.179
  100.2 29.1 %all_to_all.31 = bf16[128,3,4,128]{3,2,1,0:T(4,128)(2,1)S(1)} all-to-all(bf16[128,3,4,128]{3,2,1,0:T(4,128)(2,1)S(1)} %bitcast.15), channel_id=1, replica_groups=mesh['z'=8,'x'=4,'yg'=4,'yn'=2,'c'=2] {'z','x','yg'}, dimensions={0} | all-to-all | bytes 786432 | tf_op jit(solution)/shard_map/all_to_all | solution.py:357
  129.3 2.5 %collective-permute-start.4 = (bf16[1536,128]{1,0:T(8,128)(2,1)S(1)}, bf16[1536,128]{1,0:T(8,128)(2,1)S(1)}, u32[]{:S(2)}, u32[]{:S(2)}) collective-permute-start(bf16[1536,128]{1,0:T(8,128)(2,1)S(1)} %bitcast.11), channel_id=1, source_target_pairs={{0,2},{2,0},{1,3},{3,1},{4,6},{6,4},{5,7},{7,5},{8,10},{10,8},{9,1... | collective-permute-start | bytes 1179656 | tf_op jit(solution)/shard_map/ppermute | solution.py:362
  131.8 4.5 %collective-permute-start.3 = (bf16[1536,128]{1,0:T(8,128)(2,1)S(1)}, bf16[1536,128]{1,0:T(8,128)(2,1)S(1)}, u32[]{:S(2)}, u32[]{:S(2)}) collective-permute-start(bf16[1536,128]{1,0:T(8,128)(2,1)S(1)} %bitcast.12), channel_id=1, source_target_pairs={{0,1},{1,0},{2,3},{3,2},{4,5},{5,4},{6,7},{7,6},{8,9},{9,8},{10,11... | collective-permute-start | bytes 1179656 | tf_op jit(solution)/shard_map/ppermute | solution.py:362
  136.3 2.5 %collective-permute-done.4.refs_3_ = bf16[1536,128]{1,0:T(8,128)(2,1)S(1)} collective-permute-done((bf16[1536,128]{1,0:T(8,128)(2,1)S(1)}, bf16[1536,128]{1,0:T(8,128)(2,1)S(1)}, u32[]{:S(2)}, u32[]{:S(2)}) %collective-permute-start.4) | collective-permute-done | bytes 393248 | tf_op jit(solution)/shard_map/ppermute | solution.py:362
  138.8 5.7 %collective-permute-start.5 = (bf16[1536,128]{1,0:T(8,128)(2,1)S(1)}, bf16[1536,128]{1,0:T(8,128)(2,1)S(1)}, u32[]{:S(2)}, u32[]{:S(2)}) collective-permute-start(bf16[1536,128]{1,0:T(8,128)(2,1)S(1)} %collective-permute-done.4.refs_3_), channel_id=1, source_target_pairs={{0,1},{1,0},{2,3},{3,2},{4,5},{5,4},{6,7},{7,6},{8,9},{9,8},{10,11... | collective-permute-start | bytes 1179656 | tf_op jit(solution)/shard_map/ppermute | solution.py:362
  144.6 1.3 collective-permute-done.5.refs_4_
  145.9 1.2 copy-done.3
  147.1 2.9 %shard_map.181.h0 = bf16[384,256]{1,0:T(8,128)(2,1)S(1)} custom-call(s32[2]{0:T(128)S(1)} %pad_add_fusion.ids_ref.refs_0_, bf16[1536,128]{1,0:T(8,128)(2,1)S(1)} %bitcast.13, bf16[1536,128]{1,0:T(8,128)(2,1)S(1)} %collective-permute-done.3.refs_2_, bf16[1536,128]{1,0:T(8,128)(2,1)S(1)} %collective-permute-done.4.refs_3_, ...), custom_call_target="tpu_custom_call" | custom-call | flops 1000000 | bytes 1000000 | tf_op jit(solution)/shard_map/pallas_call | solution.py:64
  150.1 2.5 %collective-permute-start.7 = (bf16[384,256]{1,0:T(8,128)(2,1)S(1)}, bf16[384,256]{1,0:T(8,128)(2,1)S(1)}, u32[]{:S(2)}, u32[]{:S(2)}) collective-permute-start(bf16[384,256]{1,0:T(8,128)(2,1)S(1)} %shard_map.181.h0), channel_id=1, source_target_pairs={{0,2},{2,0},{1,3},{3,1},{4,6},{6,4},{5,7},{7,5},{8,10},{10,8},{9,1... | collective-permute-start | bytes 589832 | tf_op jit(solution)/shard_map/ppermute | solution.py:362
  152.6 2.6 %collective-permute-start.6 = (bf16[384,256]{1,0:T(8,128)(2,1)S(1)}, bf16[384,256]{1,0:T(8,128)(2,1)S(1)}, u32[]{:S(2)}, u32[]{:S(2)}) collective-permute-start(bf16[384,256]{1,0:T(8,128)(2,1)S(1)} %shard_map.181.h0), channel_id=1, source_target_pairs={{0,1},{1,0},{2,3},{3,2},{4,5},{5,4},{6,7},{7,6},{8,9},{9,8},{10,11... | collective-permute-start | bytes 589832 | tf_op jit(solution)/shard_map/ppermute | solution.py:362
  155.2 2.9 %collective-permute-done.7.h2 = bf16[384,256]{1,0:T(8,128)(2,1)S(1)} collective-permute-done((bf16[384,256]{1,0:T(8,128)(2,1)S(1)}, bf16[384,256]{1,0:T(8,128)(2,1)S(1)}, u32[]{:S(2)}, u32[]{:S(2)}) %collective-permute-start.7) | collective-permute-done | bytes 196640 | tf_op jit(solution)/shard_map/ppermute | solution.py:362
  158.0 3.1 %collective-permute-start.8 = (bf16[384,256]{1,0:T(8,128)(2,1)S(1)}, bf16[384,256]{1,0:T(8,128)(2,1)S(1)}, u32[]{:S(2)}, u32[]{:S(2)}) collective-permute-start(bf16[384,256]{1,0:T(8,128)(2,1)S(1)} %collective-permute-done.7.h2), channel_id=1, source_target_pairs={{0,1},{1,0},{2,3},{3,2},{4,5},{5,4},{6,7},{7,6},{8,9},{9,8},{10,11... | collective-permute-start | bytes 589832 | tf_op jit(solution)/shard_map/ppermute | solution.py:362
  161.2 1.0 collective-permute-done.8.h3
  162.2 1.4 shard_map.182
  163.6 7.7 %all-to-all-start.5 = ((bf16[128,3,4,128]{3,2,1,0:T(4,128)(2,1)}), bf16[128,3,4,128]{3,2,1,0:T(4,128)(2,1)S(1)}, u32[]{:S(2)}, u32[]{:S(2)}) async-start(bf16[128,3,4,128]{3,2,1,0:T(4,128)(2,1)} %bitcast.9), calls=%async_computation.5 | async-start | bytes 786432 | tf_op jit(solution)/shard_map/all_to_all | solution.py:357
  171.4 6.4 %collective-permute-start.10 = (bf16[256,128]{1,0:T(8,128)(2,1)S(1)}, bf16[256,128]{1,0:T(8,128)(2,1)S(1)}, u32[]{:S(2)}, u32[]{:S(2)}) collective-permute-start(bf16[256,128]{1,0:T(8,128)(2,1)S(1)} %copy-done.5), channel_id=1, source_target_pairs={{0,8},{4,12},{8,0},{12,4},{1,9},{5,13},{9,1},{13,5},{2,10},{6,14},... | collective-permute-start | bytes 196616 | tf_op jit(solution)/shard_map/ppermute | solution.py:362
  177.8 2.2 collective-permute-start.11
  180.0 4.0 %collective-permute-start.9 = (bf16[256,128]{1,0:T(8,128)(2,1)S(1)}, bf16[256,128]{1,0:T(8,128)(2,1)S(1)}, u32[]{:S(2)}, u32[]{:S(2)}) collective-permute-start(bf16[256,128]{1,0:T(8,128)(2,1)S(1)} %copy-done.5), channel_id=1, source_target_pairs={{0,4},{4,8},{8,12},{12,0},{1,5},{5,9},{9,13},{13,1},{2,6},{6,10},{... | collective-permute-start | bytes 196616 | tf_op jit(solution)/shard_map/ppermute | solution.py:362
  184.0 1.6 collective-permute-done.10.m2
  185.6 1.7 collective-permute-done.11.m3
  187.3 0.1 collective-permute-done.9.m1
  187.4 0.9 shard_map.184.r0
  188.3 5.5 %collective-permute-start.12 = (bf16[256,384]{1,0:T(8,128)(2,1)S(1)}, bf16[256,384]{1,0:T(8,128)(2,1)S(1)}, u32[]{:S(2)}, u32[]{:S(2)}) collective-permute-start(bf16[256,384]{1,0:T(8,128)(2,1)S(1)} %shard_map.184.r0), channel_id=1, source_target_pairs={{0,1},{1,0},{2,3},{3,2},{4,5},{5,4},{6,7},{7,6},{8,9},{9,8},{10,11... | collective-permute-start | bytes 589832 | tf_op jit(solution)/shard_map/ppermute | solution.py:362
  193.8 1.9 collective-permute-start.13
  195.7 3.5 %collective-permute-start.14 = (bf16[256,384]{1,0:T(8,128)(2,1)S(1)}, bf16[256,384]{1,0:T(8,128)(2,1)S(1)}, u32[]{:S(2)}, u32[]{:S(2)}) collective-permute-start(bf16[256,384]{1,0:T(8,128)(2,1)S(1)} %shard_map.184.r0), channel_id=1, source_target_pairs={{0,3},{1,2},{2,1},{3,0},{4,7},{5,6},{6,5},{7,4},{8,11},{9,10},{10,... | collective-permute-start | bytes 589832 | tf_op jit(solution)/shard_map/ppermute | solution.py:362
  199.3 2.9 %collective-permute-done.13.r2 = bf16[256,384]{1,0:T(8,128)(2,1)S(1)} collective-permute-done((bf16[256,384]{1,0:T(8,128)(2,1)S(1)}, bf16[256,384]{1,0:T(8,128)(2,1)S(1)}, u32[]{:S(2)}, u32[]{:S(2)}) %collective-permute-start.13) | collective-permute-done | bytes 196640 | tf_op jit(solution)/shard_map/ppermute | solution.py:362
  202.1 4.4 %collective-permute-done.14.r3 = bf16[256,384]{1,0:T(8,128)(2,1)S(1)} collective-permute-done((bf16[256,384]{1,0:T(8,128)(2,1)S(1)}, bf16[256,384]{1,0:T(8,128)(2,1)S(1)}, u32[]{:S(2)}, u32[]{:S(2)}) %collective-permute-start.14) | collective-permute-done | bytes 196640 | tf_op jit(solution)/shard_map/ppermute | solution.py:362
  206.5 0.1 shard_map.185.h0
  206.7 2.3 %collective-permute-start.15 = (bf16[256,128]{1,0:T(8,128)(2,1)S(1)}, bf16[256,128]{1,0:T(8,128)(2,1)S(1)}, u32[]{:S(2)}, u32[]{:S(2)}) collective-permute-start(bf16[256,128]{1,0:T(8,128)(2,1)S(1)} %shard_map.185.h0), channel_id=1, source_target_pairs={{0,4},{4,8},{8,12},{12,0},{1,5},{5,9},{9,13},{13,1},{2,6},{6,10},{... | collective-permute-start | bytes 196616 | tf_op jit(solution)/shard_map/ppermute | solution.py:362
  209.0 4.3 %collective-permute-start.16 = (bf16[256,128]{1,0:T(8,128)(2,1)S(1)}, bf16[256,128]{1,0:T(8,128)(2,1)S(1)}, u32[]{:S(2)}, u32[]{:S(2)}) collective-permute-start(bf16[256,128]{1,0:T(8,128)(2,1)S(1)} %shard_map.185.h0), channel_id=1, source_target_pairs={{0,8},{4,12},{8,0},{12,4},{1,9},{5,13},{9,1},{13,5},{2,10},{6,14},... | collective-permute-start | bytes 196616 | tf_op jit(solution)/shard_map/ppermute | solution.py:362
  213.3 5.5 %collective-permute-start.17 = (bf16[256,128]{1,0:T(8,128)(2,1)S(1)}, bf16[256,128]{1,0:T(8,128)(2,1)S(1)}, u32[]{:S(2)}, u32[]{:S(2)}) collective-permute-start(bf16[256,128]{1,0:T(8,128)(2,1)S(1)} %shard_map.185.h0), channel_id=1, source_target_pairs={{0,12},{4,0},{8,4},{12,8},{1,13},{5,1},{9,5},{13,9},{2,14},{6,2},{... | collective-permute-start | bytes 196616 | tf_op jit(solution)/shard_map/ppermute | solution.py:362
  218.7 0.1 copy.21.score_ref
  218.9 2.0 shard_map.183
  220.9 1.8 collective-permute-done.17.h3
  222.7 0.8 shard_map.186.ahead_ref
  223.5 1.2 shard_map.187
  (33 shorter events, 0.1 us)
Async XLA Ops:
  26.0 12.7 %all-to-all-start.1 = ((bf16[32,8,128]{2,1,0:T(8,128)(2,1)}), bf16[32,8,128]{2,1,0:T(8,128)(2,1)S(1)}, u32[]{:S(2)}, u32[]{:S(2)}) async-start(bf16[32,8,128]{2,1,0:T(8,128)(2,1)} %shard_map.174), calls=%async_computation.1 | async-start | bytes 131072 | tf_op jit(solution)/shard_map/all_to_all | solution.py:357
  29.9 0.7 copy-start.14
  38.8 0.6 copy-start.9
  39.4 10.0 %copy-start.10 = (bf16[2048,32]{0,1:T(8,128)(2,1)S(1)}, bf16[2048,32]{0,1:T(8,128)(2,1)}, u32[]{:S(2)}) copy-start(bf16[2048,32]{0,1:T(8,128)(2,1)} %param.34) | copy-start | bytes 393220
  39.4 10.0 %copy-start.11 = (bf16[2048,32]{0,1:T(8,128)(2,1)S(1)}, bf16[2048,32]{0,1:T(8,128)(2,1)}, u32[]{:S(2)}) copy-start(bf16[2048,32]{0,1:T(8,128)(2,1)} %param.33) | copy-start | bytes 393220
  42.4 7.0 %copy-start = (bf16[4096,128]{1,0:T(8,128)(2,1)S(1)}, bf16[4096,128]{1,0:T(8,128)(2,1)}, u32[]{:S(2)}) copy-start(bf16[4096,128]{1,0:T(8,128)(2,1)} %project_ref.1) | copy-start | bytes 3145732
  42.4 45.9 %all-to-all-start.2 = ((bf16[4,256,256]{2,1,0:T(8,128)(2,1)}), bf16[4,256,256]{2,1,0:T(8,128)(2,1)S(1)}, u32[]{:S(2)}, u32[]{:S(2)}) async-start(bf16[4,256,256]{2,1,0:T(8,128)(2,1)} %shard_map.176), calls=%async_computation.2 | async-start | bytes 1048576 | tf_op jit(solution)/shard_map/all_to_all | solution.py:357
  49.4 1.2 copy-start.1
  51.7 10.9 %collective-permute-start = (bf16[576,512]{1,0:T(8,128)(2,1)S(1)}, bf16[576,512]{1,0:T(8,128)(2,1)S(1)}, u32[]{:S(2)}, u32[]{:S(2)}) collective-permute-start(bf16[576,512]{1,0:T(8,128)(2,1)S(1)} %get-tuple-element.18), channel_id=1, source_target_pairs={{0,1},{1,0},{2,3},{3,2},{4,5},{5,4},{6,7},{7,6},{8,9},{9,8},{10,11... | collective-permute-start | bytes 1769480 | tf_op jit(solution)/shard_map/ppermute | solution.py:362
  57.1 18.6 %collective-permute-start.1 = (bf16[576,512]{1,0:T(8,128)(2,1)S(1)}, bf16[576,512]{1,0:T(8,128)(2,1)S(1)}, u32[]{:S(2)}, u32[]{:S(2)}) collective-permute-start(bf16[576,512]{1,0:T(8,128)(2,1)S(1)} %get-tuple-element.19), channel_id=1, source_target_pairs={{0,2},{1,3},{2,0},{3,1},{4,6},{5,7},{6,4},{7,5},{8,10},{9,11},{10,... | collective-permute-start | bytes 1769480 | tf_op jit(solution)/shard_map/ppermute | solution.py:362
  59.4 28.9 %collective-permute-start.2 = (bf16[576,512]{1,0:T(8,128)(2,1)S(1)}, bf16[576,512]{1,0:T(8,128)(2,1)S(1)}, u32[]{:S(2)}, u32[]{:S(2)}) collective-permute-start(bf16[576,512]{1,0:T(8,128)(2,1)S(1)} %get-tuple-element.20), channel_id=1, source_target_pairs={{0,3},{1,2},{2,1},{3,0},{4,7},{5,6},{6,5},{7,4},{8,11},{9,10},{10,... | collective-permute-start | bytes 1769480 | tf_op jit(solution)/shard_map/ppermute | solution.py:362
  90.1 3.8 %copy-start.12 = (s32[256,4]{0,1:T(4,128)S(1)}, s32[256,4]{0,1:T(4,128)}, u32[]{:S(2)}) copy-start(s32[256,4]{0,1:T(4,128)} %param.28) | copy-start | bytes 12292
  90.1 8.8 %all-to-all-start.3 = ((bf16[4,256,128]{2,1,0:T(8,128)(2,1)}), bf16[4,256,128]{2,1,0:T(8,128)(2,1)S(1)}, u32[]{:S(2)}, u32[]{:S(2)}) async-start(bf16[4,256,128]{2,1,0:T(8,128)(2,1)} %shard_map.178), calls=%async_computation.3 | async-start | bytes 524288 | tf_op jit(solution)/shard_map/all_to_all | solution.py:357
  98.9 0.8 copy-start.7
  99.8 46.1 %copy-start.2 = (bf16[2048,256]{1,0:T(8,128)(2,1)S(1)}, bf16[2048,256]{1,0:T(8,128)(2,1)}, u32[]{:S(2)}) copy-start(bf16[2048,256]{1,0:T(8,128)(2,1)} %refs_6_.1) | copy-start | bytes 3145732
  100.2 29.1 %copy-start.4 = (bf16[256,128]{1,0:T(8,128)(2,1)}, bf16[256,128]{1,0:T(8,128)(2,1)S(1)}, u32[]{:S(2)}) copy-start(bf16[256,128]{1,0:T(8,128)(2,1)S(1)} %get-tuple-element.24.m0.mid_ref) | copy-start | bytes 196612
  100.2 44.4 %copy-start.8 = (bf16[2048]{0:T(1024)(128)(2,1)S(1)}, bf16[2048]{0:T(1024)(128)(2,1)}, u32[]{:S(2)}) copy-start(bf16[2048]{0:T(1024)(128)(2,1)} %param.27) | copy-start | bytes 12292
  129.3 9.6 %collective-permute-start.4 = (bf16[1536,128]{1,0:T(8,128)(2,1)S(1)}, bf16[1536,128]{1,0:T(8,128)(2,1)S(1)}, u32[]{:S(2)}, u32[]{:S(2)}) collective-permute-start(bf16[1536,128]{1,0:T(8,128)(2,1)S(1)} %bitcast.11), channel_id=1, source_target_pairs={{0,2},{2,0},{1,3},{3,1},{4,6},{6,4},{5,7},{7,5},{8,10},{10,8},{9,1... | collective-permute-start | bytes 1179656 | tf_op jit(solution)/shard_map/ppermute | solution.py:362
  131.8 12.8 %collective-permute-start.3 = (bf16[1536,128]{1,0:T(8,128)(2,1)S(1)}, bf16[1536,128]{1,0:T(8,128)(2,1)S(1)}, u32[]{:S(2)}, u32[]{:S(2)}) collective-permute-start(bf16[1536,128]{1,0:T(8,128)(2,1)S(1)} %bitcast.12), channel_id=1, source_target_pairs={{0,1},{1,0},{2,3},{3,2},{4,5},{5,4},{6,7},{7,6},{8,9},{9,8},{10,11... | collective-permute-start | bytes 1179656 | tf_op jit(solution)/shard_map/ppermute | solution.py:362
  138.8 7.1 %collective-permute-start.5 = (bf16[1536,128]{1,0:T(8,128)(2,1)S(1)}, bf16[1536,128]{1,0:T(8,128)(2,1)S(1)}, u32[]{:S(2)}, u32[]{:S(2)}) collective-permute-start(bf16[1536,128]{1,0:T(8,128)(2,1)S(1)} %collective-permute-done.4.refs_3_), channel_id=1, source_target_pairs={{0,1},{1,0},{2,3},{3,2},{4,5},{5,4},{6,7},{7,6},{8,9},{9,8},{10,11... | collective-permute-start | bytes 1179656 | tf_op jit(solution)/shard_map/ppermute | solution.py:362
  145.9 1.2 copy-start.3
  150.1 8.0 %collective-permute-start.7 = (bf16[384,256]{1,0:T(8,128)(2,1)S(1)}, bf16[384,256]{1,0:T(8,128)(2,1)S(1)}, u32[]{:S(2)}, u32[]{:S(2)}) collective-permute-start(bf16[384,256]{1,0:T(8,128)(2,1)S(1)} %shard_map.181.h0), channel_id=1, source_target_pairs={{0,2},{2,0},{1,3},{3,1},{4,6},{6,4},{5,7},{7,5},{8,10},{10,8},{9,1... | collective-permute-start | bytes 589832 | tf_op jit(solution)/shard_map/ppermute | solution.py:362
  152.6 8.6 %collective-permute-start.6 = (bf16[384,256]{1,0:T(8,128)(2,1)S(1)}, bf16[384,256]{1,0:T(8,128)(2,1)S(1)}, u32[]{:S(2)}, u32[]{:S(2)}) collective-permute-start(bf16[384,256]{1,0:T(8,128)(2,1)S(1)} %shard_map.181.h0), channel_id=1, source_target_pairs={{0,1},{1,0},{2,3},{3,2},{4,5},{5,4},{6,7},{7,6},{8,9},{9,8},{10,11... | collective-permute-start | bytes 589832 | tf_op jit(solution)/shard_map/ppermute | solution.py:362
  158.0 4.2 %collective-permute-start.8 = (bf16[384,256]{1,0:T(8,128)(2,1)S(1)}, bf16[384,256]{1,0:T(8,128)(2,1)S(1)}, u32[]{:S(2)}, u32[]{:S(2)}) collective-permute-start(bf16[384,256]{1,0:T(8,128)(2,1)S(1)} %collective-permute-done.7.h2), channel_id=1, source_target_pairs={{0,1},{1,0},{2,3},{3,2},{4,5},{5,4},{6,7},{7,6},{8,9},{9,8},{10,11... | collective-permute-start | bytes 589832 | tf_op jit(solution)/shard_map/ppermute | solution.py:362
  163.6 7.7 %copy-start.5 = (bf16[256,128]{1,0:T(8,128)(2,1)S(1)}, bf16[256,128]{1,0:T(8,128)(2,1)}, u32[]{:S(2)}) copy-start(bf16[256,128]{1,0:T(8,128)(2,1)} %copy-done.4) | copy-start | bytes 196612
  163.6 59.9 %all-to-all-start.5 = ((bf16[128,3,4,128]{3,2,1,0:T(4,128)(2,1)}), bf16[128,3,4,128]{3,2,1,0:T(4,128)(2,1)S(1)}, u32[]{:S(2)}, u32[]{:S(2)}) async-start(bf16[128,3,4,128]{3,2,1,0:T(4,128)(2,1)} %bitcast.9), calls=%async_computation.5 | async-start | bytes 786432 | tf_op jit(solution)/shard_map/all_to_all | solution.py:357
  171.4 14.2 %collective-permute-start.10 = (bf16[256,128]{1,0:T(8,128)(2,1)S(1)}, bf16[256,128]{1,0:T(8,128)(2,1)S(1)}, u32[]{:S(2)}, u32[]{:S(2)}) collective-permute-start(bf16[256,128]{1,0:T(8,128)(2,1)S(1)} %copy-done.5), channel_id=1, source_target_pairs={{0,8},{4,12},{8,0},{12,4},{1,9},{5,13},{9,1},{13,5},{2,10},{6,14},... | collective-permute-start | bytes 196616 | tf_op jit(solution)/shard_map/ppermute | solution.py:362
  177.8 9.5 %collective-permute-start.11 = (bf16[256,128]{1,0:T(8,128)(2,1)S(1)}, bf16[256,128]{1,0:T(8,128)(2,1)S(1)}, u32[]{:S(2)}, u32[]{:S(2)}) collective-permute-start(bf16[256,128]{1,0:T(8,128)(2,1)S(1)} %copy-done.5), channel_id=1, source_target_pairs={{0,12},{4,0},{8,4},{12,8},{1,13},{5,1},{9,5},{13,9},{2,14},{6,2},{... | collective-permute-start | bytes 196616 | tf_op jit(solution)/shard_map/ppermute | solution.py:362
  180.0 7.4 %collective-permute-start.9 = (bf16[256,128]{1,0:T(8,128)(2,1)S(1)}, bf16[256,128]{1,0:T(8,128)(2,1)S(1)}, u32[]{:S(2)}, u32[]{:S(2)}) collective-permute-start(bf16[256,128]{1,0:T(8,128)(2,1)S(1)} %copy-done.5), channel_id=1, source_target_pairs={{0,4},{4,8},{8,12},{12,0},{1,5},{5,9},{9,13},{13,1},{2,6},{6,10},{... | collective-permute-start | bytes 196616 | tf_op jit(solution)/shard_map/ppermute | solution.py:362
  188.3 30.5 %copy-start.13 = (f32[256,4]{0,1:T(4,128)S(1)}, f32[256,4]{0,1:T(4,128)}, u32[]{:S(2)}) copy-start(f32[256,4]{0,1:T(4,128)} %param.29) | copy-start | bytes 12292
  188.3 11.0 %collective-permute-start.12 = (bf16[256,384]{1,0:T(8,128)(2,1)S(1)}, bf16[256,384]{1,0:T(8,128)(2,1)S(1)}, u32[]{:S(2)}, u32[]{:S(2)}) collective-permute-start(bf16[256,384]{1,0:T(8,128)(2,1)S(1)} %shard_map.184.r0), channel_id=1, source_target_pairs={{0,1},{1,0},{2,3},{3,2},{4,5},{5,4},{6,7},{7,6},{8,9},{9,8},{10,11... | collective-permute-start | bytes 589832 | tf_op jit(solution)/shard_map/ppermute | solution.py:362
  193.8 8.3 %collective-permute-start.13 = (bf16[256,384]{1,0:T(8,128)(2,1)S(1)}, bf16[256,384]{1,0:T(8,128)(2,1)S(1)}, u32[]{:S(2)}, u32[]{:S(2)}) collective-permute-start(bf16[256,384]{1,0:T(8,128)(2,1)S(1)} %shard_map.184.r0), channel_id=1, source_target_pairs={{0,2},{1,3},{2,0},{3,1},{4,6},{5,7},{6,4},{7,5},{8,10},{9,11},{10,... | collective-permute-start | bytes 589832 | tf_op jit(solution)/shard_map/ppermute | solution.py:362
  195.7 10.8 %collective-permute-start.14 = (bf16[256,384]{1,0:T(8,128)(2,1)S(1)}, bf16[256,384]{1,0:T(8,128)(2,1)S(1)}, u32[]{:S(2)}, u32[]{:S(2)}) collective-permute-start(bf16[256,384]{1,0:T(8,128)(2,1)S(1)} %shard_map.184.r0), channel_id=1, source_target_pairs={{0,3},{1,2},{2,1},{3,0},{4,7},{5,6},{6,5},{7,4},{8,11},{9,10},{10,... | collective-permute-start | bytes 589832 | tf_op jit(solution)/shard_map/ppermute | solution.py:362
  206.7 14.2 %collective-permute-start.15 = (bf16[256,128]{1,0:T(8,128)(2,1)S(1)}, bf16[256,128]{1,0:T(8,128)(2,1)S(1)}, u32[]{:S(2)}, u32[]{:S(2)}) collective-permute-start(bf16[256,128]{1,0:T(8,128)(2,1)S(1)} %shard_map.185.h0), channel_id=1, source_target_pairs={{0,4},{4,8},{8,12},{12,0},{1,5},{5,9},{9,13},{13,1},{2,6},{6,10},{... | collective-permute-start | bytes 196616 | tf_op jit(solution)/shard_map/ppermute | solution.py:362
  209.0 11.9 %collective-permute-start.16 = (bf16[256,128]{1,0:T(8,128)(2,1)S(1)}, bf16[256,128]{1,0:T(8,128)(2,1)S(1)}, u32[]{:S(2)}, u32[]{:S(2)}) collective-permute-start(bf16[256,128]{1,0:T(8,128)(2,1)S(1)} %shard_map.185.h0), channel_id=1, source_target_pairs={{0,8},{4,12},{8,0},{12,4},{1,9},{5,13},{9,1},{13,5},{2,10},{6,14},... | collective-permute-start | bytes 196616 | tf_op jit(solution)/shard_map/ppermute | solution.py:362
  213.3 9.5 %collective-permute-start.17 = (bf16[256,128]{1,0:T(8,128)(2,1)S(1)}, bf16[256,128]{1,0:T(8,128)(2,1)S(1)}, u32[]{:S(2)}, u32[]{:S(2)}) collective-permute-start(bf16[256,128]{1,0:T(8,128)(2,1)S(1)} %shard_map.185.h0), channel_id=1, source_target_pairs={{0,12},{4,0},{8,4},{12,8},{1,13},{5,1},{9,5},{13,9},{2,14},{6,2},{... | collective-permute-start | bytes 196616 | tf_op jit(solution)/shard_map/ppermute | solution.py:362
  218.9 3.8 %copy-start.6 = (bf16[512,128]{1,0:T(8,128)(2,1)S(1)}, bf16[512,128]{1,0:T(8,128)(2,1)}, u32[]{:S(2)}) copy-start(bf16[512,128]{1,0:T(8,128)(2,1)} %down_ref.3) | copy-start | bytes 393220

commit v7 on v6

--- a/solution.py
+++ b/solution.py
@@ -178,7 +178,7 @@
         before = before + cum[BLOCK - 1 : BLOCK]
 
 
-def head_kernel(gain_ref, enter_ref, local_ref, start_ref, gate_ref, out_ref):
+def head_kernel(enter_ref, gain_ref, local_ref, start_ref, gate_ref, out_ref):
     enter = enter_ref[...]
     mixed = local_ref[...] + sum(nt(piece, enter) for piece in split(start_ref[...], 3))
     scale = lax.rsqrt(jnp.mean(mixed * mixed, axis=-1, keepdims=True) + EPSILON)
@@ -201,33 +201,33 @@
         out_ref[part ^ (m + 1)] = total[:, 128:].astype(BF16)
 
 
-def places(routing_ref):
+def ranks_of(routing_ref):
     experts = lax.broadcasted_iota(jnp.int32, (TOK, 128), 1)
     hot = [(routing_ref[:, k : k + 1] == experts).astype(F32) for k in range(4)]
     named = hot[0] + hot[1] + hot[2] + hot[3]
     rows = lax.broadcasted_iota(jnp.int32, (TOK, TOK), 0)
     cols = lax.broadcasted_iota(jnp.int32, (TOK, TOK), 1)
-    earlier = (rows > cols).astype(BF16)
+    earlier = (rows > cols).astype(F32).astype(BF16)
     ranks = jnp.dot(earlier, named.astype(BF16), preferred_element_type=F32)
-    return [
-        routing_ref[:, k : k + 1] * MOST
-        + jnp.sum(hot[k] * ranks, axis=1, keepdims=True).astype(jnp.int32)
-        for k in range(4)
-    ]
-
-
-def pick_kernel(routing_ref, pick_ref):
-    place = places(routing_ref)
-    slots = lax.broadcasted_iota(jnp.int32, (TOK, 512), 1)
-    for j in range(ALL_SLOTS // 512):
-        picked = jnp.zeros((TOK, 512), F32)
-        for k in range(4):
-            picked = picked + (place[k] - j * 512 == slots).astype(F32)
-        pick_ref[j * 512 : (j + 1) * 512, :] = picked.T.astype(BF16)
+    return [jnp.sum(h * ranks, axis=1, keepdims=True).astype(jnp.int32) for h in hot]
+
+
+def pick_kernel(ids_ref, routing_ref, pick_ref):
+    group = ids_ref[1]
+    ranks = ranks_of(routing_ref)
+    slots = lax.broadcasted_iota(jnp.int32, (TOK, SLOTS), 1)
+    picked = jnp.zeros((TOK, SLOTS), F32)
+    for k in range(4):
+        expert = routing_ref[:, k : k + 1]
+        place = ranks[k] * 32 + lax.shift_right_logical(expert, 2)
+        place = jnp.where((expert & 3) == group, place, -1)
+        picked = picked + (place == slots).astype(F32)
+    pick_ref[...] = picked.T.astype(BF16)
 
 
 def weigh_kernel(routing_ref, score_ref, high_ref, low_ref):
-    place = places(routing_ref)
+    ranks = ranks_of(routing_ref)
+    place = [routing_ref[:, k : k + 1] * MOST + ranks[k] for k in range(4)]
     scores = [score_ref[:, k : k + 1] for k in range(4)]
     total = scores[0] + scores[1] + scores[2] + scores[3]
     slots = lax.broadcasted_iota(jnp.int32, (TOK, 512), 1)
@@ -241,16 +241,23 @@
         low_ref[:, j * 512 : (j + 1) * 512] = (weighted - high.astype(F32)).astype(BF16)
 
 
-def dispatch_kernel(pick_ref, in_ref, residual_ref, out_ref, mid_ref):
+def mid_kernel(in_ref, residual_ref, out_ref):
     total = residual_ref[...].astype(F32)
     for s in range(4):
         total = total + in_ref[s].astype(F32)
     mid = total.astype(BF16)
-    mid_ref[...] = mid
-    for j in range(4):
-        rows = pl.ds(j * SLOTS, SLOTS)
-        picked = jnp.dot(pick_ref[rows, :], mid, preferred_element_type=F32)
-        out_ref[rows, :] = picked.astype(BF16)
+    for dest in range(4):
+        out_ref[dest] = mid
+
+
+def dispatch_kernel(pick_ref, mid_ref, out_ref, wide_ref):
+    pick = pick_ref[...]
+    for q in range(4):
+        picked = jnp.dot(pick, mid_ref[q], preferred_element_type=F32)
+        for r in range(MOST):
+            wide_ref[pl.ds(q * MOST + r, 32, stride=PITCH), :] = picked[r * 32 : (r + 1) * 32]
+    for s in range(32):
+        out_ref[s * 48 : (s + 1) * 48, :] = wide_ref[s * PITCH : s * PITCH + 48, :].astype(BF16)
 
 
 def expert_kernel(ready, ids_ref, x0, x1, x2, x3, gain_ref, gate_ref, up_ref, out_ref, wide_ref, rows_ref):
@@ -282,7 +289,7 @@
 def down_kernel(h0, h1, h2, h3, d0, d1, d2, d3, out_ref, wide_ref):
     total = jnp.zeros((SLOTS, 512), F32)
     for h_ref, d_ref in ((h0, d0), (h1, d1), (h2, d2), (h3, d3)):
-        total = total + jnp.dot(h_ref[...], d_ref[256:512, :], preferred_element_type=F32)
+        total = total + jnp.dot(h_ref[...], d_ref[...], preferred_element_type=F32)
     for q in range(4):
         for r in range(MOST):
             wide_ref[pl.ds(q * MOST + r, 32, stride=PITCH), :] = total[
@@ -292,7 +299,7 @@
         out_ref[s * 48 : (s + 1) * 48, :] = wide_ref[s * PITCH : s * PITCH + 48, :].astype(BF16)
 
 
-def parts_kernel(ids_ref, project_ref, down_ref, shared_ref, *out_refs):
+def blocks_kernel(ids_ref, project_ref, shared_ref, *out_refs):
     part = ids_ref[0]
     for m, out_ref in enumerate(out_refs):
         for q in range(4):
@@ -300,18 +307,23 @@
             lanes = slice(q * 128, (q + 1) * 128)
             out_ref[0:256, lanes] = project_ref[pl.ds(pl.multiple_of(slab * 256, 256), 256), :]
             columns = pl.ds(pl.multiple_of(slab * 128, 128), 128)
-            out_ref[256:512, lanes] = down_ref[:, columns]
-            out_ref[512:576, lanes] = shared_ref[:, columns]
-
-
-def shared_in_kernel(ids_ref, m0, m1, m2, m3, w0, w1, w2, w3, gain_ref, out_ref, weight_ref, mid_ref):
-    part, group = ids_ref[0], ids_ref[1]
+            out_ref[256:320, lanes] = shared_ref[:, columns]
+
+
+def parts_kernel(ids_ref, down_ref, *out_refs):
+    part = ids_ref[0]
+    for m, out_ref in enumerate(out_refs):
+        for q in range(4):
+            columns = pl.ds(pl.multiple_of((q * 4 + (part ^ m)) * 128, 128), 128)
+            out_ref[:, q * 128 : (q + 1) * 128] = down_ref[:, columns]
+
+
+def shared_in_kernel(ids_ref, mid_ref, w0, w1, w2, w3, gain_ref, out_ref, weight_ref):
+    part = ids_ref[0]
     for m, w_ref in enumerate((w0, w1, w2, w3)):
         at = (part ^ m) * 32
-        weight_ref[pl.ds(pl.multiple_of(at, 32), 32), :] = w_ref[512:544, :]
-        weight_ref[pl.ds(pl.multiple_of(at + 128, 32), 32), :] = w_ref[544:576, :]
-    for d, m_ref in enumerate((m0, m1, m2, m3)):
-        mid_ref[(group - d) & 3] = m_ref[...]
+        weight_ref[pl.ds(pl.multiple_of(at, 32), 32), :] = w_ref[256:288, :]
+        weight_ref[pl.ds(pl.multiple_of(at + 128, 32), 32), :] = w_ref[288:320, :]
     squares = jnp.zeros((TOK, 128), F32)
     pre = jnp.zeros((TOK, 256), F32)
     for q in range(4):
@@ -337,7 +349,7 @@
 
 def ahead_kernel(ids_ref, h0, h1, h2, h3, down_ref, mid_ref, out_ref):
     group = ids_ref[1]
-    total = mid_ref[...].astype(F32)
+    total = mid_ref[0].astype(F32)
     for d, h in enumerate((h0, h1, h2, h3)):
         at = pl.multiple_of(((group - d) & 3) * 128, 128)
         total = total + jnp.dot(
@@ -410,40 +422,44 @@
         queries, key_matrix, value_matrix, decay_preactivation, extra,
         fetch=(whole, whole, whole, whole, (0, 2)), limit=60,
     )
-    pick = call(pick_kernel, ((ALL_SLOTS, TOK), BF16), routing)
+    pick = call(pick_kernel, ((SLOTS, TOK), BF16), ids, routing, smem=1)
     high, low = call(
         weigh_kernel, [((TOK, ALL_SLOTS), BF16), ((TOK, ALL_SLOTS), BF16)], routing, router_score
     )
     shared_in = jnp.concatenate([shared_expert_gate.T, shared_expert_up.T], axis=0)
+    own_block, *far_blocks = call(
+        blocks_kernel, [((320, 512), BF16)] * 4, ids, output_projection, shared_in, smem=1,
+    )
+    blocks = [own_block] + grouped(far_blocks)
     own_part, *far_parts = call(
-        parts_kernel, [((576, 512), BF16)] * 4,
-        ids, output_projection, expert_down_weight, shared_in, smem=1,
+        parts_kernel, [((256, 512), BF16)] * 4, ids, expert_down_weight, smem=1,
     )
     parts = [own_part] + grouped(far_parts)
 
     entering = exchange(call(scan_kernel, ((32, 8, DK), BF16), states), SP)
     head_rows = call(
         head_kernel, ((4, TOK, DV), BF16),
-        head_gain, entering.reshape(DV, DK), local, start, output_gate_preactivation,
-        fetch=(whole,) * 4, limit=60,
+        entering.reshape(DV, DK), head_gain, local, start, output_gate_preactivation,
+        fetch=(whole,) * 3,
     )
     partial = call(
         project_kernel, ((4, TOK, 128), BF16),
-        ids, exchange(head_rows, "yg"), *parts, smem=1, fetch=(whole,) * 4,
-    )
-    outgoing, mid = call(
-        dispatch_kernel, [((ALL_SLOTS, 128), BF16), ((TOK, 128), BF16)],
-        pick, exchange(partial, GROUP), residual,
-    )
-    own = exchange(outgoing.reshape(128, 3, 4, 128), SPG).reshape(ALL_SLOTS, 128)
-    mids = [mid] + shifted([mid] * 3, "yg")
+        ids, exchange(head_rows, "yg"), *blocks, smem=1, fetch=(whole,) * 4,
+    )
+    mid = call(mid_kernel, ((4, TOK, 128), BF16), exchange(partial, GROUP), residual)
+    mid_part = exchange(mid, "yg")
+    outgoing = call(
+        dispatch_kernel, ((ALL_SLOTS, 128), BF16), pick, mid_part,
+        scratch=[pltpu.VMEM((32 * PITCH, 128), F32)],
+    )
+    own = exchange(outgoing.reshape(32, 48, 128), SP).reshape(ALL_SLOTS, 128)
 
     across = swapped(own, "yn")
     beside = swapped(own, "c")
     far = swapped(across, "c")
     pre = call(
-        shared_in_kernel, ((TOK, 384), BF16), ids, *mids, *parts, gain, smem=1,
-        scratch=[pltpu.VMEM((256, 512), BF16), pltpu.VMEM((4, TOK, 128), BF16)],
+        shared_in_kernel, ((TOK, 384), BF16), ids, mid_part, *blocks, gain, smem=1,
+        scratch=[pltpu.VMEM((256, 512), BF16)],
     )
     pre = [pre] + grouped([pre] * 3)
     routed = call(

time: 226 us -> 208 us (0.920)
  waiting for transfers between devices: 53.4 us -> 41.3 us
  blocking collectives: 52.1 us -> 46.2 us
  starting transfers between devices: 89.7 us -> 93.1 us
  local copies, waits for them, and re-layouts: 5.48 us -> 2.19 us
    ppermute x18, waiting for transfers between devices: 46 us -> 29.5 us  [moved(): lax.ppermute(value, axes, [(i, target(i) % count) for i in range(count)])]
    all_to_all x4, starting transfers between devices: 22.3 us -> 28.9 us  [exchange(): return lax.all_to_all(value, axes, split_axis=0, concat_axis=0, tiled=True)]
    all_to_all x2 -> x3, blocking collectives: 52.1 us -> 46.2 us  [exchange(): return lax.all_to_all(value, axes, split_axis=0, concat_axis=0, tiled=True)]
    all_to_all x4, waiting for transfers between devices: 7.35 us -> 11.8 us  [exchange(): return lax.all_to_all(value, axes, split_axis=0, concat_axis=0, tiled=True)]
    ppermute x18, starting transfers between devices: 67.4 us -> 64.2 us  [moved(): lax.ppermute(value, axes, [(i, target(i) % count) for i in range(count)])]
    unnamed x32, local copies, waits for them, and re-layouts: 4.88 us -> 2.19 us
    pallas_call x16 -> x18, Pallas kernels: 23.5 us -> 23 us  [call(): pl.pallas_call(fetching if fetch else kernel, out_shape=shapes, in_specs=...]
  transfers between devices with their start and end apart: 22 -> 22, of which waited for: 14 -> 9; matrix products, arithmetic and copies ran while one was open for 0% -> 0% of each run, Pallas kernels for 4% -> 5%
where the time goes in v7:
time: 208 us; the launch traced here: 206 us
  starting transfers between devices  93.1 us (45%)
  blocking collectives  46.2 us (22%)
  waiting for transfers between devices  41.3 us (20%)
  Pallas kernels  23 us (11%)
  local copies, waits for them, and re-layouts  2.19 us (1%)
    ppermute x18, starting transfers between devices, moved(): lax.ppermute(value, axes, [(i, target(i) % count) for i in range(count)])  64.2 us
    all_to_all x3, blocking collectives, exchange(): return lax.all_to_all(value, axes, split_axis=0, concat_axis=0, tiled=True)  46.2 us
    ppermute x18, waiting for transfers between devices, moved(): lax.ppermute(value, axes, [(i, target(i) % count) for i in range(count)])  29.5 us
    all_to_all x4, starting transfers between devices, exchange(): return lax.all_to_all(value, axes, split_axis=0, concat_axis=0, tiled=True)  28.9 us
    pallas_call x18, Pallas kernels, call(): pl.pallas_call(fetching if fetch else kernel, out_shape=shapes, in_specs=...  23 us
    all_to_all x4, waiting for transfers between devices, exchange(): return lax.all_to_all(value, axes, split_axis=0, concat_axis=0, tiled=True)  11.8 us
  transfers between devices with their start and end apart: 22, of which 9 were waited for; matrix products, arithmetic and copies ran while one was open for 0% of the time, Pallas kernels for 5%

profile of v7, /device:TPU:1, one launch (start us, length us, event | category | flops | bytes accessed | tf_op | source)
XLA Modules:
  0.0 206.4 jit_solution(4151799418392832760)
XLA Ops:
  0.0 2.3 %shard_map.173 = bf16[32,16,128]{2,1,0:T(8,128)(2,1)} custom-call(bf16[256,128]{1,0:T(8,128)(2,1)} %refs_1_.3, bf16[256,256]{1,0:T(8,128)(2,1)} %refs_2_.3, bf16[256,128]{1,0:T(8,128)(2,1)} %refs_3_.1, f32[2,128]{1,0:T(2,128)} %bitcast.20), custom_call_target="tpu_custom_call" | custom-call | flops 1000000 | bytes 1000000 | tf_op jit(solution)/shard_map/pallas_call | solution.py:64
  2.3 23.1 %all_to_all.35.in_ref = bf16[32,16,128]{2,1,0:T(8,128)(2,1)S(1)} all-to-all(bf16[32,16,128]{2,1,0:T(8,128)(2,1)} %shard_map.173), channel_id=1, replica_groups=mesh['z'=8,'x'=4,'yg'=4,'yn'=2,'c'=2] {'z','x'}, dimensions={0} | all-to-all | bytes 262144 | tf_op jit(solution)/shard_map/all_to_all | solution.py:369
  25.3 0.7 shard_map.174
  26.0 4.0 %all-to-all-start.1 = ((bf16[32,8,128]{2,1,0:T(8,128)(2,1)}), bf16[32,8,128]{2,1,0:T(8,128)(2,1)S(1)}, u32[]{:S(2)}, u32[]{:S(2)}) async-start(bf16[32,8,128]{2,1,0:T(8,128)(2,1)} %shard_map.174), calls=%async_computation.1 | async-start | bytes 131072 | tf_op jit(solution)/shard_map/all_to_all | solution.py:369
  30.1 0.0 copy-start.5
  30.1 3.6 %shard_map.175 = (f32[256,256]{1,0:T(8,128)}, f32[256,128]{1,0:T(8,128)}) custom-call(bf16[256,128]{1,0:T(8,128)(2,1)} %refs_0_.3, bf16[256,128]{1,0:T(8,128)(2,1)} %refs_1_.3, bf16[256,256]{1,0:T(8,128)(2,1)} %refs_2_.3, bf16[256,128]{1,0:T(8,128)(2,1)} %refs_3_.1, f32[2,128]{1,0:T(2,128)} %bitcast.21), custom_call_target="tpu_custom_call" | custom-call | flops 1000000 | bytes 1000000 | tf_op jit(solution)/shard_map/pallas_call | solution.py:64
  33.6 5.3 %all-to-all-done.1 = bf16[32,8,128]{2,1,0:T(8,128)(2,1)S(1)} async-done(((bf16[32,8,128]{2,1,0:T(8,128)(2,1)}), bf16[32,8,128]{2,1,0:T(8,128)(2,1)S(1)}, u32[]{:S(2)}, u32[]{:S(2)}) %all-to-all-start.1) | async-done | bytes 65568 | tf_op jit(solution)/shard_map/all_to_all | solution.py:369
  38.9 0.9 copy-done.4
  39.9 0.9 copy-done.6
  40.8 1.5 shard_map.176
  42.3 0.0 copy-start
  42.3 7.0 %all-to-all-start.2 = ((bf16[4,256,256]{2,1,0:T(8,128)(2,1)}), bf16[4,256,256]{2,1,0:T(8,128)(2,1)S(1)}, u32[]{:S(2)}, u32[]{:S(2)}) async-start(bf16[4,256,256]{2,1,0:T(8,128)(2,1)} %shard_map.176), calls=%async_computation.2 | async-start | bytes 1048576 | tf_op jit(solution)/shard_map/all_to_all | solution.py:369
  49.3 0.1 pad_add_fusion.ids_ref.refs_0_
  49.4 0.8 shard_map.177
  50.2 5.4 %collective-permute-start = (bf16[320,512]{1,0:T(8,128)(2,1)S(1)}, bf16[320,512]{1,0:T(8,128)(2,1)S(1)}, u32[]{:S(2)}, u32[]{:S(2)}) collective-permute-start(bf16[320,512]{1,0:T(8,128)(2,1)S(1)} %get-tuple-element.20), channel_id=1, source_target_pairs={{0,1},{1,0},{2,3},{3,2},{4,5},{5,4},{6,7},{7,6},{8,9},{9,8},{10,11... | collective-permute-start | bytes 983048 | tf_op jit(solution)/shard_map/ppermute | solution.py:374
  55.6 2.3 %collective-permute-start.1 = (bf16[320,512]{1,0:T(8,128)(2,1)S(1)}, bf16[320,512]{1,0:T(8,128)(2,1)S(1)}, u32[]{:S(2)}, u32[]{:S(2)}) collective-permute-start(bf16[320,512]{1,0:T(8,128)(2,1)S(1)} %get-tuple-element.21), channel_id=1, source_target_pairs={{0,2},{1,3},{2,0},{3,1},{4,6},{5,7},{6,4},{7,5},{8,10},{9,11},{10,... | collective-permute-start | bytes 983048 | tf_op jit(solution)/shard_map/ppermute | solution.py:374
  57.9 3.2 %collective-permute-start.2 = (bf16[320,512]{1,0:T(8,128)(2,1)S(1)}, bf16[320,512]{1,0:T(8,128)(2,1)S(1)}, u32[]{:S(2)}, u32[]{:S(2)}) collective-permute-start(bf16[320,512]{1,0:T(8,128)(2,1)S(1)} %get-tuple-element.22), channel_id=1, source_target_pairs={{0,3},{1,2},{2,1},{3,0},{4,7},{5,6},{6,5},{7,4},{8,11},{9,10},{10,... | collective-permute-start | bytes 983048 | tf_op jit(solution)/shard_map/ppermute | solution.py:374
  61.1 8.3 %collective-permute-done.1.refs_4_.w2 = bf16[320,512]{1,0:T(8,128)(2,1)S(1)} collective-permute-done((bf16[320,512]{1,0:T(8,128)(2,1)S(1)}, bf16[320,512]{1,0:T(8,128)(2,1)S(1)}, u32[]{:S(2)}, u32[]{:S(2)}) %collective-permute-start.1) | collective-permute-done | bytes 327712 | tf_op jit(solution)/shard_map/ppermute | solution.py:374
  69.4 7.3 %collective-permute-done.2.refs_5_.w3 = bf16[320,512]{1,0:T(8,128)(2,1)S(1)} collective-permute-done((bf16[320,512]{1,0:T(8,128)(2,1)S(1)}, bf16[320,512]{1,0:T(8,128)(2,1)S(1)}, u32[]{:S(2)}, u32[]{:S(2)}) %collective-permute-start.2) | collective-permute-done | bytes 327712 | tf_op jit(solution)/shard_map/ppermute | solution.py:374
  76.7 1.1 shard_map.178
  77.8 0.0 copy-start.8
  77.9 7.6 %all_to_all.36.in_ref = bf16[4,256,128]{2,1,0:T(8,128)(2,1)S(1)} all-to-all(bf16[4,256,128]{2,1,0:T(8,128)(2,1)S(1)} %shard_map.178), channel_id=1, replica_groups=mesh['z'=8,'x'=4,'yg'=4,'yn'=2,'c'=2] {'yn','c'}, dimensions={0} | all-to-all | bytes 524288 | tf_op jit(solution)/shard_map/all_to_all | solution.py:369
  85.4 0.7 shard_map.179.mid_ref
  86.2 6.3 %all-to-all-start.4 = ((bf16[4,256,128]{2,1,0:T(8,128)(2,1)}), bf16[4,256,128]{2,1,0:T(8,128)(2,1)S(1)}, u32[]{:S(2)}, u32[]{:S(2)}) async-start(bf16[4,256,128]{2,1,0:T(8,128)(2,1)} %shard_map.179.mid_ref), calls=%async_computation.4 | async-start | bytes 524288 | tf_op jit(solution)/shard_map/all_to_all | solution.py:369
  92.5 0.1 copy.19.routing_ref
  92.6 1.4 shard_map.172.pick_ref
  94.0 6.6 %all-to-all-done.4.mid_ref = bf16[4,256,128]{2,1,0:T(8,128)(2,1)S(1)} async-done(((bf16[4,256,128]{2,1,0:T(8,128)(2,1)}), bf16[4,256,128]{2,1,0:T(8,128)(2,1)S(1)}, u32[]{:S(2)}, u32[]{:S(2)}) %all-to-all-start.4) | async-done | bytes 262176 | tf_op jit(solution)/shard_map/all_to_all | solution.py:369
  100.6 0.4 shard_map.180
  101.0 0.0 copy-start.9
  101.0 15.6 %all_to_all.37 = bf16[32,48,128]{2,1,0:T(8,128)(2,1)S(1)} all-to-all(bf16[32,48,128]{2,1,0:T(8,128)(2,1)S(1)} %bitcast.14), channel_id=1, replica_groups=mesh['z'=8,'x'=4,'yg'=4,'yn'=2,'c'=2] {'z','x'}, dimensions={0} | all-to-all | bytes 786432 | tf_op jit(solution)/shard_map/all_to_all | solution.py:369
  116.6 2.6 %collective-permute-start.4 = (bf16[1536,128]{1,0:T(8,128)(2,1)S(1)}, bf16[1536,128]{1,0:T(8,128)(2,1)S(1)}, u32[]{:S(2)}, u32[]{:S(2)}) collective-permute-start(bf16[1536,128]{1,0:T(8,128)(2,1)S(1)} %bitcast.11), channel_id=1, source_target_pairs={{0,2},{2,0},{1,3},{3,1},{4,6},{6,4},{5,7},{7,5},{8,10},{10,8},{9,1... | collective-permute-start | bytes 1179656 | tf_op jit(solution)/shard_map/ppermute | solution.py:374
  119.2 7.4 %collective-permute-start.3 = (bf16[1536,128]{1,0:T(8,128)(2,1)S(1)}, bf16[1536,128]{1,0:T(8,128)(2,1)S(1)}, u32[]{:S(2)}, u32[]{:S(2)}) collective-permute-start(bf16[1536,128]{1,0:T(8,128)(2,1)S(1)} %bitcast.12), channel_id=1, source_target_pairs={{0,1},{1,0},{2,3},{3,2},{4,5},{5,4},{6,7},{7,6},{8,9},{9,8},{10,11... | collective-permute-start | bytes 1179656 | tf_op jit(solution)/shard_map/ppermute | solution.py:374
  126.6 6.6 %collective-permute-start.5 = (bf16[1536,128]{1,0:T(8,128)(2,1)S(1)}, bf16[1536,128]{1,0:T(8,128)(2,1)S(1)}, u32[]{:S(2)}, u32[]{:S(2)}) collective-permute-start(bf16[1536,128]{1,0:T(8,128)(2,1)S(1)} %collective-permute-done.4.refs_3_), channel_id=1, source_target_pairs={{0,1},{1,0},{2,3},{3,2},{4,5},{5,4},{6,7},{7,6},{8,9},{9,8},{10,11... | collective-permute-start | bytes 1179656 | tf_op jit(solution)/shard_map/ppermute | solution.py:374
  133.3 0.0 copy-start.1
  133.3 1.3 collective-permute-done.5.refs_4_
  134.6 2.9 %shard_map.182.h0 = bf16[384,256]{1,0:T(8,128)(2,1)S(1)} custom-call(s32[2]{0:T(128)S(1)} %pad_add_fusion.ids_ref.refs_0_, bf16[1536,128]{1,0:T(8,128)(2,1)S(1)} %bitcast.13, bf16[1536,128]{1,0:T(8,128)(2,1)S(1)} %collective-permute-done.3.refs_2_, bf16[1536,128]{1,0:T(8,128)(2,1)S(1)} %collective-permute-done.4.refs_3_, ...), custom_call_target="tpu_custom_call" | custom-call | flops 1000000 | bytes 1000000 | tf_op jit(solution)/shard_map/pallas_call | solution.py:64
  137.5 2.7 %collective-permute-start.7 = (bf16[384,256]{1,0:T(8,128)(2,1)S(1)}, bf16[384,256]{1,0:T(8,128)(2,1)S(1)}, u32[]{:S(2)}, u32[]{:S(2)}) collective-permute-start(bf16[384,256]{1,0:T(8,128)(2,1)S(1)} %shard_map.182.h0), channel_id=1, source_target_pairs={{0,2},{2,0},{1,3},{3,1},{4,6},{6,4},{5,7},{7,5},{8,10},{10,8},{9,1... | collective-permute-start | bytes 589832 | tf_op jit(solution)/shard_map/ppermute | solution.py:374
  140.3 0.8 shard_map.183
  141.1 2.5 %collective-permute-start.10 = (bf16[256,512]{1,0:T(8,128)(2,1)S(1)}, bf16[256,512]{1,0:T(8,128)(2,1)S(1)}, u32[]{:S(2)}, u32[]{:S(2)}) collective-permute-start(bf16[256,512]{1,0:T(8,128)(2,1)S(1)} %get-tuple-element.25), channel_id=1, source_target_pairs={{0,2},{1,3},{2,0},{3,1},{4,6},{5,7},{6,4},{7,5},{8,10},{9,11},{10,... | collective-permute-start | bytes 786440 | tf_op jit(solution)/shard_map/ppermute | solution.py:374
  143.6 3.6 %collective-permute-start.11 = (bf16[256,512]{1,0:T(8,128)(2,1)S(1)}, bf16[256,512]{1,0:T(8,128)(2,1)S(1)}, u32[]{:S(2)}, u32[]{:S(2)}) collective-permute-start(bf16[256,512]{1,0:T(8,128)(2,1)S(1)} %get-tuple-element.26), channel_id=1, source_target_pairs={{0,3},{1,2},{2,1},{3,0},{4,7},{5,6},{6,5},{7,4},{8,11},{9,10},{10,... | collective-permute-start | bytes 786440 | tf_op jit(solution)/shard_map/ppermute | solution.py:374
  147.2 1.9 collective-permute-start.9
  149.1 2.4 %collective-permute-start.6 = (bf16[384,256]{1,0:T(8,128)(2,1)S(1)}, bf16[384,256]{1,0:T(8,128)(2,1)S(1)}, u32[]{:S(2)}, u32[]{:S(2)}) collective-permute-start(bf16[384,256]{1,0:T(8,128)(2,1)S(1)} %shard_map.182.h0), channel_id=1, source_target_pairs={{0,1},{1,0},{2,3},{3,2},{4,5},{5,4},{6,7},{7,6},{8,9},{9,8},{10,11... | collective-permute-start | bytes 589832 | tf_op jit(solution)/shard_map/ppermute | solution.py:374
  151.6 1.9 collective-permute-start.8
  153.5 3.8 %collective-permute-done.11.d3 = bf16[256,512]{1,0:T(8,128)(2,1)S(1)} collective-permute-done((bf16[256,512]{1,0:T(8,128)(2,1)S(1)}, bf16[256,512]{1,0:T(8,128)(2,1)S(1)}, u32[]{:S(2)}, u32[]{:S(2)}) %collective-permute-start.11) | collective-permute-done | bytes 262176 | tf_op jit(solution)/shard_map/ppermute | solution.py:374
  157.3 1.4 shard_map.184
  158.7 11.7 %all-to-all-start.6 = ((bf16[128,3,4,128]{3,2,1,0:T(4,128)(2,1)}), bf16[128,3,4,128]{3,2,1,0:T(4,128)(2,1)S(1)}, u32[]{:S(2)}, u32[]{:S(2)}) async-start(bf16[128,3,4,128]{3,2,1,0:T(4,128)(2,1)} %bitcast.9), calls=%async_computation.6 | async-start | bytes 786432 | tf_op jit(solution)/shard_map/all_to_all | solution.py:369
  170.4 0.9 shard_map.186.r0
  171.3 0.0 copy-start.13
  171.3 2.0 collective-permute-start.12
  173.4 2.1 %collective-permute-start.13 = (bf16[256,384]{1,0:T(8,128)(2,1)S(1)}, bf16[256,384]{1,0:T(8,128)(2,1)S(1)}, u32[]{:S(2)}, u32[]{:S(2)}) collective-permute-start(bf16[256,384]{1,0:T(8,128)(2,1)S(1)} %shard_map.186.r0), channel_id=1, source_target_pairs={{0,2},{1,3},{2,0},{3,1},{4,6},{5,7},{6,4},{7,5},{8,10},{9,11},{10,... | collective-permute-start | bytes 589832 | tf_op jit(solution)/shard_map/ppermute | solution.py:374
  175.5 3.7 %collective-permute-start.14 = (bf16[256,384]{1,0:T(8,128)(2,1)S(1)}, bf16[256,384]{1,0:T(8,128)(2,1)S(1)}, u32[]{:S(2)}, u32[]{:S(2)}) collective-permute-start(bf16[256,384]{1,0:T(8,128)(2,1)S(1)} %shard_map.186.r0), channel_id=1, source_target_pairs={{0,3},{1,2},{2,1},{3,0},{4,7},{5,6},{6,5},{7,4},{8,11},{9,10},{10,... | collective-permute-start | bytes 589832 | tf_op jit(solution)/shard_map/ppermute | solution.py:374
  179.2 4.2 %collective-permute-done.13.r2 = bf16[256,384]{1,0:T(8,128)(2,1)S(1)} collective-permute-done((bf16[256,384]{1,0:T(8,128)(2,1)S(1)}, bf16[256,384]{1,0:T(8,128)(2,1)S(1)}, u32[]{:S(2)}, u32[]{:S(2)}) %collective-permute-start.13) | collective-permute-done | bytes 196640 | tf_op jit(solution)/shard_map/ppermute | solution.py:374
  183.4 4.5 %collective-permute-done.14.r3 = bf16[256,384]{1,0:T(8,128)(2,1)S(1)} collective-permute-done((bf16[256,384]{1,0:T(8,128)(2,1)S(1)}, bf16[256,384]{1,0:T(8,128)(2,1)S(1)}, u32[]{:S(2)}, u32[]{:S(2)}) %collective-permute-start.14) | collective-permute-done | bytes 196640 | tf_op jit(solution)/shard_map/ppermute | solution.py:374
  187.8 0.1 shard_map.187.h0
  188.0 5.0 %collective-permute-start.15 = (bf16[256,128]{1,0:T(8,128)(2,1)S(1)}, bf16[256,128]{1,0:T(8,128)(2,1)S(1)}, u32[]{:S(2)}, u32[]{:S(2)}) collective-permute-start(bf16[256,128]{1,0:T(8,128)(2,1)S(1)} %shard_map.187.h0), channel_id=1, source_target_pairs={{0,4},{4,8},{8,12},{12,0},{1,5},{5,9},{9,13},{13,1},{2,6},{6,10},{... | collective-permute-start | bytes 196616 | tf_op jit(solution)/shard_map/ppermute | solution.py:374
  193.0 4.1 %collective-permute-start.16 = (bf16[256,128]{1,0:T(8,128)(2,1)S(1)}, bf16[256,128]{1,0:T(8,128)(2,1)S(1)}, u32[]{:S(2)}, u32[]{:S(2)}) collective-permute-start(bf16[256,128]{1,0:T(8,128)(2,1)S(1)} %shard_map.187.h0), channel_id=1, source_target_pairs={{0,8},{4,12},{8,0},{12,4},{1,9},{5,13},{9,1},{13,5},{2,10},{6,14},... | collective-permute-start | bytes 196616 | tf_op jit(solution)/shard_map/ppermute | solution.py:374
  197.1 4.7 %collective-permute-start.17 = (bf16[256,128]{1,0:T(8,128)(2,1)S(1)}, bf16[256,128]{1,0:T(8,128)(2,1)S(1)}, u32[]{:S(2)}, u32[]{:S(2)}) collective-permute-start(bf16[256,128]{1,0:T(8,128)(2,1)S(1)} %shard_map.187.h0), channel_id=1, source_target_pairs={{0,12},{4,0},{8,4},{12,8},{1,13},{5,1},{9,5},{13,9},{2,14},{6,2},{... | collective-permute-start | bytes 196616 | tf_op jit(solution)/shard_map/ppermute | solution.py:374
  201.8 0.1 copy.21.score_ref
  201.9 0.0 copy-start.7
  201.9 2.0 shard_map.185
  203.9 0.1 collective-permute-done.16.h2
  204.0 0.0 collective-permute-done.17.h3
  204.0 1.2 shard_map.188.ahead_ref
  205.2 1.2 shard_map.189
  (36 shorter events, 0.1 us)
Async XLA Ops:
  26.0 4.0 %copy-start.14 = (bf16[256]{0:T(256)(128)(2,1)S(1)}, bf16[256]{0:T(256)(128)(2,1)}, u32[]{:S(2)}) copy-start(bf16[256]{0:T(256)(128)(2,1)} %param.24) | copy-start | bytes 1540
  26.0 12.9 %all-to-all-start.1 = ((bf16[32,8,128]{2,1,0:T(8,128)(2,1)}), bf16[32,8,128]{2,1,0:T(8,128)(2,1)S(1)}, u32[]{:S(2)}, u32[]{:S(2)}) async-start(bf16[32,8,128]{2,1,0:T(8,128)(2,1)} %shard_map.174), calls=%async_computation.1 | async-start | bytes 131072 | tf_op jit(solution)/shard_map/all_to_all | solution.py:369
  30.1 8.9 %copy-start.5 = (bf16[256,256]{1,0:T(8,128)(2,1)S(1)}, bf16[256,256]{1,0:T(8,128)(2,1)}, u32[]{:S(2)}) copy-start(bf16[256,256]{1,0:T(8,128)(2,1)} %refs_4_.1) | copy-start | bytes 393220
  38.9 1.0 copy-start.4
  39.9 0.9 copy-start.6
  40.8 8.6 %copy-start.10 = (bf16[2048,32]{0,1:T(8,128)(2,1)S(1)}, bf16[2048,32]{0,1:T(8,128)(2,1)}, u32[]{:S(2)}) copy-start(bf16[2048,32]{0,1:T(8,128)(2,1)} %param.34) | copy-start | bytes 393220
  40.8 8.6 %copy-start.11 = (bf16[2048,32]{0,1:T(8,128)(2,1)S(1)}, bf16[2048,32]{0,1:T(8,128)(2,1)}, u32[]{:S(2)}) copy-start(bf16[2048,32]{0,1:T(8,128)(2,1)} %param.33) | copy-start | bytes 393220
  42.3 7.1 %copy-start = (bf16[4096,128]{1,0:T(8,128)(2,1)S(1)}, bf16[4096,128]{1,0:T(8,128)(2,1)}, u32[]{:S(2)}) copy-start(bf16[4096,128]{1,0:T(8,128)(2,1)} %project_ref.1) | copy-start | bytes 3145732
  42.3 34.4 %all-to-all-start.2 = ((bf16[4,256,256]{2,1,0:T(8,128)(2,1)}), bf16[4,256,256]{2,1,0:T(8,128)(2,1)S(1)}, u32[]{:S(2)}, u32[]{:S(2)}) async-start(bf16[4,256,256]{2,1,0:T(8,128)(2,1)} %shard_map.176), calls=%async_computation.2 | async-start | bytes 1048576 | tf_op jit(solution)/shard_map/all_to_all | solution.py:369
  50.2 10.9 %collective-permute-start = (bf16[320,512]{1,0:T(8,128)(2,1)S(1)}, bf16[320,512]{1,0:T(8,128)(2,1)S(1)}, u32[]{:S(2)}, u32[]{:S(2)}) collective-permute-start(bf16[320,512]{1,0:T(8,128)(2,1)S(1)} %get-tuple-element.20), channel_id=1, source_target_pairs={{0,1},{1,0},{2,3},{3,2},{4,5},{5,4},{6,7},{7,6},{8,9},{9,8},{10,11... | collective-permute-start | bytes 983048 | tf_op jit(solution)/shard_map/ppermute | solution.py:374
  55.6 13.8 %collective-permute-start.1 = (bf16[320,512]{1,0:T(8,128)(2,1)S(1)}, bf16[320,512]{1,0:T(8,128)(2,1)S(1)}, u32[]{:S(2)}, u32[]{:S(2)}) collective-permute-start(bf16[320,512]{1,0:T(8,128)(2,1)S(1)} %get-tuple-element.21), channel_id=1, source_target_pairs={{0,2},{1,3},{2,0},{3,1},{4,6},{5,7},{6,4},{7,5},{8,10},{9,11},{10,... | collective-permute-start | bytes 983048 | tf_op jit(solution)/shard_map/ppermute | solution.py:374
  57.9 18.8 %collective-permute-start.2 = (bf16[320,512]{1,0:T(8,128)(2,1)S(1)}, bf16[320,512]{1,0:T(8,128)(2,1)S(1)}, u32[]{:S(2)}, u32[]{:S(2)}) collective-permute-start(bf16[320,512]{1,0:T(8,128)(2,1)S(1)} %get-tuple-element.22), channel_id=1, source_target_pairs={{0,3},{1,2},{2,1},{3,0},{4,7},{5,6},{6,5},{7,4},{8,11},{9,10},{10,... | collective-permute-start | bytes 983048 | tf_op jit(solution)/shard_map/ppermute | solution.py:374
  77.8 7.6 %copy-start.8 = (bf16[256,128]{1,0:T(8,128)(2,1)S(1)}, bf16[256,128]{1,0:T(8,128)(2,1)}, u32[]{:S(2)}) copy-start(bf16[256,128]{1,0:T(8,128)(2,1)} %residual_ref.1) | copy-start | bytes 196612
  86.2 6.3 %copy-start.12 = (s32[256,4]{0,1:T(4,128)S(1)}, s32[256,4]{0,1:T(4,128)}, u32[]{:S(2)}) copy-start(s32[256,4]{0,1:T(4,128)} %param.28) | copy-start | bytes 12292
  86.2 14.4 %all-to-all-start.4 = ((bf16[4,256,128]{2,1,0:T(8,128)(2,1)}), bf16[4,256,128]{2,1,0:T(8,128)(2,1)S(1)}, u32[]{:S(2)}, u32[]{:S(2)}) async-start(bf16[4,256,128]{2,1,0:T(8,128)(2,1)} %shard_map.179.mid_ref), calls=%async_computation.4 | async-start | bytes 524288 | tf_op jit(solution)/shard_map/all_to_all | solution.py:369
  92.5 42.1 %copy-start.2 = (bf16[2048,256]{1,0:T(8,128)(2,1)S(1)}, bf16[2048,256]{1,0:T(8,128)(2,1)}, u32[]{:S(2)}) copy-start(bf16[2048,256]{1,0:T(8,128)(2,1)} %refs_6_.1) | copy-start | bytes 3145732
  100.6 34.0 %copy-start.3 = (bf16[2048,256]{1,0:T(8,128)(2,1)S(1)}, bf16[2048,256]{1,0:T(8,128)(2,1)}, u32[]{:S(2)}) copy-start(bf16[2048,256]{1,0:T(8,128)(2,1)} %refs_7_.1) | copy-start | bytes 3145732
  101.0 32.3 %copy-start.9 = (bf16[2048]{0:T(1024)(128)(2,1)S(1)}, bf16[2048]{0:T(1024)(128)(2,1)}, u32[]{:S(2)}) copy-start(bf16[2048]{0:T(1024)(128)(2,1)} %param.27) | copy-start | bytes 12292
  116.6 10.0 %collective-permute-start.4 = (bf16[1536,128]{1,0:T(8,128)(2,1)S(1)}, bf16[1536,128]{1,0:T(8,128)(2,1)S(1)}, u32[]{:S(2)}, u32[]{:S(2)}) collective-permute-start(bf16[1536,128]{1,0:T(8,128)(2,1)S(1)} %bitcast.11), channel_id=1, source_target_pairs={{0,2},{2,0},{1,3},{3,1},{4,6},{6,4},{5,7},{7,5},{8,10},{10,8},{9,1... | collective-permute-start | bytes 1179656 | tf_op jit(solution)/shard_map/ppermute | solution.py:374
  119.2 14.0 %collective-permute-start.3 = (bf16[1536,128]{1,0:T(8,128)(2,1)S(1)}, bf16[1536,128]{1,0:T(8,128)(2,1)S(1)}, u32[]{:S(2)}, u32[]{:S(2)}) collective-permute-start(bf16[1536,128]{1,0:T(8,128)(2,1)S(1)} %bitcast.12), channel_id=1, source_target_pairs={{0,1},{1,0},{2,3},{3,2},{4,5},{5,4},{6,7},{7,6},{8,9},{9,8},{10,11... | collective-permute-start | bytes 1179656 | tf_op jit(solution)/shard_map/ppermute | solution.py:374
  126.6 7.9 %collective-permute-start.5 = (bf16[1536,128]{1,0:T(8,128)(2,1)S(1)}, bf16[1536,128]{1,0:T(8,128)(2,1)S(1)}, u32[]{:S(2)}, u32[]{:S(2)}) collective-permute-start(bf16[1536,128]{1,0:T(8,128)(2,1)S(1)} %collective-permute-done.4.refs_3_), channel_id=1, source_target_pairs={{0,1},{1,0},{2,3},{3,2},{4,5},{5,4},{6,7},{7,6},{8,9},{9,8},{10,11... | collective-permute-start | bytes 1179656 | tf_op jit(solution)/shard_map/ppermute | solution.py:374
  133.3 7.0 %copy-start.1 = (bf16[256,2048]{1,0:T(8,128)(2,1)S(1)}, bf16[256,2048]{1,0:T(8,128)(2,1)}, u32[]{:S(2)}) copy-start(bf16[256,2048]{1,0:T(8,128)(2,1)} %down_ref.2) | copy-start | bytes 3145732
  137.5 14.0 %collective-permute-start.7 = (bf16[384,256]{1,0:T(8,128)(2,1)S(1)}, bf16[384,256]{1,0:T(8,128)(2,1)S(1)}, u32[]{:S(2)}, u32[]{:S(2)}) collective-permute-start(bf16[384,256]{1,0:T(8,128)(2,1)S(1)} %shard_map.182.h0), channel_id=1, source_target_pairs={{0,2},{2,0},{1,3},{3,1},{4,6},{6,4},{5,7},{7,5},{8,10},{10,8},{9,1... | collective-permute-start | bytes 589832 | tf_op jit(solution)/shard_map/ppermute | solution.py:374
  141.1 12.4 %collective-permute-start.10 = (bf16[256,512]{1,0:T(8,128)(2,1)S(1)}, bf16[256,512]{1,0:T(8,128)(2,1)S(1)}, u32[]{:S(2)}, u32[]{:S(2)}) collective-permute-start(bf16[256,512]{1,0:T(8,128)(2,1)S(1)} %get-tuple-element.25), channel_id=1, source_target_pairs={{0,2},{1,3},{2,0},{3,1},{4,6},{5,7},{6,4},{7,5},{8,10},{9,11},{10,... | collective-permute-start | bytes 786440 | tf_op jit(solution)/shard_map/ppermute | solution.py:374
  143.6 13.6 %collective-permute-start.11 = (bf16[256,512]{1,0:T(8,128)(2,1)S(1)}, bf16[256,512]{1,0:T(8,128)(2,1)S(1)}, u32[]{:S(2)}, u32[]{:S(2)}) collective-permute-start(bf16[256,512]{1,0:T(8,128)(2,1)S(1)} %get-tuple-element.26), channel_id=1, source_target_pairs={{0,3},{1,2},{2,1},{3,0},{4,7},{5,6},{6,5},{7,4},{8,11},{9,10},{10,... | collective-permute-start | bytes 786440 | tf_op jit(solution)/shard_map/ppermute | solution.py:374
  147.2 10.1 %collective-permute-start.9 = (bf16[256,512]{1,0:T(8,128)(2,1)S(1)}, bf16[256,512]{1,0:T(8,128)(2,1)S(1)}, u32[]{:S(2)}, u32[]{:S(2)}) collective-permute-start(bf16[256,512]{1,0:T(8,128)(2,1)S(1)} %get-tuple-element.24), channel_id=1, source_target_pairs={{0,1},{1,0},{2,3},{3,2},{4,5},{5,4},{6,7},{7,6},{8,9},{9,8},{10,11... | collective-permute-start | bytes 786440 | tf_op jit(solution)/shard_map/ppermute | solution.py:374
  149.1 8.1 %collective-permute-start.6 = (bf16[384,256]{1,0:T(8,128)(2,1)S(1)}, bf16[384,256]{1,0:T(8,128)(2,1)S(1)}, u32[]{:S(2)}, u32[]{:S(2)}) collective-permute-start(bf16[384,256]{1,0:T(8,128)(2,1)S(1)} %shard_map.182.h0), channel_id=1, source_target_pairs={{0,1},{1,0},{2,3},{3,2},{4,5},{5,4},{6,7},{7,6},{8,9},{9,8},{10,11... | collective-permute-start | bytes 589832 | tf_op jit(solution)/shard_map/ppermute | solution.py:374
  151.6 5.7 %collective-permute-start.8 = (bf16[384,256]{1,0:T(8,128)(2,1)S(1)}, bf16[384,256]{1,0:T(8,128)(2,1)S(1)}, u32[]{:S(2)}, u32[]{:S(2)}) collective-permute-start(bf16[384,256]{1,0:T(8,128)(2,1)S(1)} %collective-permute-done.7.h2), channel_id=1, source_target_pairs={{0,1},{1,0},{2,3},{3,2},{4,5},{5,4},{6,7},{7,6},{8,9},{9,8},{10,11... | collective-permute-start | bytes 589832 | tf_op jit(solution)/shard_map/ppermute | solution.py:374
  158.7 46.5 %all-to-all-start.6 = ((bf16[128,3,4,128]{3,2,1,0:T(4,128)(2,1)}), bf16[128,3,4,128]{3,2,1,0:T(4,128)(2,1)S(1)}, u32[]{:S(2)}, u32[]{:S(2)}) async-start(bf16[128,3,4,128]{3,2,1,0:T(4,128)(2,1)} %bitcast.9), calls=%async_computation.6 | async-start | bytes 786432 | tf_op jit(solution)/shard_map/all_to_all | solution.py:369
  171.3 30.5 %copy-start.13 = (f32[256,4]{0,1:T(4,128)S(1)}, f32[256,4]{0,1:T(4,128)}, u32[]{:S(2)}) copy-start(f32[256,4]{0,1:T(4,128)} %param.29) | copy-start | bytes 12292
  171.3 7.9 %collective-permute-start.12 = (bf16[256,384]{1,0:T(8,128)(2,1)S(1)}, bf16[256,384]{1,0:T(8,128)(2,1)S(1)}, u32[]{:S(2)}, u32[]{:S(2)}) collective-permute-start(bf16[256,384]{1,0:T(8,128)(2,1)S(1)} %shard_map.186.r0), channel_id=1, source_target_pairs={{0,1},{1,0},{2,3},{3,2},{4,5},{5,4},{6,7},{7,6},{8,9},{9,8},{10,11... | collective-permute-start | bytes 589832 | tf_op jit(solution)/shard_map/ppermute | solution.py:374
  173.4 10.0 %collective-permute-start.13 = (bf16[256,384]{1,0:T(8,128)(2,1)S(1)}, bf16[256,384]{1,0:T(8,128)(2,1)S(1)}, u32[]{:S(2)}, u32[]{:S(2)}) collective-permute-start(bf16[256,384]{1,0:T(8,128)(2,1)S(1)} %shard_map.186.r0), channel_id=1, source_target_pairs={{0,2},{1,3},{2,0},{3,1},{4,6},{5,7},{6,4},{7,5},{8,10},{9,11},{10,... | collective-permute-start | bytes 589832 | tf_op jit(solution)/shard_map/ppermute | solution.py:374
  175.5 12.4 %collective-permute-start.14 = (bf16[256,384]{1,0:T(8,128)(2,1)S(1)}, bf16[256,384]{1,0:T(8,128)(2,1)S(1)}, u32[]{:S(2)}, u32[]{:S(2)}) collective-permute-start(bf16[256,384]{1,0:T(8,128)(2,1)S(1)} %shard_map.186.r0), channel_id=1, source_target_pairs={{0,3},{1,2},{2,1},{3,0},{4,7},{5,6},{6,5},{7,4},{8,11},{9,10},{10,... | collective-permute-start | bytes 589832 | tf_op jit(solution)/shard_map/ppermute | solution.py:374
  188.0 15.9 %collective-permute-start.15 = (bf16[256,128]{1,0:T(8,128)(2,1)S(1)}, bf16[256,128]{1,0:T(8,128)(2,1)S(1)}, u32[]{:S(2)}, u32[]{:S(2)}) collective-permute-start(bf16[256,128]{1,0:T(8,128)(2,1)S(1)} %shard_map.187.h0), channel_id=1, source_target_pairs={{0,4},{4,8},{8,12},{12,0},{1,5},{5,9},{9,13},{13,1},{2,6},{6,10},{... | collective-permute-start | bytes 196616 | tf_op jit(solution)/shard_map/ppermute | solution.py:374
  193.0 11.0 %collective-permute-start.16 = (bf16[256,128]{1,0:T(8,128)(2,1)S(1)}, bf16[256,128]{1,0:T(8,128)(2,1)S(1)}, u32[]{:S(2)}, u32[]{:S(2)}) collective-permute-start(bf16[256,128]{1,0:T(8,128)(2,1)S(1)} %shard_map.187.h0), channel_id=1, source_target_pairs={{0,8},{4,12},{8,0},{12,4},{1,9},{5,13},{9,1},{13,5},{2,10},{6,14},... | collective-permute-start | bytes 196616 | tf_op jit(solution)/shard_map/ppermute | solution.py:374
  197.1 6.9 %collective-permute-start.17 = (bf16[256,128]{1,0:T(8,128)(2,1)S(1)}, bf16[256,128]{1,0:T(8,128)(2,1)S(1)}, u32[]{:S(2)}, u32[]{:S(2)}) collective-permute-start(bf16[256,128]{1,0:T(8,128)(2,1)S(1)} %shard_map.187.h0), channel_id=1, source_target_pairs={{0,12},{4,0},{8,4},{12,8},{1,13},{5,1},{9,5},{13,9},{2,14},{6,2},{... | collective-permute-start | bytes 196616 | tf_op jit(solution)/shard_map/ppermute | solution.py:374
  201.9 2.1 %copy-start.7 = (bf16[512,128]{1,0:T(8,128)(2,1)S(1)}, bf16[512,128]{1,0:T(8,128)(2,1)}, u32[]{:S(2)}) copy-start(bf16[512,128]{1,0:T(8,128)(2,1)} %down_ref.3) | copy-start | bytes 393220

commit v8 on v6

--- a/solution.py
+++ b/solution.py
@@ -13,10 +13,9 @@
 MOST = 12
 SLOTS = 384
 ALL_SLOTS = 1536
-PITCH = 56
 D = 2048
 SP = ("z", "x")
-SPG = ("z", "x", "yg")
+GSP = ("yg", "z", "x")
 TP = ("yg", "yn", "c")
 GROUP = ("yn", "c")
 F32 = jnp.float32
@@ -178,7 +177,7 @@
         before = before + cum[BLOCK - 1 : BLOCK]
 
 
-def head_kernel(gain_ref, enter_ref, local_ref, start_ref, gate_ref, out_ref):
+def head_kernel(enter_ref, gain_ref, local_ref, start_ref, gate_ref, out_ref):
     enter = enter_ref[...]
     mixed = local_ref[...] + sum(nt(piece, enter) for piece in split(start_ref[...], 3))
     scale = lax.rsqrt(jnp.mean(mixed * mixed, axis=-1, keepdims=True) + EPSILON)
@@ -209,11 +208,13 @@
     cols = lax.broadcasted_iota(jnp.int32, (TOK, TOK), 1)
     earlier = (rows > cols).astype(BF16)
     ranks = jnp.dot(earlier, named.astype(BF16), preferred_element_type=F32)
-    return [
-        routing_ref[:, k : k + 1] * MOST
-        + jnp.sum(hot[k] * ranks, axis=1, keepdims=True).astype(jnp.int32)
-        for k in range(4)
-    ]
+    slots = []
+    for k in range(4):
+        expert = routing_ref[:, k : k + 1]
+        place = (expert & 3) * 32 + lax.shift_right_logical(expert, 2)
+        rank = jnp.sum(hot[k] * ranks, axis=1, keepdims=True).astype(jnp.int32)
+        slots.append(place * MOST + rank)
+    return slots
 
 
 def pick_kernel(routing_ref, pick_ref):
@@ -253,18 +254,13 @@
         out_ref[rows, :] = picked.astype(BF16)
 
 
-def expert_kernel(ready, ids_ref, x0, x1, x2, x3, gain_ref, gate_ref, up_ref, out_ref, wide_ref, rows_ref):
+def expert_kernel(ready, ids_ref, x0, x1, x2, x3, gain_ref, gate_ref, up_ref, out_ref, rows_ref):
     part = ids_ref[0]
     squares = jnp.zeros((SLOTS, 128), F32)
     for m, x_ref in enumerate((x0, x1, x2, x3)):
-        for s in range(32):
-            wide_ref[m, s * PITCH : s * PITCH + 48, :] = x_ref[s * 48 : (s + 1) * 48, :].astype(F32)
-    for m in range(4):
         for q in range(4):
             slab = q * 4 + (part ^ m)
-            tile = jnp.concatenate(
-                [wide_ref[m, pl.ds(q * MOST + r, 32, stride=PITCH), :] for r in range(MOST)], axis=0
-            )
+            tile = x_ref[q * SLOTS : (q + 1) * SLOTS, :].astype(F32)
             squares = squares + tile * tile
             scaled = (tile * gain_ref[pl.ds(slab, 1), :]).astype(BF16)
             rows_ref[:, pl.ds(pl.multiple_of(slab * 128, 128), 128)] = scaled
@@ -279,17 +275,12 @@
     out_ref[...] = in_ref[...].astype(F32)
 
 
-def down_kernel(h0, h1, h2, h3, d0, d1, d2, d3, out_ref, wide_ref):
+def down_kernel(h0, h1, h2, h3, d0, d1, d2, d3, out_ref):
     total = jnp.zeros((SLOTS, 512), F32)
     for h_ref, d_ref in ((h0, d0), (h1, d1), (h2, d2), (h3, d3)):
         total = total + jnp.dot(h_ref[...], d_ref[256:512, :], preferred_element_type=F32)
     for q in range(4):
-        for r in range(MOST):
-            wide_ref[pl.ds(q * MOST + r, 32, stride=PITCH), :] = total[
-                r * 32 : (r + 1) * 32, q * 128 : (q + 1) * 128
-            ]
-    for s in range(32):
-        out_ref[s * 48 : (s + 1) * 48, :] = wide_ref[s * PITCH : s * PITCH + 48, :].astype(BF16)
+        out_ref[q * SLOTS : (q + 1) * SLOTS, :] = total[:, q * 128 : (q + 1) * 128].astype(BF16)
 
 
 def parts_kernel(ids_ref, project_ref, down_ref, shared_ref, *out_refs):
@@ -424,8 +415,8 @@
     entering = exchange(call(scan_kernel, ((32, 8, DK), BF16), states), SP)
     head_rows = call(
         head_kernel, ((4, TOK, DV), BF16),
-        head_gain, entering.reshape(DV, DK), local, start, output_gate_preactivation,
-        fetch=(whole,) * 4, limit=60,
+        entering.reshape(DV, DK), head_gain, local, start, output_gate_preactivation,
+        fetch=(whole,) * 3, limit=60,
     )
     partial = call(
         project_kernel, ((4, TOK, 128), BF16),
@@ -435,7 +426,7 @@
         dispatch_kernel, [((ALL_SLOTS, 128), BF16), ((TOK, 128), BF16)],
         pick, exchange(partial, GROUP), residual,
     )
-    own = exchange(outgoing.reshape(128, 3, 4, 128), SPG).reshape(ALL_SLOTS, 128)
+    own = exchange(outgoing.reshape(128, 3, 4, 128), GSP).reshape(ALL_SLOTS, 128)
     mids = [mid] + shifted([mid] * 3, "yg")
 
     across = swapped(own, "yn")
@@ -450,7 +441,7 @@
         expert_kernel, ((SLOTS, 256), BF16),
         ids, own, beside, across, far, gain, expert_gate_weight, expert_up_weight,
         smem=1, fetch=((0, D), (0, D)), late=True,
-        scratch=[pltpu.VMEM((4, 32 * PITCH, 128), F32), pltpu.VMEM((SLOTS, D), BF16)],
+        scratch=[pltpu.VMEM((SLOTS, D), BF16)],
     )
     routed_across = swapped(routed, "yn")
     routed_beside = swapped(routed, "c")
@@ -458,9 +449,8 @@
     expert_out = call(
         down_kernel, ((ALL_SLOTS, 128), BF16),
         routed, routed_beside, routed_across, routed_far, *parts,
-        scratch=[pltpu.VMEM((32 * PITCH, 128), F32)],
-    )
-    back = exchange(expert_out.reshape(128, 3, 4, 128), SPG).reshape(ALL_SLOTS, 128)
+    )
+    back = exchange(expert_out.reshape(128, 3, 4, 128), GSP).reshape(ALL_SLOTS, 128)
     hidden = call(shared_hidden_kernel, ((TOK, 128), BF16), *pre)
     hidden = [hidden] + shifted([hidden] * 3, "yg")
     ahead = call(

time: 226 us -> 225 us (level)
  transfers between devices with their start and end apart: 22 -> 22, of which waited for: 14 -> 13; matrix products, arithmetic and copies ran while one was open for 0% -> 0% of each run, Pallas kernels for 4% -> 4%
where the time goes in v8:
time: 225 us; the launch traced here: 224 us
  starting transfers between devices  90.4 us (40%)
  waiting for transfers between devices  52.3 us (23%)
  blocking collectives  51.8 us (23%)
  Pallas kernels  23.2 us (10%)
  local copies, waits for them, and re-layouts  5.48 us (2%)
    ppermute x18, starting transfers between devices, moved(): lax.ppermute(value, axes, [(i, target(i) % count) for i in range(count)])  68 us
    all_to_all x2, blocking collectives, exchange(): return lax.all_to_all(value, axes, split_axis=0, concat_axis=0, tiled=True)  51.8 us
    ppermute x18, waiting for transfers between devices, moved(): lax.ppermute(value, axes, [(i, target(i) % count) for i in range(count)])  44.9 us
    pallas_call x16, Pallas kernels, call(): pl.pallas_call(fetching if fetch else kernel, out_shape=shapes, in_specs=...  23.2 us
    all_to_all x4, starting transfers between devices, exchange(): return lax.all_to_all(value, axes, split_axis=0, concat_axis=0, tiled=True)  22.4 us
    all_to_all x4, waiting for transfers between devices, exchange(): return lax.all_to_all(value, axes, split_axis=0, concat_axis=0, tiled=True)  7.36 us
    unnamed x32, local copies, waits for them, and re-layouts  4.88 us
  transfers between devices with their start and end apart: 22, of which 13 were waited for; matrix products, arithmetic and copies ran while one was open for 0% of the time, Pallas kernels for 4%

profile of v8, /device:TPU:1, one launch (start us, length us, event | category | flops | bytes accessed | tf_op | source)
XLA Modules:
  0.0 223.7 jit_solution(15862104854769732944)
XLA Ops:
  0.0 2.3 %shard_map.173 = bf16[32,16,128]{2,1,0:T(8,128)(2,1)} custom-call(bf16[256,128]{1,0:T(8,128)(2,1)} %refs_1_.3, bf16[256,256]{1,0:T(8,128)(2,1)} %refs_2_.3, bf16[256,128]{1,0:T(8,128)(2,1)} %refs_3_.1, f32[2,128]{1,0:T(2,128)} %bitcast.20), custom_call_target="tpu_custom_call" | custom-call | flops 1000000 | bytes 1000000 | tf_op jit(solution)/shard_map/pallas_call | solution.py:63
  2.3 23.1 %all_to_all.30.in_ref = bf16[32,16,128]{2,1,0:T(8,128)(2,1)S(1)} all-to-all(bf16[32,16,128]{2,1,0:T(8,128)(2,1)} %shard_map.173), channel_id=1, replica_groups=mesh['z'=8,'x'=4,'yg'=4,'yn'=2,'c'=2] {'z','x'}, dimensions={0} | all-to-all | bytes 262144 | tf_op jit(solution)/shard_map/all_to_all | solution.py:348
  25.3 0.7 shard_map.174
  26.0 3.9 %all-to-all-start.1 = ((bf16[32,8,128]{2,1,0:T(8,128)(2,1)}), bf16[32,8,128]{2,1,0:T(8,128)(2,1)S(1)}, u32[]{:S(2)}, u32[]{:S(2)}) async-start(bf16[32,8,128]{2,1,0:T(8,128)(2,1)} %shard_map.174), calls=%async_computation.1 | async-start | bytes 131072 | tf_op jit(solution)/shard_map/all_to_all | solution.py:348
  29.9 0.0 copy-start.14
  29.9 0.6 copy-done.14
  30.6 0.6 reshape.26.refs_1_
  31.2 3.6 %shard_map.175 = (f32[256,256]{1,0:T(8,128)}, f32[256,128]{1,0:T(8,128)}) custom-call(bf16[256,128]{1,0:T(8,128)(2,1)} %refs_0_.3, bf16[256,128]{1,0:T(8,128)(2,1)} %refs_1_.3, bf16[256,256]{1,0:T(8,128)(2,1)} %refs_2_.3, bf16[256,128]{1,0:T(8,128)(2,1)} %refs_3_.1, f32[2,128]{1,0:T(2,128)} %bitcast.21), custom_call_target="tpu_custom_call" | custom-call | flops 1000000 | bytes 1000000 | tf_op jit(solution)/shard_map/pallas_call | solution.py:63
  34.7 0.1 pad_add_fusion.ids_ref.refs_0_
  34.8 4.0 %all-to-all-done.1 = bf16[32,8,128]{2,1,0:T(8,128)(2,1)S(1)} async-done(((bf16[32,8,128]{2,1,0:T(8,128)(2,1)}), bf16[32,8,128]{2,1,0:T(8,128)(2,1)S(1)}, u32[]{:S(2)}, u32[]{:S(2)}) %all-to-all-start.1) | async-done | bytes 65568 | tf_op jit(solution)/shard_map/all_to_all | solution.py:348
  38.8 0.6 copy-done.9
  39.4 3.1 %shard_map.176 = bf16[4,256,256]{2,1,0:T(8,128)(2,1)} custom-call(bf16[256,128]{1,0:T(8,128)(2,1)} %bitcast.17, bf16[1,256]{1,0:T(2,128)(2,1)} %reshape.26.refs_1_, f32[256,256]{1,0:T(8,128)} %get-tuple-element.15.refs_2_, f32[256,128]{1,0:T(8,128)} %get-tuple-element.16.refs_3_, bf16[256,256]{1,0:T(8,128)(2,1)} %refs_4_.1), custom_call_target="tpu_custom_call" | custom-call | flops 1000000 | bytes 1000000 | tf_op jit(solution)/shard_map/pallas_call | solution.py:63
  42.5 0.0 copy-start
  42.5 7.0 %all-to-all-start.2 = ((bf16[4,256,256]{2,1,0:T(8,128)(2,1)}), bf16[4,256,256]{2,1,0:T(8,128)(2,1)S(1)}, u32[]{:S(2)}, u32[]{:S(2)}) async-start(bf16[4,256,256]{2,1,0:T(8,128)(2,1)} %shard_map.176), calls=%async_computation.2 | async-start | bytes 1048576 | tf_op jit(solution)/shard_map/all_to_all | solution.py:348
  49.5 0.0 copy-start.1
  49.5 1.2 copy-done.1
  50.8 1.0 shard_map.177
  51.8 5.4 %collective-permute-start = (bf16[576,512]{1,0:T(8,128)(2,1)S(1)}, bf16[576,512]{1,0:T(8,128)(2,1)S(1)}, u32[]{:S(2)}, u32[]{:S(2)}) collective-permute-start(bf16[576,512]{1,0:T(8,128)(2,1)S(1)} %get-tuple-element.18), channel_id=1, source_target_pairs={{0,1},{1,0},{2,3},{3,2},{4,5},{5,4},{6,7},{7,6},{8,9},{9,8},{10,11... | collective-permute-start | bytes 1769480 | tf_op jit(solution)/shard_map/ppermute | solution.py:353
  57.2 2.3 %collective-permute-start.1 = (bf16[576,512]{1,0:T(8,128)(2,1)S(1)}, bf16[576,512]{1,0:T(8,128)(2,1)S(1)}, u32[]{:S(2)}, u32[]{:S(2)}) collective-permute-start(bf16[576,512]{1,0:T(8,128)(2,1)S(1)} %get-tuple-element.19), channel_id=1, source_target_pairs={{0,2},{1,3},{2,0},{3,1},{4,6},{5,7},{6,4},{7,5},{8,10},{9,11},{10,... | collective-permute-start | bytes 1769480 | tf_op jit(solution)/shard_map/ppermute | solution.py:353
  59.5 3.2 %collective-permute-start.2 = (bf16[576,512]{1,0:T(8,128)(2,1)S(1)}, bf16[576,512]{1,0:T(8,128)(2,1)S(1)}, u32[]{:S(2)}, u32[]{:S(2)}) collective-permute-start(bf16[576,512]{1,0:T(8,128)(2,1)S(1)} %get-tuple-element.20), channel_id=1, source_target_pairs={{0,3},{1,2},{2,1},{3,0},{4,7},{5,6},{6,5},{7,4},{8,11},{9,10},{10,... | collective-permute-start | bytes 1769480 | tf_op jit(solution)/shard_map/ppermute | solution.py:353
  62.7 13.1 %collective-permute-done.1.refs_4_.d2.w2 = bf16[576,512]{1,0:T(8,128)(2,1)S(1)} collective-permute-done((bf16[576,512]{1,0:T(8,128)(2,1)S(1)}, bf16[576,512]{1,0:T(8,128)(2,1)S(1)}, u32[]{:S(2)}, u32[]{:S(2)}) %collective-permute-start.1) | collective-permute-done | bytes 589856 | tf_op jit(solution)/shard_map/ppermute | solution.py:353
  75.8 12.6 %collective-permute-done.2.refs_5_.d3.w3 = bf16[576,512]{1,0:T(8,128)(2,1)S(1)} collective-permute-done((bf16[576,512]{1,0:T(8,128)(2,1)S(1)}, bf16[576,512]{1,0:T(8,128)(2,1)S(1)}, u32[]{:S(2)}, u32[]{:S(2)}) %collective-permute-start.2) | collective-permute-done | bytes 589856 | tf_op jit(solution)/shard_map/ppermute | solution.py:353
  88.4 1.8 shard_map.178
  90.2 3.8 %all-to-all-start.3 = ((bf16[4,256,128]{2,1,0:T(8,128)(2,1)}), bf16[4,256,128]{2,1,0:T(8,128)(2,1)S(1)}, u32[]{:S(2)}, u32[]{:S(2)}) async-start(bf16[4,256,128]{2,1,0:T(8,128)(2,1)} %shard_map.178), calls=%async_computation.3 | async-start | bytes 524288 | tf_op jit(solution)/shard_map/all_to_all | solution.py:348
  94.0 0.1 copy.19.routing_ref
  94.2 1.5 shard_map.172.pick_ref
  95.7 3.4 %all-to-all-done.3.in_ref = bf16[4,256,128]{2,1,0:T(8,128)(2,1)S(1)} async-done(((bf16[4,256,128]{2,1,0:T(8,128)(2,1)}), bf16[4,256,128]{2,1,0:T(8,128)(2,1)S(1)}, u32[]{:S(2)}, u32[]{:S(2)}) %all-to-all-start.3) | async-done | bytes 262176 | tf_op jit(solution)/shard_map/all_to_all | solution.py:348
  99.1 0.8 copy-done.7
  99.9 0.4 shard_map.179
  100.3 28.8 %all_to_all.31 = bf16[128,3,4,128]{3,2,1,0:T(4,128)(2,1)S(1)} all-to-all(bf16[128,3,4,128]{3,2,1,0:T(4,128)(2,1)S(1)} %bitcast.15), channel_id=1, replica_groups=mesh['z'=8,'x'=4,'yg'=4,'yn'=2,'c'=2] {'yg','z','x'}, dimensions={0} | all-to-all | bytes 786432 | tf_op jit(solution)/shard_map/all_to_all | solution.py:348
  129.1 2.1 collective-permute-start.4
  131.2 5.8 %collective-permute-start.3 = (bf16[1536,128]{1,0:T(8,128)(2,1)S(1)}, bf16[1536,128]{1,0:T(8,128)(2,1)S(1)}, u32[]{:S(2)}, u32[]{:S(2)}) collective-permute-start(bf16[1536,128]{1,0:T(8,128)(2,1)S(1)} %bitcast.12), channel_id=1, source_target_pairs={{0,1},{1,0},{2,3},{3,2},{4,5},{5,4},{6,7},{7,6},{8,9},{9,8},{10,11... | collective-permute-start | bytes 1179656 | tf_op jit(solution)/shard_map/ppermute | solution.py:353
  137.0 2.0 collective-permute-done.4.refs_3_
  139.0 5.4 %collective-permute-start.5 = (bf16[1536,128]{1,0:T(8,128)(2,1)S(1)}, bf16[1536,128]{1,0:T(8,128)(2,1)S(1)}, u32[]{:S(2)}, u32[]{:S(2)}) collective-permute-start(bf16[1536,128]{1,0:T(8,128)(2,1)S(1)} %collective-permute-done.4.refs_3_), channel_id=1, source_target_pairs={{0,1},{1,0},{2,3},{3,2},{4,5},{5,4},{6,7},{7,6},{8,9},{9,8},{10,11... | collective-permute-start | bytes 1179656 | tf_op jit(solution)/shard_map/ppermute | solution.py:353
  144.4 1.3 collective-permute-done.5.refs_4_
  145.7 1.2 copy-done.3
  147.0 2.6 %shard_map.181.h0 = bf16[384,256]{1,0:T(8,128)(2,1)S(1)} custom-call(s32[2]{0:T(128)S(1)} %pad_add_fusion.ids_ref.refs_0_, bf16[1536,128]{1,0:T(8,128)(2,1)S(1)} %bitcast.13, bf16[1536,128]{1,0:T(8,128)(2,1)S(1)} %collective-permute-done.3.refs_2_, bf16[1536,128]{1,0:T(8,128)(2,1)S(1)} %collective-permute-done.4.refs_3_, ...), custom_call_target="tpu_custom_call" | custom-call | flops 1000000 | bytes 1000000 | tf_op jit(solution)/shard_map/pallas_call | solution.py:63
  149.6 2.1 collective-permute-start.7
  151.7 2.6 %collective-permute-start.6 = (bf16[384,256]{1,0:T(8,128)(2,1)S(1)}, bf16[384,256]{1,0:T(8,128)(2,1)S(1)}, u32[]{:S(2)}, u32[]{:S(2)}) collective-permute-start(bf16[384,256]{1,0:T(8,128)(2,1)S(1)} %shard_map.181.h0), channel_id=1, source_target_pairs={{0,1},{1,0},{2,3},{3,2},{4,5},{5,4},{6,7},{7,6},{8,9},{9,8},{10,11... | collective-permute-start | bytes 589832 | tf_op jit(solution)/shard_map/ppermute | solution.py:353
  154.2 3.3 %collective-permute-done.7.h2 = bf16[384,256]{1,0:T(8,128)(2,1)S(1)} collective-permute-done((bf16[384,256]{1,0:T(8,128)(2,1)S(1)}, bf16[384,256]{1,0:T(8,128)(2,1)S(1)}, u32[]{:S(2)}, u32[]{:S(2)}) %collective-permute-start.7) | collective-permute-done | bytes 196640 | tf_op jit(solution)/shard_map/ppermute | solution.py:353
  157.5 3.1 %collective-permute-start.8 = (bf16[384,256]{1,0:T(8,128)(2,1)S(1)}, bf16[384,256]{1,0:T(8,128)(2,1)S(1)}, u32[]{:S(2)}, u32[]{:S(2)}) collective-permute-start(bf16[384,256]{1,0:T(8,128)(2,1)S(1)} %collective-permute-done.7.h2), channel_id=1, source_target_pairs={{0,1},{1,0},{2,3},{3,2},{4,5},{5,4},{6,7},{7,6},{8,9},{9,8},{10,11... | collective-permute-start | bytes 589832 | tf_op jit(solution)/shard_map/ppermute | solution.py:353
  160.7 1.0 collective-permute-done.8.h3
  161.7 1.3 shard_map.182
  163.0 7.8 %all-to-all-start.5 = ((bf16[128,3,4,128]{3,2,1,0:T(4,128)(2,1)}), bf16[128,3,4,128]{3,2,1,0:T(4,128)(2,1)S(1)}, u32[]{:S(2)}, u32[]{:S(2)}) async-start(bf16[128,3,4,128]{3,2,1,0:T(4,128)(2,1)} %bitcast.9), calls=%async_computation.5 | async-start | bytes 786432 | tf_op jit(solution)/shard_map/all_to_all | solution.py:348
  170.8 6.7 %collective-permute-start.10 = (bf16[256,128]{1,0:T(8,128)(2,1)S(1)}, bf16[256,128]{1,0:T(8,128)(2,1)S(1)}, u32[]{:S(2)}, u32[]{:S(2)}) collective-permute-start(bf16[256,128]{1,0:T(8,128)(2,1)S(1)} %copy-done.5), channel_id=1, source_target_pairs={{0,8},{4,12},{8,0},{12,4},{1,9},{5,13},{9,1},{13,5},{2,10},{6,14},... | collective-permute-start | bytes 196616 | tf_op jit(solution)/shard_map/ppermute | solution.py:353
  177.5 2.0 collective-permute-start.11
  179.5 4.2 %collective-permute-start.9 = (bf16[256,128]{1,0:T(8,128)(2,1)S(1)}, bf16[256,128]{1,0:T(8,128)(2,1)S(1)}, u32[]{:S(2)}, u32[]{:S(2)}) collective-permute-start(bf16[256,128]{1,0:T(8,128)(2,1)S(1)} %copy-done.5), channel_id=1, source_target_pairs={{0,4},{4,8},{8,12},{12,0},{1,5},{5,9},{9,13},{13,1},{2,6},{6,10},{... | collective-permute-start | bytes 196616 | tf_op jit(solution)/shard_map/ppermute | solution.py:353
  183.7 0.6 collective-permute-done.10.m2
  184.4 2.6 %collective-permute-done.9.m1 = bf16[256,128]{1,0:T(8,128)(2,1)S(1)} collective-permute-done((bf16[256,128]{1,0:T(8,128)(2,1)S(1)}, bf16[256,128]{1,0:T(8,128)(2,1)S(1)}, u32[]{:S(2)}, u32[]{:S(2)}) %collective-permute-start.9) | collective-permute-done | bytes 65568 | tf_op jit(solution)/shard_map/ppermute | solution.py:353
  187.0 0.9 shard_map.184.r0
  187.9 4.2 %collective-permute-start.12 = (bf16[256,384]{1,0:T(8,128)(2,1)S(1)}, bf16[256,384]{1,0:T(8,128)(2,1)S(1)}, u32[]{:S(2)}, u32[]{:S(2)}) collective-permute-start(bf16[256,384]{1,0:T(8,128)(2,1)S(1)} %shard_map.184.r0), channel_id=1, source_target_pairs={{0,1},{1,0},{2,3},{3,2},{4,5},{5,4},{6,7},{7,6},{8,9},{9,8},{10,11... | collective-permute-start | bytes 589832 | tf_op jit(solution)/shard_map/ppermute | solution.py:353
  192.1 2.5 %collective-permute-start.13 = (bf16[256,384]{1,0:T(8,128)(2,1)S(1)}, bf16[256,384]{1,0:T(8,128)(2,1)S(1)}, u32[]{:S(2)}, u32[]{:S(2)}) collective-permute-start(bf16[256,384]{1,0:T(8,128)(2,1)S(1)} %shard_map.184.r0), channel_id=1, source_target_pairs={{0,2},{1,3},{2,0},{3,1},{4,6},{5,7},{6,4},{7,5},{8,10},{9,11},{10,... | collective-permute-start | bytes 589832 | tf_op jit(solution)/shard_map/ppermute | solution.py:353
  194.6 3.0 %collective-permute-start.14 = (bf16[256,384]{1,0:T(8,128)(2,1)S(1)}, bf16[256,384]{1,0:T(8,128)(2,1)S(1)}, u32[]{:S(2)}, u32[]{:S(2)}) collective-permute-start(bf16[256,384]{1,0:T(8,128)(2,1)S(1)} %shard_map.184.r0), channel_id=1, source_target_pairs={{0,3},{1,2},{2,1},{3,0},{4,7},{5,6},{6,5},{7,4},{8,11},{9,10},{10,... | collective-permute-start | bytes 589832 | tf_op jit(solution)/shard_map/ppermute | solution.py:353
  197.6 2.9 %collective-permute-done.13.r2 = bf16[256,384]{1,0:T(8,128)(2,1)S(1)} collective-permute-done((bf16[256,384]{1,0:T(8,128)(2,1)S(1)}, bf16[256,384]{1,0:T(8,128)(2,1)S(1)}, u32[]{:S(2)}, u32[]{:S(2)}) %collective-permute-start.13) | collective-permute-done | bytes 196640 | tf_op jit(solution)/shard_map/ppermute | solution.py:353
  200.4 4.4 %collective-permute-done.14.r3 = bf16[256,384]{1,0:T(8,128)(2,1)S(1)} collective-permute-done((bf16[256,384]{1,0:T(8,128)(2,1)S(1)}, bf16[256,384]{1,0:T(8,128)(2,1)S(1)}, u32[]{:S(2)}, u32[]{:S(2)}) %collective-permute-start.14) | collective-permute-done | bytes 196640 | tf_op jit(solution)/shard_map/ppermute | solution.py:353
  204.8 0.1 shard_map.185.h0
  205.0 3.7 %collective-permute-start.15 = (bf16[256,128]{1,0:T(8,128)(2,1)S(1)}, bf16[256,128]{1,0:T(8,128)(2,1)S(1)}, u32[]{:S(2)}, u32[]{:S(2)}) collective-permute-start(bf16[256,128]{1,0:T(8,128)(2,1)S(1)} %shard_map.185.h0), channel_id=1, source_target_pairs={{0,4},{4,8},{8,12},{12,0},{1,5},{5,9},{9,13},{13,1},{2,6},{6,10},{... | collective-permute-start | bytes 196616 | tf_op jit(solution)/shard_map/ppermute | solution.py:353
  208.7 4.3 %collective-permute-start.16 = (bf16[256,128]{1,0:T(8,128)(2,1)S(1)}, bf16[256,128]{1,0:T(8,128)(2,1)S(1)}, u32[]{:S(2)}, u32[]{:S(2)}) collective-permute-start(bf16[256,128]{1,0:T(8,128)(2,1)S(1)} %shard_map.185.h0), channel_id=1, source_target_pairs={{0,8},{4,12},{8,0},{12,4},{1,9},{5,13},{9,1},{13,5},{2,10},{6,14},... | collective-permute-start | bytes 196616 | tf_op jit(solution)/shard_map/ppermute | solution.py:353
  213.0 5.5 %collective-permute-start.17 = (bf16[256,128]{1,0:T(8,128)(2,1)S(1)}, bf16[256,128]{1,0:T(8,128)(2,1)S(1)}, u32[]{:S(2)}, u32[]{:S(2)}) collective-permute-start(bf16[256,128]{1,0:T(8,128)(2,1)S(1)} %shard_map.185.h0), channel_id=1, source_target_pairs={{0,12},{4,0},{8,4},{12,8},{1,13},{5,1},{9,5},{13,9},{2,14},{6,2},{... | collective-permute-start | bytes 196616 | tf_op jit(solution)/shard_map/ppermute | solution.py:353
  218.5 0.1 copy.21.score_ref
  218.7 2.0 shard_map.183
  220.7 1.1 collective-permute-done.17.h3
  221.7 0.8 shard_map.186.ahead_ref
  222.5 1.2 shard_map.187
  (33 shorter events, 0.1 us)
Async XLA Ops:
  26.0 12.7 %all-to-all-start.1 = ((bf16[32,8,128]{2,1,0:T(8,128)(2,1)}), bf16[32,8,128]{2,1,0:T(8,128)(2,1)S(1)}, u32[]{:S(2)}, u32[]{:S(2)}) async-start(bf16[32,8,128]{2,1,0:T(8,128)(2,1)} %shard_map.174), calls=%async_computation.1 | async-start | bytes 131072 | tf_op jit(solution)/shard_map/all_to_all | solution.py:348
  29.9 0.7 copy-start.14
  38.8 0.6 copy-start.9
  39.4 10.1 %copy-start.10 = (bf16[2048,32]{0,1:T(8,128)(2,1)S(1)}, bf16[2048,32]{0,1:T(8,128)(2,1)}, u32[]{:S(2)}) copy-start(bf16[2048,32]{0,1:T(8,128)(2,1)} %param.34) | copy-start | bytes 393220
  39.4 10.1 %copy-start.11 = (bf16[2048,32]{0,1:T(8,128)(2,1)S(1)}, bf16[2048,32]{0,1:T(8,128)(2,1)}, u32[]{:S(2)}) copy-start(bf16[2048,32]{0,1:T(8,128)(2,1)} %param.33) | copy-start | bytes 393220
  42.5 7.0 %copy-start = (bf16[4096,128]{1,0:T(8,128)(2,1)S(1)}, bf16[4096,128]{1,0:T(8,128)(2,1)}, u32[]{:S(2)}) copy-start(bf16[4096,128]{1,0:T(8,128)(2,1)} %project_ref.1) | copy-start | bytes 3145732
  42.5 45.9 %all-to-all-start.2 = ((bf16[4,256,256]{2,1,0:T(8,128)(2,1)}), bf16[4,256,256]{2,1,0:T(8,128)(2,1)S(1)}, u32[]{:S(2)}, u32[]{:S(2)}) async-start(bf16[4,256,256]{2,1,0:T(8,128)(2,1)} %shard_map.176), calls=%async_computation.2 | async-start | bytes 1048576 | tf_op jit(solution)/shard_map/all_to_all | solution.py:348
  49.5 1.2 copy-start.1
  51.8 10.9 %collective-permute-start = (bf16[576,512]{1,0:T(8,128)(2,1)S(1)}, bf16[576,512]{1,0:T(8,128)(2,1)S(1)}, u32[]{:S(2)}, u32[]{:S(2)}) collective-permute-start(bf16[576,512]{1,0:T(8,128)(2,1)S(1)} %get-tuple-element.18), channel_id=1, source_target_pairs={{0,1},{1,0},{2,3},{3,2},{4,5},{5,4},{6,7},{7,6},{8,9},{9,8},{10,11... | collective-permute-start | bytes 1769480 | tf_op jit(solution)/shard_map/ppermute | solution.py:353
  57.2 18.6 %collective-permute-start.1 = (bf16[576,512]{1,0:T(8,128)(2,1)S(1)}, bf16[576,512]{1,0:T(8,128)(2,1)S(1)}, u32[]{:S(2)}, u32[]{:S(2)}) collective-permute-start(bf16[576,512]{1,0:T(8,128)(2,1)S(1)} %get-tuple-element.19), channel_id=1, source_target_pairs={{0,2},{1,3},{2,0},{3,1},{4,6},{5,7},{6,4},{7,5},{8,10},{9,11},{10,... | collective-permute-start | bytes 1769480 | tf_op jit(solution)/shard_map/ppermute | solution.py:353
  59.5 28.9 %collective-permute-start.2 = (bf16[576,512]{1,0:T(8,128)(2,1)S(1)}, bf16[576,512]{1,0:T(8,128)(2,1)S(1)}, u32[]{:S(2)}, u32[]{:S(2)}) collective-permute-start(bf16[576,512]{1,0:T(8,128)(2,1)S(1)} %get-tuple-element.20), channel_id=1, source_target_pairs={{0,3},{1,2},{2,1},{3,0},{4,7},{5,6},{6,5},{7,4},{8,11},{9,10},{10,... | collective-permute-start | bytes 1769480 | tf_op jit(solution)/shard_map/ppermute | solution.py:353
  90.2 3.8 %copy-start.12 = (s32[256,4]{0,1:T(4,128)S(1)}, s32[256,4]{0,1:T(4,128)}, u32[]{:S(2)}) copy-start(s32[256,4]{0,1:T(4,128)} %param.28) | copy-start | bytes 12292
  90.2 8.8 %all-to-all-start.3 = ((bf16[4,256,128]{2,1,0:T(8,128)(2,1)}), bf16[4,256,128]{2,1,0:T(8,128)(2,1)S(1)}, u32[]{:S(2)}, u32[]{:S(2)}) async-start(bf16[4,256,128]{2,1,0:T(8,128)(2,1)} %shard_map.178), calls=%async_computation.3 | async-start | bytes 524288 | tf_op jit(solution)/shard_map/all_to_all | solution.py:348
  99.1 0.8 copy-start.7
  99.9 45.8 %copy-start.2 = (bf16[2048,256]{1,0:T(8,128)(2,1)S(1)}, bf16[2048,256]{1,0:T(8,128)(2,1)}, u32[]{:S(2)}) copy-start(bf16[2048,256]{1,0:T(8,128)(2,1)} %refs_6_.1) | copy-start | bytes 3145732
  100.3 28.8 %copy-start.4 = (bf16[256,128]{1,0:T(8,128)(2,1)}, bf16[256,128]{1,0:T(8,128)(2,1)S(1)}, u32[]{:S(2)}) copy-start(bf16[256,128]{1,0:T(8,128)(2,1)S(1)} %get-tuple-element.24.m0.mid_ref) | copy-start | bytes 196612
  100.3 44.1 %copy-start.8 = (bf16[2048]{0:T(1024)(128)(2,1)S(1)}, bf16[2048]{0:T(1024)(128)(2,1)}, u32[]{:S(2)}) copy-start(bf16[2048]{0:T(1024)(128)(2,1)} %param.27) | copy-start | bytes 12292
  129.1 9.9 %collective-permute-start.4 = (bf16[1536,128]{1,0:T(8,128)(2,1)S(1)}, bf16[1536,128]{1,0:T(8,128)(2,1)S(1)}, u32[]{:S(2)}, u32[]{:S(2)}) collective-permute-start(bf16[1536,128]{1,0:T(8,128)(2,1)S(1)} %bitcast.11), channel_id=1, source_target_pairs={{0,2},{2,0},{1,3},{3,1},{4,6},{6,4},{5,7},{7,5},{8,10},{10,8},{9,1... | collective-permute-start | bytes 1179656 | tf_op jit(solution)/shard_map/ppermute | solution.py:353
  131.2 13.2 %collective-permute-start.3 = (bf16[1536,128]{1,0:T(8,128)(2,1)S(1)}, bf16[1536,128]{1,0:T(8,128)(2,1)S(1)}, u32[]{:S(2)}, u32[]{:S(2)}) collective-permute-start(bf16[1536,128]{1,0:T(8,128)(2,1)S(1)} %bitcast.12), channel_id=1, source_target_pairs={{0,1},{1,0},{2,3},{3,2},{4,5},{5,4},{6,7},{7,6},{8,9},{9,8},{10,11... | collective-permute-start | bytes 1179656 | tf_op jit(solution)/shard_map/ppermute | solution.py:353
  139.0 6.8 %collective-permute-start.5 = (bf16[1536,128]{1,0:T(8,128)(2,1)S(1)}, bf16[1536,128]{1,0:T(8,128)(2,1)S(1)}, u32[]{:S(2)}, u32[]{:S(2)}) collective-permute-start(bf16[1536,128]{1,0:T(8,128)(2,1)S(1)} %collective-permute-done.4.refs_3_), channel_id=1, source_target_pairs={{0,1},{1,0},{2,3},{3,2},{4,5},{5,4},{6,7},{7,6},{8,9},{9,8},{10,11... | collective-permute-start | bytes 1179656 | tf_op jit(solution)/shard_map/ppermute | solution.py:353
  145.7 1.2 copy-start.3
  149.6 8.0 %collective-permute-start.7 = (bf16[384,256]{1,0:T(8,128)(2,1)S(1)}, bf16[384,256]{1,0:T(8,128)(2,1)S(1)}, u32[]{:S(2)}, u32[]{:S(2)}) collective-permute-start(bf16[384,256]{1,0:T(8,128)(2,1)S(1)} %shard_map.181.h0), channel_id=1, source_target_pairs={{0,2},{2,0},{1,3},{3,1},{4,6},{6,4},{5,7},{7,5},{8,10},{10,8},{9,1... | collective-permute-start | bytes 589832 | tf_op jit(solution)/shard_map/ppermute | solution.py:353
  151.7 9.0 %collective-permute-start.6 = (bf16[384,256]{1,0:T(8,128)(2,1)S(1)}, bf16[384,256]{1,0:T(8,128)(2,1)S(1)}, u32[]{:S(2)}, u32[]{:S(2)}) collective-permute-start(bf16[384,256]{1,0:T(8,128)(2,1)S(1)} %shard_map.181.h0), channel_id=1, source_target_pairs={{0,1},{1,0},{2,3},{3,2},{4,5},{5,4},{6,7},{7,6},{8,9},{9,8},{10,11... | collective-permute-start | bytes 589832 | tf_op jit(solution)/shard_map/ppermute | solution.py:353
  157.5 4.2 %collective-permute-start.8 = (bf16[384,256]{1,0:T(8,128)(2,1)S(1)}, bf16[384,256]{1,0:T(8,128)(2,1)S(1)}, u32[]{:S(2)}, u32[]{:S(2)}) collective-permute-start(bf16[384,256]{1,0:T(8,128)(2,1)S(1)} %collective-permute-done.7.h2), channel_id=1, source_target_pairs={{0,1},{1,0},{2,3},{3,2},{4,5},{5,4},{6,7},{7,6},{8,9},{9,8},{10,11... | collective-permute-start | bytes 589832 | tf_op jit(solution)/shard_map/ppermute | solution.py:353
  163.0 7.8 %copy-start.5 = (bf16[256,128]{1,0:T(8,128)(2,1)S(1)}, bf16[256,128]{1,0:T(8,128)(2,1)}, u32[]{:S(2)}) copy-start(bf16[256,128]{1,0:T(8,128)(2,1)} %copy-done.4) | copy-start | bytes 196612
  163.0 59.5 %all-to-all-start.5 = ((bf16[128,3,4,128]{3,2,1,0:T(4,128)(2,1)}), bf16[128,3,4,128]{3,2,1,0:T(4,128)(2,1)S(1)}, u32[]{:S(2)}, u32[]{:S(2)}) async-start(bf16[128,3,4,128]{3,2,1,0:T(4,128)(2,1)} %bitcast.9), calls=%async_computation.5 | async-start | bytes 786432 | tf_op jit(solution)/shard_map/all_to_all | solution.py:348
  170.8 13.6 %collective-permute-start.10 = (bf16[256,128]{1,0:T(8,128)(2,1)S(1)}, bf16[256,128]{1,0:T(8,128)(2,1)S(1)}, u32[]{:S(2)}, u32[]{:S(2)}) collective-permute-start(bf16[256,128]{1,0:T(8,128)(2,1)S(1)} %copy-done.5), channel_id=1, source_target_pairs={{0,8},{4,12},{8,0},{12,4},{1,9},{5,13},{9,1},{13,5},{2,10},{6,14},... | collective-permute-start | bytes 196616 | tf_op jit(solution)/shard_map/ppermute | solution.py:353
  177.5 6.8 %collective-permute-start.11 = (bf16[256,128]{1,0:T(8,128)(2,1)S(1)}, bf16[256,128]{1,0:T(8,128)(2,1)S(1)}, u32[]{:S(2)}, u32[]{:S(2)}) collective-permute-start(bf16[256,128]{1,0:T(8,128)(2,1)S(1)} %copy-done.5), channel_id=1, source_target_pairs={{0,12},{4,0},{8,4},{12,8},{1,13},{5,1},{9,5},{13,9},{2,14},{6,2},{... | collective-permute-start | bytes 196616 | tf_op jit(solution)/shard_map/ppermute | solution.py:353
  179.5 7.5 %collective-permute-start.9 = (bf16[256,128]{1,0:T(8,128)(2,1)S(1)}, bf16[256,128]{1,0:T(8,128)(2,1)S(1)}, u32[]{:S(2)}, u32[]{:S(2)}) collective-permute-start(bf16[256,128]{1,0:T(8,128)(2,1)S(1)} %copy-done.5), channel_id=1, source_target_pairs={{0,4},{4,8},{8,12},{12,0},{1,5},{5,9},{9,13},{13,1},{2,6},{6,10},{... | collective-permute-start | bytes 196616 | tf_op jit(solution)/shard_map/ppermute | solution.py:353
  187.9 30.6 %copy-start.13 = (f32[256,4]{0,1:T(4,128)S(1)}, f32[256,4]{0,1:T(4,128)}, u32[]{:S(2)}) copy-start(f32[256,4]{0,1:T(4,128)} %param.29) | copy-start | bytes 12292
  187.9 9.7 %collective-permute-start.12 = (bf16[256,384]{1,0:T(8,128)(2,1)S(1)}, bf16[256,384]{1,0:T(8,128)(2,1)S(1)}, u32[]{:S(2)}, u32[]{:S(2)}) collective-permute-start(bf16[256,384]{1,0:T(8,128)(2,1)S(1)} %shard_map.184.r0), channel_id=1, source_target_pairs={{0,1},{1,0},{2,3},{3,2},{4,5},{5,4},{6,7},{7,6},{8,9},{9,8},{10,11... | collective-permute-start | bytes 589832 | tf_op jit(solution)/shard_map/ppermute | solution.py:353
  192.1 8.3 %collective-permute-start.13 = (bf16[256,384]{1,0:T(8,128)(2,1)S(1)}, bf16[256,384]{1,0:T(8,128)(2,1)S(1)}, u32[]{:S(2)}, u32[]{:S(2)}) collective-permute-start(bf16[256,384]{1,0:T(8,128)(2,1)S(1)} %shard_map.184.r0), channel_id=1, source_target_pairs={{0,2},{1,3},{2,0},{3,1},{4,6},{5,7},{6,4},{7,5},{8,10},{9,11},{10,... | collective-permute-start | bytes 589832 | tf_op jit(solution)/shard_map/ppermute | solution.py:353
  194.6 10.3 %collective-permute-start.14 = (bf16[256,384]{1,0:T(8,128)(2,1)S(1)}, bf16[256,384]{1,0:T(8,128)(2,1)S(1)}, u32[]{:S(2)}, u32[]{:S(2)}) collective-permute-start(bf16[256,384]{1,0:T(8,128)(2,1)S(1)} %shard_map.184.r0), channel_id=1, source_target_pairs={{0,3},{1,2},{2,1},{3,0},{4,7},{5,6},{6,5},{7,4},{8,11},{9,10},{10,... | collective-permute-start | bytes 589832 | tf_op jit(solution)/shard_map/ppermute | solution.py:353
  205.0 15.7 %collective-permute-start.15 = (bf16[256,128]{1,0:T(8,128)(2,1)S(1)}, bf16[256,128]{1,0:T(8,128)(2,1)S(1)}, u32[]{:S(2)}, u32[]{:S(2)}) collective-permute-start(bf16[256,128]{1,0:T(8,128)(2,1)S(1)} %shard_map.185.h0), channel_id=1, source_target_pairs={{0,4},{4,8},{8,12},{12,0},{1,5},{5,9},{9,13},{13,1},{2,6},{6,10},{... | collective-permute-start | bytes 196616 | tf_op jit(solution)/shard_map/ppermute | solution.py:353
  208.7 12.0 %collective-permute-start.16 = (bf16[256,128]{1,0:T(8,128)(2,1)S(1)}, bf16[256,128]{1,0:T(8,128)(2,1)S(1)}, u32[]{:S(2)}, u32[]{:S(2)}) collective-permute-start(bf16[256,128]{1,0:T(8,128)(2,1)S(1)} %shard_map.185.h0), channel_id=1, source_target_pairs={{0,8},{4,12},{8,0},{12,4},{1,9},{5,13},{9,1},{13,5},{2,10},{6,14},... | collective-permute-start | bytes 196616 | tf_op jit(solution)/shard_map/ppermute | solution.py:353
  213.0 8.7 %collective-permute-start.17 = (bf16[256,128]{1,0:T(8,128)(2,1)S(1)}, bf16[256,128]{1,0:T(8,128)(2,1)S(1)}, u32[]{:S(2)}, u32[]{:S(2)}) collective-permute-start(bf16[256,128]{1,0:T(8,128)(2,1)S(1)} %shard_map.185.h0), channel_id=1, source_target_pairs={{0,12},{4,0},{8,4},{12,8},{1,13},{5,1},{9,5},{13,9},{2,14},{6,2},{... | collective-permute-start | bytes 196616 | tf_op jit(solution)/shard_map/ppermute | solution.py:353
  218.6 3.1 %copy-start.6 = (bf16[512,128]{1,0:T(8,128)(2,1)S(1)}, bf16[512,128]{1,0:T(8,128)(2,1)}, u32[]{:S(2)}) copy-start(bf16[512,128]{1,0:T(8,128)(2,1)} %down_ref.3) | copy-start | bytes 393220
